TPU v7x, 32 devices: a whole 2x2x4 slice. The times are simulated.
32 devices in a mesh: grp: 2 (over y), kv: 4 (over z), tp: 4 (over x, core).
Axes of the slice: x: 2, y: 2, z: 4, core: 2. Of those that a mesh axis runs over, the one named last changes fastest.
Arguments:
- tokens: bfloat16 [32, 4096], P('grp', 'kv'), parts along dimension 0, may hold values from -16 to 16
- positions: int32 [32], P(('grp', 'kv')), parts along dimension 0, may hold values from 512 to 8191
- state: float32 [32, 16, 128, 128], P(('grp', 'kv'), 'tp'), parts along dimension 0, may hold values from -3 to 3
- norm_gain: float32 [4096], P('kv'), may hold values from 0.1 to 1.9
- w_query: bfloat16 [4096, 2048], P('kv', 'tp'), may hold values from -0.09375 to 0.09375
- w_key: bfloat16 [4096, 2048], P('kv', 'tp'), may hold values from -0.09375 to 0.09375
- w_value: bfloat16 [4096, 2048], P('kv', 'tp'), may hold values from -0.09375 to 0.09375
- w_gate: bfloat16 [4096, 2048], P('kv', 'tp'), may hold values from -0.09375 to 0.09375
- w_out: bfloat16 [2048, 4096], P('tp', 'kv'), may hold values from -0.125 to 0.125
- mlp_gain: float32 [4096], P('kv'), may hold values from 0.1 to 1.9
- w_up: bfloat16 [4096, 16384], P('kv', 'tp'), may hold values from -0.09375 to 0.09375
- w_down: bfloat16 [16384, 4096], P('tp', 'kv'), may hold values from -0.046875 to 0.046875
Outputs:
- layer_out: bfloat16 [32, 4096], P('grp', 'kv'), parts along dimension 0
- new_state: float32 [32, 16, 128, 128], P(('grp', 'kv'), 'tp'), parts along dimension 0
There are 2 independent parts, one for each index of `grp`. A program takes and returns all parts, laid end to end along the dimension named above; an argument that names none is the same for every part. Nothing has to cross between parts.
All inputs are finite; a program needn't handle non-finite values.
Results may differ from a plain program's by a relative error of at most 0.007.
Values may be sent and summed in bfloat16 or wider, within the bound.
No kernel may reach another device: no remote copies, remote signals or barrier semaphores. Data moves between devices by JAX's collectives and lax.ppermute only.
A program may use at most 64 MiB of HBM per device.

v0:
```python
import jax
import jax.numpy as jnp
from jax import lax
from jax.sharding import PartitionSpec as P

D = 4096
HEADS = 16


def turn(values, positions):
    half = values.shape[-1] // 2
    freq = 10000.0 ** (-(jnp.arange(half, dtype=jnp.float32) * 2.0) / values.shape[-1])
    angle = positions.astype(jnp.float32)[:, None, None] * freq[None, None, :]
    cosine = jnp.cos(angle)
    sine = jnp.sin(angle)
    first = values[..., :half]
    second = values[..., half:]
    return jnp.concatenate(
        [first * cosine - second * sine, first * sine + second * cosine], axis=-1
    )


def shards(
    tokens,
    positions,
    state,
    norm_gain,
    w_query,
    w_key,
    w_value,
    w_gate,
    w_out,
    mlp_gain,
    w_up,
    w_down,
):
    local_seqs, head_dev, head_size, _ = state.shape
    inputs = tokens.astype(jnp.float32)
    squares = jnp.sum(inputs * inputs, axis=1)
    normed = (inputs * norm_gain).astype(jnp.bfloat16)
    terms = jnp.stack(
        [
            jnp.dot(normed, weight, preferred_element_type=jnp.float32)
            for weight in (w_query, w_key, w_value, w_gate)
        ],
        axis=1,
    )
    summed, total_sq = (
        lax.psum_scatter(terms, "kv", scatter_dimension=0, tiled=True),
        lax.psum_scatter(squares, "kv", scatter_dimension=0, tiled=True),
    )
    scale1 = lax.rsqrt(total_sq / D + 1e-06)
    summed = (summed * scale1[:, None, None]).reshape(local_seqs, 4, head_dev, head_size)
    query = turn(summed[:, 0], positions)
    key_rows = turn(summed[:, 1], positions) * head_size ** (-0.5)
    value = summed[:, 2]
    gate = summed[:, 3]
    heads = (lax.axis_index("tp") * head_dev + jnp.arange(head_dev)).astype(jnp.float32)
    gamma = 1.0 - 2.0 ** (-5.0 - 5.0 * heads / (HEADS - 1))
    new_state = gamma[None, :, None, None] * state + key_rows[:, :, :, None] * value[:, :, None, :]
    read = jnp.einsum("bhd,bhde->bhe", query, new_state, precision=lax.Precision.HIGHEST)
    read = read * lax.rsqrt(jnp.mean(read * read, axis=-1, keepdims=True) + 1e-06)
    retained = (
        (read * jax.nn.silu(gate)).reshape(local_seqs, head_dev * head_size).astype(jnp.bfloat16)
    )
    head_terms = jnp.dot(
        lax.all_gather(retained, "kv", axis=0, tiled=True),
        w_out,
        preferred_element_type=jnp.float32,
    )
    mixed = (inputs + lax.psum(head_terms, "tp")).astype(jnp.bfloat16)
    middle = mixed.astype(jnp.float32)
    squares2 = jnp.sum(middle * middle, axis=1)
    normed2 = (middle * mlp_gain).astype(jnp.bfloat16)
    upward = jnp.dot(normed2, w_up, preferred_element_type=jnp.float32)
    up_full, total_sq2 = lax.psum((upward, squares2), "kv")
    scale2 = lax.rsqrt(total_sq2 / D + 1e-06)
    hidden = jnp.square(jax.nn.relu(up_full * scale2[:, None])).astype(jnp.bfloat16)
    down_terms = jnp.dot(hidden, w_down, preferred_element_type=jnp.float32)
    layer_out = (middle + lax.psum(down_terms, "tp")).astype(jnp.bfloat16)
    return (layer_out, new_state)


def solution(mesh):
    return jax.shard_map(
        shards,
        mesh=mesh,
        in_specs=(
            P("grp", "kv"),
            P(("grp", "kv")),
            P(("grp", "kv"), "tp", None, None),
            P("kv"),
            P("kv", "tp"),
            P("kv", "tp"),
            P("kv", "tp"),
            P("kv", "tp"),
            P("tp", "kv"),
            P("kv"),
            P("kv", "tp"),
            P("tp", "kv"),
        ),
        out_specs=(P("grp", "kv"), P(("grp", "kv"), "tp", None, None)),
        check_vma=False,
    )
```

profile of v0, /device:TPU:0, one launch (start us, length us, event | category | flops | bytes accessed | tf_op | source)
XLA Modules:
  0.0 187.9 jit_solution(12907306079230193447)
XLA Ops:
  7.2 0.0 copy-start
  7.2 0.0 copy-start.2
  7.2 0.0 copy-start.3
  7.2 0.0 all-reduce.13.cloned.1.call-start
  7.2 1.6 convolution_bitcast_fusion.3
  8.8 1.5 convolution_bitcast_fusion.2
  10.3 1.5 convolution_bitcast_fusion.1
  11.8 1.5 convolution_bitcast_fusion
  13.4 0.7 pad_maximum_fusion
  14.0 0.0 all-reduce.13.cloned.1.call-update
  14.1 0.0 all-reduce.7.cloned.1.call-start
  14.1 0.9 fusion.4
  15.0 0.7 convert_element_type.40
  15.7 0.1 multiply_cosine_fusion
  15.8 1.2 dynamic-slice
  17.7 13.5 %all-reduce.1 = f32[16]{0:T(128)S(1)} all-reduce(f32[16]{0:T(128)S(1)} %fusion.4), channel_id=3, replica_groups=mesh['grp'=2,'kv'=4,'tp'=4] {'kv'}, use_global_device_ids=true, to_apply=%region_2.0.clone | all-reduce | flops 16 | bytes 128
  31.2 0.1 fusion.19
  31.3 20.3 %all-reduce.13.cloned.1.call-done = f32[16,4,512]{2,0,1:T(8,128)} async-done(((f32[16,4,512]{2,0,1:T(8,128)}), f32[16,4,512]{2,0,1:T(8,128)}) %all-reduce.13.cloned.1.call-update) | async-done | bytes 131088
  51.6 0.9 dynamic-slice_multiply_fusion
  52.5 0.1 multiply_subtract_fusion
  52.6 0.1 pad_maximum_fusion.1
  52.7 1.6 multiply_add_fusion
  54.3 0.0 copy-start.1
  54.3 1.0 fusion.22
  55.3 0.1 multiply_reduce_fusion
  55.4 0.1 fusion.17
  55.5 13.2 %all-gather = bf16[4,4,512]{2,1,0:T(4,128)(2,1)S(1)} all-gather(bf16[1,4,512]{2,1,0:T(4,128)(2,1)S(1)} %reshape.108), channel_id=1, replica_groups=mesh['grp'=2,'kv'=4,'tp'=4] {'kv'}, dimensions={0}, use_global_device_ids=true | all-gather | bytes 20480 | tf_op jit(solution)/shard_map/all_gather | solution.py:67
  68.7 0.0 copy-done
  68.7 0.9 fusion.23
  69.6 0.0 all-reduce.7.cloned.1.call-update
  69.6 0.0 all-reduce.9.cloned.1.call-start
  69.6 31.3 %all-reduce.7.cloned.1.call-done = f32[16,1024]{1,0:T(8,128)} async-done(((f32[16,1024]{1,0:T(8,128)}), f32[16,1024]{1,0:T(8,128)}) %all-reduce.7.cloned.1.call-update) | async-done | bytes 65552 | tf_op jit(solution)/shard_map/psum | solution.py:71
  101.0 0.0 copy-done.2
  101.0 1.0 fusion.7
  101.9 0.0 copy-done.3
  101.9 5.3 %fusion.9 = f32[16,4096]{1,0:T(8,128)} fusion(bf16[1024,4096]{1,0:T(8,128)(2,1)} %param.22, bf16[16,1024]{1,0:T(8,128)(2,1)S(1)} %get-tuple-element.3, f32[1024]{0:T(1024)S(1)} %copy-done.3), kind=kOutput, calls=%fused_computation.22 | convolution fusion | flops 134266880 | bytes 8687616 | tf_op jit(solution)/shard_map/dot_general | solution.py:75
  107.2 0.0 copy-done.1
  107.2 0.0 all-reduce.9.cloned.1.call-update
  107.2 0.0 all-reduce.11.cloned.1.call-start
  107.3 11.8 %psum.30 = f32[16]{0:T(128)S(1)} all-reduce(f32[16]{0:T(128)S(1)} %get-tuple-element.2), channel_id=1, replica_groups=mesh['grp'=2,'kv'=4,'tp'=4] {'kv'}, use_global_device_ids=true, to_apply=%region_7.8 | all-reduce | flops 16 | bytes 128 | tf_op jit(solution)/shard_map/psum | solution.py:76
  119.1 23.9 %all-reduce.9.cloned.1.call-done = f32[16,4096]{1,0:T(8,128)} async-done(((f32[16,4096]{1,0:T(8,128)}), f32[16,4096]{1,0:T(8,128)}) %all-reduce.9.cloned.1.call-update) | async-done | bytes 262160 | tf_op jit(solution)/shard_map/psum | solution.py:76
  143.0 5.3 %fusion = f32[16,1024]{1,0:T(8,128)} fusion(bf16[4096,1024]{1,0:T(8,128)(2,1)} %param.23, f32[16,4096]{1,0:T(8,128)} %all-reduce.9.cloned.1.call-done, f32[16]{0:T(128)S(1)} %add_rsqrt_fusion.1), kind=kOutput, calls=%fused_computation.6 | convolution fusion | flops 134479872 | bytes 8716352 | tf_op jit(solution)/shard_map/dot_general | solution.py:79
  148.3 0.0 all-reduce.11.cloned.1.call-update
  148.4 31.6 %all-reduce.11.cloned.1.call-done = f32[16,1024]{1,0:T(8,128)} async-done(((f32[16,1024]{1,0:T(8,128)}), f32[16,1024]{1,0:T(8,128)}) %all-reduce.11.cloned.1.call-update) | async-done | bytes 65552 | tf_op jit(solution)/shard_map/psum | solution.py:80
  179.9 1.5 fusion.8
  (8 shorter events, 0.1 us)
Async XLA Ops:
  7.2 61.5 %copy-start = (bf16[512,1024]{1,0:T(8,128)(2,1)S(1)}, bf16[512,1024]{1,0:T(8,128)(2,1)}, u32[]{:S(2)}) copy-start(bf16[512,1024]{1,0:T(8,128)(2,1)} %param.20) | copy-start | bytes 3145732
  7.2 93.8 %copy-start.2 = (bf16[16,1024]{1,0:T(8,128)(2,1)S(1)}, bf16[16,1024]{1,0:T(8,128)(2,1)}, u32[]{:S(2)}) copy-start(bf16[16,1024]{1,0:T(8,128)(2,1)} %param.12) | copy-start | bytes 98308
  7.2 94.7 %copy-start.3 = (f32[1024]{0:T(1024)S(1)}, f32[1024]{0:T(1024)}, u32[]{:S(2)}) copy-start(f32[1024]{0:T(1024)} %param.21) | copy-start | bytes 12292
  7.2 44.4 %all-reduce.13.cloned.1.call-start = ((), (), s32[]{:S(2)}) async-start(), calls=%async_computation.3 | async-start | bytes 262144
  14.1 86.9 %all-reduce.7.cloned.1.call-start = ((), (), s32[]{:S(2)}) async-start(), calls=%async_computation | async-start | bytes 131072 | tf_op jit(solution)/shard_map/psum | solution.py:71
  54.3 52.9 %copy-start.1 = (f32[4,4,128,128]{3,2,1,0:T(8,128)}, f32[4,4,128,128]{3,2,1,0:T(8,128)S(1)}, u32[]{:S(2)}) copy-start(f32[4,4,128,128]{3,2,1,0:T(8,128)S(1)} %multiply_add_fusion) | copy-start | bytes 3145732
  69.6 73.4 %all-reduce.9.cloned.1.call-start = ((), (), s32[]{:S(2)}) async-start(), calls=%async_computation.1 | async-start | bytes 524288 | tf_op jit(solution)/shard_map/psum | solution.py:76
  107.2 72.7 %all-reduce.11.cloned.1.call-start = ((), (), s32[]{:S(2)}) async-start(), calls=%async_computation.2 | async-start | bytes 131072 | tf_op jit(solution)/shard_map/psum | solution.py:80
Sparse Core Ops, SparseCore 0:
  14.2 37.3 all-reduce.12
  69.7 31.1 all-reduce.6
  107.4 35.5 all-reduce.8
  148.5 31.3 all-reduce.10
where the time goes:
time: 189 us; the launch traced here: 188 us
  waiting for transfers between devices  107 us (57%)
  blocking collectives  38.5 us (20%)
  matrix products  18.6 us (10%)
  between operations  14.5 us (8%)
  other arithmetic  7.69 us (4%)
    psum x1, waiting for transfers between devices, shards(): layer_out = (middle + lax.psum(down_terms, 'tp')).astype(jnp.bfloat16)  31.6 us
    psum x1, waiting for transfers between devices, shards(): mixed = (inputs + lax.psum(head_terms, 'tp')).astype(jnp.bfloat16)  31.3 us
    psum x1, waiting for transfers between devices, shards(): up_full, total_sq2 = lax.psum((upward, squares2), 'kv')  23.9 us
    unnamed x5, waiting for transfers between devices  20.4 us
    unnamed x1, blocking collectives  13.5 us
    all_gather x1, blocking collectives, shards(): lax.all_gather(retained, 'kv', axis=0, tiled=True)  13.2 us
    psum x1, blocking collectives, shards(): up_full, total_sq2 = lax.psum((upward, squares2), 'kv')  11.8 us
    dot_general x4, matrix products, shards(): jnp.dot(normed, weight, preferred_element_type=jnp.float32)  6.11 us
  transfers between devices with their start and end apart: 4, of which 4 were waited for; matrix products, arithmetic and copies ran while one was open for 2% of the time, Pallas kernels for 0%

commit v1 on v0

v1 whole, which is shorter than its diff:
```python
import jax
import jax.numpy as jnp
from jax import lax
from jax.sharding import PartitionSpec as P

D = 4096
HEADS = 16
DIRECT = 8


def turn(values, positions):
    half = values.shape[-1] // 2
    freq = 10000.0 ** (-(jnp.arange(half, dtype=jnp.float32) * 2.0) / values.shape[-1])
    angle = positions.astype(jnp.float32)[:, None, None] * freq[None, None, :]
    cosine = jnp.cos(angle)
    sine = jnp.sin(angle)
    first = values[..., :half]
    second = values[..., half:]
    return jnp.concatenate(
        [first * cosine - second * sine, first * sine + second * cosine], axis=-1
    )


def swap(value, axis, n, step):
    return lax.ppermute(value, axis, [(i, i ^ step) for i in range(n)])


def pieces(value):
    high = lax.reduce_precision(value, 8, 7)
    rest = value - high
    middle = lax.reduce_precision(rest, 8, 7)
    return [p.astype(jnp.bfloat16) for p in (high, middle, rest - middle)]


def scatter_sum(chunk, axis, n):
    me = lax.axis_index(axis)
    mine = chunk(me)
    got = [swap(chunk(me ^ s).astype(jnp.bfloat16), axis, n, s) for s in range(1, n)]
    total = mine
    for g in got:
        total = total + g.astype(jnp.float32)
    return total


def all_sum(value, axis, n):
    sent = value.astype(jnp.bfloat16)
    total = value
    for g in [swap(sent, axis, n, s) for s in range(1, n)]:
        total = total + g.astype(jnp.float32)
    return total


def gather(value, axis, n):
    me = lax.axis_index(axis)
    got = [value] + [swap(value, axis, n, s) for s in range(1, n)]
    out = jnp.zeros((n, *value.shape), value.dtype)
    for s, g in enumerate(got):
        out = lax.dynamic_update_slice_in_dim(out, g[None], me ^ s, 0)
    return out


def make(mesh):
    n_kv, n_tp = mesh.shape["kv"], mesh.shape["tp"]

    def shards(
        tokens, positions, state, norm_gain, w_query, w_key, w_value, w_gate, w_out, mlp_gain, w_up, w_down
    ):
        local_seqs, head_dev, head_size, _ = state.shape
        rows = tokens.shape[0]
        width = head_dev * head_size
        inputs = tokens.astype(jnp.float32)
        squares = jnp.sum(inputs * inputs, axis=1)
        normed = (inputs * norm_gain).astype(jnp.bfloat16)
        terms = jnp.concatenate(
            [
                jnp.dot(normed, weight, preferred_element_type=jnp.float32)
                for weight in (w_query, w_key, w_value, w_gate)
            ]
            + [jnp.broadcast_to(p.astype(jnp.float32)[:, None], (rows, 128)) for p in pieces(squares)],
            axis=1,
        )
        total = scatter_sum(
            lambda i: lax.dynamic_slice_in_dim(terms, i * local_seqs, local_seqs, 0), "kv", n_kv
        )
        total_sq = total[:, 4 * width] + total[:, 4 * width + 128] + total[:, 4 * width + 256]
        scale1 = lax.rsqrt(total_sq / D + 1e-06)
        summed = (total[:, : 4 * width] * scale1[:, None]).reshape(local_seqs, 4, head_dev, head_size)
        query = turn(summed[:, 0], positions)
        key_rows = turn(summed[:, 1], positions) * head_size ** (-0.5)
        value = summed[:, 2]
        gate = summed[:, 3]
        heads = (lax.axis_index("tp") * head_dev + jnp.arange(head_dev)).astype(jnp.float32)
        gamma = 1.0 - 2.0 ** (-5.0 - 5.0 * heads / (HEADS - 1))
        new_state = gamma[None, :, None, None] * state + key_rows[:, :, :, None] * value[:, :, None, :]
        read = jnp.einsum("bhd,bhde->bhe", query, new_state, precision=lax.Precision.HIGHEST)
        read = read * lax.rsqrt(jnp.mean(read * read, axis=-1, keepdims=True) + 1e-06)
        retained = (read * jax.nn.silu(gate)).reshape(local_seqs, width).astype(jnp.bfloat16)
        head_terms = jnp.dot(
            gather(retained, "kv", n_kv).reshape(rows, width), w_out, preferred_element_type=jnp.float32
        )
        mixed = (inputs + all_sum(head_terms, "tp", n_tp)).astype(jnp.bfloat16)
        middle = mixed.astype(jnp.float32)
        squares2 = jnp.sum(middle * middle, axis=1)
        normed2 = (middle * mlp_gain).astype(jnp.bfloat16)
        upward = jnp.dot(normed2, w_up, preferred_element_type=jnp.float32)
        part = upward.shape[1] // n_kv
        extra = jnp.concatenate(
            [jnp.broadcast_to(p.astype(jnp.float32)[:, None], (rows, 128)) for p in pieces(squares2)], axis=1
        )
        total2 = scatter_sum(
            lambda i: jnp.concatenate([lax.dynamic_slice_in_dim(upward, i * part, part, 1), extra], axis=1),
            "kv",
            n_kv,
        )
        total_sq2 = total2[:, part] + total2[:, part + 128] + total2[:, part + 256]
        scale2 = lax.rsqrt(total_sq2 / D + 1e-06)
        hidden = jnp.square(jax.nn.relu(total2[:, :part] * scale2[:, None])).astype(jnp.bfloat16)
        full = gather(hidden, "kv", n_kv).transpose(1, 0, 2).reshape(rows, n_kv * part)
        down_terms = jnp.dot(full, w_down, preferred_element_type=jnp.float32)
        layer_out = (middle + all_sum(down_terms, "tp", n_tp)).astype(jnp.bfloat16)
        return (layer_out, new_state)

    return shards


def solution(mesh):
    return jax.shard_map(
        make(mesh),
        mesh=mesh,
        in_specs=(
            P("grp", "kv"),
            P(("grp", "kv")),
            P(("grp", "kv"), "tp", None, None),
            P("kv"),
            P("kv", "tp"),
            P("kv", "tp"),
            P("kv", "tp"),
            P("kv", "tp"),
            P("tp", "kv"),
            P("kv"),
            P("kv", "tp"),
            P("tp", "kv"),
        ),
        out_specs=(P("grp", "kv"), P(("grp", "kv"), "tp", None, None)),
        check_vma=False,
    )
```

time: 189 us -> 67.5 us (0.36)
  waiting for transfers between devices: 107 us -> 19.1 us
  blocking collectives: 38.5 us -> 0 us
  starting transfers between devices: 0.16 us -> 22.6 us
  between operations: 14.5 us -> 0.95 us
  matrix products: 18.6 us -> 15.9 us
  other arithmetic: 7.69 us -> 5.06 us
  local copies, waits for them, and re-layouts: 1.33 us -> 3.47 us
    psum x3 -> x0, waiting for transfers between devices: 86.8 us -> none  [the longest x1 31.6 us: shards(): layer_out = (middle + lax.psum(down_terms, 'tp')).astype(jnp.bfloat16)]
    ppermute x0 -> x18, starting transfers between devices: none -> 22.6 us  [swap(): return lax.ppermute(value, axis, [(i, i ^ step) for i in range(n)])]
    unnamed x5 -> x0, waiting for transfers between devices: 20.4 us -> none
    ppermute x0 -> x18, waiting for transfers between devices: none -> 19.1 us  [swap(): return lax.ppermute(value, axis, [(i, i ^ step) for i in range(n)])]
    unnamed x1 -> x0, blocking collectives: 13.5 us -> none
    all_gather x1 -> x0, blocking collectives: 13.2 us -> none  [shards(): lax.all_gather(retained, 'kv', axis=0, tiled=True)]
    psum x1 -> x0, blocking collectives: 11.8 us -> none  [shards(): up_full, total_sq2 = lax.psum((upward, squares2), 'kv')]
    dynamic_update_slice x0 -> x8, local copies, waits for them, and re-layouts: none -> 1.91 us  [gather(): out = lax.dynamic_update_slice_in_dim(out, g[None], me ^ s, 0)]
  transfers between devices with their start and end apart: 4 -> 18, of which waited for: 4 -> 12; matrix products, arithmetic and copies ran while one was open for 2% -> 2% of each run, Pallas kernels for 0% -> 0%
where the time goes in v1:
time: 67.5 us; the launch traced here: 67 us
  starting transfers between devices  22.6 us (33%)
  waiting for transfers between devices  19.1 us (28%)
  matrix products  15.9 us (24%)
  other arithmetic  5.06 us (7%)
  local copies, waits for them, and re-layouts  3.47 us (5%)
  between operations  0.95 us (1%)
    ppermute x18, starting transfers between devices, swap(): return lax.ppermute(value, axis, [(i, i ^ step) for i in range(n)])  22.6 us
    ppermute x18, waiting for transfers between devices, swap(): return lax.ppermute(value, axis, [(i, i ^ step) for i in range(n)])  19.1 us
    dot_general x4, matrix products, shards(): jnp.dot(normed, weight, preferred_element_type=jnp.float32)  5.53 us
    dot_general x1, matrix products, shards(): upward = jnp.dot(normed2, w_up, preferred_element_type=jnp.float32)  4.58 us
    dot_general x1, matrix products, shards(): down_terms = jnp.dot(full, w_down, preferred_element_type=jnp.float32)  4.58 us
    dynamic_update_slice x8, local copies, waits for them, and re-layouts, gather(): out = lax.dynamic_update_slice_in_dim(out, g[None], me ^ s, 0)  1.91 us
    add x1, other arithmetic, shards(): gamma[None, :, None, None] * state  1.57 us
  transfers between devices with their start and end apart: 18, of which 12 were waited for; matrix products, arithmetic and copies ran while one was open for 2% of the time, Pallas kernels for 0%

profile of v1, /device:TPU:0, one launch (start us, length us, event | category | flops | bytes accessed | tf_op | source)
XLA Modules:
  0.0 67.0 jit_solution(7946527294787739206)
XLA Ops:
  0.7 1.0 %fusion.3 = f32[16]{0:T(128)S(1)} fusion(bf16[16,1024]{1,0:T(8,128)(2,1)} %param.12), kind=kLoop, calls=%fused_computation.24 | loop fusion | flops 49136 | bytes 32832 | tf_op jit(solution)/shard_map/reduce_sum | solution.py:72
  1.7 0.5 copy-done
  2.2 1.0 %convolution_dynamic-update-slice_fusion.3 = f32[16,2432]{1,0:T(8,128)S(1)} fusion(bf16[1024,512]{1,0:T(8,128)(2,1)S(1)} %copy-done, bf16[16,1024]{1,0:T(8,128)(2,1)} %param.12, f32[1024]{0:T(1024)} %param.15), kind=kOutput, calls=%fused_computation.3 | convolution fusion | flops 16826368 | bytes 1118208 | tf_op jit(solution)/shard_map/dot_general | solution.py:76
  3.2 1.5 %convolution_dynamic-update-slice_fusion.2 = f32[16,2432]{1,0:T(8,128)S(1)} fusion(f32[16,2432]{1,0:T(8,128)S(1)} %convolution_dynamic-update-slice_fusion.3, bf16[1024,512]{1,0:T(8,128)(2,1)} %param.17, bf16[16,1024]{1,0:T(8,128)(2,1)} %param.12, f32[1024]{0:T(1024)} %param.15), kind=kOutput, calls=%fused_computation.2 | convolution fusion | flops 16826368 | bytes 1118208 | tf_op jit(solution)/shard_map/dot_general | solution.py:76
  4.7 1.5 %convolution_dynamic-update-slice_fusion.1 = f32[16,2432]{1,0:T(8,128)S(1)} fusion(f32[16,2432]{1,0:T(8,128)S(1)} %convolution_dynamic-update-slice_fusion.2, bf16[1024,512]{1,0:T(8,128)(2,1)} %param.18, bf16[16,1024]{1,0:T(8,128)(2,1)} %param.12, f32[1024]{0:T(1024)} %param.15), kind=kOutput, calls=%fused_computation.1 | convolution fusion | flops 16826368 | bytes 1118208 | tf_op jit(solution)/shard_map/dot_general | solution.py:76
  6.2 1.5 %convolution_dynamic-update-slice_fusion = f32[16,2432]{1,0:T(8,128)S(1)} fusion(f32[16,2432]{1,0:T(8,128)S(1)} %convolution_dynamic-update-slice_fusion.1, bf16[1024,512]{1,0:T(8,128)(2,1)} %param.19, bf16[16,1024]{1,0:T(8,128)(2,1)} %param.12, f32[1024]{0:T(1024)} %param.15), kind=kOutput, calls=%fused_computation | convolution fusion | flops 16826368 | bytes 1118208 | tf_op jit(solution)/shard_map/dot_general | solution.py:76
  7.7 0.1 constant_dynamic-update-slice_fusion.2
  7.8 0.1 constant_dynamic-update-slice_fusion.1
  7.9 0.1 constant_dynamic-update-slice_fusion
  8.0 3.1 %collective-permute-start = (bf16[4,2432]{1,0:T(4,128)(2,1)S(1)}, bf16[4,2432]{1,0:T(4,128)(2,1)S(1)}, u32[]{:S(2)}, u32[]{:S(2)}) collective-permute-start(bf16[4,2432]{1,0:T(4,128)(2,1)S(1)} %get-tuple-element.7), channel_id=1, source_target_pairs={{0,4},{4,0},{8,12},{12,8},{1,5},{5,1},{9,13},{13,9},{2,6},{6,2},{1... | collective-permute-start | bytes 58376 | tf_op jit(solution)/shard_map/ppermute | solution.py:25
  11.1 2.6 %collective-permute-start.1 = (bf16[4,2432]{1,0:T(4,128)(2,1)S(1)}, bf16[4,2432]{1,0:T(4,128)(2,1)S(1)}, u32[]{:S(2)}, u32[]{:S(2)}) collective-permute-start(bf16[4,2432]{1,0:T(4,128)(2,1)S(1)} %get-tuple-element.9), channel_id=1, source_target_pairs={{0,8},{4,12},{8,0},{12,4},{1,9},{5,13},{9,1},{13,5},{2,10},{6,14},... | collective-permute-start | bytes 58376 | tf_op jit(solution)/shard_map/ppermute | solution.py:25
  13.7 0.7 convert_element_type.200
  14.4 0.1 multiply_cosine_fusion
  14.5 1.4 %collective-permute-done.1 = bf16[4,2432]{1,0:T(4,128)(2,1)S(1)} collective-permute-done((bf16[4,2432]{1,0:T(4,128)(2,1)S(1)}, bf16[4,2432]{1,0:T(4,128)(2,1)S(1)}, u32[]{:S(2)}, u32[]{:S(2)}) %collective-permute-start.1) | collective-permute-done | bytes 19488 | tf_op jit(solution)/shard_map/ppermute | solution.py:25
  16.0 3.3 %collective-permute-done.2 = bf16[4,2432]{1,0:T(4,128)(2,1)S(1)} collective-permute-done((bf16[4,2432]{1,0:T(4,128)(2,1)S(1)}, bf16[4,2432]{1,0:T(4,128)(2,1)S(1)}, u32[]{:S(2)}, u32[]{:S(2)}) %collective-permute-start.2) | collective-permute-done | bytes 19488 | tf_op jit(solution)/shard_map/ppermute | solution.py:25
  19.3 0.1 fusion.27
  19.4 0.1 slice_multiply_fusion.1
  19.6 0.1 multiply_subtract_fusion
  19.6 0.1 pad_maximum_fusion.9
  19.7 1.6 %multiply_add_fusion = f32[4,4,128,128]{3,2,1,0:T(8,128)S(1)} fusion(f32[4,4,128,128]{3,2,1,0:T(8,128)} %param.14, f32[4,4,128]{2,1,0:T(4,128)S(1)} %get-tuple-element.11, f32[4,4,128]{2,1,0:T(4,128)S(1)} %get-tuple-element.37, f32[4]{0:T(128)S(1)} %power_subtract_fusion), kind=kLoop, calls=%fused_computation.4 | loop fusion | flops 786432 | bytes 2113552 | tf_op jit(solution)/shard_map/add | solution.py:94
  21.3 1.0 %fusion.38 = f32[4,4,1,128]{3,2,1,0:T(1,128)S(1)} fusion(f32[4,4,128,1]{2,3,1,0:T(1,128)S(1)} %bitcast.53, f32[4,4,128,128]{3,2,1,0:T(8,128)S(1)} %multiply_add_fusion), kind=kOutput, calls=%fused_computation.100 | convolution fusion | flops 3145728 | bytes 1064960 | tf_op jit(solution)/shard_map/bhd,bhde->bhe/dot_general | solution.py:95
  22.3 0.1 multiply_reduce_fusion
  22.4 0.1 fusion.23
  22.5 0.1 collective-permute-start.3
  22.6 0.8 %collective-permute-start.4 = (bf16[4,512]{1,0:T(4,128)(2,1)S(1)}, bf16[4,512]{1,0:T(4,128)(2,1)S(1)}, u32[]{:S(2)}, u32[]{:S(2)}) collective-permute-start(bf16[4,512]{1,0:T(4,128)(2,1)S(1)} %bitcast.58), channel_id=1, source_target_pairs={{0,8},{4,12},{8,0},{12,4},{1,9},{5,13},{9,1},{13,5},{2,10},{6,14},... | collective-permute-start | bytes 12296 | tf_op jit(solution)/shard_map/ppermute | solution.py:25
  23.3 3.6 %collective-permute-start.5 = (bf16[4,512]{1,0:T(4,128)(2,1)S(1)}, bf16[4,512]{1,0:T(4,128)(2,1)S(1)}, u32[]{:S(2)}, u32[]{:S(2)}) collective-permute-start(bf16[4,512]{1,0:T(4,128)(2,1)S(1)} %bitcast.59), channel_id=1, source_target_pairs={{0,12},{4,8},{8,4},{12,0},{1,13},{5,9},{9,5},{13,1},{2,14},{6,10},... | collective-permute-start | bytes 12296 | tf_op jit(solution)/shard_map/ppermute | solution.py:25
  27.0 0.2 collective-permute-done.4
  27.1 1.6 %collective-permute-done.5 = bf16[4,512]{1,0:T(4,128)(2,1)S(1)} collective-permute-done((bf16[4,512]{1,0:T(4,128)(2,1)S(1)}, bf16[4,512]{1,0:T(4,128)(2,1)S(1)}, u32[]{:S(2)}, u32[]{:S(2)}) %collective-permute-start.5) | collective-permute-done | bytes 4128 | tf_op jit(solution)/shard_map/ppermute | solution.py:25
  28.8 0.3 fusion.36
  29.0 1.6 %collective-permute-start.7 = (bf16[16,1024]{1,0:T(8,128)(2,1)S(1)}, bf16[16,1024]{1,0:T(8,128)(2,1)S(1)}, u32[]{:S(2)}, u32[]{:S(2)}) collective-permute-start(bf16[16,1024]{1,0:T(8,128)(2,1)S(1)} %get-tuple-element.32), channel_id=1, source_target_pairs={{0,2},{1,3},{2,0},{3,1},{4,6},{5,7},{6,4},{7,5},{8,10},{9,11},{10,... | collective-permute-start | bytes 98312 | tf_op jit(solution)/shard_map/ppermute | solution.py:25
  30.6 0.3 collective-permute-start.8
  30.9 2.1 %collective-permute-done.7 = bf16[16,1024]{1,0:T(8,128)(2,1)S(1)} collective-permute-done((bf16[16,1024]{1,0:T(8,128)(2,1)S(1)}, bf16[16,1024]{1,0:T(8,128)(2,1)S(1)}, u32[]{:S(2)}, u32[]{:S(2)}) %collective-permute-start.7) | collective-permute-done | bytes 32800 | tf_op jit(solution)/shard_map/ppermute | solution.py:25
  33.0 0.9 %collective-permute-done.8 = bf16[16,1024]{1,0:T(8,128)(2,1)S(1)} collective-permute-done((bf16[16,1024]{1,0:T(8,128)(2,1)S(1)}, bf16[16,1024]{1,0:T(8,128)(2,1)S(1)}, u32[]{:S(2)}, u32[]{:S(2)}) %collective-permute-start.8) | collective-permute-done | bytes 32800 | tf_op jit(solution)/shard_map/ppermute | solution.py:25
  33.9 0.1 fusion.6
  34.1 4.6 %fusion.11 = f32[16,4096]{1,0:T(8,128)S(1)} fusion(bf16[1024,4096]{1,0:T(8,128)(2,1)} %param.22, bf16[16,1024]{1,0:T(8,128)(2,1)S(1)} %get-tuple-element.3, f32[1024]{0:T(1024)S(1)} %copy-done.4), kind=kOutput, calls=%fused_computation.40 | convolution fusion | flops 134266880 | bytes 8687616 | tf_op jit(solution)/shard_map/dot_general | solution.py:105
  38.7 0.1 broadcast_in_dim.92
  38.8 0.1 broadcast_in_dim.93
  38.8 0.1 broadcast_in_dim.94
  38.9 0.5 collective-permute-start.10
  39.4 3.3 %collective-permute-start.11 = (bf16[16,1408]{1,0:T(8,128)(2,1)S(1)}, bf16[16,1408]{1,0:T(8,128)(2,1)S(1)}, u32[]{:S(2)}, u32[]{:S(2)}) collective-permute-start(bf16[16,1408]{1,0:T(8,128)(2,1)S(1)} %get-tuple-element.15), channel_id=1, source_target_pairs={{0,12},{4,8},{8,4},{12,0},{1,13},{5,9},{9,5},{13,1},{2,14},{6,10},... | collective-permute-start | bytes 135176 | tf_op jit(solution)/shard_map/ppermute | solution.py:25
  42.7 0.5 collective-permute-start.9
  43.2 2.9 %collective-permute-done.10 = bf16[16,1408]{1,0:T(8,128)(2,1)S(1)} collective-permute-done((bf16[16,1408]{1,0:T(8,128)(2,1)S(1)}, bf16[16,1408]{1,0:T(8,128)(2,1)S(1)}, u32[]{:S(2)}, u32[]{:S(2)}) %collective-permute-start.10) | collective-permute-done | bytes 45088 | tf_op jit(solution)/shard_map/ppermute | solution.py:25
  46.1 0.7 %collective-permute-done.9 = bf16[16,1408]{1,0:T(8,128)(2,1)S(1)} collective-permute-done((bf16[16,1408]{1,0:T(8,128)(2,1)S(1)}, bf16[16,1408]{1,0:T(8,128)(2,1)S(1)}, u32[]{:S(2)}, u32[]{:S(2)}) %collective-permute-start.9) | collective-permute-done | bytes 45088 | tf_op jit(solution)/shard_map/ppermute | solution.py:25
  46.8 0.1 broadcast_in_dim.44
  46.9 0.1 broadcast_in_dim.90
  47.0 0.1 broadcast_in_dim.91
  47.1 0.1 fusion.22
  47.2 0.1 fusion.10
  47.3 0.6 collective-permute-start.12
  47.9 2.3 %collective-permute-start.13 = (bf16[16,1024]{1,0:T(8,128)(2,1)S(1)}, bf16[16,1024]{1,0:T(8,128)(2,1)S(1)}, u32[]{:S(2)}, u32[]{:S(2)}) collective-permute-start(bf16[16,1024]{1,0:T(8,128)(2,1)S(1)} %fusion.10), channel_id=1, source_target_pairs={{0,8},{4,12},{8,0},{12,4},{1,9},{5,13},{9,1},{13,5},{2,10},{6,14},... | collective-permute-start | bytes 98312 | tf_op jit(solution)/shard_map/ppermute | solution.py:25
  50.2 1.5 %collective-permute-start.14 = (bf16[16,1024]{1,0:T(8,128)(2,1)S(1)}, bf16[16,1024]{1,0:T(8,128)(2,1)S(1)}, u32[]{:S(2)}, u32[]{:S(2)}) collective-permute-start(bf16[16,1024]{1,0:T(8,128)(2,1)S(1)} %fusion.10), channel_id=1, source_target_pairs={{0,12},{4,8},{8,4},{12,0},{1,13},{5,9},{9,5},{13,1},{2,14},{6,10},... | collective-permute-start | bytes 98312 | tf_op jit(solution)/shard_map/ppermute | solution.py:25
  51.7 0.1 fusion.50
  51.9 0.5 dynamic_update_slice.28
  52.5 0.3 collective-permute-done.13
  52.8 3.1 %collective-permute-done.14 = bf16[16,1024]{1,0:T(8,128)(2,1)S(1)} collective-permute-done((bf16[16,1024]{1,0:T(8,128)(2,1)S(1)}, bf16[16,1024]{1,0:T(8,128)(2,1)S(1)}, u32[]{:S(2)}, u32[]{:S(2)}) %collective-permute-start.14) | collective-permute-done | bytes 32800 | tf_op jit(solution)/shard_map/ppermute | solution.py:25
  56.0 0.5 dynamic_update_slice.29
  56.5 0.5 dynamic_update_slice.30
  57.0 0.5 dynamic_update_slice.31
  57.5 4.6 %fusion.37 = (bf16[16,1024]{1,0:T(8,128)(2,1)S(1)}, f32[16,1024]{1,0:T(8,128)S(1)}) fusion(bf16[16,4096]{1,0:T(8,128)(2,1)S(1)} %bitcast.48, bf16[4096,1024]{1,0:T(8,128)(2,1)} %param.23), kind=kOutput, calls=%fused_computation.99 | convolution fusion | flops 134234112 | bytes 8617984 | tf_op jit(solution)/shard_map/dot_general | solution.py:119
  62.1 0.9 %collective-permute-start.16 = (bf16[16,1024]{1,0:T(8,128)(2,1)S(1)}, bf16[16,1024]{1,0:T(8,128)(2,1)S(1)}, u32[]{:S(2)}, u32[]{:S(2)}) collective-permute-start(bf16[16,1024]{1,0:T(8,128)(2,1)S(1)} %get-tuple-element.34), channel_id=1, source_target_pairs={{0,2},{1,3},{2,0},{3,1},{4,6},{5,7},{6,4},{7,5},{8,10},{9,11},{10,... | collective-permute-start | bytes 98312 | tf_op jit(solution)/shard_map/ppermute | solution.py:25
  63.0 0.9 %collective-permute-start.17 = (bf16[16,1024]{1,0:T(8,128)(2,1)S(1)}, bf16[16,1024]{1,0:T(8,128)(2,1)S(1)}, u32[]{:S(2)}, u32[]{:S(2)}) collective-permute-start(bf16[16,1024]{1,0:T(8,128)(2,1)S(1)} %get-tuple-element.34), channel_id=1, source_target_pairs={{0,3},{1,2},{2,1},{3,0},{4,7},{5,6},{6,5},{7,4},{8,11},{9,10},{10,... | collective-permute-start | bytes 98312 | tf_op jit(solution)/shard_map/ppermute | solution.py:25
  63.9 2.1 %collective-permute-done.16 = bf16[16,1024]{1,0:T(8,128)(2,1)S(1)} collective-permute-done((bf16[16,1024]{1,0:T(8,128)(2,1)S(1)}, bf16[16,1024]{1,0:T(8,128)(2,1)S(1)}, u32[]{:S(2)}, u32[]{:S(2)}) %collective-permute-start.16) | collective-permute-done | bytes 32800 | tf_op jit(solution)/shard_map/ppermute | solution.py:25
  66.1 0.3 collective-permute-done.17
  66.4 0.6 fusion.7
  (45 shorter events, 0.7 us)
Async XLA Ops:
  0.6 1.6 %copy-start = (bf16[1024,512]{1,0:T(8,128)(2,1)S(1)}, bf16[1024,512]{1,0:T(8,128)(2,1)}, u32[]{:S(2)}) copy-start(bf16[1024,512]{1,0:T(8,128)(2,1)} %param.16) | copy-start | bytes 3145732
  0.6 33.3 %copy-start.2 = (bf16[16,1024]{1,0:T(8,128)(2,1)S(1)}, bf16[16,1024]{1,0:T(8,128)(2,1)}, u32[]{:S(2)}) copy-start(bf16[16,1024]{1,0:T(8,128)(2,1)} %param.12) | copy-start | bytes 98308
  0.7 28.1 %copy-start.3 = (bf16[512,1024]{1,0:T(8,128)(2,1)S(1)}, bf16[512,1024]{1,0:T(8,128)(2,1)}, u32[]{:S(2)}) copy-start(bf16[512,1024]{1,0:T(8,128)(2,1)} %param.20) | copy-start | bytes 3145732
  0.7 33.4 %copy-start.4 = (f32[1024]{0:T(1024)S(1)}, f32[1024]{0:T(1024)}, u32[]{:S(2)}) copy-start(f32[1024]{0:T(1024)} %param.21) | copy-start | bytes 12292
  8.0 6.5 %collective-permute-start = (bf16[4,2432]{1,0:T(4,128)(2,1)S(1)}, bf16[4,2432]{1,0:T(4,128)(2,1)S(1)}, u32[]{:S(2)}, u32[]{:S(2)}) collective-permute-start(bf16[4,2432]{1,0:T(4,128)(2,1)S(1)} %get-tuple-element.7), channel_id=1, source_target_pairs={{0,4},{4,0},{8,12},{12,8},{1,5},{5,1},{9,13},{13,9},{2,6},{6,2},{1... | collective-permute-start | bytes 58376 | tf_op jit(solution)/shard_map/ppermute | solution.py:25
  11.1 4.8 %collective-permute-start.1 = (bf16[4,2432]{1,0:T(4,128)(2,1)S(1)}, bf16[4,2432]{1,0:T(4,128)(2,1)S(1)}, u32[]{:S(2)}, u32[]{:S(2)}) collective-permute-start(bf16[4,2432]{1,0:T(4,128)(2,1)S(1)} %get-tuple-element.9), channel_id=1, source_target_pairs={{0,8},{4,12},{8,0},{12,4},{1,9},{5,13},{9,1},{13,5},{2,10},{6,14},... | collective-permute-start | bytes 58376 | tf_op jit(solution)/shard_map/ppermute | solution.py:25
  13.7 5.6 %collective-permute-start.2 = (bf16[4,2432]{1,0:T(4,128)(2,1)S(1)}, bf16[4,2432]{1,0:T(4,128)(2,1)S(1)}, u32[]{:S(2)}, u32[]{:S(2)}) collective-permute-start(bf16[4,2432]{1,0:T(4,128)(2,1)S(1)} %get-tuple-element.8), channel_id=1, source_target_pairs={{0,12},{4,8},{8,4},{12,0},{1,13},{5,9},{9,5},{13,1},{2,14},{6,10},... | collective-permute-start | bytes 58376 | tf_op jit(solution)/shard_map/ppermute | solution.py:25
  21.3 17.4 %copy-start.1 = (f32[4,4,128,128]{3,2,1,0:T(8,128)}, f32[4,4,128,128]{3,2,1,0:T(8,128)S(1)}, u32[]{:S(2)}) copy-start(f32[4,4,128,128]{3,2,1,0:T(8,128)S(1)} %multiply_add_fusion) | copy-start | bytes 3145732
  22.5 4.5 %collective-permute-start.3 = (bf16[4,512]{1,0:T(4,128)(2,1)S(1)}, bf16[4,512]{1,0:T(4,128)(2,1)S(1)}, u32[]{:S(2)}, u32[]{:S(2)}) collective-permute-start(bf16[4,512]{1,0:T(4,128)(2,1)S(1)} %bitcast.57), channel_id=1, source_target_pairs={{0,4},{4,0},{8,12},{12,8},{1,5},{5,1},{9,13},{13,9},{2,6},{6,2},{1... | collective-permute-start | bytes 12296 | tf_op jit(solution)/shard_map/ppermute | solution.py:25
  22.6 4.6 %collective-permute-start.4 = (bf16[4,512]{1,0:T(4,128)(2,1)S(1)}, bf16[4,512]{1,0:T(4,128)(2,1)S(1)}, u32[]{:S(2)}, u32[]{:S(2)}) collective-permute-start(bf16[4,512]{1,0:T(4,128)(2,1)S(1)} %bitcast.58), channel_id=1, source_target_pairs={{0,8},{4,12},{8,0},{12,4},{1,9},{5,13},{9,1},{13,5},{2,10},{6,14},... | collective-permute-start | bytes 12296 | tf_op jit(solution)/shard_map/ppermute | solution.py:25
  23.3 5.4 %collective-permute-start.5 = (bf16[4,512]{1,0:T(4,128)(2,1)S(1)}, bf16[4,512]{1,0:T(4,128)(2,1)S(1)}, u32[]{:S(2)}, u32[]{:S(2)}) collective-permute-start(bf16[4,512]{1,0:T(4,128)(2,1)S(1)} %bitcast.59), channel_id=1, source_target_pairs={{0,12},{4,8},{8,4},{12,0},{1,13},{5,9},{9,5},{13,1},{2,14},{6,10},... | collective-permute-start | bytes 12296 | tf_op jit(solution)/shard_map/ppermute | solution.py:25
  29.0 1.9 %collective-permute-start.6 = (bf16[16,1024]{1,0:T(8,128)(2,1)S(1)}, bf16[16,1024]{1,0:T(8,128)(2,1)S(1)}, u32[]{:S(2)}, u32[]{:S(2)}) collective-permute-start(bf16[16,1024]{1,0:T(8,128)(2,1)S(1)} %get-tuple-element.32), channel_id=1, source_target_pairs={{0,1},{1,0},{2,3},{3,2},{4,5},{5,4},{6,7},{7,6},{8,9},{9,8},{10,11... | collective-permute-start | bytes 98312 | tf_op jit(solution)/shard_map/ppermute | solution.py:25
  29.0 4.0 %collective-permute-start.7 = (bf16[16,1024]{1,0:T(8,128)(2,1)S(1)}, bf16[16,1024]{1,0:T(8,128)(2,1)S(1)}, u32[]{:S(2)}, u32[]{:S(2)}) collective-permute-start(bf16[16,1024]{1,0:T(8,128)(2,1)S(1)} %get-tuple-element.32), channel_id=1, source_target_pairs={{0,2},{1,3},{2,0},{3,1},{4,6},{5,7},{6,4},{7,5},{8,10},{9,11},{10,... | collective-permute-start | bytes 98312 | tf_op jit(solution)/shard_map/ppermute | solution.py:25
  30.6 3.3 %collective-permute-start.8 = (bf16[16,1024]{1,0:T(8,128)(2,1)S(1)}, bf16[16,1024]{1,0:T(8,128)(2,1)S(1)}, u32[]{:S(2)}, u32[]{:S(2)}) collective-permute-start(bf16[16,1024]{1,0:T(8,128)(2,1)S(1)} %get-tuple-element.32), channel_id=1, source_target_pairs={{0,3},{1,2},{2,1},{3,0},{4,7},{5,6},{6,5},{7,4},{8,11},{9,10},{10,... | collective-permute-start | bytes 98312 | tf_op jit(solution)/shard_map/ppermute | solution.py:25
  38.9 7.2 %collective-permute-start.10 = (bf16[16,1408]{1,0:T(8,128)(2,1)S(1)}, bf16[16,1408]{1,0:T(8,128)(2,1)S(1)}, u32[]{:S(2)}, u32[]{:S(2)}) collective-permute-start(bf16[16,1408]{1,0:T(8,128)(2,1)S(1)} %get-tuple-element.14), channel_id=1, source_target_pairs={{0,8},{4,12},{8,0},{12,4},{1,9},{5,13},{9,1},{13,5},{2,10},{6,14},... | collective-permute-start | bytes 135176 | tf_op jit(solution)/shard_map/ppermute | solution.py:25
  39.4 6.7 %collective-permute-start.11 = (bf16[16,1408]{1,0:T(8,128)(2,1)S(1)}, bf16[16,1408]{1,0:T(8,128)(2,1)S(1)}, u32[]{:S(2)}, u32[]{:S(2)}) collective-permute-start(bf16[16,1408]{1,0:T(8,128)(2,1)S(1)} %get-tuple-element.15), channel_id=1, source_target_pairs={{0,12},{4,8},{8,4},{12,0},{1,13},{5,9},{9,5},{13,1},{2,14},{6,10},... | collective-permute-start | bytes 135176 | tf_op jit(solution)/shard_map/ppermute | solution.py:25
  42.7 4.2 %collective-permute-start.9 = (bf16[16,1408]{1,0:T(8,128)(2,1)S(1)}, bf16[16,1408]{1,0:T(8,128)(2,1)S(1)}, u32[]{:S(2)}, u32[]{:S(2)}) collective-permute-start(bf16[16,1408]{1,0:T(8,128)(2,1)S(1)} %get-tuple-element.13), channel_id=1, source_target_pairs={{0,4},{4,0},{8,12},{12,8},{1,5},{5,1},{9,13},{13,9},{2,6},{6,2},{1... | collective-permute-start | bytes 135176 | tf_op jit(solution)/shard_map/ppermute | solution.py:25
  47.3 5.1 %collective-permute-start.12 = (bf16[16,1024]{1,0:T(8,128)(2,1)S(1)}, bf16[16,1024]{1,0:T(8,128)(2,1)S(1)}, u32[]{:S(2)}, u32[]{:S(2)}) collective-permute-start(bf16[16,1024]{1,0:T(8,128)(2,1)S(1)} %fusion.10), channel_id=1, source_target_pairs={{0,4},{4,0},{8,12},{12,8},{1,5},{5,1},{9,13},{13,9},{2,6},{6,2},{1... | collective-permute-start | bytes 98312 | tf_op jit(solution)/shard_map/ppermute | solution.py:25
  47.9 4.9 %collective-permute-start.13 = (bf16[16,1024]{1,0:T(8,128)(2,1)S(1)}, bf16[16,1024]{1,0:T(8,128)(2,1)S(1)}, u32[]{:S(2)}, u32[]{:S(2)}) collective-permute-start(bf16[16,1024]{1,0:T(8,128)(2,1)S(1)} %fusion.10), channel_id=1, source_target_pairs={{0,8},{4,12},{8,0},{12,4},{1,9},{5,13},{9,1},{13,5},{2,10},{6,14},... | collective-permute-start | bytes 98312 | tf_op jit(solution)/shard_map/ppermute | solution.py:25
  50.2 5.7 %collective-permute-start.14 = (bf16[16,1024]{1,0:T(8,128)(2,1)S(1)}, bf16[16,1024]{1,0:T(8,128)(2,1)S(1)}, u32[]{:S(2)}, u32[]{:S(2)}) collective-permute-start(bf16[16,1024]{1,0:T(8,128)(2,1)S(1)} %fusion.10), channel_id=1, source_target_pairs={{0,12},{4,8},{8,4},{12,0},{1,13},{5,9},{9,5},{13,1},{2,14},{6,10},... | collective-permute-start | bytes 98312 | tf_op jit(solution)/shard_map/ppermute | solution.py:25
  62.1 1.9 %collective-permute-start.15 = (bf16[16,1024]{1,0:T(8,128)(2,1)S(1)}, bf16[16,1024]{1,0:T(8,128)(2,1)S(1)}, u32[]{:S(2)}, u32[]{:S(2)}) collective-permute-start(bf16[16,1024]{1,0:T(8,128)(2,1)S(1)} %get-tuple-element.34), channel_id=1, source_target_pairs={{0,1},{1,0},{2,3},{3,2},{4,5},{5,4},{6,7},{7,6},{8,9},{9,8},{10,11... | collective-permute-start | bytes 98312 | tf_op jit(solution)/shard_map/ppermute | solution.py:25
  62.1 4.0 %collective-permute-start.16 = (bf16[16,1024]{1,0:T(8,128)(2,1)S(1)}, bf16[16,1024]{1,0:T(8,128)(2,1)S(1)}, u32[]{:S(2)}, u32[]{:S(2)}) collective-permute-start(bf16[16,1024]{1,0:T(8,128)(2,1)S(1)} %get-tuple-element.34), channel_id=1, source_target_pairs={{0,2},{1,3},{2,0},{3,1},{4,6},{5,7},{6,4},{7,5},{8,10},{9,11},{10,... | collective-permute-start | bytes 98312 | tf_op jit(solution)/shard_map/ppermute | solution.py:25
  63.0 3.4 %collective-permute-start.17 = (bf16[16,1024]{1,0:T(8,128)(2,1)S(1)}, bf16[16,1024]{1,0:T(8,128)(2,1)S(1)}, u32[]{:S(2)}, u32[]{:S(2)}) collective-permute-start(bf16[16,1024]{1,0:T(8,128)(2,1)S(1)} %get-tuple-element.34), channel_id=1, source_target_pairs={{0,3},{1,2},{2,1},{3,0},{4,7},{5,6},{6,5},{7,4},{8,11},{9,10},{10,... | collective-permute-start | bytes 98312 | tf_op jit(solution)/shard_map/ppermute | solution.py:25

commit v2 on v0

--- a/solution.py
+++ b/solution.py
@@ -1,10 +1,17 @@
+import functools
+
 import jax
 import jax.numpy as jnp
 from jax import lax
+from jax.experimental import pallas as pl
+from jax.experimental.pallas import tpu as pltpu
 from jax.sharding import PartitionSpec as P
 
 D = 4096
 HEADS = 16
+DIRECT = 8
+LANES = 128
+F32, BF16 = jnp.float32, jnp.bfloat16
 
 
 def turn(values, positions):
@@ -20,7 +27,7 @@
     )
 
 
-def shards(
+def shards_large(
     tokens,
     positions,
     state,
@@ -81,9 +88,258 @@
     return (layer_out, new_state)
 
 
+def swap(value, axis, n, step):
+    return lax.ppermute(value, axis, [(i, i ^ step) for i in range(n)])
+
+
+def pieces(value):
+    high = value.astype(BF16).astype(F32)
+    rest = value - high
+    middle = rest.astype(BF16).astype(F32)
+    return high, middle, rest - middle
+
+
+def reorder(n, values):
+    me = lax.axis_index("kv")
+    rows = values.shape[0]
+    block = rows // n
+    to = lax.broadcasted_iota(jnp.int32, (rows, rows), 0)
+    of = lax.broadcasted_iota(jnp.int32, (rows, rows), 1)
+    hot = ((to // block) ^ me) * block + to % block == of
+    return jnp.dot(hot.astype(F32).astype(BF16), values, preferred_element_type=F32)
+
+
+def project_kernel(n, x_ref, gain_ref, *refs):
+    weights, (own_ref, *sent), (held, sems) = refs[:4], refs[4 : 4 + n], refs[4 + n :]
+    copies = []
+    depth = x_ref.shape[1]
+    half = depth // 2
+    for i, w in enumerate(weights):
+        for j in range(2):
+            part = pl.ds(j * half, half)
+            copies.append(pltpu.make_async_copy(w.at[part], held.at[i, part], sems.at[i, j]))
+    for copy in copies:
+        copy.start()
+    x = reorder(n, x_ref[...])
+    squares = jnp.sum(x * x, axis=1, keepdims=True)
+    normed = (x * gain_ref[...]).astype(BF16)
+    rows, width = x.shape[0], held.shape[2]
+    block = rows // n
+    split = [jnp.broadcast_to(p, (rows, LANES)) for p in pieces(squares)]
+    split.append(jnp.zeros((rows, LANES), F32))
+    outs = (own_ref, *sent)
+    for i in range(4):
+        total = None
+        for j in range(2):
+            copies[2 * i + j].wait()
+            part = slice(j * half, (j + 1) * half)
+            term = jnp.dot(normed[:, part], held[i, part], preferred_element_type=F32)
+            total = term if total is None else total + term
+        for s, out in enumerate(outs):
+            here = slice(i * block, (i + 1) * block)
+            out[here, :width] = total[s * block : (s + 1) * block].astype(out.dtype)
+            out[here, width:] = split[i][s * block : (s + 1) * block].astype(out.dtype)
+
+
+def retain_kernel(n, own_ref, *refs):
+    got, (cos_ref, sin_ref, gamma_ref, state_ref, new_ref, kept_ref) = refs[: n - 1], refs[n - 1 :]
+    block, head_dev, size, _ = state_ref.shape
+    width = head_dev * size
+    total = own_ref[...]
+    for g in got:
+        total = total + g[...].astype(F32)
+    sq = total[:, width : width + 1]
+    total_sq = sq[:block] + sq[block : 2 * block] + sq[2 * block : 3 * block]
+    scale = lax.rsqrt(total_sq / D + 1e-06)
+    query, key, value, gate = (total[i * block : (i + 1) * block, :width] * scale for i in range(4))
+    cos, sin = cos_ref[...], sin_ref[...]
+    gate = gate / (1.0 + jnp.exp(-gate))
+    for h in range(head_dev):
+        at = slice(h * size, (h + 1) * size)
+        q, k = query[:, at], key[:, at]
+        q = q * cos + pltpu.roll(q, size // 2, 1) * sin
+        k = (k * cos + pltpu.roll(k, size // 2, 1) * sin) * size ** (-0.5)
+        columns = jnp.concatenate([q, k], axis=0).T
+        v = value[:, at]
+        gamma = gamma_ref[h : h + 1, :]
+        reads = []
+        for b in range(block):
+            new = gamma * state_ref[b, h] + columns[:, block + b : block + b + 1] * v[b : b + 1]
+            new_ref[b, h] = new
+            reads.append(jnp.sum(columns[:, b : b + 1] * new, axis=0, keepdims=True))
+        read = jnp.concatenate(reads, axis=0)
+        read = read * lax.rsqrt(jnp.mean(read * read, axis=1, keepdims=True) + 1e-06)
+        kept_ref[:, at] = (read * gate[:, at]).astype(BF16)
+
+
+def out_kernel(n, *refs):
+    parts, (w_ref, own_ref, sent_ref) = refs[:n], refs[n:]
+    kept = jnp.concatenate([p[...].astype(F32) for p in parts], axis=0).astype(BF16)
+    kept = reorder(n, kept).astype(BF16)
+    terms = jnp.dot(kept, w_ref[...], preferred_element_type=F32)
+    own_ref[...] = terms
+    sent_ref[...] = terms.astype(BF16)
+
+
+def up_kernel(n_tp, n, x_ref, gain_ref, w_ref, own_ref, *refs):
+    got, (mixed_ref, total_ref, *sent) = refs[: n_tp - 1], refs[n_tp - 1 :]
+    total = own_ref[...]
+    for g in got:
+        total = total + g[...].astype(F32)
+    mixed = (x_ref[...].astype(F32) + total).astype(BF16)
+    mixed_ref[...] = mixed
+    middle = mixed.astype(F32)
+    normed = (middle * gain_ref[...]).astype(BF16)
+    rows = middle.shape[0]
+    high, mid, low = pieces(jnp.sum(middle * middle, axis=1, keepdims=True))
+    lane = lax.broadcasted_iota(jnp.int32, (rows, LANES), 1)
+    split = jnp.where(lane == 0, high, jnp.where(lane == 1, mid, jnp.where(lane == 2, low, 0.0)))
+    part = w_ref.shape[1] // n
+    me = lax.axis_index("kv")
+    for s in reversed(range(n)):
+        at = pl.ds(pl.multiple_of((me ^ s) * part, part), part)
+        out = sent[s - 1] if s else total_ref
+        out[:, :part] = jnp.dot(normed, w_ref[:, at], preferred_element_type=F32).astype(out.dtype)
+        out[:, part:] = split.astype(out.dtype)
+
+
+def hidden_kernel(own_ref, *refs):
+    *got, out_ref = refs
+    total = own_ref[...]
+    for g in got:
+        total = total + g[...].astype(F32)
+    part = out_ref.shape[1]
+    sq = total[:, part : part + 1] + total[:, part + 1 : part + 2] + total[:, part + 2 : part + 3]
+    scale = lax.rsqrt(sq / D + 1e-06)
+    out_ref[...] = jnp.square(jnp.maximum(total[:, :part] * scale, 0.0)).astype(BF16)
+
+
+def down_kernel(n, *refs):
+    parts, (w_ref, own_ref, sent_ref) = refs[:n], refs[n:]
+    me = lax.axis_index("kv")
+    part = w_ref.shape[0] // n
+    total = None
+    for s, p in enumerate(parts):
+        at = pl.ds(pl.multiple_of((me ^ s) * part, part), part)
+        term = jnp.dot(p[...], w_ref[at, :], preferred_element_type=F32)
+        total = term if total is None else total + term
+    own_ref[...] = total
+    sent_ref[...] = total.astype(BF16)
+
+
+def final_kernel(mixed_ref, own_ref, *refs):
+    *got, out_ref = refs
+    total = own_ref[...]
+    for g in got:
+        total = total + g[...].astype(F32)
+    out_ref[...] = (mixed_ref[...].astype(F32) + total).astype(BF16)
+
+
+VMEM = pl.BlockSpec(memory_space=pltpu.VMEM)
+HBM = pl.BlockSpec(memory_space=pltpu.HBM)
+
+
+def call(kernel, name, outs, *args, specs=None, scratch=(), limit=8):
+    return pl.pallas_call(
+        kernel,
+        name=name,
+        out_shape=[jax.ShapeDtypeStruct(*o) for o in outs],
+        in_specs=specs or [VMEM] * len(args),
+        out_specs=[VMEM] * len(outs),
+        scratch_shapes=scratch,
+        compiler_params=pltpu.CompilerParams(vmem_limit_bytes=limit << 20),
+    )(*args)
+
+
+def near(value):
+    return pltpu.with_memory_space_constraint(value, pltpu.VMEM)
+
+
+def make_direct(n, n_tp):
+    def shards(
+        tokens, positions, state, norm_gain, w_query, w_key, w_value, w_gate, w_out, mlp_gain, w_up, w_down
+    ):
+        block, head_dev, size, _ = state.shape
+        rows, depth = tokens.shape
+        width = head_dev * size
+        wide = width + LANES
+        own, *sent = call(
+            functools.partial(project_kernel, n),
+            "project",
+            [((4 * block, wide), F32)] + [((4 * block, wide), BF16)] * (n - 1),
+            tokens,
+            norm_gain[None],
+            w_query,
+            w_key,
+            w_value,
+            w_gate,
+            specs=[VMEM, VMEM] + [HBM] * 4,
+            scratch=[pltpu.VMEM((4, depth, width), BF16), pltpu.SemaphoreType.DMA((4, 2))],
+            limit=8,
+        )
+        got = [swap(v, "kv", n, s) for s, v in enumerate(sent, 1)]
+        half = size // 2
+        freq = 10000.0 ** (-(jnp.arange(half, dtype=F32) * 2.0) / size)
+        angle = positions.astype(F32)[:, None] * freq[None, :]
+        cosine, sine = jnp.cos(angle), jnp.sin(angle)
+        cosine = jnp.concatenate([cosine, cosine], axis=1)
+        sine = jnp.concatenate([-sine, sine], axis=1)
+        heads = (lax.axis_index("tp") * head_dev + jnp.arange(head_dev)).astype(F32)
+        gamma = 1.0 - 2.0 ** (-5.0 - 5.0 * heads / (HEADS - 1))
+        gamma = jnp.broadcast_to(gamma[:, None], (head_dev, size))
+        new_state, kept = call(
+            functools.partial(retain_kernel, n),
+            "retain",
+            [(state.shape, F32), ((block, width), BF16)],
+            own,
+            *got,
+            cosine,
+            sine,
+            gamma,
+            near(state),
+        )
+        kept = [kept] + [swap(kept, "kv", n, s) for s in range(1, n)]
+        own, sent = call(
+            functools.partial(out_kernel, n),
+            "out",
+            [((rows, depth), F32), ((rows, depth), BF16)],
+            *kept,
+            near(w_out),
+        )
+        got = [swap(sent, "tp", n_tp, s) for s in range(1, n_tp)]
+        part = w_up.shape[1] // n
+        mixed, own, *sent = call(
+            functools.partial(up_kernel, n_tp, n),
+            "up",
+            [((rows, depth), BF16), ((rows, part + LANES), F32)] + [((rows, part + LANES), BF16)] * (n - 1),
+            tokens,
+            mlp_gain[None],
+            near(w_up),
+            own,
+            *got,
+        )
+        got = [swap(v, "kv", n, s) for s, v in enumerate(sent, 1)]
+        (hidden,) = call(hidden_kernel, "hidden", [((rows, part), BF16)], own, *got)
+        hidden = [hidden] + [swap(hidden, "kv", n, s) for s in range(1, n)]
+        own, sent = call(
+            functools.partial(down_kernel, n),
+            "down",
+            [((rows, depth), F32), ((rows, depth), BF16)],
+            *hidden,
+            near(w_down),
+        )
+        got = [swap(sent, "tp", n_tp, s) for s in range(1, n_tp)]
+        (layer_out,) = call(final_kernel, "final", [((rows, depth), BF16)], mixed, own, *got)
+        return (layer_out, new_state)
+
+    return shards
+
+
 def solution(mesh):
+    n_kv, n_tp = mesh.shape["kv"], mesh.shape["tp"]
+    direct = all(n <= DIRECT and n & (n - 1) == 0 for n in (n_kv, n_tp))
     return jax.shard_map(
-        shards,
+        make_direct(n_kv, n_tp) if direct else shards_large,
         mesh=mesh,
         in_specs=(
             P("grp", "kv"),

time: 189 us -> 63.3 us (0.33)
  waiting for transfers between devices: 107 us -> 17.1 us
  blocking collectives: 38.5 us -> 0 us
  starting transfers between devices: 0.16 us -> 22.7 us
  matrix products: 18.6 us -> 0 us
  between operations: 14.5 us -> 0.69 us
  local copies, waits for them, and re-layouts: 1.33 us -> 13.7 us
  Pallas kernels: 0 us -> 7.55 us
  other arithmetic: 7.69 us -> 0.87 us
    psum x3 -> x0, waiting for transfers between devices: 86.8 us -> none  [the longest x1 31.6 us: shards(): layer_out = (middle + lax.psum(down_terms, 'tp')).astype(jnp.bfloat16)]
    ppermute x0 -> x18, starting transfers between devices: none -> 22.7 us  [swap(): return lax.ppermute(value, axis, [(i, i ^ step) for i in range(n)])]
    unnamed x5 -> x0, waiting for transfers between devices: 20.4 us -> none
    dot_general x8 -> x0, matrix products: 18.6 us -> none  [the longest x4 6.11 us: shards(): jnp.dot(normed, weight, preferred_element_type=jnp.float32)]
    ppermute x0 -> x18, waiting for transfers between devices: none -> 17.1 us  [swap(): return lax.ppermute(value, axis, [(i, i ^ step) for i in range(n)])]
    unnamed x1 -> x0, blocking collectives: 13.5 us -> none
    all_gather x1 -> x0, blocking collectives: 13.2 us -> none  [shards(): lax.all_gather(retained, 'kv', axis=0, tiled=True)]
    unnamed x11 -> x24, local copies, waits for them, and re-layouts: 1.3 us -> 13.6 us
  transfers between devices with their start and end apart: 4 -> 18, of which waited for: 4 -> 13; matrix products, arithmetic and copies ran while one was open for 2% -> 1% of each run, Pallas kernels for 0% -> 0%
where the time goes in v2:
time: 63.3 us; the launch traced here: 62.7 us
  starting transfers between devices  22.7 us (36%)
  waiting for transfers between devices  17.1 us (27%)
  local copies, waits for them, and re-layouts  13.7 us (22%)
  Pallas kernels  7.55 us (12%)
  other arithmetic  0.87 us (1%)
  between operations  0.69 us (1%)
    ppermute x18, starting transfers between devices, swap(): return lax.ppermute(value, axis, [(i, i ^ step) for i in range(n)])  22.7 us
    ppermute x18, waiting for transfers between devices, swap(): return lax.ppermute(value, axis, [(i, i ^ step) for i in range(n)])  17.1 us
    unnamed x24, local copies, waits for them, and re-layouts  13.6 us
    pallas_call x7, Pallas kernels, call(): pl.pallas_call(kernel, name=name, out_shape=[jax.ShapeDtypeStruct(*o) for...  7.55 us
  transfers between devices with their start and end apart: 18, of which 13 were waited for; matrix products, arithmetic and copies ran while one was open for 1% of the time, Pallas kernels for 0%

profile of v2, /device:TPU:0, one launch (start us, length us, event | category | flops | bytes accessed | tf_op | source)
XLA Modules:
  0.0 62.7 jit_solution(1450644518436374478)
XLA Ops:
  0.6 0.0 copy-start.2
  0.6 1.2 %copy-done.2 = bf16[1024,512]{1,0:T(8,128)(2,1)S(1)} copy-done((bf16[1024,512]{1,0:T(8,128)(2,1)S(1)}, bf16[1024,512]{1,0:T(8,128)(2,1)}, u32[]{:S(2)}) %copy-start.2) | copy-done | bytes 1048600
  1.9 0.0 copy-start.3
  1.9 1.2 %copy-done.3 = bf16[1024,512]{1,0:T(8,128)(2,1)S(1)} copy-done((bf16[1024,512]{1,0:T(8,128)(2,1)S(1)}, bf16[1024,512]{1,0:T(8,128)(2,1)}, u32[]{:S(2)}) %copy-start.3) | copy-done | bytes 1048600
  3.1 0.0 copy-start.4
  3.1 1.2 %copy-done.4 = bf16[1024,512]{1,0:T(8,128)(2,1)S(1)} copy-done((bf16[1024,512]{1,0:T(8,128)(2,1)S(1)}, bf16[1024,512]{1,0:T(8,128)(2,1)}, u32[]{:S(2)}) %copy-start.4) | copy-done | bytes 1048600
  4.3 0.0 copy-start.5
  4.3 1.2 %copy-done.5 = bf16[1024,512]{1,0:T(8,128)(2,1)S(1)} copy-done((bf16[1024,512]{1,0:T(8,128)(2,1)S(1)}, bf16[1024,512]{1,0:T(8,128)(2,1)}, u32[]{:S(2)}) %copy-start.5) | copy-done | bytes 1048600
  5.5 0.0 copy-start.8
  5.5 0.8 %copy-done.8 = bf16[16,1024]{1,0:T(8,128)(2,1)S(1)} copy-done((bf16[16,1024]{1,0:T(8,128)(2,1)S(1)}, bf16[16,1024]{1,0:T(8,128)(2,1)}, u32[]{:S(2)}) %copy-start.8) | copy-done | bytes 32792
  6.3 0.7 %copy-done.10 = f32[1024]{0:T(1024)S(1)} copy-done((f32[1024]{0:T(1024)S(1)}, f32[1024]{0:T(1024)}, u32[]{:S(2)}) %copy-start.10) | copy-done | bytes 4120
  7.0 1.7 %project.1 = (f32[16,640]{1,0:T(8,128)S(1)}, bf16[16,640]{1,0:T(8,128)(2,1)S(1)}, bf16[16,640]{1,0:T(8,128)(2,1)S(1)}, bf16[16,640]{1,0:T(8,128)(2,1)S(1)}) custom-call(bf16[16,1024]{1,0:T(8,128)(2,1)S(1)} %copy-done.8, f32[1,1024]{1,0:T(1,128)S(1)} %bitcast.2, bf16[1024,512]{1,0:T(8,128)(2,1)S(1)} %copy-done.2, bf16[1024,512]{1,0:T(8,128)(2,1)S(1)} %copy-done.3, ...), custom_call_target="tpu_custom_call" | custom-call | tf_op jit(solution)/shard_map/project/pallas_call | solution.py:243
  8.7 3.1 %collective-permute-start = (bf16[16,640]{1,0:T(8,128)(2,1)S(1)}, bf16[16,640]{1,0:T(8,128)(2,1)S(1)}, u32[]{:S(2)}, u32[]{:S(2)}) collective-permute-start(bf16[16,640]{1,0:T(8,128)(2,1)S(1)} %get-tuple-element.18), channel_id=1, source_target_pairs={{0,4},{4,0},{8,12},{12,8},{1,5},{5,1},{9,13},{13,9},{2,6},{6,2},{1... | collective-permute-start | bytes 61448 | tf_op jit(solution)/shard_map/ppermute | solution.py:92
  11.8 2.6 %collective-permute-start.1 = (bf16[16,640]{1,0:T(8,128)(2,1)S(1)}, bf16[16,640]{1,0:T(8,128)(2,1)S(1)}, u32[]{:S(2)}, u32[]{:S(2)}) collective-permute-start(bf16[16,640]{1,0:T(8,128)(2,1)S(1)} %get-tuple-element.19), channel_id=1, source_target_pairs={{0,8},{4,12},{8,0},{12,4},{1,9},{5,13},{9,1},{13,5},{2,10},{6,14},... | collective-permute-start | bytes 61448 | tf_op jit(solution)/shard_map/ppermute | solution.py:92
  14.4 0.0 collective-permute-start.2
  14.4 0.7 %convert_element_type.10 = f32[4]{0:T(128)S(1)} convert(s32[4]{0:T(128)} %param.13) | non-fusion elementwise | flops 4 | bytes 32 | tf_op jit(solution)/shard_map/convert_element_type | solution.py:283
  15.1 0.1 fusion
  15.2 0.1 pad_maximum_fusion
  15.3 0.0 collective-permute-done.refs_0_
  15.3 1.4 %collective-permute-done.1.refs_1_ = bf16[16,640]{1,0:T(8,128)(2,1)S(1)} collective-permute-done((bf16[16,640]{1,0:T(8,128)(2,1)S(1)}, bf16[16,640]{1,0:T(8,128)(2,1)S(1)}, u32[]{:S(2)}, u32[]{:S(2)}) %collective-permute-start.1) | collective-permute-done | bytes 20512 | tf_op jit(solution)/shard_map/ppermute | solution.py:92
  16.7 3.3 %collective-permute-done.2.refs_2_ = bf16[16,640]{1,0:T(8,128)(2,1)S(1)} collective-permute-done((bf16[16,640]{1,0:T(8,128)(2,1)S(1)}, bf16[16,640]{1,0:T(8,128)(2,1)S(1)}, u32[]{:S(2)}, u32[]{:S(2)}) %collective-permute-start.2) | collective-permute-done | bytes 20512 | tf_op jit(solution)/shard_map/ppermute | solution.py:92
  20.0 0.1 broadcast_in_dim.16.refs_5_
  20.1 1.2 %copy-done.6 = f32[4,4,128,128]{3,2,1,0:T(8,128)S(1)} copy-done((f32[4,4,128,128]{3,2,1,0:T(8,128)S(1)}, f32[4,4,128,128]{3,2,1,0:T(8,128)}, u32[]{:S(2)}) %copy-start.6) | copy-done | bytes 1048600
  21.3 2.3 %retain.1 = (f32[4,4,128,128]{3,2,1,0:T(8,128)}, bf16[4,512]{1,0:T(4,128)(2,1)S(1)}) custom-call(f32[16,640]{1,0:T(8,128)S(1)} %get-tuple-element.17.own_ref, bf16[16,640]{1,0:T(8,128)(2,1)S(1)} %collective-permute-done.refs_0_, bf16[16,640]{1,0:T(8,128)(2,1)S(1)} %collective-permute-done.1.refs_1_, bf16[16,640]{1,0:T(8,128)(2,1)S(1)} %collective-permute-done.2.refs_2_, ...), custom_call_target="tpu_custom_call" | custom-call | tf_op jit(solution)/shard_map/retain/pallas_call | solution.py:243
  23.6 0.2 collective-permute-start.5
  23.8 0.0 collective-permute-start.4
  23.8 4.2 %collective-permute-start.3 = (bf16[4,512]{1,0:T(4,128)(2,1)S(1)}, bf16[4,512]{1,0:T(4,128)(2,1)S(1)}, u32[]{:S(2)}, u32[]{:S(2)}) collective-permute-start(bf16[4,512]{1,0:T(4,128)(2,1)S(1)} %get-tuple-element.21.refs_0_), channel_id=1, source_target_pairs={{0,4},{4,0},{8,12},{12,8},{1,5},{5,1},{9,13},{13,9},{2,6},{6,2},{1... | collective-permute-start | bytes 12296 | tf_op jit(solution)/shard_map/ppermute | solution.py:92
  28.0 1.0 %collective-permute-done.5.refs_3_ = bf16[4,512]{1,0:T(4,128)(2,1)S(1)} collective-permute-done((bf16[4,512]{1,0:T(4,128)(2,1)S(1)}, bf16[4,512]{1,0:T(4,128)(2,1)S(1)}, u32[]{:S(2)}, u32[]{:S(2)}) %collective-permute-start.5) | collective-permute-done | bytes 4128 | tf_op jit(solution)/shard_map/ppermute | solution.py:92
  29.0 0.0 collective-permute-done.4.refs_2_
  29.0 0.6 collective-permute-done.3.refs_1_
  29.6 1.2 %copy-done.7 = bf16[512,1024]{1,0:T(8,128)(2,1)S(1)} copy-done((bf16[512,1024]{1,0:T(8,128)(2,1)S(1)}, bf16[512,1024]{1,0:T(8,128)(2,1)}, u32[]{:S(2)}) %copy-start.7) | copy-done | bytes 1048600
  30.8 0.3 out.1
  31.1 0.0 collective-permute-start.8
  31.1 1.5 %collective-permute-start.7 = (bf16[16,1024]{1,0:T(8,128)(2,1)S(1)}, bf16[16,1024]{1,0:T(8,128)(2,1)S(1)}, u32[]{:S(2)}, u32[]{:S(2)}) collective-permute-start(bf16[16,1024]{1,0:T(8,128)(2,1)S(1)} %get-tuple-element.23), channel_id=1, source_target_pairs={{0,2},{1,3},{2,0},{3,1},{4,6},{5,7},{6,4},{7,5},{8,10},{9,11},{10,... | collective-permute-start | bytes 98312 | tf_op jit(solution)/shard_map/ppermute | solution.py:92
  32.7 0.3 collective-permute-start.6
  33.0 1.8 %collective-permute-done.8.refs_2_ = bf16[16,1024]{1,0:T(8,128)(2,1)S(1)} collective-permute-done((bf16[16,1024]{1,0:T(8,128)(2,1)S(1)}, bf16[16,1024]{1,0:T(8,128)(2,1)S(1)}, u32[]{:S(2)}, u32[]{:S(2)}) %collective-permute-start.8) | collective-permute-done | bytes 32800 | tf_op jit(solution)/shard_map/ppermute | solution.py:92
  34.8 0.4 collective-permute-done.7.refs_1_
  35.2 0.0 collective-permute-done.6.refs_0_
  35.2 3.4 %copy-done = bf16[1024,4096]{1,0:T(8,128)(2,1)S(1)} copy-done((bf16[1024,4096]{1,0:T(8,128)(2,1)S(1)}, bf16[1024,4096]{1,0:T(8,128)(2,1)}, u32[]{:S(2)}) %copy-start) | copy-done | bytes 8388632
  38.6 0.8 %copy-done.9 = bf16[16,1024]{1,0:T(8,128)(2,1)S(1)} copy-done((bf16[16,1024]{1,0:T(8,128)(2,1)S(1)}, bf16[16,1024]{1,0:T(8,128)(2,1)}, u32[]{:S(2)}) %copy-start.9) | copy-done | bytes 32792
  39.3 0.7 %copy-done.11 = f32[1024]{0:T(1024)S(1)} copy-done((f32[1024]{0:T(1024)S(1)}, f32[1024]{0:T(1024)}, u32[]{:S(2)}) %copy-start.11) | copy-done | bytes 4120
  40.0 1.2 %up.1 = (bf16[16,1024]{1,0:T(8,128)(2,1)S(1)}, f32[16,1152]{1,0:T(8,128)S(1)}, bf16[16,1152]{1,0:T(8,128)(2,1)S(1)}, bf16[16,1152]{1,0:T(8,128)(2,1)S(1)}, bf16[16,1152]{1,0:T(8,128)(2,1)S(1)}) custom-call(bf16[16,1024]{1,0:T(8,128)(2,1)S(1)} %copy-done.9, f32[1,1024]{1,0:T(1,128)S(1)} %bitcast.3, bf16[1024,4096]{1,0:T(8,128)(2,1)S(1)} %copy-done, ...), custom_call_target="tpu_custom_call" | custom-call | tf_op jit(solution)/shard_map/up/pallas_call | solution.py:243
  41.2 2.0 %collective-permute-start.9 = (bf16[16,1152]{1,0:T(8,128)(2,1)S(1)}, bf16[16,1152]{1,0:T(8,128)(2,1)S(1)}, u32[]{:S(2)}, u32[]{:S(2)}) collective-permute-start(bf16[16,1152]{1,0:T(8,128)(2,1)S(1)} %get-tuple-element.26), channel_id=1, source_target_pairs={{0,4},{4,0},{8,12},{12,8},{1,5},{5,1},{9,13},{13,9},{2,6},{6,2},{1... | collective-permute-start | bytes 110600 | tf_op jit(solution)/shard_map/ppermute | solution.py:92
  43.3 0.9 %collective-permute-start.10 = (bf16[16,1152]{1,0:T(8,128)(2,1)S(1)}, bf16[16,1152]{1,0:T(8,128)(2,1)S(1)}, u32[]{:S(2)}, u32[]{:S(2)}) collective-permute-start(bf16[16,1152]{1,0:T(8,128)(2,1)S(1)} %get-tuple-element.27), channel_id=1, source_target_pairs={{0,8},{4,12},{8,0},{12,4},{1,9},{5,13},{9,1},{13,5},{2,10},{6,14},... | collective-permute-start | bytes 110600 | tf_op jit(solution)/shard_map/ppermute | solution.py:92
  44.2 1.5 %collective-permute-start.11 = (bf16[16,1152]{1,0:T(8,128)(2,1)S(1)}, bf16[16,1152]{1,0:T(8,128)(2,1)S(1)}, u32[]{:S(2)}, u32[]{:S(2)}) collective-permute-start(bf16[16,1152]{1,0:T(8,128)(2,1)S(1)} %get-tuple-element.28), channel_id=1, source_target_pairs={{0,12},{4,8},{8,4},{12,0},{1,13},{5,9},{9,5},{13,1},{2,14},{6,10},... | collective-permute-start | bytes 110600 | tf_op jit(solution)/shard_map/ppermute | solution.py:92
  45.7 0.0 collective-permute-done.9.refs_0_
  45.7 3.2 %collective-permute-done.10.refs_1_ = bf16[16,1152]{1,0:T(8,128)(2,1)S(1)} collective-permute-done((bf16[16,1152]{1,0:T(8,128)(2,1)S(1)}, bf16[16,1152]{1,0:T(8,128)(2,1)S(1)}, u32[]{:S(2)}, u32[]{:S(2)}) %collective-permute-start.10) | collective-permute-done | bytes 36896 | tf_op jit(solution)/shard_map/ppermute | solution.py:92
  48.9 1.0 %collective-permute-done.11.refs_2_ = bf16[16,1152]{1,0:T(8,128)(2,1)S(1)} collective-permute-done((bf16[16,1152]{1,0:T(8,128)(2,1)S(1)}, bf16[16,1152]{1,0:T(8,128)(2,1)S(1)}, u32[]{:S(2)}, u32[]{:S(2)}) %collective-permute-start.11) | collective-permute-done | bytes 36896 | tf_op jit(solution)/shard_map/ppermute | solution.py:92
  49.9 0.2 hidden.1.refs_0_
  50.1 1.6 %collective-permute-start.14 = (bf16[16,1024]{1,0:T(8,128)(2,1)S(1)}, bf16[16,1024]{1,0:T(8,128)(2,1)S(1)}, u32[]{:S(2)}, u32[]{:S(2)}) collective-permute-start(bf16[16,1024]{1,0:T(8,128)(2,1)S(1)} %hidden.1.refs_0_), channel_id=1, source_target_pairs={{0,12},{4,8},{8,4},{12,0},{1,13},{5,9},{9,5},{13,1},{2,14},{6,10},... | collective-permute-start | bytes 98312 | tf_op jit(solution)/shard_map/ppermute | solution.py:92
  51.7 0.0 collective-permute-start.13
  51.7 2.9 %collective-permute-start.12 = (bf16[16,1024]{1,0:T(8,128)(2,1)S(1)}, bf16[16,1024]{1,0:T(8,128)(2,1)S(1)}, u32[]{:S(2)}, u32[]{:S(2)}) collective-permute-start(bf16[16,1024]{1,0:T(8,128)(2,1)S(1)} %hidden.1.refs_0_), channel_id=1, source_target_pairs={{0,4},{4,0},{8,12},{12,8},{1,5},{5,1},{9,13},{13,9},{2,6},{6,2},{1... | collective-permute-start | bytes 98312 | tf_op jit(solution)/shard_map/ppermute | solution.py:92
  54.5 1.3 %collective-permute-done.14.refs_3_ = bf16[16,1024]{1,0:T(8,128)(2,1)S(1)} collective-permute-done((bf16[16,1024]{1,0:T(8,128)(2,1)S(1)}, bf16[16,1024]{1,0:T(8,128)(2,1)S(1)}, u32[]{:S(2)}, u32[]{:S(2)}) %collective-permute-start.14) | collective-permute-done | bytes 32800 | tf_op jit(solution)/shard_map/ppermute | solution.py:92
  55.9 0.8 %collective-permute-done.13.refs_2_ = bf16[16,1024]{1,0:T(8,128)(2,1)S(1)} collective-permute-done((bf16[16,1024]{1,0:T(8,128)(2,1)S(1)}, bf16[16,1024]{1,0:T(8,128)(2,1)S(1)}, u32[]{:S(2)}, u32[]{:S(2)}) %collective-permute-start.13) | collective-permute-done | bytes 32800 | tf_op jit(solution)/shard_map/ppermute | solution.py:92
  56.7 0.1 collective-permute-done.12.refs_1_
  56.8 0.0 copy-done.1
  56.8 1.2 %down.1 = (f32[16,1024]{1,0:T(8,128)S(1)}, bf16[16,1024]{1,0:T(8,128)(2,1)S(1)}) custom-call(bf16[16,1024]{1,0:T(8,128)(2,1)S(1)} %hidden.1.refs_0_, bf16[16,1024]{1,0:T(8,128)(2,1)S(1)} %collective-permute-done.12.refs_1_, bf16[16,1024]{1,0:T(8,128)(2,1)S(1)} %collective-permute-done.13.refs_2_, bf16[16,1024]{1,0:T(8,128)(2,1)S(1)} %collective-permute-done.14.refs_3_, ...), custom_call_target="tpu_custom_call" | custom-call | tf_op jit(solution)/shard_map/down/pallas_call | solution.py:243
  58.0 0.0 collective-permute-start.17
  58.0 1.5 %collective-permute-start.16 = (bf16[16,1024]{1,0:T(8,128)(2,1)S(1)}, bf16[16,1024]{1,0:T(8,128)(2,1)S(1)}, u32[]{:S(2)}, u32[]{:S(2)}) collective-permute-start(bf16[16,1024]{1,0:T(8,128)(2,1)S(1)} %get-tuple-element.30), channel_id=1, source_target_pairs={{0,2},{1,3},{2,0},{3,1},{4,6},{5,7},{6,4},{7,5},{8,10},{9,11},{10,... | collective-permute-start | bytes 98312 | tf_op jit(solution)/shard_map/ppermute | solution.py:92
  59.5 0.3 collective-permute-start.15
  59.9 1.8 %collective-permute-done.17.refs_2_ = bf16[16,1024]{1,0:T(8,128)(2,1)S(1)} collective-permute-done((bf16[16,1024]{1,0:T(8,128)(2,1)S(1)}, bf16[16,1024]{1,0:T(8,128)(2,1)S(1)}, u32[]{:S(2)}, u32[]{:S(2)}) %collective-permute-start.17) | collective-permute-done | bytes 32800 | tf_op jit(solution)/shard_map/ppermute | solution.py:92
  61.6 0.4 collective-permute-done.16.refs_1_
  62.0 0.0 collective-permute-done.15.refs_0_
  62.0 0.6 %final.1 = bf16[16,1024]{1,0:T(8,128)(2,1)} custom-call(bf16[16,1024]{1,0:T(8,128)(2,1)S(1)} %get-tuple-element.24.mixed_ref, f32[16,1024]{1,0:T(8,128)S(1)} %get-tuple-element.29.own_ref, bf16[16,1024]{1,0:T(8,128)(2,1)S(1)} %collective-permute-done.15.refs_0_, bf16[16,1024]{1,0:T(8,128)(2,1)S(1)} %collective-permute-done.16.refs_1_, ...), custom_call_target="tpu_custom_call" | custom-call | tf_op jit(solution)/shard_map/final/pallas_call | solution.py:243
  (9 shorter events, 0.0 us)
Async XLA Ops:
  0.6 1.2 %copy-start.2 = (bf16[1024,512]{1,0:T(8,128)(2,1)S(1)}, bf16[1024,512]{1,0:T(8,128)(2,1)}, u32[]{:S(2)}) copy-start(bf16[1024,512]{1,0:T(8,128)(2,1)} %refs_0_.1) | copy-start | bytes 3145732
  1.9 1.2 %copy-start.3 = (bf16[1024,512]{1,0:T(8,128)(2,1)S(1)}, bf16[1024,512]{1,0:T(8,128)(2,1)}, u32[]{:S(2)}) copy-start(bf16[1024,512]{1,0:T(8,128)(2,1)} %refs_1_.1) | copy-start | bytes 3145732
  3.1 1.2 %copy-start.4 = (bf16[1024,512]{1,0:T(8,128)(2,1)S(1)}, bf16[1024,512]{1,0:T(8,128)(2,1)}, u32[]{:S(2)}) copy-start(bf16[1024,512]{1,0:T(8,128)(2,1)} %refs_2_.1) | copy-start | bytes 3145732
  4.3 1.2 %copy-start.5 = (bf16[1024,512]{1,0:T(8,128)(2,1)S(1)}, bf16[1024,512]{1,0:T(8,128)(2,1)}, u32[]{:S(2)}) copy-start(bf16[1024,512]{1,0:T(8,128)(2,1)} %refs_3_.1) | copy-start | bytes 3145732
  5.5 0.8 %copy-start.8 = (bf16[16,1024]{1,0:T(8,128)(2,1)S(1)}, bf16[16,1024]{1,0:T(8,128)(2,1)}, u32[]{:S(2)}) copy-start(bf16[16,1024]{1,0:T(8,128)(2,1)} %x_ref.3) | copy-start | bytes 98308
  6.3 0.7 %copy-start.10 = (f32[1024]{0:T(1024)S(1)}, f32[1024]{0:T(1024)}, u32[]{:S(2)}) copy-start(f32[1024]{0:T(1024)} %param.15) | copy-start | bytes 12292
  8.7 6.6 %collective-permute-start = (bf16[16,640]{1,0:T(8,128)(2,1)S(1)}, bf16[16,640]{1,0:T(8,128)(2,1)S(1)}, u32[]{:S(2)}, u32[]{:S(2)}) collective-permute-start(bf16[16,640]{1,0:T(8,128)(2,1)S(1)} %get-tuple-element.18), channel_id=1, source_target_pairs={{0,4},{4,0},{8,12},{12,8},{1,5},{5,1},{9,13},{13,9},{2,6},{6,2},{1... | collective-permute-start | bytes 61448 | tf_op jit(solution)/shard_map/ppermute | solution.py:92
  11.8 4.9 %collective-permute-start.1 = (bf16[16,640]{1,0:T(8,128)(2,1)S(1)}, bf16[16,640]{1,0:T(8,128)(2,1)S(1)}, u32[]{:S(2)}, u32[]{:S(2)}) collective-permute-start(bf16[16,640]{1,0:T(8,128)(2,1)S(1)} %get-tuple-element.19), channel_id=1, source_target_pairs={{0,8},{4,12},{8,0},{12,4},{1,9},{5,13},{9,1},{13,5},{2,10},{6,14},... | collective-permute-start | bytes 61448 | tf_op jit(solution)/shard_map/ppermute | solution.py:92
  14.4 5.6 %collective-permute-start.2 = (bf16[16,640]{1,0:T(8,128)(2,1)S(1)}, bf16[16,640]{1,0:T(8,128)(2,1)S(1)}, u32[]{:S(2)}, u32[]{:S(2)}) collective-permute-start(bf16[16,640]{1,0:T(8,128)(2,1)S(1)} %get-tuple-element.20), channel_id=1, source_target_pairs={{0,12},{4,8},{8,4},{12,0},{1,13},{5,9},{9,5},{13,1},{2,14},{6,10},... | collective-permute-start | bytes 61448 | tf_op jit(solution)/shard_map/ppermute | solution.py:92
  20.1 1.2 %copy-start.6 = (f32[4,4,128,128]{3,2,1,0:T(8,128)S(1)}, f32[4,4,128,128]{3,2,1,0:T(8,128)}, u32[]{:S(2)}) copy-start(f32[4,4,128,128]{3,2,1,0:T(8,128)} %refs_6_.1) | copy-start | bytes 3145732
  23.6 5.4 %collective-permute-start.5 = (bf16[4,512]{1,0:T(4,128)(2,1)S(1)}, bf16[4,512]{1,0:T(4,128)(2,1)S(1)}, u32[]{:S(2)}, u32[]{:S(2)}) collective-permute-start(bf16[4,512]{1,0:T(4,128)(2,1)S(1)} %get-tuple-element.21.refs_0_), channel_id=1, source_target_pairs={{0,12},{4,8},{8,4},{12,0},{1,13},{5,9},{9,5},{13,1},{2,14},{6,10},... | collective-permute-start | bytes 12296 | tf_op jit(solution)/shard_map/ppermute | solution.py:92
  23.8 5.2 %collective-permute-start.4 = (bf16[4,512]{1,0:T(4,128)(2,1)S(1)}, bf16[4,512]{1,0:T(4,128)(2,1)S(1)}, u32[]{:S(2)}, u32[]{:S(2)}) collective-permute-start(bf16[4,512]{1,0:T(4,128)(2,1)S(1)} %get-tuple-element.21.refs_0_), channel_id=1, source_target_pairs={{0,8},{4,12},{8,0},{12,4},{1,9},{5,13},{9,1},{13,5},{2,10},{6,14},... | collective-permute-start | bytes 12296 | tf_op jit(solution)/shard_map/ppermute | solution.py:92
  23.8 5.8 %collective-permute-start.3 = (bf16[4,512]{1,0:T(4,128)(2,1)S(1)}, bf16[4,512]{1,0:T(4,128)(2,1)S(1)}, u32[]{:S(2)}, u32[]{:S(2)}) collective-permute-start(bf16[4,512]{1,0:T(4,128)(2,1)S(1)} %get-tuple-element.21.refs_0_), channel_id=1, source_target_pairs={{0,4},{4,0},{8,12},{12,8},{1,5},{5,1},{9,13},{13,9},{2,6},{6,2},{1... | collective-permute-start | bytes 12296 | tf_op jit(solution)/shard_map/ppermute | solution.py:92
  29.6 1.2 %copy-start.7 = (bf16[512,1024]{1,0:T(8,128)(2,1)S(1)}, bf16[512,1024]{1,0:T(8,128)(2,1)}, u32[]{:S(2)}) copy-start(bf16[512,1024]{1,0:T(8,128)(2,1)} %refs_4_.2) | copy-start | bytes 3145732
  31.1 3.7 %collective-permute-start.8 = (bf16[16,1024]{1,0:T(8,128)(2,1)S(1)}, bf16[16,1024]{1,0:T(8,128)(2,1)S(1)}, u32[]{:S(2)}, u32[]{:S(2)}) collective-permute-start(bf16[16,1024]{1,0:T(8,128)(2,1)S(1)} %get-tuple-element.23), channel_id=1, source_target_pairs={{0,3},{1,2},{2,1},{3,0},{4,7},{5,6},{6,5},{7,4},{8,11},{9,10},{10,... | collective-permute-start | bytes 98312 | tf_op jit(solution)/shard_map/ppermute | solution.py:92
  31.1 4.0 %collective-permute-start.7 = (bf16[16,1024]{1,0:T(8,128)(2,1)S(1)}, bf16[16,1024]{1,0:T(8,128)(2,1)S(1)}, u32[]{:S(2)}, u32[]{:S(2)}) collective-permute-start(bf16[16,1024]{1,0:T(8,128)(2,1)S(1)} %get-tuple-element.23), channel_id=1, source_target_pairs={{0,2},{1,3},{2,0},{3,1},{4,6},{5,7},{6,4},{7,5},{8,10},{9,11},{10,... | collective-permute-start | bytes 98312 | tf_op jit(solution)/shard_map/ppermute | solution.py:92
  32.7 2.5 %collective-permute-start.6 = (bf16[16,1024]{1,0:T(8,128)(2,1)S(1)}, bf16[16,1024]{1,0:T(8,128)(2,1)S(1)}, u32[]{:S(2)}, u32[]{:S(2)}) collective-permute-start(bf16[16,1024]{1,0:T(8,128)(2,1)S(1)} %get-tuple-element.23), channel_id=1, source_target_pairs={{0,1},{1,0},{2,3},{3,2},{4,5},{5,4},{6,7},{7,6},{8,9},{9,8},{10,11... | collective-permute-start | bytes 98312 | tf_op jit(solution)/shard_map/ppermute | solution.py:92
  35.2 3.4 %copy-start = (bf16[1024,4096]{1,0:T(8,128)(2,1)S(1)}, bf16[1024,4096]{1,0:T(8,128)(2,1)}, u32[]{:S(2)}) copy-start(bf16[1024,4096]{1,0:T(8,128)(2,1)} %w_ref.1) | copy-start | bytes 25165828
  38.6 0.8 %copy-start.9 = (bf16[16,1024]{1,0:T(8,128)(2,1)S(1)}, bf16[16,1024]{1,0:T(8,128)(2,1)}, u32[]{:S(2)}) copy-start(bf16[16,1024]{1,0:T(8,128)(2,1)} %x_ref.3) | copy-start | bytes 98308
  39.3 0.7 %copy-start.11 = (f32[1024]{0:T(1024)S(1)}, f32[1024]{0:T(1024)}, u32[]{:S(2)}) copy-start(f32[1024]{0:T(1024)} %param.21) | copy-start | bytes 12292
  40.0 16.8 %copy-start.1 = (bf16[4096,1024]{1,0:T(8,128)(2,1)S(1)}, bf16[4096,1024]{1,0:T(8,128)(2,1)}, u32[]{:S(2)}) copy-start(bf16[4096,1024]{1,0:T(8,128)(2,1)} %refs_4_.3) | copy-start | bytes 25165828
  41.2 4.5 %collective-permute-start.9 = (bf16[16,1152]{1,0:T(8,128)(2,1)S(1)}, bf16[16,1152]{1,0:T(8,128)(2,1)S(1)}, u32[]{:S(2)}, u32[]{:S(2)}) collective-permute-start(bf16[16,1152]{1,0:T(8,128)(2,1)S(1)} %get-tuple-element.26), channel_id=1, source_target_pairs={{0,4},{4,0},{8,12},{12,8},{1,5},{5,1},{9,13},{13,9},{2,6},{6,2},{1... | collective-permute-start | bytes 110600 | tf_op jit(solution)/shard_map/ppermute | solution.py:92
  43.3 5.6 %collective-permute-start.10 = (bf16[16,1152]{1,0:T(8,128)(2,1)S(1)}, bf16[16,1152]{1,0:T(8,128)(2,1)S(1)}, u32[]{:S(2)}, u32[]{:S(2)}) collective-permute-start(bf16[16,1152]{1,0:T(8,128)(2,1)S(1)} %get-tuple-element.27), channel_id=1, source_target_pairs={{0,8},{4,12},{8,0},{12,4},{1,9},{5,13},{9,1},{13,5},{2,10},{6,14},... | collective-permute-start | bytes 110600 | tf_op jit(solution)/shard_map/ppermute | solution.py:92
  44.2 5.8 %collective-permute-start.11 = (bf16[16,1152]{1,0:T(8,128)(2,1)S(1)}, bf16[16,1152]{1,0:T(8,128)(2,1)S(1)}, u32[]{:S(2)}, u32[]{:S(2)}) collective-permute-start(bf16[16,1152]{1,0:T(8,128)(2,1)S(1)} %get-tuple-element.28), channel_id=1, source_target_pairs={{0,12},{4,8},{8,4},{12,0},{1,13},{5,9},{9,5},{13,1},{2,14},{6,10},... | collective-permute-start | bytes 110600 | tf_op jit(solution)/shard_map/ppermute | solution.py:92
  50.1 5.8 %collective-permute-start.14 = (bf16[16,1024]{1,0:T(8,128)(2,1)S(1)}, bf16[16,1024]{1,0:T(8,128)(2,1)S(1)}, u32[]{:S(2)}, u32[]{:S(2)}) collective-permute-start(bf16[16,1024]{1,0:T(8,128)(2,1)S(1)} %hidden.1.refs_0_), channel_id=1, source_target_pairs={{0,12},{4,8},{8,4},{12,0},{1,13},{5,9},{9,5},{13,1},{2,14},{6,10},... | collective-permute-start | bytes 98312 | tf_op jit(solution)/shard_map/ppermute | solution.py:92
  51.7 5.0 %collective-permute-start.13 = (bf16[16,1024]{1,0:T(8,128)(2,1)S(1)}, bf16[16,1024]{1,0:T(8,128)(2,1)S(1)}, u32[]{:S(2)}, u32[]{:S(2)}) collective-permute-start(bf16[16,1024]{1,0:T(8,128)(2,1)S(1)} %hidden.1.refs_0_), channel_id=1, source_target_pairs={{0,8},{4,12},{8,0},{12,4},{1,9},{5,13},{9,1},{13,5},{2,10},{6,14},... | collective-permute-start | bytes 98312 | tf_op jit(solution)/shard_map/ppermute | solution.py:92
  51.7 5.1 %collective-permute-start.12 = (bf16[16,1024]{1,0:T(8,128)(2,1)S(1)}, bf16[16,1024]{1,0:T(8,128)(2,1)S(1)}, u32[]{:S(2)}, u32[]{:S(2)}) collective-permute-start(bf16[16,1024]{1,0:T(8,128)(2,1)S(1)} %hidden.1.refs_0_), channel_id=1, source_target_pairs={{0,4},{4,0},{8,12},{12,8},{1,5},{5,1},{9,13},{13,9},{2,6},{6,2},{1... | collective-permute-start | bytes 98312 | tf_op jit(solution)/shard_map/ppermute | solution.py:92
  58.0 3.7 %collective-permute-start.17 = (bf16[16,1024]{1,0:T(8,128)(2,1)S(1)}, bf16[16,1024]{1,0:T(8,128)(2,1)S(1)}, u32[]{:S(2)}, u32[]{:S(2)}) collective-permute-start(bf16[16,1024]{1,0:T(8,128)(2,1)S(1)} %get-tuple-element.30), channel_id=1, source_target_pairs={{0,3},{1,2},{2,1},{3,0},{4,7},{5,6},{6,5},{7,4},{8,11},{9,10},{10,... | collective-permute-start | bytes 98312 | tf_op jit(solution)/shard_map/ppermute | solution.py:92
  58.0 4.1 %collective-permute-start.16 = (bf16[16,1024]{1,0:T(8,128)(2,1)S(1)}, bf16[16,1024]{1,0:T(8,128)(2,1)S(1)}, u32[]{:S(2)}, u32[]{:S(2)}) collective-permute-start(bf16[16,1024]{1,0:T(8,128)(2,1)S(1)} %get-tuple-element.30), channel_id=1, source_target_pairs={{0,2},{1,3},{2,0},{3,1},{4,6},{5,7},{6,4},{7,5},{8,10},{9,11},{10,... | collective-permute-start | bytes 98312 | tf_op jit(solution)/shard_map/ppermute | solution.py:92
  59.5 2.5 %collective-permute-start.15 = (bf16[16,1024]{1,0:T(8,128)(2,1)S(1)}, bf16[16,1024]{1,0:T(8,128)(2,1)S(1)}, u32[]{:S(2)}, u32[]{:S(2)}) collective-permute-start(bf16[16,1024]{1,0:T(8,128)(2,1)S(1)} %get-tuple-element.30), channel_id=1, source_target_pairs={{0,1},{1,0},{2,3},{3,2},{4,5},{5,4},{6,7},{7,6},{8,9},{9,8},{10,11... | collective-permute-start | bytes 98312 | tf_op jit(solution)/shard_map/ppermute | solution.py:92

commit v3 on v2

--- a/solution.py
+++ b/solution.py
@@ -11,6 +11,7 @@
 HEADS = 16
 DIRECT = 8
 LANES = 128
+RATE = 1 << 36
 F32, BF16 = jnp.float32, jnp.bfloat16
 
 
@@ -109,19 +110,25 @@
     return jnp.dot(hot.astype(F32).astype(BF16), values, preferred_element_type=F32)
 
 
-def project_kernel(n, x_ref, gain_ref, *refs):
-    weights, (own_ref, *sent), (held, sems) = refs[:4], refs[4 : 4 + n], refs[4 + n :]
-    copies = []
+def project_kernel(n, x_hbm, gain_hbm, *refs):
+    weights, (own_ref, *sent), (x_ref, gain_ref, held, sems, small) = refs[:4], refs[4 : 4 + n], refs[4 + n :]
+    first = [
+        pltpu.make_async_copy(x_hbm, x_ref, small.at[0]),
+        pltpu.make_async_copy(gain_hbm, gain_ref, small.at[1]),
+    ]
     depth = x_ref.shape[1]
     half = depth // 2
+    copies = []
     for i, w in enumerate(weights):
         for j in range(2):
             part = pl.ds(j * half, half)
             copies.append(pltpu.make_async_copy(w.at[part], held.at[i, part], sems.at[i, j]))
-    for copy in copies:
+    for copy in first + copies:
         copy.start()
+    first[0].wait()
     x = reorder(n, x_ref[...])
     squares = jnp.sum(x * x, axis=1, keepdims=True)
+    first[1].wait()
     normed = (x * gain_ref[...]).astype(BF16)
     rows, width = x.shape[0], held.shape[2]
     block = rows // n
@@ -141,8 +148,8 @@
             out[here, width:] = split[i][s * block : (s + 1) * block].astype(out.dtype)
 
 
-def retain_kernel(n, own_ref, *refs):
-    got, (cos_ref, sin_ref, gamma_ref, state_ref, new_ref, kept_ref) = refs[: n - 1], refs[n - 1 :]
+def read_kernel(n, own_ref, *refs):
+    got, (cos_ref, sin_ref, gamma_ref, state_ref, kept_ref, key_ref, value_ref) = refs[: n - 1], refs[n - 1 :]
     block, head_dev, size, _ = state_ref.shape
     width = head_dev * size
     total = own_ref[...]
@@ -152,6 +159,7 @@
     total_sq = sq[:block] + sq[block : 2 * block] + sq[2 * block : 3 * block]
     scale = lax.rsqrt(total_sq / D + 1e-06)
     query, key, value, gate = (total[i * block : (i + 1) * block, :width] * scale for i in range(4))
+    value_ref[...] = value
     cos, sin = cos_ref[...], sin_ref[...]
     gate = gate / (1.0 + jnp.exp(-gate))
     for h in range(head_dev):
@@ -159,17 +167,32 @@
         q, k = query[:, at], key[:, at]
         q = q * cos + pltpu.roll(q, size // 2, 1) * sin
         k = (k * cos + pltpu.roll(k, size // 2, 1) * sin) * size ** (-0.5)
+        key_ref[:, at] = k
         columns = jnp.concatenate([q, k], axis=0).T
-        v = value[:, at]
-        gamma = gamma_ref[h : h + 1, :]
         reads = []
         for b in range(block):
-            new = gamma * state_ref[b, h] + columns[:, block + b : block + b + 1] * v[b : b + 1]
-            new_ref[b, h] = new
-            reads.append(jnp.sum(columns[:, b : b + 1] * new, axis=0, keepdims=True))
-        read = jnp.concatenate(reads, axis=0)
+            reads.append(jnp.sum(columns[:, b : b + 1] * state_ref[b, h], axis=0, keepdims=True))
+        match = jnp.sum(q * k, axis=1, keepdims=True)
+        read = gamma_ref[h : h + 1, :] * jnp.concatenate(reads, axis=0) + match * value[:, at]
         read = read * lax.rsqrt(jnp.mean(read * read, axis=1, keepdims=True) + 1e-06)
         kept_ref[:, at] = (read * gate[:, at]).astype(BF16)
+
+
+def update_kernel(key_ref, value_ref, gamma_ref, after_ref, state_ref, new_hbm, new_ref, sems):
+    del after_ref
+    block, head_dev, size, _ = state_ref.shape
+    copies = []
+    for h in range(head_dev):
+        at = slice(h * size, (h + 1) * size)
+        k = key_ref[:, at]
+        columns = jnp.concatenate([k, k], axis=0).T
+        gamma = gamma_ref[h : h + 1, :]
+        for b in range(block):
+            new_ref[b, h] = gamma * state_ref[b, h] + columns[:, b : b + 1] * value_ref[b : b + 1, at]
+            copies.append(pltpu.make_async_copy(new_ref.at[b, h], new_hbm.at[b, h], sems.at[b, h]))
+            copies[-1].start()
+    for copy in copies:
+        copy.wait()
 
 
 def out_kernel(n, *refs):
@@ -182,7 +205,7 @@
 
 
 def up_kernel(n_tp, n, x_ref, gain_ref, w_ref, own_ref, *refs):
-    got, (mixed_ref, total_ref, *sent) = refs[: n_tp - 1], refs[n_tp - 1 :]
+    got, (mixed_ref, normed_ref, split_ref, *sent) = refs[: n_tp - 1], refs[n_tp - 1 :]
     total = own_ref[...]
     for g in got:
         total = total + g[...].astype(F32)
@@ -190,39 +213,53 @@
     mixed_ref[...] = mixed
     middle = mixed.astype(F32)
     normed = (middle * gain_ref[...]).astype(BF16)
+    normed_ref[...] = normed
     rows = middle.shape[0]
     high, mid, low = pieces(jnp.sum(middle * middle, axis=1, keepdims=True))
     lane = lax.broadcasted_iota(jnp.int32, (rows, LANES), 1)
     split = jnp.where(lane == 0, high, jnp.where(lane == 1, mid, jnp.where(lane == 2, low, 0.0)))
+    split_ref[...] = split
     part = w_ref.shape[1] // n
     me = lax.axis_index("kv")
-    for s in reversed(range(n)):
+    for s in reversed(range(1, n)):
         at = pl.ds(pl.multiple_of((me ^ s) * part, part), part)
-        out = sent[s - 1] if s else total_ref
+        out = sent[s - 1]
         out[:, :part] = jnp.dot(normed, w_ref[:, at], preferred_element_type=F32).astype(out.dtype)
         out[:, part:] = split.astype(out.dtype)
 
 
-def hidden_kernel(own_ref, *refs):
+def up_own_kernel(n, normed_ref, w_ref, out_ref):
+    part = w_ref.shape[1] // n
+    at = pl.ds(pl.multiple_of(lax.axis_index("kv") * part, part), part)
+    out_ref[...] = jnp.dot(normed_ref[...], w_ref[:, at], preferred_element_type=F32)
+
+
+def hidden_kernel(own_ref, split_ref, *refs):
     *got, out_ref = refs
-    total = own_ref[...]
+    part = out_ref.shape[1]
+    total, split = own_ref[...], split_ref[...]
     for g in got:
-        total = total + g[...].astype(F32)
-    part = out_ref.shape[1]
-    sq = total[:, part : part + 1] + total[:, part + 1 : part + 2] + total[:, part + 2 : part + 3]
+        total = total + g[:, :part].astype(F32)
+        split = split + g[:, part:].astype(F32)
+    sq = split[:, 0:1] + split[:, 1:2] + split[:, 2:3]
     scale = lax.rsqrt(sq / D + 1e-06)
-    out_ref[...] = jnp.square(jnp.maximum(total[:, :part] * scale, 0.0)).astype(BF16)
-
-
-def down_kernel(n, *refs):
-    parts, (w_ref, own_ref, sent_ref) = refs[:n], refs[n:]
+    out_ref[...] = jnp.square(jnp.maximum(total * scale, 0.0)).astype(BF16)
+
+
+def down_own_kernel(n, hidden_ref, w_ref, out_ref):
+    part = w_ref.shape[0] // n
+    at = pl.ds(pl.multiple_of(lax.axis_index("kv") * part, part), part)
+    out_ref[...] = jnp.dot(hidden_ref[...], w_ref[at, :], preferred_element_type=F32)
+
+
+def down_kernel(n, start_ref, *refs):
+    parts, (w_ref, own_ref, sent_ref) = refs[: n - 1], refs[n - 1 :]
     me = lax.axis_index("kv")
     part = w_ref.shape[0] // n
-    total = None
-    for s, p in enumerate(parts):
+    total = start_ref[...]
+    for s, p in enumerate(parts, 1):
         at = pl.ds(pl.multiple_of((me ^ s) * part, part), part)
-        term = jnp.dot(p[...], w_ref[at, :], preferred_element_type=F32)
-        total = term if total is None else total + term
+        total = total + jnp.dot(p[...], w_ref[at, :], preferred_element_type=F32)
     own_ref[...] = total
     sent_ref[...] = total.astype(BF16)
 
@@ -239,16 +276,21 @@
 HBM = pl.BlockSpec(memory_space=pltpu.HBM)
 
 
-def call(kernel, name, outs, *args, specs=None, scratch=(), limit=8):
+def call(kernel, name, outs, *args, specs=None, out_specs=None, scratch=(), limit=8, us=1):
     return pl.pallas_call(
         kernel,
         name=name,
         out_shape=[jax.ShapeDtypeStruct(*o) for o in outs],
         in_specs=specs or [VMEM] * len(args),
-        out_specs=[VMEM] * len(outs),
+        out_specs=out_specs or [VMEM] * len(outs),
         scratch_shapes=scratch,
         compiler_params=pltpu.CompilerParams(vmem_limit_bytes=limit << 20),
+        cost_estimate=pl.CostEstimate(flops=int(us * RATE), bytes_accessed=0, transcendentals=0),
     )(*args)
+
+
+def far(value):
+    return pltpu.with_memory_space_constraint(value, pltpu.HBM)
 
 
 def near(value):
@@ -267,15 +309,21 @@
             functools.partial(project_kernel, n),
             "project",
             [((4 * block, wide), F32)] + [((4 * block, wide), BF16)] * (n - 1),
-            tokens,
-            norm_gain[None],
-            w_query,
-            w_key,
-            w_value,
-            w_gate,
-            specs=[VMEM, VMEM] + [HBM] * 4,
-            scratch=[pltpu.VMEM((4, depth, width), BF16), pltpu.SemaphoreType.DMA((4, 2))],
-            limit=8,
+            far(tokens),
+            far(norm_gain[None]),
+            far(w_query),
+            far(w_key),
+            far(w_value),
+            far(w_gate),
+            specs=[HBM] * 6,
+            scratch=[
+                pltpu.VMEM((rows, depth), BF16),
+                pltpu.VMEM((1, depth), F32),
+                pltpu.VMEM((4, depth, width), BF16),
+                pltpu.SemaphoreType.DMA((4, 2)),
+                pltpu.SemaphoreType.DMA((2,)),
+            ],
+            us=2,
         )
         got = [swap(v, "kv", n, s) for s, v in enumerate(sent, 1)]
         half = size // 2
@@ -287,16 +335,18 @@
         heads = (lax.axis_index("tp") * head_dev + jnp.arange(head_dev)).astype(F32)
         gamma = 1.0 - 2.0 ** (-5.0 - 5.0 * heads / (HEADS - 1))
         gamma = jnp.broadcast_to(gamma[:, None], (head_dev, size))
-        new_state, kept = call(
-            functools.partial(retain_kernel, n),
-            "retain",
-            [(state.shape, F32), ((block, width), BF16)],
+        state = near(state)
+        kept, key, value = call(
+            functools.partial(read_kernel, n),
+            "read",
+            [((block, width), BF16), ((block, width), F32), ((block, width), F32)],
             own,
             *got,
             cosine,
             sine,
             gamma,
-            near(state),
+            state,
+            us=1,
         )
         kept = [kept] + [swap(kept, "kv", n, s) for s in range(1, n)]
         own, sent = call(
@@ -308,25 +358,47 @@
         )
         got = [swap(sent, "tp", n_tp, s) for s in range(1, n_tp)]
         part = w_up.shape[1] // n
-        mixed, own, *sent = call(
+        w_up = near(w_up)
+        mixed, normed, split, *sent = call(
             functools.partial(up_kernel, n_tp, n),
             "up",
-            [((rows, depth), BF16), ((rows, part + LANES), F32)] + [((rows, part + LANES), BF16)] * (n - 1),
+            [((rows, depth), BF16), ((rows, depth), BF16), ((rows, LANES), F32)]
+            + [((rows, part + LANES), BF16)] * (n - 1),
             tokens,
             mlp_gain[None],
-            near(w_up),
+            w_up,
             own,
             *got,
         )
         got = [swap(v, "kv", n, s) for s, v in enumerate(sent, 1)]
-        (hidden,) = call(hidden_kernel, "hidden", [((rows, part), BF16)], own, *got)
-        hidden = [hidden] + [swap(hidden, "kv", n, s) for s in range(1, n)]
+        (new_state,) = call(
+            update_kernel,
+            "update",
+            [(state.shape, F32)],
+            key,
+            value,
+            gamma,
+            split,
+            state,
+            out_specs=[HBM],
+            scratch=[pltpu.VMEM(state.shape, F32), pltpu.SemaphoreType.DMA((block, head_dev))],
+        )
+        (own,) = call(
+            functools.partial(up_own_kernel, n), "up_own", [((rows, part), F32)], normed, w_up
+        )
+        (hidden,) = call(hidden_kernel, "hidden", [((rows, part), BF16)], own, split, *got)
+        got = [swap(hidden, "kv", n, s) for s in range(1, n)]
+        w_down = near(w_down)
+        (own,) = call(
+            functools.partial(down_own_kernel, n), "down_own", [((rows, depth), F32)], hidden, w_down
+        )
         own, sent = call(
             functools.partial(down_kernel, n),
             "down",
             [((rows, depth), F32), ((rows, depth), BF16)],
-            *hidden,
-            near(w_down),
+            own,
+            *got,
+            w_down,
         )
         got = [swap(sent, "tp", n_tp, s) for s in range(1, n_tp)]
         (layer_out,) = call(final_kernel, "final", [((rows, depth), BF16)], mixed, own, *got)

time: 63.3 us -> 49.3 us (0.78)
  local copies, waits for them, and re-layouts: 13.7 us -> 0.12 us
  Pallas kernels: 7.55 us -> 9.75 us
  waiting for transfers between devices: 17.1 us -> 15.5 us
  other arithmetic: 0.87 us -> 0.21 us
    unnamed x24 -> x22, local copies, waits for them, and re-layouts: 13.6 us -> 0.05 us
    pallas_call x7 -> x10, Pallas kernels: 7.55 us -> 9.75 us  [call(): pl.pallas_call(kernel, name=name, out_shape=[jax.ShapeDtypeStruct(*o) for...]
    ppermute x18, waiting for transfers between devices: 17.1 us -> 15.5 us  [swap(): return lax.ppermute(value, axis, [(i, i ^ step) for i in range(n)])]
    convert_element_type x1, other arithmetic: 0.66 us -> 0.01 us  [shards(): angle = positions.astype(F32)[:, None] * freq[None, :]]
  transfers between devices with their start and end apart: 18 -> 18, of which waited for: 13 -> 13; matrix products, arithmetic and copies ran while one was open for 1% -> 0% of each run, Pallas kernels for 0% -> 5%
where the time goes in v3:
time: 49.3 us; the launch traced here: 49.1 us
  starting transfers between devices  22.8 us (46%)
  waiting for transfers between devices  15.5 us (31%)
  Pallas kernels  9.75 us (20%)
  between operations  0.78 us (2%)
    ppermute x18, starting transfers between devices, swap(): return lax.ppermute(value, axis, [(i, i ^ step) for i in range(n)])  22.8 us
    ppermute x18, waiting for transfers between devices, swap(): return lax.ppermute(value, axis, [(i, i ^ step) for i in range(n)])  15.5 us
    pallas_call x10, Pallas kernels, call(): pl.pallas_call(kernel, name=name, out_shape=[jax.ShapeDtypeStruct(*o) for...  9.75 us
  transfers between devices with their start and end apart: 18, of which 13 were waited for; matrix products, arithmetic and copies ran while one was open for 0% of the time, Pallas kernels for 5%

profile of v3, /device:TPU:0, one launch (start us, length us, event | category | flops | bytes accessed | tf_op | source)
XLA Modules:
  0.0 49.1 jit_solution(10908858998582047905)
XLA Ops:
  0.6 0.0 copy-start.6
  0.6 0.0 copy-start.3
  0.7 3.2 %project.1 = (f32[16,640]{1,0:T(8,128)S(1)}, bf16[16,640]{1,0:T(8,128)(2,1)S(1)}, bf16[16,640]{1,0:T(8,128)(2,1)S(1)}, bf16[16,640]{1,0:T(8,128)(2,1)S(1)}) custom-call(bf16[16,1024]{1,0:T(8,128)(2,1)} %x_ref.1, f32[1,1024]{1,0:T(1,128)} %bitcast.7, bf16[1024,512]{1,0:T(8,128)(2,1)} %refs_0_.1, bf16[1024,512]{1,0:T(8,128)(2,1)} %refs_1_.1, ...), custom_call_target="tpu_custom_call" | custom-call | flops 137438953472 | tf_op jit(solution)/shard_map/project/pallas_call | solution.py:280
  3.9 3.1 %collective-permute-start = (bf16[16,640]{1,0:T(8,128)(2,1)S(1)}, bf16[16,640]{1,0:T(8,128)(2,1)S(1)}, u32[]{:S(2)}, u32[]{:S(2)}) collective-permute-start(bf16[16,640]{1,0:T(8,128)(2,1)S(1)} %get-tuple-element.20), channel_id=1, source_target_pairs={{0,4},{4,0},{8,12},{12,8},{1,5},{5,1},{9,13},{13,9},{2,6},{6,2},{1... | collective-permute-start | bytes 61448 | tf_op jit(solution)/shard_map/ppermute | solution.py:93
  7.0 2.6 %collective-permute-start.1 = (bf16[16,640]{1,0:T(8,128)(2,1)S(1)}, bf16[16,640]{1,0:T(8,128)(2,1)S(1)}, u32[]{:S(2)}, u32[]{:S(2)}) collective-permute-start(bf16[16,640]{1,0:T(8,128)(2,1)S(1)} %get-tuple-element.21), channel_id=1, source_target_pairs={{0,8},{4,12},{8,0},{12,4},{1,9},{5,13},{9,1},{13,5},{2,10},{6,14},... | collective-permute-start | bytes 61448 | tf_op jit(solution)/shard_map/ppermute | solution.py:93
  9.6 0.0 collective-permute-start.2
  9.6 0.0 copy-done.6
  9.7 0.1 fusion
  9.8 0.1 pad_maximum_fusion
  9.8 0.0 collective-permute-done.refs_0_
  9.9 2.1 %collective-permute-done.1.refs_1_ = bf16[16,640]{1,0:T(8,128)(2,1)S(1)} collective-permute-done((bf16[16,640]{1,0:T(8,128)(2,1)S(1)}, bf16[16,640]{1,0:T(8,128)(2,1)S(1)}, u32[]{:S(2)}, u32[]{:S(2)}) %collective-permute-start.1) | collective-permute-done | bytes 20512 | tf_op jit(solution)/shard_map/ppermute | solution.py:93
  11.9 3.3 %collective-permute-done.2.refs_2_ = bf16[16,640]{1,0:T(8,128)(2,1)S(1)} collective-permute-done((bf16[16,640]{1,0:T(8,128)(2,1)S(1)}, bf16[16,640]{1,0:T(8,128)(2,1)S(1)}, u32[]{:S(2)}, u32[]{:S(2)}) %collective-permute-start.2) | collective-permute-done | bytes 20512 | tf_op jit(solution)/shard_map/ppermute | solution.py:93
  15.2 0.1 broadcast_in_dim.16.refs_5_.gamma_ref
  15.3 0.0 copy-done.3
  15.3 1.2 %read.1 = (bf16[4,512]{1,0:T(4,128)(2,1)S(1)}, f32[4,512]{1,0:T(4,128)S(1)}, f32[4,512]{1,0:T(4,128)S(1)}) custom-call(f32[16,640]{1,0:T(8,128)S(1)} %get-tuple-element.19.own_ref, bf16[16,640]{1,0:T(8,128)(2,1)S(1)} %collective-permute-done.refs_0_, bf16[16,640]{1,0:T(8,128)(2,1)S(1)} %collective-permute-done.1.refs_1_, ...), custom_call_target="tpu_custom_call" | custom-call | flops 68719476736 | tf_op jit(solution)/shard_map/read/pallas_call | solution.py:280
  16.5 0.0 copy-done
  16.5 0.0 slice-start.1
  16.5 0.0 copy-start.4
  16.5 0.0 copy-start.5
  16.5 0.3 collective-permute-start.5
  16.8 0.0 collective-permute-start.4
  16.8 4.2 %collective-permute-start.3 = (bf16[4,512]{1,0:T(4,128)(2,1)S(1)}, bf16[4,512]{1,0:T(4,128)(2,1)S(1)}, u32[]{:S(2)}, u32[]{:S(2)}) collective-permute-start(bf16[4,512]{1,0:T(4,128)(2,1)S(1)} %get-tuple-element.23.refs_0_), channel_id=1, source_target_pairs={{0,4},{4,0},{8,12},{12,8},{1,5},{5,1},{9,13},{13,9},{2,6},{6,2},{1... | collective-permute-start | bytes 12296 | tf_op jit(solution)/shard_map/ppermute | solution.py:93
  21.0 1.0 %collective-permute-done.5.refs_3_ = bf16[4,512]{1,0:T(4,128)(2,1)S(1)} collective-permute-done((bf16[4,512]{1,0:T(4,128)(2,1)S(1)}, bf16[4,512]{1,0:T(4,128)(2,1)S(1)}, u32[]{:S(2)}, u32[]{:S(2)}) %collective-permute-start.5) | collective-permute-done | bytes 4128 | tf_op jit(solution)/shard_map/ppermute | solution.py:93
  22.0 0.0 collective-permute-done.4.refs_2_
  22.0 0.6 %collective-permute-done.3.refs_1_ = bf16[4,512]{1,0:T(4,128)(2,1)S(1)} collective-permute-done((bf16[4,512]{1,0:T(4,128)(2,1)S(1)}, bf16[4,512]{1,0:T(4,128)(2,1)S(1)}, u32[]{:S(2)}, u32[]{:S(2)}) %collective-permute-start.3) | collective-permute-done | bytes 4128 | tf_op jit(solution)/shard_map/ppermute | solution.py:93
  22.6 0.0 copy-done.2
  22.6 0.3 out.1
  22.9 0.0 collective-permute-start.8
  22.9 1.5 %collective-permute-start.7 = (bf16[16,1024]{1,0:T(8,128)(2,1)S(1)}, bf16[16,1024]{1,0:T(8,128)(2,1)S(1)}, u32[]{:S(2)}, u32[]{:S(2)}) collective-permute-start(bf16[16,1024]{1,0:T(8,128)(2,1)S(1)} %get-tuple-element.25), channel_id=1, source_target_pairs={{0,2},{1,3},{2,0},{3,1},{4,6},{5,7},{6,4},{7,5},{8,10},{9,11},{10,... | collective-permute-start | bytes 98312 | tf_op jit(solution)/shard_map/ppermute | solution.py:93
  24.5 0.3 collective-permute-start.6
  24.8 1.8 %collective-permute-done.8.refs_2_ = bf16[16,1024]{1,0:T(8,128)(2,1)S(1)} collective-permute-done((bf16[16,1024]{1,0:T(8,128)(2,1)S(1)}, bf16[16,1024]{1,0:T(8,128)(2,1)S(1)}, u32[]{:S(2)}, u32[]{:S(2)}) %collective-permute-start.8) | collective-permute-done | bytes 32800 | tf_op jit(solution)/shard_map/ppermute | solution.py:93
  26.6 0.4 collective-permute-done.7.refs_1_
  27.0 0.0 collective-permute-done.6.refs_0_
  27.0 0.0 slice-done
  27.0 0.0 slice-done.1
  27.0 0.0 copy-done.4
  27.0 0.0 copy-done.5
  27.0 0.9 %up.1 = (bf16[16,1024]{1,0:T(8,128)(2,1)S(1)}, bf16[16,1024]{1,0:T(8,128)(2,1)S(1)}, f32[16,128]{1,0:T(8,128)S(1)}, bf16[16,1152]{1,0:T(8,128)(2,1)S(1)}, bf16[1...) custom-call(bf16[16,1024]{1,0:T(8,128)(2,1)S(1)} %copy-done.4, f32[1,1024]{1,0:T(1,128)S(1)} %bitcast.6, ...), custom_call_target="tpu_custom_call" | custom-call | flops 68719476736 | tf_op jit(solution)/shard_map/up/pallas_call | solution.py:280
  28.0 2.0 %collective-permute-start.9 = (bf16[16,1152]{1,0:T(8,128)(2,1)S(1)}, bf16[16,1152]{1,0:T(8,128)(2,1)S(1)}, u32[]{:S(2)}, u32[]{:S(2)}) collective-permute-start(bf16[16,1152]{1,0:T(8,128)(2,1)S(1)} %get-tuple-element.29), channel_id=1, source_target_pairs={{0,4},{4,0},{8,12},{12,8},{1,5},{5,1},{9,13},{13,9},{2,6},{6,2},{1... | collective-permute-start | bytes 110600 | tf_op jit(solution)/shard_map/ppermute | solution.py:93
  30.0 0.9 %collective-permute-start.10 = (bf16[16,1152]{1,0:T(8,128)(2,1)S(1)}, bf16[16,1152]{1,0:T(8,128)(2,1)S(1)}, u32[]{:S(2)}, u32[]{:S(2)}) collective-permute-start(bf16[16,1152]{1,0:T(8,128)(2,1)S(1)} %get-tuple-element.30), channel_id=1, source_target_pairs={{0,8},{4,12},{8,0},{12,4},{1,9},{5,13},{9,1},{13,5},{2,10},{6,14},... | collective-permute-start | bytes 110600 | tf_op jit(solution)/shard_map/ppermute | solution.py:93
  30.9 1.5 %collective-permute-start.11 = (bf16[16,1152]{1,0:T(8,128)(2,1)S(1)}, bf16[16,1152]{1,0:T(8,128)(2,1)S(1)}, u32[]{:S(2)}, u32[]{:S(2)}) collective-permute-start(bf16[16,1152]{1,0:T(8,128)(2,1)S(1)} %get-tuple-element.31), channel_id=1, source_target_pairs={{0,12},{4,8},{8,4},{12,0},{1,13},{5,9},{9,5},{13,1},{2,14},{6,10},... | collective-permute-start | bytes 110600 | tf_op jit(solution)/shard_map/ppermute | solution.py:93
  32.4 0.4 up_own.1.own_ref
  32.8 0.0 collective-permute-done.9.refs_0_
  32.8 2.8 %collective-permute-done.10.refs_1_ = bf16[16,1152]{1,0:T(8,128)(2,1)S(1)} collective-permute-done((bf16[16,1152]{1,0:T(8,128)(2,1)S(1)}, bf16[16,1152]{1,0:T(8,128)(2,1)S(1)}, u32[]{:S(2)}, u32[]{:S(2)}) %collective-permute-start.10) | collective-permute-done | bytes 36896 | tf_op jit(solution)/shard_map/ppermute | solution.py:93
  35.6 1.0 %collective-permute-done.11.refs_2_ = bf16[16,1152]{1,0:T(8,128)(2,1)S(1)} collective-permute-done((bf16[16,1152]{1,0:T(8,128)(2,1)S(1)}, bf16[16,1152]{1,0:T(8,128)(2,1)S(1)}, u32[]{:S(2)}, u32[]{:S(2)}) %collective-permute-start.11) | collective-permute-done | bytes 36896 | tf_op jit(solution)/shard_map/ppermute | solution.py:93
  36.7 0.2 hidden.1.hidden_ref
  36.8 1.6 %collective-permute-start.14 = (bf16[16,1024]{1,0:T(8,128)(2,1)S(1)}, bf16[16,1024]{1,0:T(8,128)(2,1)S(1)}, u32[]{:S(2)}, u32[]{:S(2)}) collective-permute-start(bf16[16,1024]{1,0:T(8,128)(2,1)S(1)} %hidden.1.hidden_ref), channel_id=1, source_target_pairs={{0,12},{4,8},{8,4},{12,0},{1,13},{5,9},{9,5},{13,1},{2,14},{6,10},... | collective-permute-start | bytes 98312 | tf_op jit(solution)/shard_map/ppermute | solution.py:93
  38.4 0.0 collective-permute-start.13
  38.4 2.9 %collective-permute-start.12 = (bf16[16,1024]{1,0:T(8,128)(2,1)S(1)}, bf16[16,1024]{1,0:T(8,128)(2,1)S(1)}, u32[]{:S(2)}, u32[]{:S(2)}) collective-permute-start(bf16[16,1024]{1,0:T(8,128)(2,1)S(1)} %hidden.1.hidden_ref), channel_id=1, source_target_pairs={{0,4},{4,0},{8,12},{12,8},{1,5},{5,1},{9,13},{13,9},{2,6},{6,2},{1... | collective-permute-start | bytes 98312 | tf_op jit(solution)/shard_map/ppermute | solution.py:93
  41.3 0.0 slice-done.2
  41.3 0.4 down_own.1.start_ref
  41.7 0.9 %collective-permute-done.14.refs_2_ = bf16[16,1024]{1,0:T(8,128)(2,1)S(1)} collective-permute-done((bf16[16,1024]{1,0:T(8,128)(2,1)S(1)}, bf16[16,1024]{1,0:T(8,128)(2,1)S(1)}, u32[]{:S(2)}, u32[]{:S(2)}) %collective-permute-start.14) | collective-permute-done | bytes 32800 | tf_op jit(solution)/shard_map/ppermute | solution.py:93
  42.6 0.8 %collective-permute-done.13.refs_1_ = bf16[16,1024]{1,0:T(8,128)(2,1)S(1)} collective-permute-done((bf16[16,1024]{1,0:T(8,128)(2,1)S(1)}, bf16[16,1024]{1,0:T(8,128)(2,1)S(1)}, u32[]{:S(2)}, u32[]{:S(2)}) %collective-permute-start.13) | collective-permute-done | bytes 32800 | tf_op jit(solution)/shard_map/ppermute | solution.py:93
  43.4 0.1 collective-permute-done.12.refs_0_
  43.5 0.9 %down.1 = (f32[16,1024]{1,0:T(8,128)S(1)}, bf16[16,1024]{1,0:T(8,128)(2,1)S(1)}) custom-call(f32[16,1024]{1,0:T(8,128)S(1)} %down_own.1.start_ref, bf16[16,1024]{1,0:T(8,128)(2,1)S(1)} %collective-permute-done.12.refs_0_, bf16[16,1024]{1,0:T(8,128)(2,1)S(1)} %collective-permute-done.13.refs_1_, bf16[16,1024]{1,0:T(8,128)(2,1)S(1)} %collective-permute-done.14.refs_2_, ...), custom_call_target="tpu_custom_call" | custom-call | flops 68719476736 | tf_op jit(solution)/shard_map/down/pallas_call | solution.py:280
  44.4 0.0 collective-permute-start.17
  44.4 1.5 %collective-permute-start.16 = (bf16[16,1024]{1,0:T(8,128)(2,1)S(1)}, bf16[16,1024]{1,0:T(8,128)(2,1)S(1)}, u32[]{:S(2)}, u32[]{:S(2)}) collective-permute-start(bf16[16,1024]{1,0:T(8,128)(2,1)S(1)} %get-tuple-element.33), channel_id=1, source_target_pairs={{0,2},{1,3},{2,0},{3,1},{4,6},{5,7},{6,4},{7,5},{8,10},{9,11},{10,... | collective-permute-start | bytes 98312 | tf_op jit(solution)/shard_map/ppermute | solution.py:93
  46.0 0.3 collective-permute-start.15
  46.3 0.0 copy-done.1
  46.3 1.5 %update.1 = f32[4,4,128,128]{3,2,1,0:T(8,128)} custom-call(f32[4,512]{1,0:T(4,128)S(1)} %get-tuple-element.34.key_ref, f32[4,512]{1,0:T(4,128)S(1)} %get-tuple-element.35.value_ref, f32[4,128]{1,0:T(4,128)S(1)} %copy-done.1, f32[16,128]{1,0:T(8,128)S(1)} %get-tuple-element.28.split_ref.after_ref, f32[4,4,128,128]{3,2,1,0:T(8,128)S(1)} %copy-done.3), custom_call_target="tpu_custom_call" | custom-call | flops 68719476736 | tf_op jit(solution)/shard_map/update/pallas_call | solution.py:280
  47.8 0.3 collective-permute-done.17.refs_2_
  48.1 0.4 collective-permute-done.16.refs_1_
  48.5 0.0 collective-permute-done.15.refs_0_
  48.5 0.6 %final.1 = bf16[16,1024]{1,0:T(8,128)(2,1)} custom-call(bf16[16,1024]{1,0:T(8,128)(2,1)S(1)} %get-tuple-element.26.mixed_ref, f32[16,1024]{1,0:T(8,128)S(1)} %get-tuple-element.32.own_ref, bf16[16,1024]{1,0:T(8,128)(2,1)S(1)} %collective-permute-done.15.refs_0_, bf16[16,1024]{1,0:T(8,128)(2,1)S(1)} %collective-permute-done.16.refs_1_, ...), custom_call_target="tpu_custom_call" | custom-call | flops 68719476736 | tf_op jit(solution)/shard_map/final/pallas_call | solution.py:280
  (12 shorter events, 0.0 us)
Async XLA Ops:
  0.6 9.0 %copy-start.6 = (s32[4]{0:T(128)S(1)}, s32[4]{0:T(128)}, u32[]{:S(2)}) copy-start(s32[4]{0:T(128)} %param.13) | copy-start | bytes 52
  0.6 14.6 %copy-start.3 = (f32[4,4,128,128]{3,2,1,0:T(8,128)S(1)}, f32[4,4,128,128]{3,2,1,0:T(8,128)}, u32[]{:S(2)}) copy-start(f32[4,4,128,128]{3,2,1,0:T(8,128)} %state_ref.1) | copy-start | bytes 3145732
  3.9 5.9 %collective-permute-start = (bf16[16,640]{1,0:T(8,128)(2,1)S(1)}, bf16[16,640]{1,0:T(8,128)(2,1)S(1)}, u32[]{:S(2)}, u32[]{:S(2)}) collective-permute-start(bf16[16,640]{1,0:T(8,128)(2,1)S(1)} %get-tuple-element.20), channel_id=1, source_target_pairs={{0,4},{4,0},{8,12},{12,8},{1,5},{5,1},{9,13},{13,9},{2,6},{6,2},{1... | collective-permute-start | bytes 61448 | tf_op jit(solution)/shard_map/ppermute | solution.py:93
  7.0 4.9 %collective-permute-start.1 = (bf16[16,640]{1,0:T(8,128)(2,1)S(1)}, bf16[16,640]{1,0:T(8,128)(2,1)S(1)}, u32[]{:S(2)}, u32[]{:S(2)}) collective-permute-start(bf16[16,640]{1,0:T(8,128)(2,1)S(1)} %get-tuple-element.21), channel_id=1, source_target_pairs={{0,8},{4,12},{8,0},{12,4},{1,9},{5,13},{9,1},{13,5},{2,10},{6,14},... | collective-permute-start | bytes 61448 | tf_op jit(solution)/shard_map/ppermute | solution.py:93
  9.6 5.6 %collective-permute-start.2 = (bf16[16,640]{1,0:T(8,128)(2,1)S(1)}, bf16[16,640]{1,0:T(8,128)(2,1)S(1)}, u32[]{:S(2)}, u32[]{:S(2)}) collective-permute-start(bf16[16,640]{1,0:T(8,128)(2,1)S(1)} %get-tuple-element.22), channel_id=1, source_target_pairs={{0,12},{4,8},{8,4},{12,0},{1,13},{5,9},{9,5},{13,1},{2,14},{6,10},... | collective-permute-start | bytes 61448 | tf_op jit(solution)/shard_map/ppermute | solution.py:93
  15.3 1.2 %copy-start = (f32[4,128]{1,0:T(4,128)}, f32[4,128]{1,0:T(4,128)S(1)}, u32[]{:S(2)}) copy-start(f32[4,128]{1,0:T(4,128)S(1)} %broadcast_in_dim.16.refs_5_.gamma_ref) | copy-start | bytes 6148
  15.3 7.3 %copy-start.2 = (bf16[512,1024]{1,0:T(8,128)(2,1)S(1)}, bf16[512,1024]{1,0:T(8,128)(2,1)}, u32[]{:S(2)}) copy-start(bf16[512,1024]{1,0:T(8,128)(2,1)} %refs_4_.1) | copy-start | bytes 3145732
  16.5 10.5 %slice-start = ((s8[8388608]{0:T(1024)(128)(4,1)}), s8[4194304]{0:T(1024)(128)(4,1)S(1)}, s32[]{:S(2)}) async-start(s8[8388608]{0:T(1024)(128)(4,1)} %bitcast.2), calls=%async_computation | async-start | bytes 8388608
  16.5 10.5 %slice-start.1 = ((s8[8388608]{0:T(1024)(128)(4,1)}), s8[4194304]{0:T(1024)(128)(4,1)S(1)}, s32[]{:S(2)}) async-start(s8[8388608]{0:T(1024)(128)(4,1)} %bitcast.2), calls=%async_computation.1 | async-start | bytes 8388608
  16.5 10.5 %copy-start.4 = (bf16[16,1024]{1,0:T(8,128)(2,1)S(1)}, bf16[16,1024]{1,0:T(8,128)(2,1)}, u32[]{:S(2)}) copy-start(bf16[16,1024]{1,0:T(8,128)(2,1)} %x_ref.1) | copy-start | bytes 98308
  16.5 10.5 %copy-start.5 = (f32[1024]{0:T(1024)S(1)}, f32[1024]{0:T(1024)}, u32[]{:S(2)}) copy-start(f32[1024]{0:T(1024)} %param.21) | copy-start | bytes 12292
  16.5 5.5 %collective-permute-start.5 = (bf16[4,512]{1,0:T(4,128)(2,1)S(1)}, bf16[4,512]{1,0:T(4,128)(2,1)S(1)}, u32[]{:S(2)}, u32[]{:S(2)}) collective-permute-start(bf16[4,512]{1,0:T(4,128)(2,1)S(1)} %get-tuple-element.23.refs_0_), channel_id=1, source_target_pairs={{0,12},{4,8},{8,4},{12,0},{1,13},{5,9},{9,5},{13,1},{2,14},{6,10},... | collective-permute-start | bytes 12296 | tf_op jit(solution)/shard_map/ppermute | solution.py:93
  16.8 5.2 %collective-permute-start.4 = (bf16[4,512]{1,0:T(4,128)(2,1)S(1)}, bf16[4,512]{1,0:T(4,128)(2,1)S(1)}, u32[]{:S(2)}, u32[]{:S(2)}) collective-permute-start(bf16[4,512]{1,0:T(4,128)(2,1)S(1)} %get-tuple-element.23.refs_0_), channel_id=1, source_target_pairs={{0,8},{4,12},{8,0},{12,4},{1,9},{5,13},{9,1},{13,5},{2,10},{6,14},... | collective-permute-start | bytes 12296 | tf_op jit(solution)/shard_map/ppermute | solution.py:93
  16.8 5.8 %collective-permute-start.3 = (bf16[4,512]{1,0:T(4,128)(2,1)S(1)}, bf16[4,512]{1,0:T(4,128)(2,1)S(1)}, u32[]{:S(2)}, u32[]{:S(2)}) collective-permute-start(bf16[4,512]{1,0:T(4,128)(2,1)S(1)} %get-tuple-element.23.refs_0_), channel_id=1, source_target_pairs={{0,4},{4,0},{8,12},{12,8},{1,5},{5,1},{9,13},{13,9},{2,6},{6,2},{1... | collective-permute-start | bytes 12296 | tf_op jit(solution)/shard_map/ppermute | solution.py:93
  22.9 3.7 %collective-permute-start.8 = (bf16[16,1024]{1,0:T(8,128)(2,1)S(1)}, bf16[16,1024]{1,0:T(8,128)(2,1)S(1)}, u32[]{:S(2)}, u32[]{:S(2)}) collective-permute-start(bf16[16,1024]{1,0:T(8,128)(2,1)S(1)} %get-tuple-element.25), channel_id=1, source_target_pairs={{0,3},{1,2},{2,1},{3,0},{4,7},{5,6},{6,5},{7,4},{8,11},{9,10},{10,... | collective-permute-start | bytes 98312 | tf_op jit(solution)/shard_map/ppermute | solution.py:93
  22.9 4.0 %collective-permute-start.7 = (bf16[16,1024]{1,0:T(8,128)(2,1)S(1)}, bf16[16,1024]{1,0:T(8,128)(2,1)S(1)}, u32[]{:S(2)}, u32[]{:S(2)}) collective-permute-start(bf16[16,1024]{1,0:T(8,128)(2,1)S(1)} %get-tuple-element.25), channel_id=1, source_target_pairs={{0,2},{1,3},{2,0},{3,1},{4,6},{5,7},{6,4},{7,5},{8,10},{9,11},{10,... | collective-permute-start | bytes 98312 | tf_op jit(solution)/shard_map/ppermute | solution.py:93
  24.5 2.5 %collective-permute-start.6 = (bf16[16,1024]{1,0:T(8,128)(2,1)S(1)}, bf16[16,1024]{1,0:T(8,128)(2,1)S(1)}, u32[]{:S(2)}, u32[]{:S(2)}) collective-permute-start(bf16[16,1024]{1,0:T(8,128)(2,1)S(1)} %get-tuple-element.25), channel_id=1, source_target_pairs={{0,1},{1,0},{2,3},{3,2},{4,5},{5,4},{6,7},{7,6},{8,9},{9,8},{10,11... | collective-permute-start | bytes 98312 | tf_op jit(solution)/shard_map/ppermute | solution.py:93
  28.0 4.8 %collective-permute-start.9 = (bf16[16,1152]{1,0:T(8,128)(2,1)S(1)}, bf16[16,1152]{1,0:T(8,128)(2,1)S(1)}, u32[]{:S(2)}, u32[]{:S(2)}) collective-permute-start(bf16[16,1152]{1,0:T(8,128)(2,1)S(1)} %get-tuple-element.29), channel_id=1, source_target_pairs={{0,4},{4,0},{8,12},{12,8},{1,5},{5,1},{9,13},{13,9},{2,6},{6,2},{1... | collective-permute-start | bytes 110600 | tf_op jit(solution)/shard_map/ppermute | solution.py:93
  30.0 5.6 %collective-permute-start.10 = (bf16[16,1152]{1,0:T(8,128)(2,1)S(1)}, bf16[16,1152]{1,0:T(8,128)(2,1)S(1)}, u32[]{:S(2)}, u32[]{:S(2)}) collective-permute-start(bf16[16,1152]{1,0:T(8,128)(2,1)S(1)} %get-tuple-element.30), channel_id=1, source_target_pairs={{0,8},{4,12},{8,0},{12,4},{1,9},{5,13},{9,1},{13,5},{2,10},{6,14},... | collective-permute-start | bytes 110600 | tf_op jit(solution)/shard_map/ppermute | solution.py:93
  30.9 5.8 %collective-permute-start.11 = (bf16[16,1152]{1,0:T(8,128)(2,1)S(1)}, bf16[16,1152]{1,0:T(8,128)(2,1)S(1)}, u32[]{:S(2)}, u32[]{:S(2)}) collective-permute-start(bf16[16,1152]{1,0:T(8,128)(2,1)S(1)} %get-tuple-element.31), channel_id=1, source_target_pairs={{0,12},{4,8},{8,4},{12,0},{1,13},{5,9},{9,5},{13,1},{2,14},{6,10},... | collective-permute-start | bytes 110600 | tf_op jit(solution)/shard_map/ppermute | solution.py:93
  32.4 8.9 %slice-start.2 = ((s8[8388608]{0:T(1024)(128)(4,1)}), s8[4194304]{0:T(1024)(128)(4,1)S(1)}, s32[]{:S(2)}) async-start(s8[8388608]{0:T(1024)(128)(4,1)} %bitcast.4), calls=%async_computation.2 | async-start | bytes 8388608
  32.8 8.5 %slice-start.3 = ((s8[8388608]{0:T(1024)(128)(4,1)}), s8[4194304]{0:T(1024)(128)(4,1)S(1)}, s32[]{:S(2)}) async-start(s8[8388608]{0:T(1024)(128)(4,1)} %bitcast.4), calls=%async_computation.3 | async-start | bytes 8388608
  36.8 5.8 %collective-permute-start.14 = (bf16[16,1024]{1,0:T(8,128)(2,1)S(1)}, bf16[16,1024]{1,0:T(8,128)(2,1)S(1)}, u32[]{:S(2)}, u32[]{:S(2)}) collective-permute-start(bf16[16,1024]{1,0:T(8,128)(2,1)S(1)} %hidden.1.hidden_ref), channel_id=1, source_target_pairs={{0,12},{4,8},{8,4},{12,0},{1,13},{5,9},{9,5},{13,1},{2,14},{6,10},... | collective-permute-start | bytes 98312 | tf_op jit(solution)/shard_map/ppermute | solution.py:93
  38.4 5.0 %collective-permute-start.13 = (bf16[16,1024]{1,0:T(8,128)(2,1)S(1)}, bf16[16,1024]{1,0:T(8,128)(2,1)S(1)}, u32[]{:S(2)}, u32[]{:S(2)}) collective-permute-start(bf16[16,1024]{1,0:T(8,128)(2,1)S(1)} %hidden.1.hidden_ref), channel_id=1, source_target_pairs={{0,8},{4,12},{8,0},{12,4},{1,9},{5,13},{9,1},{13,5},{2,10},{6,14},... | collective-permute-start | bytes 98312 | tf_op jit(solution)/shard_map/ppermute | solution.py:93
  38.4 5.1 %collective-permute-start.12 = (bf16[16,1024]{1,0:T(8,128)(2,1)S(1)}, bf16[16,1024]{1,0:T(8,128)(2,1)S(1)}, u32[]{:S(2)}, u32[]{:S(2)}) collective-permute-start(bf16[16,1024]{1,0:T(8,128)(2,1)S(1)} %hidden.1.hidden_ref), channel_id=1, source_target_pairs={{0,4},{4,0},{8,12},{12,8},{1,5},{5,1},{9,13},{13,9},{2,6},{6,2},{1... | collective-permute-start | bytes 98312 | tf_op jit(solution)/shard_map/ppermute | solution.py:93
  41.7 4.7 %copy-start.1 = (f32[4,128]{1,0:T(4,128)S(1)}, f32[4,128]{1,0:T(4,128)}, u32[]{:S(2)}) copy-start(f32[4,128]{1,0:T(4,128)} %copy-done) | copy-start | bytes 6148
  44.4 3.7 %collective-permute-start.17 = (bf16[16,1024]{1,0:T(8,128)(2,1)S(1)}, bf16[16,1024]{1,0:T(8,128)(2,1)S(1)}, u32[]{:S(2)}, u32[]{:S(2)}) collective-permute-start(bf16[16,1024]{1,0:T(8,128)(2,1)S(1)} %get-tuple-element.33), channel_id=1, source_target_pairs={{0,3},{1,2},{2,1},{3,0},{4,7},{5,6},{6,5},{7,4},{8,11},{9,10},{10,... | collective-permute-start | bytes 98312 | tf_op jit(solution)/shard_map/ppermute | solution.py:93
  44.4 4.1 %collective-permute-start.16 = (bf16[16,1024]{1,0:T(8,128)(2,1)S(1)}, bf16[16,1024]{1,0:T(8,128)(2,1)S(1)}, u32[]{:S(2)}, u32[]{:S(2)}) collective-permute-start(bf16[16,1024]{1,0:T(8,128)(2,1)S(1)} %get-tuple-element.33), channel_id=1, source_target_pairs={{0,2},{1,3},{2,0},{3,1},{4,6},{5,7},{6,4},{7,5},{8,10},{9,11},{10,... | collective-permute-start | bytes 98312 | tf_op jit(solution)/shard_map/ppermute | solution.py:93
  46.0 2.5 %collective-permute-start.15 = (bf16[16,1024]{1,0:T(8,128)(2,1)S(1)}, bf16[16,1024]{1,0:T(8,128)(2,1)S(1)}, u32[]{:S(2)}, u32[]{:S(2)}) collective-permute-start(bf16[16,1024]{1,0:T(8,128)(2,1)S(1)} %get-tuple-element.33), channel_id=1, source_target_pairs={{0,1},{1,0},{2,3},{3,2},{4,5},{5,4},{6,7},{7,6},{8,9},{9,8},{10,11... | collective-permute-start | bytes 98312 | tf_op jit(solution)/shard_map/ppermute | solution.py:93

commit v4 on v3

--- a/solution.py
+++ b/solution.py
@@ -246,22 +246,16 @@
     out_ref[...] = jnp.square(jnp.maximum(total * scale, 0.0)).astype(BF16)
 
 
-def down_own_kernel(n, hidden_ref, w_ref, out_ref):
+def down_kernel(n, s, last, *refs):
+    part_ref, w_ref, *refs = refs
     part = w_ref.shape[0] // n
-    at = pl.ds(pl.multiple_of(lax.axis_index("kv") * part, part), part)
-    out_ref[...] = jnp.dot(hidden_ref[...], w_ref[at, :], preferred_element_type=F32)
-
-
-def down_kernel(n, start_ref, *refs):
-    parts, (w_ref, own_ref, sent_ref) = refs[: n - 1], refs[n - 1 :]
-    me = lax.axis_index("kv")
-    part = w_ref.shape[0] // n
-    total = start_ref[...]
-    for s, p in enumerate(parts, 1):
-        at = pl.ds(pl.multiple_of((me ^ s) * part, part), part)
-        total = total + jnp.dot(p[...], w_ref[at, :], preferred_element_type=F32)
-    own_ref[...] = total
-    sent_ref[...] = total.astype(BF16)
+    at = pl.ds(pl.multiple_of((lax.axis_index("kv") ^ s) * part, part), part)
+    total = jnp.dot(part_ref[...], w_ref[at, :], preferred_element_type=F32)
+    if s:
+        total = total + refs.pop(0)[...]
+    refs[0][...] = total
+    if last:
+        refs[1][...] = total.astype(BF16)
 
 
 def final_kernel(mixed_ref, own_ref, *refs):
@@ -325,7 +319,7 @@
             ],
             us=2,
         )
-        got = [swap(v, "kv", n, s) for s, v in enumerate(sent, 1)]
+        got = [swap(sent[s - 1], "kv", n, s) for s in reversed(range(1, n))]
         half = size // 2
         freq = 10000.0 ** (-(jnp.arange(half, dtype=F32) * 2.0) / size)
         angle = positions.astype(F32)[:, None] * freq[None, :]
@@ -370,7 +364,7 @@
             own,
             *got,
         )
-        got = [swap(v, "kv", n, s) for s, v in enumerate(sent, 1)]
+        got = [swap(sent[s - 1], "kv", n, s) for s in reversed(range(1, n))]
         (new_state,) = call(
             update_kernel,
             "update",
@@ -390,16 +384,19 @@
         got = [swap(hidden, "kv", n, s) for s in range(1, n)]
         w_down = near(w_down)
         (own,) = call(
-            functools.partial(down_own_kernel, n), "down_own", [((rows, depth), F32)], hidden, w_down
-        )
-        own, sent = call(
-            functools.partial(down_kernel, n),
-            "down",
-            [((rows, depth), F32), ((rows, depth), BF16)],
-            own,
-            *got,
-            w_down,
-        )
+            functools.partial(down_kernel, n, 0, False), "down_own", [((rows, depth), F32)], hidden, w_down
+        )
+        for s in reversed(range(1, n)):
+            last = s == 1
+            own, *sent = call(
+                functools.partial(down_kernel, n, s, last),
+                f"down_{s}",
+                [((rows, depth), F32)] + [((rows, depth), BF16)] * last,
+                got[s - 1],
+                w_down,
+                own,
+            )
+        (sent,) = sent
         got = [swap(sent, "tp", n_tp, s) for s in range(1, n_tp)]
         (layer_out,) = call(final_kernel, "final", [((rows, depth), BF16)], mixed, own, *got)
         return (layer_out, new_state)

time: 49.3 us -> 48.8 us (0.990)
  waiting for transfers between devices: 15.5 us -> 12.5 us
  Pallas kernels: 9.75 us -> 12.1 us
    ppermute x18, waiting for transfers between devices: 15.5 us -> 12.5 us  [swap(): return lax.ppermute(value, axis, [(i, i ^ step) for i in range(n)])]
    pallas_call x10 -> x12, Pallas kernels: 9.75 us -> 12.1 us  [call(): pl.pallas_call(kernel, name=name, out_shape=[jax.ShapeDtypeStruct(*o) for...]
  transfers between devices with their start and end apart: 18 -> 18, of which waited for: 13 -> 12; matrix products, arithmetic and copies ran while one was open for 0% -> 0% of each run, Pallas kernels for 5% -> 8%
where the time goes in v4:
time: 48.8 us; the launch traced here: 48.5 us
  starting transfers between devices  22.8 us (47%)
  waiting for transfers between devices  12.5 us (26%)
  Pallas kernels  12.1 us (25%)
  between operations  0.77 us (2%)
    ppermute x18, starting transfers between devices, swap(): return lax.ppermute(value, axis, [(i, i ^ step) for i in range(n)])  22.8 us
    ppermute x18, waiting for transfers between devices, swap(): return lax.ppermute(value, axis, [(i, i ^ step) for i in range(n)])  12.5 us
    pallas_call x12, Pallas kernels, call(): pl.pallas_call(kernel, name=name, out_shape=[jax.ShapeDtypeStruct(*o) for...  12.1 us
  transfers between devices with their start and end apart: 18, of which 12 were waited for; matrix products, arithmetic and copies ran while one was open for 0% of the time, Pallas kernels for 8%

profile of v4, /device:TPU:0, one launch (start us, length us, event | category | flops | bytes accessed | tf_op | source)
XLA Modules:
  0.0 48.5 jit_solution(3628326282132930358)
XLA Ops:
  0.6 0.0 copy-start.8
  0.6 0.0 copy-start.3
  0.7 3.2 %project.1 = (f32[16,640]{1,0:T(8,128)S(1)}, bf16[16,640]{1,0:T(8,128)(2,1)S(1)}, bf16[16,640]{1,0:T(8,128)(2,1)S(1)}, bf16[16,640]{1,0:T(8,128)(2,1)S(1)}) custom-call(bf16[16,1024]{1,0:T(8,128)(2,1)} %x_ref.1, f32[1,1024]{1,0:T(1,128)} %bitcast.7, bf16[1024,512]{1,0:T(8,128)(2,1)} %refs_0_.1, bf16[1024,512]{1,0:T(8,128)(2,1)} %refs_1_.5, ...), custom_call_target="tpu_custom_call" | custom-call | flops 137438953472 | tf_op jit(solution)/shard_map/project/pallas_call | solution.py:274
  3.9 5.1 %collective-permute-start = (bf16[16,640]{1,0:T(8,128)(2,1)S(1)}, bf16[16,640]{1,0:T(8,128)(2,1)S(1)}, u32[]{:S(2)}, u32[]{:S(2)}) collective-permute-start(bf16[16,640]{1,0:T(8,128)(2,1)S(1)} %get-tuple-element.20), channel_id=1, source_target_pairs={{0,12},{4,8},{8,4},{12,0},{1,13},{5,9},{9,5},{13,1},{2,14},{6,10},... | collective-permute-start | bytes 61448 | tf_op jit(solution)/shard_map/ppermute | solution.py:93
  9.0 0.0 collective-permute-start.1
  9.1 0.6 %collective-permute-start.2 = (bf16[16,640]{1,0:T(8,128)(2,1)S(1)}, bf16[16,640]{1,0:T(8,128)(2,1)S(1)}, u32[]{:S(2)}, u32[]{:S(2)}) collective-permute-start(bf16[16,640]{1,0:T(8,128)(2,1)S(1)} %get-tuple-element.22), channel_id=1, source_target_pairs={{0,4},{4,0},{8,12},{12,8},{1,5},{5,1},{9,13},{13,9},{2,6},{6,2},{1... | collective-permute-start | bytes 61448 | tf_op jit(solution)/shard_map/ppermute | solution.py:93
  9.7 0.0 copy-done.8
  9.7 0.1 fusion
  9.8 0.1 pad_maximum_fusion
  9.9 0.9 %collective-permute-done.refs_0_ = bf16[16,640]{1,0:T(8,128)(2,1)S(1)} collective-permute-done((bf16[16,640]{1,0:T(8,128)(2,1)S(1)}, bf16[16,640]{1,0:T(8,128)(2,1)S(1)}, u32[]{:S(2)}, u32[]{:S(2)}) %collective-permute-start) | collective-permute-done | bytes 20512 | tf_op jit(solution)/shard_map/ppermute | solution.py:93
  10.8 2.9 %collective-permute-done.1.refs_1_ = bf16[16,640]{1,0:T(8,128)(2,1)S(1)} collective-permute-done((bf16[16,640]{1,0:T(8,128)(2,1)S(1)}, bf16[16,640]{1,0:T(8,128)(2,1)S(1)}, u32[]{:S(2)}, u32[]{:S(2)}) %collective-permute-start.1) | collective-permute-done | bytes 20512 | tf_op jit(solution)/shard_map/ppermute | solution.py:93
  13.7 0.0 collective-permute-done.2.refs_2_
  13.7 0.1 broadcast_in_dim.16.refs_5_.gamma_ref
  13.8 0.0 copy-done.3
  13.8 1.2 %read.1 = (bf16[4,512]{1,0:T(4,128)(2,1)S(1)}, f32[4,512]{1,0:T(4,128)S(1)}, f32[4,512]{1,0:T(4,128)S(1)}) custom-call(f32[16,640]{1,0:T(8,128)S(1)} %get-tuple-element.19.own_ref, bf16[16,640]{1,0:T(8,128)(2,1)S(1)} %collective-permute-done.refs_0_, bf16[16,640]{1,0:T(8,128)(2,1)S(1)} %collective-permute-done.1.refs_1_, ...), custom_call_target="tpu_custom_call" | custom-call | flops 68719476736 | tf_op jit(solution)/shard_map/read/pallas_call | solution.py:274
  15.0 0.0 copy-done
  15.0 0.0 slice-start.1
  15.1 0.0 copy-start.4
  15.1 0.0 copy-start.5
  15.1 1.5 %collective-permute-start.5 = (bf16[4,512]{1,0:T(4,128)(2,1)S(1)}, bf16[4,512]{1,0:T(4,128)(2,1)S(1)}, u32[]{:S(2)}, u32[]{:S(2)}) collective-permute-start(bf16[4,512]{1,0:T(4,128)(2,1)S(1)} %get-tuple-element.23.refs_0_), channel_id=1, source_target_pairs={{0,12},{4,8},{8,4},{12,0},{1,13},{5,9},{9,5},{13,1},{2,14},{6,10},... | collective-permute-start | bytes 12296 | tf_op jit(solution)/shard_map/ppermute | solution.py:93
  16.6 0.6 %collective-permute-start.4 = (bf16[4,512]{1,0:T(4,128)(2,1)S(1)}, bf16[4,512]{1,0:T(4,128)(2,1)S(1)}, u32[]{:S(2)}, u32[]{:S(2)}) collective-permute-start(bf16[4,512]{1,0:T(4,128)(2,1)S(1)} %get-tuple-element.23.refs_0_), channel_id=1, source_target_pairs={{0,8},{4,12},{8,0},{12,4},{1,9},{5,13},{9,1},{13,5},{2,10},{6,14},... | collective-permute-start | bytes 12296 | tf_op jit(solution)/shard_map/ppermute | solution.py:93
  17.2 2.3 %collective-permute-start.3 = (bf16[4,512]{1,0:T(4,128)(2,1)S(1)}, bf16[4,512]{1,0:T(4,128)(2,1)S(1)}, u32[]{:S(2)}, u32[]{:S(2)}) collective-permute-start(bf16[4,512]{1,0:T(4,128)(2,1)S(1)} %get-tuple-element.23.refs_0_), channel_id=1, source_target_pairs={{0,4},{4,0},{8,12},{12,8},{1,5},{5,1},{9,13},{13,9},{2,6},{6,2},{1... | collective-permute-start | bytes 12296 | tf_op jit(solution)/shard_map/ppermute | solution.py:93
  19.5 1.0 %collective-permute-done.5.refs_3_ = bf16[4,512]{1,0:T(4,128)(2,1)S(1)} collective-permute-done((bf16[4,512]{1,0:T(4,128)(2,1)S(1)}, bf16[4,512]{1,0:T(4,128)(2,1)S(1)}, u32[]{:S(2)}, u32[]{:S(2)}) %collective-permute-start.5) | collective-permute-done | bytes 4128 | tf_op jit(solution)/shard_map/ppermute | solution.py:93
  20.5 0.6 %collective-permute-done.4.refs_2_ = bf16[4,512]{1,0:T(4,128)(2,1)S(1)} collective-permute-done((bf16[4,512]{1,0:T(4,128)(2,1)S(1)}, bf16[4,512]{1,0:T(4,128)(2,1)S(1)}, u32[]{:S(2)}, u32[]{:S(2)}) %collective-permute-start.4) | collective-permute-done | bytes 4128 | tf_op jit(solution)/shard_map/ppermute | solution.py:93
  21.1 0.0 collective-permute-done.3.refs_1_
  21.2 0.0 copy-done.2
  21.2 0.3 out.1
  21.5 0.0 collective-permute-start.8
  21.5 1.5 %collective-permute-start.7 = (bf16[16,1024]{1,0:T(8,128)(2,1)S(1)}, bf16[16,1024]{1,0:T(8,128)(2,1)S(1)}, u32[]{:S(2)}, u32[]{:S(2)}) collective-permute-start(bf16[16,1024]{1,0:T(8,128)(2,1)S(1)} %get-tuple-element.25), channel_id=1, source_target_pairs={{0,2},{1,3},{2,0},{3,1},{4,6},{5,7},{6,4},{7,5},{8,10},{9,11},{10,... | collective-permute-start | bytes 98312 | tf_op jit(solution)/shard_map/ppermute | solution.py:93
  23.0 0.3 collective-permute-start.6
  23.4 1.8 %collective-permute-done.8.refs_2_ = bf16[16,1024]{1,0:T(8,128)(2,1)S(1)} collective-permute-done((bf16[16,1024]{1,0:T(8,128)(2,1)S(1)}, bf16[16,1024]{1,0:T(8,128)(2,1)S(1)}, u32[]{:S(2)}, u32[]{:S(2)}) %collective-permute-start.8) | collective-permute-done | bytes 32800 | tf_op jit(solution)/shard_map/ppermute | solution.py:93
  25.2 0.4 collective-permute-done.7.refs_1_
  25.6 0.0 collective-permute-done.6.refs_0_
  25.6 0.0 slice-done
  25.6 0.0 slice-done.1
  25.6 0.0 copy-done.4
  25.6 0.9 %up.1 = (bf16[16,1024]{1,0:T(8,128)(2,1)S(1)}, bf16[16,1024]{1,0:T(8,128)(2,1)S(1)}, f32[16,128]{1,0:T(8,128)S(1)}, bf16[16,1152]{1,0:T(8,128)(2,1)S(1)}, bf16[1...) custom-call(bf16[16,1024]{1,0:T(8,128)(2,1)S(1)} %copy-done.4, f32[1,1024]{1,0:T(1,128)S(1)} %bitcast.6, ...), custom_call_target="tpu_custom_call" | custom-call | flops 68719476736 | tf_op jit(solution)/shard_map/up/pallas_call | solution.py:274
  26.5 2.6 %collective-permute-start.9 = (bf16[16,1152]{1,0:T(8,128)(2,1)S(1)}, bf16[16,1152]{1,0:T(8,128)(2,1)S(1)}, u32[]{:S(2)}, u32[]{:S(2)}) collective-permute-start(bf16[16,1152]{1,0:T(8,128)(2,1)S(1)} %get-tuple-element.29), channel_id=1, source_target_pairs={{0,12},{4,8},{8,4},{12,0},{1,13},{5,9},{9,5},{13,1},{2,14},{6,10},... | collective-permute-start | bytes 110600 | tf_op jit(solution)/shard_map/ppermute | solution.py:93
  29.1 0.9 %collective-permute-start.10 = (bf16[16,1152]{1,0:T(8,128)(2,1)S(1)}, bf16[16,1152]{1,0:T(8,128)(2,1)S(1)}, u32[]{:S(2)}, u32[]{:S(2)}) collective-permute-start(bf16[16,1152]{1,0:T(8,128)(2,1)S(1)} %get-tuple-element.30), channel_id=1, source_target_pairs={{0,8},{4,12},{8,0},{12,4},{1,9},{5,13},{9,1},{13,5},{2,10},{6,14},... | collective-permute-start | bytes 110600 | tf_op jit(solution)/shard_map/ppermute | solution.py:93
  30.0 0.9 %collective-permute-start.11 = (bf16[16,1152]{1,0:T(8,128)(2,1)S(1)}, bf16[16,1152]{1,0:T(8,128)(2,1)S(1)}, u32[]{:S(2)}, u32[]{:S(2)}) collective-permute-start(bf16[16,1152]{1,0:T(8,128)(2,1)S(1)} %get-tuple-element.31), channel_id=1, source_target_pairs={{0,4},{4,0},{8,12},{12,8},{1,5},{5,1},{9,13},{13,9},{2,6},{6,2},{1... | collective-permute-start | bytes 110600 | tf_op jit(solution)/shard_map/ppermute | solution.py:93
  30.9 0.4 up_own.1.own_ref
  31.3 1.2 %collective-permute-done.9.refs_0_ = bf16[16,1152]{1,0:T(8,128)(2,1)S(1)} collective-permute-done((bf16[16,1152]{1,0:T(8,128)(2,1)S(1)}, bf16[16,1152]{1,0:T(8,128)(2,1)S(1)}, u32[]{:S(2)}, u32[]{:S(2)}) %collective-permute-start.9) | collective-permute-done | bytes 36896 | tf_op jit(solution)/shard_map/ppermute | solution.py:93
  32.5 1.6 %collective-permute-done.10.refs_1_ = bf16[16,1152]{1,0:T(8,128)(2,1)S(1)} collective-permute-done((bf16[16,1152]{1,0:T(8,128)(2,1)S(1)}, bf16[16,1152]{1,0:T(8,128)(2,1)S(1)}, u32[]{:S(2)}, u32[]{:S(2)}) %collective-permute-start.10) | collective-permute-done | bytes 36896 | tf_op jit(solution)/shard_map/ppermute | solution.py:93
  34.1 0.3 collective-permute-done.11.refs_2_
  34.5 0.8 %hidden.1.refs_0_ = bf16[16,1024]{1,0:T(8,128)(2,1)} custom-call(f32[16,1024]{1,0:T(8,128)S(1)} %up_own.1.own_ref, f32[16,128]{1,0:T(8,128)S(1)} %get-tuple-element.28.split_ref.after_ref, bf16[16,1152]{1,0:T(8,128)(2,1)S(1)} %collective-permute-done.9.refs_0_, bf16[16,1152]{1,0:T(8,128)(2,1)S(1)} %collective-permute-done.10.refs_1_, ...), custom_call_target="tpu_custom_call" | custom-call | flops 68719476736 | tf_op jit(solution)/shard_map/hidden/pallas_call | solution.py:274
  35.2 1.7 %collective-permute-start.14 = (bf16[16,1024]{1,0:T(8,128)(2,1)}, bf16[16,1024]{1,0:T(8,128)(2,1)S(1)}, u32[]{:S(2)}, u32[]{:S(2)}) collective-permute-start(bf16[16,1024]{1,0:T(8,128)(2,1)} %hidden.1.refs_0_), channel_id=1, source_target_pairs={{0,12},{4,8},{8,4},{12,0},{1,13},{5,9},{9,5},{13,1},{2,14},{6,10},... | collective-permute-start | bytes 98312 | tf_op jit(solution)/shard_map/ppermute | solution.py:93
  37.0 0.2 collective-permute-start.13
  37.1 2.5 %collective-permute-start.12 = (bf16[16,1024]{1,0:T(8,128)(2,1)}, bf16[16,1024]{1,0:T(8,128)(2,1)}, u32[]{:S(2)}, u32[]{:S(2)}) collective-permute-start(bf16[16,1024]{1,0:T(8,128)(2,1)} %hidden.1.refs_0_), channel_id=1, source_target_pairs={{0,4},{4,0},{8,12},{12,8},{1,5},{5,1},{9,13},{13,9},{2,6},{6,2},{1... | collective-permute-start | bytes 98312 | tf_op jit(solution)/shard_map/ppermute | solution.py:93
  39.6 1.2 %down_own.1.refs_2_ = f32[16,1024]{1,0:T(8,128)S(1)} custom-call(bf16[16,1024]{1,0:T(8,128)(2,1)} %hidden.1.refs_0_, bf16[4096,1024]{1,0:T(8,128)(2,1)S(1)} %bitcast.5), custom_call_target="tpu_custom_call" | custom-call | flops 68719476736 | tf_op jit(solution)/shard_map/down_own/pallas_call | solution.py:274
  40.8 0.4 collective-permute-done.14.refs_0_
  41.2 0.4 down_3.1.refs_2_
  41.5 0.7 %collective-permute-done.13.refs_0_ = bf16[16,1024]{1,0:T(8,128)(2,1)S(1)} collective-permute-done((bf16[16,1024]{1,0:T(8,128)(2,1)}, bf16[16,1024]{1,0:T(8,128)(2,1)S(1)}, u32[]{:S(2)}, u32[]{:S(2)}) %collective-permute-start.13) | collective-permute-done | bytes 32800 | tf_op jit(solution)/shard_map/ppermute | solution.py:93
  42.2 0.4 down_2.1.refs_2_
  42.6 0.0 collective-permute-done.12.refs_0_
  42.6 1.1 %down_1.1 = (f32[16,1024]{1,0:T(8,128)S(1)}, bf16[16,1024]{1,0:T(8,128)(2,1)S(1)}) custom-call(bf16[16,1024]{1,0:T(8,128)(2,1)} %collective-permute-done.12.refs_0_, bf16[4096,1024]{1,0:T(8,128)(2,1)S(1)} %bitcast.5, f32[16,1024]{1,0:T(8,128)S(1)} %down_2.1.refs_2_), custom_call_target="tpu_custom_call" | custom-call | flops 68719476736 | tf_op jit(solution)/shard_map/down_1/pallas_call | solution.py:274
  43.8 0.0 collective-permute-start.17
  43.8 1.2 %collective-permute-start.16 = (bf16[16,1024]{1,0:T(8,128)(2,1)S(1)}, bf16[16,1024]{1,0:T(8,128)(2,1)S(1)}, u32[]{:S(2)}, u32[]{:S(2)}) collective-permute-start(bf16[16,1024]{1,0:T(8,128)(2,1)S(1)} %get-tuple-element.33), channel_id=1, source_target_pairs={{0,2},{1,3},{2,0},{3,1},{4,6},{5,7},{6,4},{7,5},{8,10},{9,11},{10,... | collective-permute-start | bytes 98312 | tf_op jit(solution)/shard_map/ppermute | solution.py:93
  45.0 0.6 %collective-permute-start.15 = (bf16[16,1024]{1,0:T(8,128)(2,1)S(1)}, bf16[16,1024]{1,0:T(8,128)(2,1)S(1)}, u32[]{:S(2)}, u32[]{:S(2)}) collective-permute-start(bf16[16,1024]{1,0:T(8,128)(2,1)S(1)} %get-tuple-element.33), channel_id=1, source_target_pairs={{0,1},{1,0},{2,3},{3,2},{4,5},{5,4},{6,7},{7,6},{8,9},{9,8},{10,11... | collective-permute-start | bytes 98312 | tf_op jit(solution)/shard_map/ppermute | solution.py:93
  45.7 0.0 copy-done.7
  45.7 1.5 %update.1 = f32[4,4,128,128]{3,2,1,0:T(8,128)} custom-call(f32[4,512]{1,0:T(4,128)S(1)} %get-tuple-element.34.key_ref, f32[4,512]{1,0:T(4,128)S(1)} %get-tuple-element.35.value_ref, f32[4,128]{1,0:T(4,128)S(1)} %copy-done.1, f32[16,128]{1,0:T(8,128)S(1)} %copy-done.7, f32[4,4,128,128]{3,2,1,0:T(8,128)S(1)} %copy-done.3), custom_call_target="tpu_custom_call" | custom-call | flops 68719476736 | tf_op jit(solution)/shard_map/update/pallas_call | solution.py:274
  47.2 0.0 collective-permute-done.17.refs_2_
  47.2 0.6 %collective-permute-done.16.refs_1_ = bf16[16,1024]{1,0:T(8,128)(2,1)S(1)} collective-permute-done((bf16[16,1024]{1,0:T(8,128)(2,1)S(1)}, bf16[16,1024]{1,0:T(8,128)(2,1)S(1)}, u32[]{:S(2)}, u32[]{:S(2)}) %collective-permute-start.16) | collective-permute-done | bytes 32800 | tf_op jit(solution)/shard_map/ppermute | solution.py:93
  47.9 0.0 collective-permute-done.15.refs_0_
  47.9 0.6 %final.1 = bf16[16,1024]{1,0:T(8,128)(2,1)} custom-call(bf16[16,1024]{1,0:T(8,128)(2,1)S(1)} %get-tuple-element.26.mixed_ref, f32[16,1024]{1,0:T(8,128)S(1)} %get-tuple-element.32.own_ref, bf16[16,1024]{1,0:T(8,128)(2,1)S(1)} %collective-permute-done.15.refs_0_, bf16[16,1024]{1,0:T(8,128)(2,1)S(1)} %collective-permute-done.16.refs_1_, ...), custom_call_target="tpu_custom_call" | custom-call | flops 68719476736 | tf_op jit(solution)/shard_map/final/pallas_call | solution.py:274
  (18 shorter events, 0.0 us)
Async XLA Ops:
  0.6 9.1 %copy-start.8 = (s32[4]{0:T(128)S(1)}, s32[4]{0:T(128)}, u32[]{:S(2)}) copy-start(s32[4]{0:T(128)} %param.13) | copy-start | bytes 52
  0.6 13.2 %copy-start.3 = (f32[4,4,128,128]{3,2,1,0:T(8,128)S(1)}, f32[4,4,128,128]{3,2,1,0:T(8,128)}, u32[]{:S(2)}) copy-start(f32[4,4,128,128]{3,2,1,0:T(8,128)} %state_ref.1) | copy-start | bytes 3145732
  3.9 6.9 %collective-permute-start = (bf16[16,640]{1,0:T(8,128)(2,1)S(1)}, bf16[16,640]{1,0:T(8,128)(2,1)S(1)}, u32[]{:S(2)}, u32[]{:S(2)}) collective-permute-start(bf16[16,640]{1,0:T(8,128)(2,1)S(1)} %get-tuple-element.20), channel_id=1, source_target_pairs={{0,12},{4,8},{8,4},{12,0},{1,13},{5,9},{9,5},{13,1},{2,14},{6,10},... | collective-permute-start | bytes 61448 | tf_op jit(solution)/shard_map/ppermute | solution.py:93
  9.0 4.7 %collective-permute-start.1 = (bf16[16,640]{1,0:T(8,128)(2,1)S(1)}, bf16[16,640]{1,0:T(8,128)(2,1)S(1)}, u32[]{:S(2)}, u32[]{:S(2)}) collective-permute-start(bf16[16,640]{1,0:T(8,128)(2,1)S(1)} %get-tuple-element.21), channel_id=1, source_target_pairs={{0,8},{4,12},{8,0},{12,4},{1,9},{5,13},{9,1},{13,5},{2,10},{6,14},... | collective-permute-start | bytes 61448 | tf_op jit(solution)/shard_map/ppermute | solution.py:93
  9.1 4.7 %collective-permute-start.2 = (bf16[16,640]{1,0:T(8,128)(2,1)S(1)}, bf16[16,640]{1,0:T(8,128)(2,1)S(1)}, u32[]{:S(2)}, u32[]{:S(2)}) collective-permute-start(bf16[16,640]{1,0:T(8,128)(2,1)S(1)} %get-tuple-element.22), channel_id=1, source_target_pairs={{0,4},{4,0},{8,12},{12,8},{1,5},{5,1},{9,13},{13,9},{2,6},{6,2},{1... | collective-permute-start | bytes 61448 | tf_op jit(solution)/shard_map/ppermute | solution.py:93
  13.8 1.2 %copy-start = (f32[4,128]{1,0:T(4,128)}, f32[4,128]{1,0:T(4,128)S(1)}, u32[]{:S(2)}) copy-start(f32[4,128]{1,0:T(4,128)S(1)} %broadcast_in_dim.16.refs_5_.gamma_ref) | copy-start | bytes 6148
  13.8 7.3 %copy-start.2 = (bf16[512,1024]{1,0:T(8,128)(2,1)S(1)}, bf16[512,1024]{1,0:T(8,128)(2,1)}, u32[]{:S(2)}) copy-start(bf16[512,1024]{1,0:T(8,128)(2,1)} %refs_4_.1) | copy-start | bytes 3145732
  15.0 10.5 %slice-start = ((s8[8388608]{0:T(1024)(128)(4,1)}), s8[4194304]{0:T(1024)(128)(4,1)S(1)}, s32[]{:S(2)}) async-start(s8[8388608]{0:T(1024)(128)(4,1)} %bitcast.2), calls=%async_computation | async-start | bytes 8388608
  15.0 10.5 %slice-start.1 = ((s8[8388608]{0:T(1024)(128)(4,1)}), s8[4194304]{0:T(1024)(128)(4,1)S(1)}, s32[]{:S(2)}) async-start(s8[8388608]{0:T(1024)(128)(4,1)} %bitcast.2), calls=%async_computation.1 | async-start | bytes 8388608
  15.1 10.5 %copy-start.4 = (bf16[16,1024]{1,0:T(8,128)(2,1)S(1)}, bf16[16,1024]{1,0:T(8,128)(2,1)}, u32[]{:S(2)}) copy-start(bf16[16,1024]{1,0:T(8,128)(2,1)} %x_ref.1) | copy-start | bytes 98308
  15.1 10.5 %copy-start.5 = (f32[1024]{0:T(1024)S(1)}, f32[1024]{0:T(1024)}, u32[]{:S(2)}) copy-start(f32[1024]{0:T(1024)} %param.21) | copy-start | bytes 12292
  15.1 5.5 %collective-permute-start.5 = (bf16[4,512]{1,0:T(4,128)(2,1)S(1)}, bf16[4,512]{1,0:T(4,128)(2,1)S(1)}, u32[]{:S(2)}, u32[]{:S(2)}) collective-permute-start(bf16[4,512]{1,0:T(4,128)(2,1)S(1)} %get-tuple-element.23.refs_0_), channel_id=1, source_target_pairs={{0,12},{4,8},{8,4},{12,0},{1,13},{5,9},{9,5},{13,1},{2,14},{6,10},... | collective-permute-start | bytes 12296 | tf_op jit(solution)/shard_map/ppermute | solution.py:93
  16.6 4.5 %collective-permute-start.4 = (bf16[4,512]{1,0:T(4,128)(2,1)S(1)}, bf16[4,512]{1,0:T(4,128)(2,1)S(1)}, u32[]{:S(2)}, u32[]{:S(2)}) collective-permute-start(bf16[4,512]{1,0:T(4,128)(2,1)S(1)} %get-tuple-element.23.refs_0_), channel_id=1, source_target_pairs={{0,8},{4,12},{8,0},{12,4},{1,9},{5,13},{9,1},{13,5},{2,10},{6,14},... | collective-permute-start | bytes 12296 | tf_op jit(solution)/shard_map/ppermute | solution.py:93
  17.2 3.9 %collective-permute-start.3 = (bf16[4,512]{1,0:T(4,128)(2,1)S(1)}, bf16[4,512]{1,0:T(4,128)(2,1)S(1)}, u32[]{:S(2)}, u32[]{:S(2)}) collective-permute-start(bf16[4,512]{1,0:T(4,128)(2,1)S(1)} %get-tuple-element.23.refs_0_), channel_id=1, source_target_pairs={{0,4},{4,0},{8,12},{12,8},{1,5},{5,1},{9,13},{13,9},{2,6},{6,2},{1... | collective-permute-start | bytes 12296 | tf_op jit(solution)/shard_map/ppermute | solution.py:93
  21.5 3.7 %collective-permute-start.8 = (bf16[16,1024]{1,0:T(8,128)(2,1)S(1)}, bf16[16,1024]{1,0:T(8,128)(2,1)S(1)}, u32[]{:S(2)}, u32[]{:S(2)}) collective-permute-start(bf16[16,1024]{1,0:T(8,128)(2,1)S(1)} %get-tuple-element.25), channel_id=1, source_target_pairs={{0,3},{1,2},{2,1},{3,0},{4,7},{5,6},{6,5},{7,4},{8,11},{9,10},{10,... | collective-permute-start | bytes 98312 | tf_op jit(solution)/shard_map/ppermute | solution.py:93
  21.5 4.0 %collective-permute-start.7 = (bf16[16,1024]{1,0:T(8,128)(2,1)S(1)}, bf16[16,1024]{1,0:T(8,128)(2,1)S(1)}, u32[]{:S(2)}, u32[]{:S(2)}) collective-permute-start(bf16[16,1024]{1,0:T(8,128)(2,1)S(1)} %get-tuple-element.25), channel_id=1, source_target_pairs={{0,2},{1,3},{2,0},{3,1},{4,6},{5,7},{6,4},{7,5},{8,10},{9,11},{10,... | collective-permute-start | bytes 98312 | tf_op jit(solution)/shard_map/ppermute | solution.py:93
  23.0 2.5 %collective-permute-start.6 = (bf16[16,1024]{1,0:T(8,128)(2,1)S(1)}, bf16[16,1024]{1,0:T(8,128)(2,1)S(1)}, u32[]{:S(2)}, u32[]{:S(2)}) collective-permute-start(bf16[16,1024]{1,0:T(8,128)(2,1)S(1)} %get-tuple-element.25), channel_id=1, source_target_pairs={{0,1},{1,0},{2,3},{3,2},{4,5},{5,4},{6,7},{7,6},{8,9},{9,8},{10,11... | collective-permute-start | bytes 98312 | tf_op jit(solution)/shard_map/ppermute | solution.py:93
  26.5 7.9 %copy-start.6 = (f32[16,128]{1,0:T(8,128)}, f32[16,128]{1,0:T(8,128)S(1)}, u32[]{:S(2)}) copy-start(f32[16,128]{1,0:T(8,128)S(1)} %get-tuple-element.28.split_ref.after_ref) | copy-start | bytes 24580
  26.5 6.0 %collective-permute-start.9 = (bf16[16,1152]{1,0:T(8,128)(2,1)S(1)}, bf16[16,1152]{1,0:T(8,128)(2,1)S(1)}, u32[]{:S(2)}, u32[]{:S(2)}) collective-permute-start(bf16[16,1152]{1,0:T(8,128)(2,1)S(1)} %get-tuple-element.29), channel_id=1, source_target_pairs={{0,12},{4,8},{8,4},{12,0},{1,13},{5,9},{9,5},{13,1},{2,14},{6,10},... | collective-permute-start | bytes 110600 | tf_op jit(solution)/shard_map/ppermute | solution.py:93
  29.1 5.0 %collective-permute-start.10 = (bf16[16,1152]{1,0:T(8,128)(2,1)S(1)}, bf16[16,1152]{1,0:T(8,128)(2,1)S(1)}, u32[]{:S(2)}, u32[]{:S(2)}) collective-permute-start(bf16[16,1152]{1,0:T(8,128)(2,1)S(1)} %get-tuple-element.30), channel_id=1, source_target_pairs={{0,8},{4,12},{8,0},{12,4},{1,9},{5,13},{9,1},{13,5},{2,10},{6,14},... | collective-permute-start | bytes 110600 | tf_op jit(solution)/shard_map/ppermute | solution.py:93
  30.0 4.5 %collective-permute-start.11 = (bf16[16,1152]{1,0:T(8,128)(2,1)S(1)}, bf16[16,1152]{1,0:T(8,128)(2,1)S(1)}, u32[]{:S(2)}, u32[]{:S(2)}) collective-permute-start(bf16[16,1152]{1,0:T(8,128)(2,1)S(1)} %get-tuple-element.31), channel_id=1, source_target_pairs={{0,4},{4,0},{8,12},{12,8},{1,5},{5,1},{9,13},{13,9},{2,6},{6,2},{1... | collective-permute-start | bytes 110600 | tf_op jit(solution)/shard_map/ppermute | solution.py:93
  30.9 8.7 %slice-start.2 = ((s8[8388608]{0:T(1024)(128)(4,1)}), s8[4194304]{0:T(1024)(128)(4,1)S(1)}, s32[]{:S(2)}) async-start(s8[8388608]{0:T(1024)(128)(4,1)} %bitcast.4), calls=%async_computation.2 | async-start | bytes 8388608
  31.3 8.3 %slice-start.3 = ((s8[8388608]{0:T(1024)(128)(4,1)}), s8[4194304]{0:T(1024)(128)(4,1)S(1)}, s32[]{:S(2)}) async-start(s8[8388608]{0:T(1024)(128)(4,1)} %bitcast.4), calls=%async_computation.3 | async-start | bytes 8388608
  35.2 5.9 %collective-permute-start.14 = (bf16[16,1024]{1,0:T(8,128)(2,1)}, bf16[16,1024]{1,0:T(8,128)(2,1)S(1)}, u32[]{:S(2)}, u32[]{:S(2)}) collective-permute-start(bf16[16,1024]{1,0:T(8,128)(2,1)} %hidden.1.refs_0_), channel_id=1, source_target_pairs={{0,12},{4,8},{8,4},{12,0},{1,13},{5,9},{9,5},{13,1},{2,14},{6,10},... | collective-permute-start | bytes 98312 | tf_op jit(solution)/shard_map/ppermute | solution.py:93
  37.0 5.3 %collective-permute-start.13 = (bf16[16,1024]{1,0:T(8,128)(2,1)}, bf16[16,1024]{1,0:T(8,128)(2,1)S(1)}, u32[]{:S(2)}, u32[]{:S(2)}) collective-permute-start(bf16[16,1024]{1,0:T(8,128)(2,1)} %hidden.1.refs_0_), channel_id=1, source_target_pairs={{0,8},{4,12},{8,0},{12,4},{1,9},{5,13},{9,1},{13,5},{2,10},{6,14},... | collective-permute-start | bytes 98312 | tf_op jit(solution)/shard_map/ppermute | solution.py:93
  37.1 5.5 %collective-permute-start.12 = (bf16[16,1024]{1,0:T(8,128)(2,1)}, bf16[16,1024]{1,0:T(8,128)(2,1)}, u32[]{:S(2)}, u32[]{:S(2)}) collective-permute-start(bf16[16,1024]{1,0:T(8,128)(2,1)} %hidden.1.refs_0_), channel_id=1, source_target_pairs={{0,4},{4,0},{8,12},{12,8},{1,5},{5,1},{9,13},{13,9},{2,6},{6,2},{1... | collective-permute-start | bytes 98312 | tf_op jit(solution)/shard_map/ppermute | solution.py:93
  42.6 3.0 %copy-start.1 = (f32[4,128]{1,0:T(4,128)S(1)}, f32[4,128]{1,0:T(4,128)}, u32[]{:S(2)}) copy-start(f32[4,128]{1,0:T(4,128)} %copy-done) | copy-start | bytes 6148
  42.6 3.1 %copy-start.7 = (f32[16,128]{1,0:T(8,128)S(1)}, f32[16,128]{1,0:T(8,128)}, u32[]{:S(2)}) copy-start(f32[16,128]{1,0:T(8,128)} %copy-done.6) | copy-start | bytes 24580
  43.8 3.4 %collective-permute-start.17 = (bf16[16,1024]{1,0:T(8,128)(2,1)S(1)}, bf16[16,1024]{1,0:T(8,128)(2,1)S(1)}, u32[]{:S(2)}, u32[]{:S(2)}) collective-permute-start(bf16[16,1024]{1,0:T(8,128)(2,1)S(1)} %get-tuple-element.33), channel_id=1, source_target_pairs={{0,3},{1,2},{2,1},{3,0},{4,7},{5,6},{6,5},{7,4},{8,11},{9,10},{10,... | collective-permute-start | bytes 98312 | tf_op jit(solution)/shard_map/ppermute | solution.py:93
  43.8 4.1 %collective-permute-start.16 = (bf16[16,1024]{1,0:T(8,128)(2,1)S(1)}, bf16[16,1024]{1,0:T(8,128)(2,1)S(1)}, u32[]{:S(2)}, u32[]{:S(2)}) collective-permute-start(bf16[16,1024]{1,0:T(8,128)(2,1)S(1)} %get-tuple-element.33), channel_id=1, source_target_pairs={{0,2},{1,3},{2,0},{3,1},{4,6},{5,7},{6,4},{7,5},{8,10},{9,11},{10,... | collective-permute-start | bytes 98312 | tf_op jit(solution)/shard_map/ppermute | solution.py:93
  45.0 2.8 %collective-permute-start.15 = (bf16[16,1024]{1,0:T(8,128)(2,1)S(1)}, bf16[16,1024]{1,0:T(8,128)(2,1)S(1)}, u32[]{:S(2)}, u32[]{:S(2)}) collective-permute-start(bf16[16,1024]{1,0:T(8,128)(2,1)S(1)} %get-tuple-element.33), channel_id=1, source_target_pairs={{0,1},{1,0},{2,3},{3,2},{4,5},{5,4},{6,7},{7,6},{8,9},{9,8},{10,11... | collective-permute-start | bytes 98312 | tf_op jit(solution)/shard_map/ppermute | solution.py:93

commit v5 on v4

--- a/solution.py
+++ b/solution.py
@@ -11,7 +11,7 @@
 HEADS = 16
 DIRECT = 8
 LANES = 128
-RATE = 1 << 36
+RATE = 1 << 33
 F32, BF16 = jnp.float32, jnp.bfloat16
 
 
@@ -270,11 +270,11 @@
 HBM = pl.BlockSpec(memory_space=pltpu.HBM)
 
 
-def call(kernel, name, outs, *args, specs=None, out_specs=None, scratch=(), limit=8, us=1):
+def call(kernel, name, outs, *args, specs=None, out_specs=None, scratch=(), limit=8, us=1, kept=True):
     return pl.pallas_call(
         kernel,
         name=name,
-        out_shape=[jax.ShapeDtypeStruct(*o) for o in outs],
+        out_shape=[(pltpu.VMEM if kept else jax.ShapeDtypeStruct)(*o) for o in outs],
         in_specs=specs or [VMEM] * len(args),
         out_specs=out_specs or [VMEM] * len(outs),
         scratch_shapes=scratch,
@@ -376,6 +376,7 @@
             state,
             out_specs=[HBM],
             scratch=[pltpu.VMEM(state.shape, F32), pltpu.SemaphoreType.DMA((block, head_dev))],
+            kept=False,
         )
         (own,) = call(
             functools.partial(up_own_kernel, n), "up_own", [((rows, part), F32)], normed, w_up
@@ -398,7 +399,7 @@
             )
         (sent,) = sent
         got = [swap(sent, "tp", n_tp, s) for s in range(1, n_tp)]
-        (layer_out,) = call(final_kernel, "final", [((rows, depth), BF16)], mixed, own, *got)
+        (layer_out,) = call(final_kernel, "final", [((rows, depth), BF16)], mixed, own, *got, kept=False)
         return (layer_out, new_state)
 
     return shards

time: 48.8 us -> 47.1 us (0.965)
  Pallas kernels: 12.1 us -> 9.98 us
  waiting for transfers between devices: 12.5 us -> 13.1 us
    pallas_call x12, Pallas kernels: 12.1 us -> 9.98 us  [call(): pl.pallas_call(kernel, name=name, out_shape=[(pltpu.VMEM if kept else jax...]
    ppermute x18, waiting for transfers between devices: 12.5 us -> 13.1 us  [swap(): return lax.ppermute(value, axis, [(i, i ^ step) for i in range(n)])]
  transfers between devices with their start and end apart: 18 -> 18, of which waited for: 12 -> 12; matrix products, arithmetic and copies ran while one was open for 0% -> 0% of each run, Pallas kernels for 8% -> 6%
where the time goes in v5:
time: 47.1 us; the launch traced here: 46.9 us
  starting transfers between devices  22.8 us (48%)
  waiting for transfers between devices  13.1 us (28%)
  Pallas kernels  9.98 us (21%)
  between operations  0.75 us (2%)
    ppermute x18, starting transfers between devices, swap(): return lax.ppermute(value, axis, [(i, i ^ step) for i in range(n)])  22.8 us
    ppermute x18, waiting for transfers between devices, swap(): return lax.ppermute(value, axis, [(i, i ^ step) for i in range(n)])  13.1 us
    pallas_call x12, Pallas kernels, call(): pl.pallas_call(kernel, name=name, out_shape=[(pltpu.VMEM if kept else jax...  9.98 us
  transfers between devices with their start and end apart: 18, of which 12 were waited for; matrix products, arithmetic and copies ran while one was open for 0% of the time, Pallas kernels for 6%

profile of v5, /device:TPU:0, one launch (start us, length us, event | category | flops | bytes accessed | tf_op | source)
XLA Modules:
  0.0 46.9 jit_solution(18034787363551561982)
XLA Ops:
  0.6 0.0 copy-start.4
  0.6 0.0 copy-start.1
  0.7 3.2 %project.1 = (f32[16,640]{1,0:T(8,128)S(1)}, bf16[16,640]{1,0:T(8,128)(2,1)S(1)}, bf16[16,640]{1,0:T(8,128)(2,1)S(1)}, bf16[16,640]{1,0:T(8,128)(2,1)S(1)}) custom-call(bf16[16,1024]{1,0:T(8,128)(2,1)} %x_ref.1, f32[1,1024]{1,0:T(1,128)} %bitcast.7, bf16[1024,512]{1,0:T(8,128)(2,1)} %refs_0_.1, bf16[1024,512]{1,0:T(8,128)(2,1)} %refs_1_.5, ...), custom_call_target="tpu_custom_call" | custom-call | flops 17179869184 | tf_op jit(solution)/shard_map/project/pallas_call | solution.py:274
  3.9 5.1 %collective-permute-start = (bf16[16,640]{1,0:T(8,128)(2,1)S(1)}, bf16[16,640]{1,0:T(8,128)(2,1)S(1)}, u32[]{:S(2)}, u32[]{:S(2)}) collective-permute-start(bf16[16,640]{1,0:T(8,128)(2,1)S(1)} %get-tuple-element.20), channel_id=1, source_target_pairs={{0,12},{4,8},{8,4},{12,0},{1,13},{5,9},{9,5},{13,1},{2,14},{6,10},... | collective-permute-start | bytes 61448 | tf_op jit(solution)/shard_map/ppermute | solution.py:93
  9.0 0.0 collective-permute-start.1
  9.1 0.6 %collective-permute-start.2 = (bf16[16,640]{1,0:T(8,128)(2,1)S(1)}, bf16[16,640]{1,0:T(8,128)(2,1)S(1)}, u32[]{:S(2)}, u32[]{:S(2)}) collective-permute-start(bf16[16,640]{1,0:T(8,128)(2,1)S(1)} %get-tuple-element.22), channel_id=1, source_target_pairs={{0,4},{4,0},{8,12},{12,8},{1,5},{5,1},{9,13},{13,9},{2,6},{6,2},{1... | collective-permute-start | bytes 61448 | tf_op jit(solution)/shard_map/ppermute | solution.py:93
  9.7 0.0 copy-done.4
  9.7 0.1 fusion
  9.8 0.1 pad_maximum_fusion
  9.9 0.9 %collective-permute-done.refs_0_ = bf16[16,640]{1,0:T(8,128)(2,1)S(1)} collective-permute-done((bf16[16,640]{1,0:T(8,128)(2,1)S(1)}, bf16[16,640]{1,0:T(8,128)(2,1)S(1)}, u32[]{:S(2)}, u32[]{:S(2)}) %collective-permute-start) | collective-permute-done | bytes 20512 | tf_op jit(solution)/shard_map/ppermute | solution.py:93
  10.8 2.9 %collective-permute-done.1.refs_1_ = bf16[16,640]{1,0:T(8,128)(2,1)S(1)} collective-permute-done((bf16[16,640]{1,0:T(8,128)(2,1)S(1)}, bf16[16,640]{1,0:T(8,128)(2,1)S(1)}, u32[]{:S(2)}, u32[]{:S(2)}) %collective-permute-start.1) | collective-permute-done | bytes 20512 | tf_op jit(solution)/shard_map/ppermute | solution.py:93
  13.7 0.0 collective-permute-done.2.refs_2_
  13.7 0.1 broadcast_in_dim.16.refs_5_.gamma_ref
  13.8 0.0 copy-done.1
  13.8 1.2 %read.1 = (bf16[4,512]{1,0:T(4,128)(2,1)S(1)}, f32[4,512]{1,0:T(4,128)S(1)}, f32[4,512]{1,0:T(4,128)S(1)}) custom-call(f32[16,640]{1,0:T(8,128)S(1)} %get-tuple-element.19.own_ref, bf16[16,640]{1,0:T(8,128)(2,1)S(1)} %collective-permute-done.refs_0_, bf16[16,640]{1,0:T(8,128)(2,1)S(1)} %collective-permute-done.1.refs_1_, ...), custom_call_target="tpu_custom_call" | custom-call | flops 8589934592 | tf_op jit(solution)/shard_map/read/pallas_call | solution.py:274
  15.0 0.0 copy-start.2
  15.1 0.0 copy-start.3
  15.1 1.5 %collective-permute-start.5 = (bf16[4,512]{1,0:T(4,128)(2,1)S(1)}, bf16[4,512]{1,0:T(4,128)(2,1)S(1)}, u32[]{:S(2)}, u32[]{:S(2)}) collective-permute-start(bf16[4,512]{1,0:T(4,128)(2,1)S(1)} %get-tuple-element.23.refs_0_), channel_id=1, source_target_pairs={{0,12},{4,8},{8,4},{12,0},{1,13},{5,9},{9,5},{13,1},{2,14},{6,10},... | collective-permute-start | bytes 12296 | tf_op jit(solution)/shard_map/ppermute | solution.py:93
  16.6 0.6 %collective-permute-start.4 = (bf16[4,512]{1,0:T(4,128)(2,1)S(1)}, bf16[4,512]{1,0:T(4,128)(2,1)S(1)}, u32[]{:S(2)}, u32[]{:S(2)}) collective-permute-start(bf16[4,512]{1,0:T(4,128)(2,1)S(1)} %get-tuple-element.23.refs_0_), channel_id=1, source_target_pairs={{0,8},{4,12},{8,0},{12,4},{1,9},{5,13},{9,1},{13,5},{2,10},{6,14},... | collective-permute-start | bytes 12296 | tf_op jit(solution)/shard_map/ppermute | solution.py:93
  17.2 2.3 %collective-permute-start.3 = (bf16[4,512]{1,0:T(4,128)(2,1)S(1)}, bf16[4,512]{1,0:T(4,128)(2,1)S(1)}, u32[]{:S(2)}, u32[]{:S(2)}) collective-permute-start(bf16[4,512]{1,0:T(4,128)(2,1)S(1)} %get-tuple-element.23.refs_0_), channel_id=1, source_target_pairs={{0,4},{4,0},{8,12},{12,8},{1,5},{5,1},{9,13},{13,9},{2,6},{6,2},{1... | collective-permute-start | bytes 12296 | tf_op jit(solution)/shard_map/ppermute | solution.py:93
  19.5 1.0 %collective-permute-done.5.refs_3_ = bf16[4,512]{1,0:T(4,128)(2,1)S(1)} collective-permute-done((bf16[4,512]{1,0:T(4,128)(2,1)S(1)}, bf16[4,512]{1,0:T(4,128)(2,1)S(1)}, u32[]{:S(2)}, u32[]{:S(2)}) %collective-permute-start.5) | collective-permute-done | bytes 4128 | tf_op jit(solution)/shard_map/ppermute | solution.py:93
  20.5 0.6 %collective-permute-done.4.refs_2_ = bf16[4,512]{1,0:T(4,128)(2,1)S(1)} collective-permute-done((bf16[4,512]{1,0:T(4,128)(2,1)S(1)}, bf16[4,512]{1,0:T(4,128)(2,1)S(1)}, u32[]{:S(2)}, u32[]{:S(2)}) %collective-permute-start.4) | collective-permute-done | bytes 4128 | tf_op jit(solution)/shard_map/ppermute | solution.py:93
  21.1 0.0 collective-permute-done.3.refs_1_
  21.1 0.0 copy-done
  21.1 0.3 out.1
  21.5 0.0 collective-permute-start.8
  21.5 1.5 %collective-permute-start.7 = (bf16[16,1024]{1,0:T(8,128)(2,1)S(1)}, bf16[16,1024]{1,0:T(8,128)(2,1)S(1)}, u32[]{:S(2)}, u32[]{:S(2)}) collective-permute-start(bf16[16,1024]{1,0:T(8,128)(2,1)S(1)} %get-tuple-element.25), channel_id=1, source_target_pairs={{0,2},{1,3},{2,0},{3,1},{4,6},{5,7},{6,4},{7,5},{8,10},{9,11},{10,... | collective-permute-start | bytes 98312 | tf_op jit(solution)/shard_map/ppermute | solution.py:93
  23.0 0.3 collective-permute-start.6
  23.4 1.8 %collective-permute-done.8.refs_2_ = bf16[16,1024]{1,0:T(8,128)(2,1)S(1)} collective-permute-done((bf16[16,1024]{1,0:T(8,128)(2,1)S(1)}, bf16[16,1024]{1,0:T(8,128)(2,1)S(1)}, u32[]{:S(2)}, u32[]{:S(2)}) %collective-permute-start.8) | collective-permute-done | bytes 32800 | tf_op jit(solution)/shard_map/ppermute | solution.py:93
  25.1 0.4 collective-permute-done.7.refs_1_
  25.5 0.0 collective-permute-done.6.refs_0_
  25.5 0.0 slice-done
  25.5 0.0 slice-done.1
  25.5 0.0 copy-done.2
  25.6 0.0 copy-done.3
  25.6 0.9 %up.1 = (bf16[16,1024]{1,0:T(8,128)(2,1)S(1)}, bf16[16,1024]{1,0:T(8,128)(2,1)S(1)}, f32[16,128]{1,0:T(8,128)S(1)}, bf16[16,1152]{1,0:T(8,128)(2,1)S(1)}, bf16[1...) custom-call(bf16[16,1024]{1,0:T(8,128)(2,1)S(1)} %copy-done.2, f32[1,1024]{1,0:T(1,128)S(1)} %bitcast.6, ...), custom_call_target="tpu_custom_call" | custom-call | flops 8589934592 | tf_op jit(solution)/shard_map/up/pallas_call | solution.py:274
  26.5 2.6 %collective-permute-start.9 = (bf16[16,1152]{1,0:T(8,128)(2,1)S(1)}, bf16[16,1152]{1,0:T(8,128)(2,1)S(1)}, u32[]{:S(2)}, u32[]{:S(2)}) collective-permute-start(bf16[16,1152]{1,0:T(8,128)(2,1)S(1)} %get-tuple-element.29), channel_id=1, source_target_pairs={{0,12},{4,8},{8,4},{12,0},{1,13},{5,9},{9,5},{13,1},{2,14},{6,10},... | collective-permute-start | bytes 110600 | tf_op jit(solution)/shard_map/ppermute | solution.py:93
  29.1 0.9 %collective-permute-start.10 = (bf16[16,1152]{1,0:T(8,128)(2,1)S(1)}, bf16[16,1152]{1,0:T(8,128)(2,1)S(1)}, u32[]{:S(2)}, u32[]{:S(2)}) collective-permute-start(bf16[16,1152]{1,0:T(8,128)(2,1)S(1)} %get-tuple-element.30), channel_id=1, source_target_pairs={{0,8},{4,12},{8,0},{12,4},{1,9},{5,13},{9,1},{13,5},{2,10},{6,14},... | collective-permute-start | bytes 110600 | tf_op jit(solution)/shard_map/ppermute | solution.py:93
  30.0 0.9 %collective-permute-start.11 = (bf16[16,1152]{1,0:T(8,128)(2,1)S(1)}, bf16[16,1152]{1,0:T(8,128)(2,1)S(1)}, u32[]{:S(2)}, u32[]{:S(2)}) collective-permute-start(bf16[16,1152]{1,0:T(8,128)(2,1)S(1)} %get-tuple-element.31), channel_id=1, source_target_pairs={{0,4},{4,0},{8,12},{12,8},{1,5},{5,1},{9,13},{13,9},{2,6},{6,2},{1... | collective-permute-start | bytes 110600 | tf_op jit(solution)/shard_map/ppermute | solution.py:93
  30.9 0.4 up_own.1.own_ref
  31.3 1.2 %collective-permute-done.9.refs_0_ = bf16[16,1152]{1,0:T(8,128)(2,1)S(1)} collective-permute-done((bf16[16,1152]{1,0:T(8,128)(2,1)S(1)}, bf16[16,1152]{1,0:T(8,128)(2,1)S(1)}, u32[]{:S(2)}, u32[]{:S(2)}) %collective-permute-start.9) | collective-permute-done | bytes 36896 | tf_op jit(solution)/shard_map/ppermute | solution.py:93
  32.5 1.6 %collective-permute-done.10.refs_1_ = bf16[16,1152]{1,0:T(8,128)(2,1)S(1)} collective-permute-done((bf16[16,1152]{1,0:T(8,128)(2,1)S(1)}, bf16[16,1152]{1,0:T(8,128)(2,1)S(1)}, u32[]{:S(2)}, u32[]{:S(2)}) %collective-permute-start.10) | collective-permute-done | bytes 36896 | tf_op jit(solution)/shard_map/ppermute | solution.py:93
  34.1 0.3 collective-permute-done.11.refs_2_
  34.4 0.2 hidden.1.refs_0_
  34.6 1.8 %collective-permute-start.14 = (bf16[16,1024]{1,0:T(8,128)(2,1)S(1)}, bf16[16,1024]{1,0:T(8,128)(2,1)S(1)}, u32[]{:S(2)}, u32[]{:S(2)}) collective-permute-start(bf16[16,1024]{1,0:T(8,128)(2,1)S(1)} %hidden.1.refs_0_), channel_id=1, source_target_pairs={{0,12},{4,8},{8,4},{12,0},{1,13},{5,9},{9,5},{13,1},{2,14},{6,10},... | collective-permute-start | bytes 98312 | tf_op jit(solution)/shard_map/ppermute | solution.py:93
  36.4 0.2 collective-permute-start.13
  36.6 2.5 %collective-permute-start.12 = (bf16[16,1024]{1,0:T(8,128)(2,1)S(1)}, bf16[16,1024]{1,0:T(8,128)(2,1)S(1)}, u32[]{:S(2)}, u32[]{:S(2)}) collective-permute-start(bf16[16,1024]{1,0:T(8,128)(2,1)S(1)} %hidden.1.refs_0_), channel_id=1, source_target_pairs={{0,4},{4,0},{8,12},{12,8},{1,5},{5,1},{9,13},{13,9},{2,6},{6,2},{1... | collective-permute-start | bytes 98312 | tf_op jit(solution)/shard_map/ppermute | solution.py:93
  39.1 0.0 slice-done.2
  39.1 0.0 slice-done.3
  39.1 0.4 down_own.1.refs_2_
  39.4 0.9 %collective-permute-done.14.refs_0_ = bf16[16,1024]{1,0:T(8,128)(2,1)S(1)} collective-permute-done((bf16[16,1024]{1,0:T(8,128)(2,1)S(1)}, bf16[16,1024]{1,0:T(8,128)(2,1)S(1)}, u32[]{:S(2)}, u32[]{:S(2)}) %collective-permute-start.14) | collective-permute-done | bytes 32800 | tf_op jit(solution)/shard_map/ppermute | solution.py:93
  40.4 0.4 down_3.1.refs_2_
  40.8 0.7 %collective-permute-done.13.refs_0_ = bf16[16,1024]{1,0:T(8,128)(2,1)S(1)} collective-permute-done((bf16[16,1024]{1,0:T(8,128)(2,1)S(1)}, bf16[16,1024]{1,0:T(8,128)(2,1)S(1)}, u32[]{:S(2)}, u32[]{:S(2)}) %collective-permute-start.13) | collective-permute-done | bytes 32800 | tf_op jit(solution)/shard_map/ppermute | solution.py:93
  41.5 0.4 down_2.1.refs_2_
  41.8 0.0 collective-permute-done.12.refs_0_
  41.9 0.4 down_1.1
  42.2 0.0 collective-permute-start.17
  42.2 1.2 %collective-permute-start.16 = (bf16[16,1024]{1,0:T(8,128)(2,1)S(1)}, bf16[16,1024]{1,0:T(8,128)(2,1)S(1)}, u32[]{:S(2)}, u32[]{:S(2)}) collective-permute-start(bf16[16,1024]{1,0:T(8,128)(2,1)S(1)} %get-tuple-element.33), channel_id=1, source_target_pairs={{0,2},{1,3},{2,0},{3,1},{4,6},{5,7},{6,4},{7,5},{8,10},{9,11},{10,... | collective-permute-start | bytes 98312 | tf_op jit(solution)/shard_map/ppermute | solution.py:93
  43.5 0.6 %collective-permute-start.15 = (bf16[16,1024]{1,0:T(8,128)(2,1)S(1)}, bf16[16,1024]{1,0:T(8,128)(2,1)S(1)}, u32[]{:S(2)}, u32[]{:S(2)}) collective-permute-start(bf16[16,1024]{1,0:T(8,128)(2,1)S(1)} %get-tuple-element.33), channel_id=1, source_target_pairs={{0,1},{1,0},{2,3},{3,2},{4,5},{5,4},{6,7},{7,6},{8,9},{9,8},{10,11... | collective-permute-start | bytes 98312 | tf_op jit(solution)/shard_map/ppermute | solution.py:93
  44.1 1.5 %update.1 = f32[4,4,128,128]{3,2,1,0:T(8,128)} custom-call(f32[4,512]{1,0:T(4,128)S(1)} %get-tuple-element.34.key_ref, f32[4,512]{1,0:T(4,128)S(1)} %get-tuple-element.35.value_ref, f32[4,128]{1,0:T(4,128)S(1)} %broadcast_in_dim.16.refs_5_.gamma_ref, f32[16,128]{1,0:T(8,128)S(1)} %get-tuple-element.28.split_ref.after_ref, f32[4,4,128,128]{3,2,1,0:T(8,128)S(1)} %copy-done.1), custom_call_target="tpu_custom_call" | custom-call | flops 8589934592 | tf_op jit(solution)/shard_map/update/pallas_call | solution.py:274
  45.6 0.0 collective-permute-done.17.refs_2_
  45.7 0.6 %collective-permute-done.16.refs_1_ = bf16[16,1024]{1,0:T(8,128)(2,1)S(1)} collective-permute-done((bf16[16,1024]{1,0:T(8,128)(2,1)S(1)}, bf16[16,1024]{1,0:T(8,128)(2,1)S(1)}, u32[]{:S(2)}, u32[]{:S(2)}) %collective-permute-start.16) | collective-permute-done | bytes 32800 | tf_op jit(solution)/shard_map/ppermute | solution.py:93
  46.3 0.0 collective-permute-done.15.refs_0_
  46.3 0.6 %final.1 = bf16[16,1024]{1,0:T(8,128)(2,1)} custom-call(bf16[16,1024]{1,0:T(8,128)(2,1)S(1)} %get-tuple-element.26.mixed_ref, f32[16,1024]{1,0:T(8,128)S(1)} %get-tuple-element.32.own_ref, bf16[16,1024]{1,0:T(8,128)(2,1)S(1)} %collective-permute-done.15.refs_0_, bf16[16,1024]{1,0:T(8,128)(2,1)S(1)} %collective-permute-done.16.refs_1_, ...), custom_call_target="tpu_custom_call" | custom-call | flops 8589934592 | tf_op jit(solution)/shard_map/final/pallas_call | solution.py:274
  (10 shorter events, 0.0 us)
Async XLA Ops:
  0.6 9.1 %copy-start.4 = (s32[4]{0:T(128)S(1)}, s32[4]{0:T(128)}, u32[]{:S(2)}) copy-start(s32[4]{0:T(128)} %param.13) | copy-start | bytes 52
  0.6 13.2 %copy-start.1 = (f32[4,4,128,128]{3,2,1,0:T(8,128)S(1)}, f32[4,4,128,128]{3,2,1,0:T(8,128)}, u32[]{:S(2)}) copy-start(f32[4,4,128,128]{3,2,1,0:T(8,128)} %state_ref.1) | copy-start | bytes 3145732
  3.9 6.9 %collective-permute-start = (bf16[16,640]{1,0:T(8,128)(2,1)S(1)}, bf16[16,640]{1,0:T(8,128)(2,1)S(1)}, u32[]{:S(2)}, u32[]{:S(2)}) collective-permute-start(bf16[16,640]{1,0:T(8,128)(2,1)S(1)} %get-tuple-element.20), channel_id=1, source_target_pairs={{0,12},{4,8},{8,4},{12,0},{1,13},{5,9},{9,5},{13,1},{2,14},{6,10},... | collective-permute-start | bytes 61448 | tf_op jit(solution)/shard_map/ppermute | solution.py:93
  9.0 4.7 %collective-permute-start.1 = (bf16[16,640]{1,0:T(8,128)(2,1)S(1)}, bf16[16,640]{1,0:T(8,128)(2,1)S(1)}, u32[]{:S(2)}, u32[]{:S(2)}) collective-permute-start(bf16[16,640]{1,0:T(8,128)(2,1)S(1)} %get-tuple-element.21), channel_id=1, source_target_pairs={{0,8},{4,12},{8,0},{12,4},{1,9},{5,13},{9,1},{13,5},{2,10},{6,14},... | collective-permute-start | bytes 61448 | tf_op jit(solution)/shard_map/ppermute | solution.py:93
  9.1 4.7 %collective-permute-start.2 = (bf16[16,640]{1,0:T(8,128)(2,1)S(1)}, bf16[16,640]{1,0:T(8,128)(2,1)S(1)}, u32[]{:S(2)}, u32[]{:S(2)}) collective-permute-start(bf16[16,640]{1,0:T(8,128)(2,1)S(1)} %get-tuple-element.22), channel_id=1, source_target_pairs={{0,4},{4,0},{8,12},{12,8},{1,5},{5,1},{9,13},{13,9},{2,6},{6,2},{1... | collective-permute-start | bytes 61448 | tf_op jit(solution)/shard_map/ppermute | solution.py:93
  13.8 7.3 %copy-start = (bf16[512,1024]{1,0:T(8,128)(2,1)S(1)}, bf16[512,1024]{1,0:T(8,128)(2,1)}, u32[]{:S(2)}) copy-start(bf16[512,1024]{1,0:T(8,128)(2,1)} %refs_4_.1) | copy-start | bytes 3145732
  15.0 10.5 %slice-start = ((s8[8388608]{0:T(1024)(128)(4,1)}), s8[4194304]{0:T(1024)(128)(4,1)S(1)}, s32[]{:S(2)}) async-start(s8[8388608]{0:T(1024)(128)(4,1)} %bitcast.2), calls=%async_computation | async-start | bytes 8388608
  15.0 10.5 %slice-start.1 = ((s8[8388608]{0:T(1024)(128)(4,1)}), s8[4194304]{0:T(1024)(128)(4,1)S(1)}, s32[]{:S(2)}) async-start(s8[8388608]{0:T(1024)(128)(4,1)} %bitcast.2), calls=%async_computation.1 | async-start | bytes 8388608
  15.0 10.5 %copy-start.2 = (bf16[16,1024]{1,0:T(8,128)(2,1)S(1)}, bf16[16,1024]{1,0:T(8,128)(2,1)}, u32[]{:S(2)}) copy-start(bf16[16,1024]{1,0:T(8,128)(2,1)} %x_ref.1) | copy-start | bytes 98308
  15.1 10.5 %copy-start.3 = (f32[1024]{0:T(1024)S(1)}, f32[1024]{0:T(1024)}, u32[]{:S(2)}) copy-start(f32[1024]{0:T(1024)} %param.21) | copy-start | bytes 12292
  15.1 5.5 %collective-permute-start.5 = (bf16[4,512]{1,0:T(4,128)(2,1)S(1)}, bf16[4,512]{1,0:T(4,128)(2,1)S(1)}, u32[]{:S(2)}, u32[]{:S(2)}) collective-permute-start(bf16[4,512]{1,0:T(4,128)(2,1)S(1)} %get-tuple-element.23.refs_0_), channel_id=1, source_target_pairs={{0,12},{4,8},{8,4},{12,0},{1,13},{5,9},{9,5},{13,1},{2,14},{6,10},... | collective-permute-start | bytes 12296 | tf_op jit(solution)/shard_map/ppermute | solution.py:93
  16.6 4.5 %collective-permute-start.4 = (bf16[4,512]{1,0:T(4,128)(2,1)S(1)}, bf16[4,512]{1,0:T(4,128)(2,1)S(1)}, u32[]{:S(2)}, u32[]{:S(2)}) collective-permute-start(bf16[4,512]{1,0:T(4,128)(2,1)S(1)} %get-tuple-element.23.refs_0_), channel_id=1, source_target_pairs={{0,8},{4,12},{8,0},{12,4},{1,9},{5,13},{9,1},{13,5},{2,10},{6,14},... | collective-permute-start | bytes 12296 | tf_op jit(solution)/shard_map/ppermute | solution.py:93
  17.2 3.9 %collective-permute-start.3 = (bf16[4,512]{1,0:T(4,128)(2,1)S(1)}, bf16[4,512]{1,0:T(4,128)(2,1)S(1)}, u32[]{:S(2)}, u32[]{:S(2)}) collective-permute-start(bf16[4,512]{1,0:T(4,128)(2,1)S(1)} %get-tuple-element.23.refs_0_), channel_id=1, source_target_pairs={{0,4},{4,0},{8,12},{12,8},{1,5},{5,1},{9,13},{13,9},{2,6},{6,2},{1... | collective-permute-start | bytes 12296 | tf_op jit(solution)/shard_map/ppermute | solution.py:93
  21.5 3.7 %collective-permute-start.8 = (bf16[16,1024]{1,0:T(8,128)(2,1)S(1)}, bf16[16,1024]{1,0:T(8,128)(2,1)S(1)}, u32[]{:S(2)}, u32[]{:S(2)}) collective-permute-start(bf16[16,1024]{1,0:T(8,128)(2,1)S(1)} %get-tuple-element.25), channel_id=1, source_target_pairs={{0,3},{1,2},{2,1},{3,0},{4,7},{5,6},{6,5},{7,4},{8,11},{9,10},{10,... | collective-permute-start | bytes 98312 | tf_op jit(solution)/shard_map/ppermute | solution.py:93
  21.5 4.0 %collective-permute-start.7 = (bf16[16,1024]{1,0:T(8,128)(2,1)S(1)}, bf16[16,1024]{1,0:T(8,128)(2,1)S(1)}, u32[]{:S(2)}, u32[]{:S(2)}) collective-permute-start(bf16[16,1024]{1,0:T(8,128)(2,1)S(1)} %get-tuple-element.25), channel_id=1, source_target_pairs={{0,2},{1,3},{2,0},{3,1},{4,6},{5,7},{6,4},{7,5},{8,10},{9,11},{10,... | collective-permute-start | bytes 98312 | tf_op jit(solution)/shard_map/ppermute | solution.py:93
  23.0 2.5 %collective-permute-start.6 = (bf16[16,1024]{1,0:T(8,128)(2,1)S(1)}, bf16[16,1024]{1,0:T(8,128)(2,1)S(1)}, u32[]{:S(2)}, u32[]{:S(2)}) collective-permute-start(bf16[16,1024]{1,0:T(8,128)(2,1)S(1)} %get-tuple-element.25), channel_id=1, source_target_pairs={{0,1},{1,0},{2,3},{3,2},{4,5},{5,4},{6,7},{7,6},{8,9},{9,8},{10,11... | collective-permute-start | bytes 98312 | tf_op jit(solution)/shard_map/ppermute | solution.py:93
  26.5 6.0 %collective-permute-start.9 = (bf16[16,1152]{1,0:T(8,128)(2,1)S(1)}, bf16[16,1152]{1,0:T(8,128)(2,1)S(1)}, u32[]{:S(2)}, u32[]{:S(2)}) collective-permute-start(bf16[16,1152]{1,0:T(8,128)(2,1)S(1)} %get-tuple-element.29), channel_id=1, source_target_pairs={{0,12},{4,8},{8,4},{12,0},{1,13},{5,9},{9,5},{13,1},{2,14},{6,10},... | collective-permute-start | bytes 110600 | tf_op jit(solution)/shard_map/ppermute | solution.py:93
  29.1 5.0 %collective-permute-start.10 = (bf16[16,1152]{1,0:T(8,128)(2,1)S(1)}, bf16[16,1152]{1,0:T(8,128)(2,1)S(1)}, u32[]{:S(2)}, u32[]{:S(2)}) collective-permute-start(bf16[16,1152]{1,0:T(8,128)(2,1)S(1)} %get-tuple-element.30), channel_id=1, source_target_pairs={{0,8},{4,12},{8,0},{12,4},{1,9},{5,13},{9,1},{13,5},{2,10},{6,14},... | collective-permute-start | bytes 110600 | tf_op jit(solution)/shard_map/ppermute | solution.py:93
  30.0 4.5 %collective-permute-start.11 = (bf16[16,1152]{1,0:T(8,128)(2,1)S(1)}, bf16[16,1152]{1,0:T(8,128)(2,1)S(1)}, u32[]{:S(2)}, u32[]{:S(2)}) collective-permute-start(bf16[16,1152]{1,0:T(8,128)(2,1)S(1)} %get-tuple-element.31), channel_id=1, source_target_pairs={{0,4},{4,0},{8,12},{12,8},{1,5},{5,1},{9,13},{13,9},{2,6},{6,2},{1... | collective-permute-start | bytes 110600 | tf_op jit(solution)/shard_map/ppermute | solution.py:93
  30.9 8.1 %slice-start.2 = ((s8[8388608]{0:T(1024)(128)(4,1)}), s8[4194304]{0:T(1024)(128)(4,1)S(1)}, s32[]{:S(2)}) async-start(s8[8388608]{0:T(1024)(128)(4,1)} %bitcast.4), calls=%async_computation.2 | async-start | bytes 8388608
  31.3 7.8 %slice-start.3 = ((s8[8388608]{0:T(1024)(128)(4,1)}), s8[4194304]{0:T(1024)(128)(4,1)S(1)}, s32[]{:S(2)}) async-start(s8[8388608]{0:T(1024)(128)(4,1)} %bitcast.4), calls=%async_computation.3 | async-start | bytes 8388608
  34.6 5.8 %collective-permute-start.14 = (bf16[16,1024]{1,0:T(8,128)(2,1)S(1)}, bf16[16,1024]{1,0:T(8,128)(2,1)S(1)}, u32[]{:S(2)}, u32[]{:S(2)}) collective-permute-start(bf16[16,1024]{1,0:T(8,128)(2,1)S(1)} %hidden.1.refs_0_), channel_id=1, source_target_pairs={{0,12},{4,8},{8,4},{12,0},{1,13},{5,9},{9,5},{13,1},{2,14},{6,10},... | collective-permute-start | bytes 98312 | tf_op jit(solution)/shard_map/ppermute | solution.py:93
  36.4 5.1 %collective-permute-start.13 = (bf16[16,1024]{1,0:T(8,128)(2,1)S(1)}, bf16[16,1024]{1,0:T(8,128)(2,1)S(1)}, u32[]{:S(2)}, u32[]{:S(2)}) collective-permute-start(bf16[16,1024]{1,0:T(8,128)(2,1)S(1)} %hidden.1.refs_0_), channel_id=1, source_target_pairs={{0,8},{4,12},{8,0},{12,4},{1,9},{5,13},{9,1},{13,5},{2,10},{6,14},... | collective-permute-start | bytes 98312 | tf_op jit(solution)/shard_map/ppermute | solution.py:93
  36.6 5.3 %collective-permute-start.12 = (bf16[16,1024]{1,0:T(8,128)(2,1)S(1)}, bf16[16,1024]{1,0:T(8,128)(2,1)S(1)}, u32[]{:S(2)}, u32[]{:S(2)}) collective-permute-start(bf16[16,1024]{1,0:T(8,128)(2,1)S(1)} %hidden.1.refs_0_), channel_id=1, source_target_pairs={{0,4},{4,0},{8,12},{12,8},{1,5},{5,1},{9,13},{13,9},{2,6},{6,2},{1... | collective-permute-start | bytes 98312 | tf_op jit(solution)/shard_map/ppermute | solution.py:93
  42.2 3.4 %collective-permute-start.17 = (bf16[16,1024]{1,0:T(8,128)(2,1)S(1)}, bf16[16,1024]{1,0:T(8,128)(2,1)S(1)}, u32[]{:S(2)}, u32[]{:S(2)}) collective-permute-start(bf16[16,1024]{1,0:T(8,128)(2,1)S(1)} %get-tuple-element.33), channel_id=1, source_target_pairs={{0,3},{1,2},{2,1},{3,0},{4,7},{5,6},{6,5},{7,4},{8,11},{9,10},{10,... | collective-permute-start | bytes 98312 | tf_op jit(solution)/shard_map/ppermute | solution.py:93
  42.2 4.0 %collective-permute-start.16 = (bf16[16,1024]{1,0:T(8,128)(2,1)S(1)}, bf16[16,1024]{1,0:T(8,128)(2,1)S(1)}, u32[]{:S(2)}, u32[]{:S(2)}) collective-permute-start(bf16[16,1024]{1,0:T(8,128)(2,1)S(1)} %get-tuple-element.33), channel_id=1, source_target_pairs={{0,2},{1,3},{2,0},{3,1},{4,6},{5,7},{6,4},{7,5},{8,10},{9,11},{10,... | collective-permute-start | bytes 98312 | tf_op jit(solution)/shard_map/ppermute | solution.py:93
  43.5 2.8 %collective-permute-start.15 = (bf16[16,1024]{1,0:T(8,128)(2,1)S(1)}, bf16[16,1024]{1,0:T(8,128)(2,1)S(1)}, u32[]{:S(2)}, u32[]{:S(2)}) collective-permute-start(bf16[16,1024]{1,0:T(8,128)(2,1)S(1)} %get-tuple-element.33), channel_id=1, source_target_pairs={{0,1},{1,0},{2,3},{3,2},{4,5},{5,4},{6,7},{7,6},{8,9},{9,8},{10,11... | collective-permute-start | bytes 98312 | tf_op jit(solution)/shard_map/ppermute | solution.py:93

commit v6 on v5

--- a/solution.py
+++ b/solution.py
@@ -110,72 +110,101 @@
     return jnp.dot(hot.astype(F32).astype(BF16), values, preferred_element_type=F32)
 
 
-def project_kernel(n, x_hbm, gain_hbm, *refs):
-    weights, (own_ref, *sent), (x_ref, gain_ref, held, sems, small) = refs[:4], refs[4 : 4 + n], refs[4 + n :]
+def project_kernel(n, chunks, flight, x_hbm, gain_hbm, *refs):
+    weights, outs, (x_ref, gain_ref, held, sems, small) = refs[:4], refs[4 : 4 + n], refs[4 + n :]
     first = [
         pltpu.make_async_copy(x_hbm, x_ref, small.at[0]),
         pltpu.make_async_copy(gain_hbm, gain_ref, small.at[1]),
     ]
-    depth = x_ref.shape[1]
-    half = depth // 2
+    rows, depth = x_ref.shape
+    width = held.shape[2]
+    block, heads = rows // n, width // LANES
+    step = depth // chunks
     copies = []
     for i, w in enumerate(weights):
-        for j in range(2):
-            part = pl.ds(j * half, half)
+        for j in range(chunks):
+            part = pl.ds(j * step, step)
             copies.append(pltpu.make_async_copy(w.at[part], held.at[i, part], sems.at[i, j]))
-    for copy in first + copies:
+    for copy in first + copies[:flight]:
         copy.start()
     first[0].wait()
     x = reorder(n, x_ref[...])
-    squares = jnp.sum(x * x, axis=1, keepdims=True)
+    lane = lax.broadcasted_iota(jnp.int32, (rows, LANES), 1)
+    high, mid, low = pieces(jnp.sum(x * x, axis=1, keepdims=True))
+    split = jnp.where(lane == 0, high, jnp.where(lane == 1, mid, jnp.where(lane == 2, low, 0.0)))
+    group = heads * block
+    for s, out in enumerate(outs):
+        mine = split[s * block : (s + 1) * block]
+        out[4 * group :] = jnp.concatenate([mine] * heads, axis=0).astype(out.dtype)
     first[1].wait()
     normed = (x * gain_ref[...]).astype(BF16)
-    rows, width = x.shape[0], held.shape[2]
-    block = rows // n
-    split = [jnp.broadcast_to(p, (rows, LANES)) for p in pieces(squares)]
-    split.append(jnp.zeros((rows, LANES), F32))
-    outs = (own_ref, *sent)
     for i in range(4):
         total = None
-        for j in range(2):
-            copies[2 * i + j].wait()
-            part = slice(j * half, (j + 1) * half)
+        for j in range(chunks):
+            at = chunks * i + j
+            copies[at].wait()
+            if at + flight < len(copies):
+                copies[at + flight].start()
+            part = slice(j * step, (j + 1) * step)
             term = jnp.dot(normed[:, part], held[i, part], preferred_element_type=F32)
             total = term if total is None else total + term
         for s, out in enumerate(outs):
-            here = slice(i * block, (i + 1) * block)
-            out[here, :width] = total[s * block : (s + 1) * block].astype(out.dtype)
-            out[here, width:] = split[i][s * block : (s + 1) * block].astype(out.dtype)
-
-
-def read_kernel(n, own_ref, *refs):
-    got, (cos_ref, sin_ref, gamma_ref, state_ref, kept_ref, key_ref, value_ref) = refs[: n - 1], refs[n - 1 :]
+            mine = total[s * block : (s + 1) * block]
+            mine = jnp.concatenate([mine[:, h * LANES : (h + 1) * LANES] for h in range(heads)], axis=0)
+            out[i * group : (i + 1) * group] = mine.astype(out.dtype)
+
+
+def prepare_kernel(state_ref, cos_ref, sin_ref, out_ref, cosine_ref, sine_ref, gamma_ref):
     block, head_dev, size, _ = state_ref.shape
-    width = head_dev * size
+    for h in range(head_dev):
+        for b in range(block):
+            value = state_ref[b, h]
+            high = value.astype(BF16)
+            at = slice(b * size, (b + 1) * size)
+            out_ref[h, :size, at] = high
+            out_ref[h, size:, at] = (value - high.astype(F32)).astype(BF16)
+    cos, sin = cos_ref[...], sin_ref[...]
+    cosine_ref[...] = jnp.concatenate([jnp.concatenate([cos, cos], axis=1)] * head_dev, axis=0)
+    sine_ref[...] = jnp.concatenate([jnp.concatenate([-sin, sin], axis=1)] * head_dev, axis=0)
+    row = lax.broadcasted_iota(jnp.int32, gamma_ref.shape, 0)
+    head = lax.axis_index("tp") * head_dev + row // block
+    gamma_ref[...] = 1.0 - jnp.exp2(-5.0 - 5.0 * head.astype(F32) / (HEADS - 1))
+
+
+def read_kernel(n, block, own_ref, *refs):
+    got, (cos_ref, sin_ref, gamma_ref, prep_ref, kept_ref, key_ref, value_ref) = refs[: n - 1], refs[n - 1 :]
+    head_dev, _, wide = prep_ref.shape
+    size = wide // block
     total = own_ref[...]
     for g in got:
         total = total + g[...].astype(F32)
-    sq = total[:, width : width + 1]
-    total_sq = sq[:block] + sq[block : 2 * block] + sq[2 * block : 3 * block]
-    scale = lax.rsqrt(total_sq / D + 1e-06)
-    query, key, value, gate = (total[i * block : (i + 1) * block, :width] * scale for i in range(4))
+    group = head_dev * block
+    sq = total[4 * group :]
+    scale = lax.rsqrt((sq[:, 0:1] + sq[:, 1:2] + sq[:, 2:3]) / D + 1e-06)
+    query, key, value, gate = (total[i * group : (i + 1) * group] * scale for i in range(4))
+    cos, sin = cos_ref[...], sin_ref[...]
+    query = query * cos + pltpu.roll(query, size // 2, 1) * sin
+    high = query.astype(BF16).astype(F32)
+    low = query - high
+    row = lax.broadcasted_iota(jnp.int32, (2 * block, size), 0)
+    reads = []
+    for h in range(head_dev):
+        at = slice(h * block, (h + 1) * block)
+        both = jnp.concatenate([high[at], low[at]], axis=0).astype(BF16)
+        both = jnp.concatenate([both, both], axis=1)
+        product = jnp.dot(both, prep_ref[h], preferred_element_type=F32)
+        picked = jnp.zeros((2 * block, size), F32)
+        for b in range(block):
+            picked = jnp.where(row % block == b, product[:, b * size : (b + 1) * size], picked)
+        reads.append(picked[:block] + picked[block:])
+    key = (key * cos + pltpu.roll(key, size // 2, 1) * sin) * size ** (-0.5)
+    key_ref[...] = key
     value_ref[...] = value
-    cos, sin = cos_ref[...], sin_ref[...]
+    match = jnp.sum(query * key, axis=1, keepdims=True)
     gate = gate / (1.0 + jnp.exp(-gate))
-    for h in range(head_dev):
-        at = slice(h * size, (h + 1) * size)
-        q, k = query[:, at], key[:, at]
-        q = q * cos + pltpu.roll(q, size // 2, 1) * sin
-        k = (k * cos + pltpu.roll(k, size // 2, 1) * sin) * size ** (-0.5)
-        key_ref[:, at] = k
-        columns = jnp.concatenate([q, k], axis=0).T
-        reads = []
-        for b in range(block):
-            reads.append(jnp.sum(columns[:, b : b + 1] * state_ref[b, h], axis=0, keepdims=True))
-        match = jnp.sum(q * k, axis=1, keepdims=True)
-        read = gamma_ref[h : h + 1, :] * jnp.concatenate(reads, axis=0) + match * value[:, at]
-        read = read * lax.rsqrt(jnp.mean(read * read, axis=1, keepdims=True) + 1e-06)
-        kept_ref[:, at] = (read * gate[:, at]).astype(BF16)
+    read = gamma_ref[...] * jnp.concatenate(reads, axis=0) + match * value
+    read = read * lax.rsqrt(jnp.mean(read * read, axis=1, keepdims=True) + 1e-06)
+    kept_ref[...] = (read * gate).astype(BF16)
 
 
 def update_kernel(key_ref, value_ref, gamma_ref, after_ref, state_ref, new_hbm, new_ref, sems):
@@ -183,12 +212,12 @@
     block, head_dev, size, _ = state_ref.shape
     copies = []
     for h in range(head_dev):
-        at = slice(h * size, (h + 1) * size)
-        k = key_ref[:, at]
+        rows = slice(h * block, (h + 1) * block)
+        k, v = key_ref[rows], value_ref[rows]
         columns = jnp.concatenate([k, k], axis=0).T
-        gamma = gamma_ref[h : h + 1, :]
+        gamma = gamma_ref[h * block : h * block + 1, :]
         for b in range(block):
-            new_ref[b, h] = gamma * state_ref[b, h] + columns[:, b : b + 1] * value_ref[b : b + 1, at]
+            new_ref[b, h] = gamma * state_ref[b, h] + columns[:, b : b + 1] * v[b : b + 1]
             copies.append(pltpu.make_async_copy(new_ref.at[b, h], new_hbm.at[b, h], sems.at[b, h]))
             copies[-1].start()
     for copy in copies:
@@ -197,8 +226,18 @@
 
 def out_kernel(n, *refs):
     parts, (w_ref, own_ref, sent_ref) = refs[:n], refs[n:]
-    kept = jnp.concatenate([p[...].astype(F32) for p in parts], axis=0).astype(BF16)
-    kept = reorder(n, kept).astype(BF16)
+    kept = jnp.concatenate([p[...] for p in parts], axis=0)
+    many, size = kept.shape
+    heads = w_ref.shape[0] // size
+    block = many // n // heads
+    rows = n * block
+    me = lax.axis_index("kv")
+    to = lax.broadcasted_iota(jnp.int32, (many, many), 0)
+    of = lax.broadcasted_iota(jnp.int32, (many, many), 1)
+    head, row = to // rows, to % rows
+    hot = ((row // block) ^ me) * (heads * block) + head * block + row % block == of
+    kept = jnp.dot(hot.astype(F32).astype(BF16), kept, preferred_element_type=F32).astype(BF16)
+    kept = jnp.concatenate([kept[h * rows : (h + 1) * rows] for h in range(heads)], axis=1)
     terms = jnp.dot(kept, w_ref[...], preferred_element_type=F32)
     own_ref[...] = terms
     sent_ref[...] = terms.astype(BF16)
@@ -298,11 +337,12 @@
         block, head_dev, size, _ = state.shape
         rows, depth = tokens.shape
         width = head_dev * size
-        wide = width + LANES
+        group = head_dev * block
+        chunks, flight = 1, 4
         own, *sent = call(
-            functools.partial(project_kernel, n),
+            functools.partial(project_kernel, n, chunks, flight),
             "project",
-            [((4 * block, wide), F32)] + [((4 * block, wide), BF16)] * (n - 1),
+            [((5 * group, size), F32)] + [((5 * group, size), BF16)] * (n - 1),
             far(tokens),
             far(norm_gain[None]),
             far(w_query),
@@ -314,7 +354,7 @@
                 pltpu.VMEM((rows, depth), BF16),
                 pltpu.VMEM((1, depth), F32),
                 pltpu.VMEM((4, depth, width), BF16),
-                pltpu.SemaphoreType.DMA((4, 2)),
+                pltpu.SemaphoreType.DMA((4, chunks)),
                 pltpu.SemaphoreType.DMA((2,)),
             ],
             us=2,
@@ -324,23 +364,25 @@
         freq = 10000.0 ** (-(jnp.arange(half, dtype=F32) * 2.0) / size)
         angle = positions.astype(F32)[:, None] * freq[None, :]
         cosine, sine = jnp.cos(angle), jnp.sin(angle)
-        cosine = jnp.concatenate([cosine, cosine], axis=1)
-        sine = jnp.concatenate([-sine, sine], axis=1)
-        heads = (lax.axis_index("tp") * head_dev + jnp.arange(head_dev)).astype(F32)
-        gamma = 1.0 - 2.0 ** (-5.0 - 5.0 * heads / (HEADS - 1))
-        gamma = jnp.broadcast_to(gamma[:, None], (head_dev, size))
         state = near(state)
+        prepared, cosine, sine, gamma = call(
+            prepare_kernel,
+            "prepare",
+            [((head_dev, 2 * size, block * size), BF16)] + [((group, size), F32)] * 3,
+            state,
+            cosine,
+            sine,
+        )
         kept, key, value = call(
-            functools.partial(read_kernel, n),
+            functools.partial(read_kernel, n, block),
             "read",
-            [((block, width), BF16), ((block, width), F32), ((block, width), F32)],
+            [((group, size), BF16), ((group, size), F32), ((group, size), F32)],
             own,
             *got,
             cosine,
             sine,
             gamma,
-            state,
-            us=1,
+            prepared,
         )
         kept = [kept] + [swap(kept, "kv", n, s) for s in range(1, n)]
         own, sent = call(

time: 47.1 us -> 45.9 us (0.975)
  Pallas kernels: 9.98 us -> 9.05 us
    pallas_call x12 -> x13, Pallas kernels: 9.98 us -> 9.05 us  [call(): pl.pallas_call(kernel, name=name, out_shape=[(pltpu.VMEM if kept else jax...]
  transfers between devices with their start and end apart: 18 -> 18, of which waited for: 12 -> 12; matrix products, arithmetic and copies ran while one was open for 0% -> 0% of each run, Pallas kernels for 6% -> 7%
where the time goes in v6:
time: 45.9 us; the launch traced here: 45.7 us
  starting transfers between devices  22.8 us (50%)
  waiting for transfers between devices  12.9 us (28%)
  Pallas kernels  9.05 us (20%)
  between operations  0.76 us (2%)
    ppermute x18, starting transfers between devices, swap(): return lax.ppermute(value, axis, [(i, i ^ step) for i in range(n)])  22.8 us
    ppermute x18, waiting for transfers between devices, swap(): return lax.ppermute(value, axis, [(i, i ^ step) for i in range(n)])  12.9 us
    pallas_call x13, Pallas kernels, call(): pl.pallas_call(kernel, name=name, out_shape=[(pltpu.VMEM if kept else jax...  9.05 us
  transfers between devices with their start and end apart: 18, of which 12 were waited for; matrix products, arithmetic and copies ran while one was open for 0% of the time, Pallas kernels for 7%

profile of v6, /device:TPU:0, one launch (start us, length us, event | category | flops | bytes accessed | tf_op | source)
XLA Modules:
  0.0 45.7 jit_solution(15528612931041741839)
XLA Ops:
  0.6 0.0 copy-start.4
  0.6 0.0 copy-start.1
  0.7 2.8 %project.1 = (f32[80,128]{1,0:T(8,128)S(1)}, bf16[80,128]{1,0:T(8,128)(2,1)S(1)}, bf16[80,128]{1,0:T(8,128)(2,1)S(1)}, bf16[80,128]{1,0:T(8,128)(2,1)S(1)}) custom-call(bf16[16,1024]{1,0:T(8,128)(2,1)} %x_ref.1, f32[1,1024]{1,0:T(1,128)} %bitcast.7, bf16[1024,512]{1,0:T(8,128)(2,1)} %refs_0_.1, bf16[1024,512]{1,0:T(8,128)(2,1)} %refs_1_.5, ...), custom_call_target="tpu_custom_call" | custom-call | flops 17179869184 | tf_op jit(solution)/shard_map/project/pallas_call | solution.py:313
  3.5 5.1 %collective-permute-start = (bf16[80,128]{1,0:T(8,128)(2,1)S(1)}, bf16[80,128]{1,0:T(8,128)(2,1)S(1)}, u32[]{:S(2)}, u32[]{:S(2)}) collective-permute-start(bf16[80,128]{1,0:T(8,128)(2,1)S(1)} %get-tuple-element.24), channel_id=1, source_target_pairs={{0,12},{4,8},{8,4},{12,0},{1,13},{5,9},{9,5},{13,1},{2,14},{6,10},... | collective-permute-start | bytes 61448 | tf_op jit(solution)/shard_map/ppermute | solution.py:93
  8.6 0.0 collective-permute-start.1
  8.6 0.6 %collective-permute-start.2 = (bf16[80,128]{1,0:T(8,128)(2,1)S(1)}, bf16[80,128]{1,0:T(8,128)(2,1)S(1)}, u32[]{:S(2)}, u32[]{:S(2)}) collective-permute-start(bf16[80,128]{1,0:T(8,128)(2,1)S(1)} %get-tuple-element.26), channel_id=1, source_target_pairs={{0,4},{4,0},{8,12},{12,8},{1,5},{5,1},{9,13},{13,9},{2,6},{6,2},{1... | collective-permute-start | bytes 61448 | tf_op jit(solution)/shard_map/ppermute | solution.py:93
  9.3 0.0 copy-done.4
  9.3 0.1 multiply_sine_fusion
  9.4 0.0 copy-done.1
  9.4 0.2 prepare.1
  9.6 0.8 %collective-permute-done.refs_0_ = bf16[80,128]{1,0:T(8,128)(2,1)S(1)} collective-permute-done((bf16[80,128]{1,0:T(8,128)(2,1)S(1)}, bf16[80,128]{1,0:T(8,128)(2,1)S(1)}, u32[]{:S(2)}, u32[]{:S(2)}) %collective-permute-start) | collective-permute-done | bytes 20512 | tf_op jit(solution)/shard_map/ppermute | solution.py:93
  10.4 2.9 %collective-permute-done.1.refs_1_ = bf16[80,128]{1,0:T(8,128)(2,1)S(1)} collective-permute-done((bf16[80,128]{1,0:T(8,128)(2,1)S(1)}, bf16[80,128]{1,0:T(8,128)(2,1)S(1)}, u32[]{:S(2)}, u32[]{:S(2)}) %collective-permute-start.1) | collective-permute-done | bytes 20512 | tf_op jit(solution)/shard_map/ppermute | solution.py:93
  13.3 0.0 collective-permute-done.2.refs_2_
  13.3 0.0 copy-start
  13.3 0.5 %read.1 = (bf16[16,128]{1,0:T(8,128)(2,1)S(1)}, f32[16,128]{1,0:T(8,128)S(1)}, f32[16,128]{1,0:T(8,128)S(1)}) custom-call(f32[80,128]{1,0:T(8,128)S(1)} %get-tuple-element.23.own_ref, bf16[80,128]{1,0:T(8,128)(2,1)S(1)} %collective-permute-done.refs_0_, bf16[80,128]{1,0:T(8,128)(2,1)S(1)} %collective-permute-done.1.refs_1_, ...), custom_call_target="tpu_custom_call" | custom-call | flops 8589934592 | tf_op jit(solution)/shard_map/read/pallas_call | solution.py:313
  13.8 0.0 copy-start.2
  13.9 0.0 copy-start.3
  13.9 1.5 %collective-permute-start.5 = (bf16[16,128]{1,0:T(8,128)(2,1)S(1)}, bf16[16,128]{1,0:T(8,128)(2,1)S(1)}, u32[]{:S(2)}, u32[]{:S(2)}) collective-permute-start(bf16[16,128]{1,0:T(8,128)(2,1)S(1)} %get-tuple-element.31.refs_0_), channel_id=1, source_target_pairs={{0,12},{4,8},{8,4},{12,0},{1,13},{5,9},{9,5},{13,1},{2,14},{6,10},... | collective-permute-start | bytes 12296 | tf_op jit(solution)/shard_map/ppermute | solution.py:93
  15.4 0.6 %collective-permute-start.4 = (bf16[16,128]{1,0:T(8,128)(2,1)S(1)}, bf16[16,128]{1,0:T(8,128)(2,1)S(1)}, u32[]{:S(2)}, u32[]{:S(2)}) collective-permute-start(bf16[16,128]{1,0:T(8,128)(2,1)S(1)} %get-tuple-element.31.refs_0_), channel_id=1, source_target_pairs={{0,8},{4,12},{8,0},{12,4},{1,9},{5,13},{9,1},{13,5},{2,10},{6,14},... | collective-permute-start | bytes 12296 | tf_op jit(solution)/shard_map/ppermute | solution.py:93
  16.0 2.3 %collective-permute-start.3 = (bf16[16,128]{1,0:T(8,128)(2,1)S(1)}, bf16[16,128]{1,0:T(8,128)(2,1)S(1)}, u32[]{:S(2)}, u32[]{:S(2)}) collective-permute-start(bf16[16,128]{1,0:T(8,128)(2,1)S(1)} %get-tuple-element.31.refs_0_), channel_id=1, source_target_pairs={{0,4},{4,0},{8,12},{12,8},{1,5},{5,1},{9,13},{13,9},{2,6},{6,2},{1... | collective-permute-start | bytes 12296 | tf_op jit(solution)/shard_map/ppermute | solution.py:93
  18.3 1.0 %collective-permute-done.5.refs_3_ = bf16[16,128]{1,0:T(8,128)(2,1)S(1)} collective-permute-done((bf16[16,128]{1,0:T(8,128)(2,1)S(1)}, bf16[16,128]{1,0:T(8,128)(2,1)S(1)}, u32[]{:S(2)}, u32[]{:S(2)}) %collective-permute-start.5) | collective-permute-done | bytes 4128 | tf_op jit(solution)/shard_map/ppermute | solution.py:93
  19.3 0.6 %collective-permute-done.4.refs_2_ = bf16[16,128]{1,0:T(8,128)(2,1)S(1)} collective-permute-done((bf16[16,128]{1,0:T(8,128)(2,1)S(1)}, bf16[16,128]{1,0:T(8,128)(2,1)S(1)}, u32[]{:S(2)}, u32[]{:S(2)}) %collective-permute-start.4) | collective-permute-done | bytes 4128 | tf_op jit(solution)/shard_map/ppermute | solution.py:93
  19.9 0.0 collective-permute-done.3.refs_1_
  19.9 0.0 copy-done
  19.9 0.3 out.1
  20.3 0.0 collective-permute-start.8
  20.3 1.5 %collective-permute-start.7 = (bf16[16,1024]{1,0:T(8,128)(2,1)S(1)}, bf16[16,1024]{1,0:T(8,128)(2,1)S(1)}, u32[]{:S(2)}, u32[]{:S(2)}) collective-permute-start(bf16[16,1024]{1,0:T(8,128)(2,1)S(1)} %get-tuple-element.33), channel_id=1, source_target_pairs={{0,2},{1,3},{2,0},{3,1},{4,6},{5,7},{6,4},{7,5},{8,10},{9,11},{10,... | collective-permute-start | bytes 98312 | tf_op jit(solution)/shard_map/ppermute | solution.py:93
  21.8 0.3 collective-permute-start.6
  22.2 1.8 %collective-permute-done.8.refs_2_ = bf16[16,1024]{1,0:T(8,128)(2,1)S(1)} collective-permute-done((bf16[16,1024]{1,0:T(8,128)(2,1)S(1)}, bf16[16,1024]{1,0:T(8,128)(2,1)S(1)}, u32[]{:S(2)}, u32[]{:S(2)}) %collective-permute-start.8) | collective-permute-done | bytes 32800 | tf_op jit(solution)/shard_map/ppermute | solution.py:93
  23.9 0.4 collective-permute-done.7.refs_1_
  24.3 0.0 collective-permute-done.6.refs_0_
  24.3 0.0 slice-done
  24.3 0.0 slice-done.1
  24.4 0.0 copy-done.2
  24.4 0.0 copy-done.3
  24.4 0.9 %up.1 = (bf16[16,1024]{1,0:T(8,128)(2,1)S(1)}, bf16[16,1024]{1,0:T(8,128)(2,1)S(1)}, f32[16,128]{1,0:T(8,128)S(1)}, bf16[16,1152]{1,0:T(8,128)(2,1)S(1)}, bf16[1...) custom-call(bf16[16,1024]{1,0:T(8,128)(2,1)S(1)} %copy-done.2, f32[1,1024]{1,0:T(1,128)S(1)} %bitcast.6, ...), custom_call_target="tpu_custom_call" | custom-call | flops 8589934592 | tf_op jit(solution)/shard_map/up/pallas_call | solution.py:313
  25.3 2.6 %collective-permute-start.9 = (bf16[16,1152]{1,0:T(8,128)(2,1)S(1)}, bf16[16,1152]{1,0:T(8,128)(2,1)S(1)}, u32[]{:S(2)}, u32[]{:S(2)}) collective-permute-start(bf16[16,1152]{1,0:T(8,128)(2,1)S(1)} %get-tuple-element.37), channel_id=1, source_target_pairs={{0,12},{4,8},{8,4},{12,0},{1,13},{5,9},{9,5},{13,1},{2,14},{6,10},... | collective-permute-start | bytes 110600 | tf_op jit(solution)/shard_map/ppermute | solution.py:93
  27.9 0.9 %collective-permute-start.10 = (bf16[16,1152]{1,0:T(8,128)(2,1)S(1)}, bf16[16,1152]{1,0:T(8,128)(2,1)S(1)}, u32[]{:S(2)}, u32[]{:S(2)}) collective-permute-start(bf16[16,1152]{1,0:T(8,128)(2,1)S(1)} %get-tuple-element.38), channel_id=1, source_target_pairs={{0,8},{4,12},{8,0},{12,4},{1,9},{5,13},{9,1},{13,5},{2,10},{6,14},... | collective-permute-start | bytes 110600 | tf_op jit(solution)/shard_map/ppermute | solution.py:93
  28.8 0.9 %collective-permute-start.11 = (bf16[16,1152]{1,0:T(8,128)(2,1)S(1)}, bf16[16,1152]{1,0:T(8,128)(2,1)S(1)}, u32[]{:S(2)}, u32[]{:S(2)}) collective-permute-start(bf16[16,1152]{1,0:T(8,128)(2,1)S(1)} %get-tuple-element.39), channel_id=1, source_target_pairs={{0,4},{4,0},{8,12},{12,8},{1,5},{5,1},{9,13},{13,9},{2,6},{6,2},{1... | collective-permute-start | bytes 110600 | tf_op jit(solution)/shard_map/ppermute | solution.py:93
  29.7 0.4 up_own.1.own_ref
  30.1 1.2 %collective-permute-done.9.refs_0_ = bf16[16,1152]{1,0:T(8,128)(2,1)S(1)} collective-permute-done((bf16[16,1152]{1,0:T(8,128)(2,1)S(1)}, bf16[16,1152]{1,0:T(8,128)(2,1)S(1)}, u32[]{:S(2)}, u32[]{:S(2)}) %collective-permute-start.9) | collective-permute-done | bytes 36896 | tf_op jit(solution)/shard_map/ppermute | solution.py:93
  31.3 1.6 %collective-permute-done.10.refs_1_ = bf16[16,1152]{1,0:T(8,128)(2,1)S(1)} collective-permute-done((bf16[16,1152]{1,0:T(8,128)(2,1)S(1)}, bf16[16,1152]{1,0:T(8,128)(2,1)S(1)}, u32[]{:S(2)}, u32[]{:S(2)}) %collective-permute-start.10) | collective-permute-done | bytes 36896 | tf_op jit(solution)/shard_map/ppermute | solution.py:93
  32.9 0.3 collective-permute-done.11.refs_2_
  33.2 0.2 hidden.1.refs_0_
  33.4 1.8 %collective-permute-start.14 = (bf16[16,1024]{1,0:T(8,128)(2,1)S(1)}, bf16[16,1024]{1,0:T(8,128)(2,1)S(1)}, u32[]{:S(2)}, u32[]{:S(2)}) collective-permute-start(bf16[16,1024]{1,0:T(8,128)(2,1)S(1)} %hidden.1.refs_0_), channel_id=1, source_target_pairs={{0,12},{4,8},{8,4},{12,0},{1,13},{5,9},{9,5},{13,1},{2,14},{6,10},... | collective-permute-start | bytes 98312 | tf_op jit(solution)/shard_map/ppermute | solution.py:93
  35.2 0.2 collective-permute-start.13
  35.4 2.5 %collective-permute-start.12 = (bf16[16,1024]{1,0:T(8,128)(2,1)S(1)}, bf16[16,1024]{1,0:T(8,128)(2,1)S(1)}, u32[]{:S(2)}, u32[]{:S(2)}) collective-permute-start(bf16[16,1024]{1,0:T(8,128)(2,1)S(1)} %hidden.1.refs_0_), channel_id=1, source_target_pairs={{0,4},{4,0},{8,12},{12,8},{1,5},{5,1},{9,13},{13,9},{2,6},{6,2},{1... | collective-permute-start | bytes 98312 | tf_op jit(solution)/shard_map/ppermute | solution.py:93
  37.9 0.0 slice-done.2
  37.9 0.0 slice-done.3
  37.9 0.4 down_own.1.refs_2_
  38.2 0.9 %collective-permute-done.14.refs_0_ = bf16[16,1024]{1,0:T(8,128)(2,1)S(1)} collective-permute-done((bf16[16,1024]{1,0:T(8,128)(2,1)S(1)}, bf16[16,1024]{1,0:T(8,128)(2,1)S(1)}, u32[]{:S(2)}, u32[]{:S(2)}) %collective-permute-start.14) | collective-permute-done | bytes 32800 | tf_op jit(solution)/shard_map/ppermute | solution.py:93
  39.2 0.4 down_3.1.refs_2_
  39.6 0.7 %collective-permute-done.13.refs_0_ = bf16[16,1024]{1,0:T(8,128)(2,1)S(1)} collective-permute-done((bf16[16,1024]{1,0:T(8,128)(2,1)S(1)}, bf16[16,1024]{1,0:T(8,128)(2,1)S(1)}, u32[]{:S(2)}, u32[]{:S(2)}) %collective-permute-start.13) | collective-permute-done | bytes 32800 | tf_op jit(solution)/shard_map/ppermute | solution.py:93
  40.3 0.4 down_2.1.refs_2_
  40.6 0.0 collective-permute-done.12.refs_0_
  40.7 0.4 down_1.1
  41.0 0.0 collective-permute-start.17
  41.1 1.2 %collective-permute-start.16 = (bf16[16,1024]{1,0:T(8,128)(2,1)S(1)}, bf16[16,1024]{1,0:T(8,128)(2,1)S(1)}, u32[]{:S(2)}, u32[]{:S(2)}) collective-permute-start(bf16[16,1024]{1,0:T(8,128)(2,1)S(1)} %get-tuple-element.41), channel_id=1, source_target_pairs={{0,2},{1,3},{2,0},{3,1},{4,6},{5,7},{6,4},{7,5},{8,10},{9,11},{10,... | collective-permute-start | bytes 98312 | tf_op jit(solution)/shard_map/ppermute | solution.py:93
  42.3 0.6 %collective-permute-start.15 = (bf16[16,1024]{1,0:T(8,128)(2,1)S(1)}, bf16[16,1024]{1,0:T(8,128)(2,1)S(1)}, u32[]{:S(2)}, u32[]{:S(2)}) collective-permute-start(bf16[16,1024]{1,0:T(8,128)(2,1)S(1)} %get-tuple-element.41), channel_id=1, source_target_pairs={{0,1},{1,0},{2,3},{3,2},{4,5},{5,4},{6,7},{7,6},{8,9},{9,8},{10,11... | collective-permute-start | bytes 98312 | tf_op jit(solution)/shard_map/ppermute | solution.py:93
  42.9 1.5 %update.1 = f32[4,4,128,128]{3,2,1,0:T(8,128)} custom-call(f32[16,128]{1,0:T(8,128)S(1)} %get-tuple-element.42.key_ref, f32[16,128]{1,0:T(8,128)S(1)} %get-tuple-element.43.value_ref, f32[16,128]{1,0:T(8,128)S(1)} %get-tuple-element.29.refs_5_.gamma_ref, f32[16,128]{1,0:T(8,128)S(1)} %get-tuple-element.36.split_ref.after_ref, f32[4,4,128,128]{3,2,1,0:T(8,128)S(1)} %copy-done.1), custom_call_target="tpu_custom_call" | custom-call | flops 8589934592 | tf_op jit(solution)/shard_map/update/pallas_call | solution.py:313
  44.5 0.0 collective-permute-done.17.refs_2_
  44.5 0.6 %collective-permute-done.16.refs_1_ = bf16[16,1024]{1,0:T(8,128)(2,1)S(1)} collective-permute-done((bf16[16,1024]{1,0:T(8,128)(2,1)S(1)}, bf16[16,1024]{1,0:T(8,128)(2,1)S(1)}, u32[]{:S(2)}, u32[]{:S(2)}) %collective-permute-start.16) | collective-permute-done | bytes 32800 | tf_op jit(solution)/shard_map/ppermute | solution.py:93
  45.1 0.0 collective-permute-done.15.refs_0_
  45.1 0.6 %final.1 = bf16[16,1024]{1,0:T(8,128)(2,1)} custom-call(bf16[16,1024]{1,0:T(8,128)(2,1)S(1)} %get-tuple-element.34.mixed_ref, f32[16,1024]{1,0:T(8,128)S(1)} %get-tuple-element.40.own_ref, bf16[16,1024]{1,0:T(8,128)(2,1)S(1)} %collective-permute-done.15.refs_0_, bf16[16,1024]{1,0:T(8,128)(2,1)S(1)} %collective-permute-done.16.refs_1_, ...), custom_call_target="tpu_custom_call" | custom-call | flops 8589934592 | tf_op jit(solution)/shard_map/final/pallas_call | solution.py:313
  (8 shorter events, 0.0 us)
Async XLA Ops:
  0.6 8.6 %copy-start.4 = (s32[4]{0:T(128)S(1)}, s32[4]{0:T(128)}, u32[]{:S(2)}) copy-start(s32[4]{0:T(128)} %param.13) | copy-start | bytes 52
  0.6 8.8 %copy-start.1 = (f32[4,4,128,128]{3,2,1,0:T(8,128)S(1)}, f32[4,4,128,128]{3,2,1,0:T(8,128)}, u32[]{:S(2)}) copy-start(f32[4,4,128,128]{3,2,1,0:T(8,128)} %state_ref.3) | copy-start | bytes 3145732
  3.5 6.9 %collective-permute-start = (bf16[80,128]{1,0:T(8,128)(2,1)S(1)}, bf16[80,128]{1,0:T(8,128)(2,1)S(1)}, u32[]{:S(2)}, u32[]{:S(2)}) collective-permute-start(bf16[80,128]{1,0:T(8,128)(2,1)S(1)} %get-tuple-element.24), channel_id=1, source_target_pairs={{0,12},{4,8},{8,4},{12,0},{1,13},{5,9},{9,5},{13,1},{2,14},{6,10},... | collective-permute-start | bytes 61448 | tf_op jit(solution)/shard_map/ppermute | solution.py:93
  8.6 4.7 %collective-permute-start.1 = (bf16[80,128]{1,0:T(8,128)(2,1)S(1)}, bf16[80,128]{1,0:T(8,128)(2,1)S(1)}, u32[]{:S(2)}, u32[]{:S(2)}) collective-permute-start(bf16[80,128]{1,0:T(8,128)(2,1)S(1)} %get-tuple-element.25), channel_id=1, source_target_pairs={{0,8},{4,12},{8,0},{12,4},{1,9},{5,13},{9,1},{13,5},{2,10},{6,14},... | collective-permute-start | bytes 61448 | tf_op jit(solution)/shard_map/ppermute | solution.py:93
  8.6 4.7 %collective-permute-start.2 = (bf16[80,128]{1,0:T(8,128)(2,1)S(1)}, bf16[80,128]{1,0:T(8,128)(2,1)S(1)}, u32[]{:S(2)}, u32[]{:S(2)}) collective-permute-start(bf16[80,128]{1,0:T(8,128)(2,1)S(1)} %get-tuple-element.26), channel_id=1, source_target_pairs={{0,4},{4,0},{8,12},{12,8},{1,5},{5,1},{9,13},{13,9},{2,6},{6,2},{1... | collective-permute-start | bytes 61448 | tf_op jit(solution)/shard_map/ppermute | solution.py:93
  13.3 6.6 %copy-start = (bf16[512,1024]{1,0:T(8,128)(2,1)S(1)}, bf16[512,1024]{1,0:T(8,128)(2,1)}, u32[]{:S(2)}) copy-start(bf16[512,1024]{1,0:T(8,128)(2,1)} %refs_4_.1) | copy-start | bytes 3145732
  13.8 10.5 %slice-start = ((s8[8388608]{0:T(1024)(128)(4,1)}), s8[4194304]{0:T(1024)(128)(4,1)S(1)}, s32[]{:S(2)}) async-start(s8[8388608]{0:T(1024)(128)(4,1)} %bitcast.2), calls=%async_computation | async-start | bytes 8388608
  13.8 10.5 %slice-start.1 = ((s8[8388608]{0:T(1024)(128)(4,1)}), s8[4194304]{0:T(1024)(128)(4,1)S(1)}, s32[]{:S(2)}) async-start(s8[8388608]{0:T(1024)(128)(4,1)} %bitcast.2), calls=%async_computation.1 | async-start | bytes 8388608
  13.8 10.5 %copy-start.2 = (bf16[16,1024]{1,0:T(8,128)(2,1)S(1)}, bf16[16,1024]{1,0:T(8,128)(2,1)}, u32[]{:S(2)}) copy-start(bf16[16,1024]{1,0:T(8,128)(2,1)} %x_ref.1) | copy-start | bytes 98308
  13.9 10.5 %copy-start.3 = (f32[1024]{0:T(1024)S(1)}, f32[1024]{0:T(1024)}, u32[]{:S(2)}) copy-start(f32[1024]{0:T(1024)} %param.21) | copy-start | bytes 12292
  13.9 5.5 %collective-permute-start.5 = (bf16[16,128]{1,0:T(8,128)(2,1)S(1)}, bf16[16,128]{1,0:T(8,128)(2,1)S(1)}, u32[]{:S(2)}, u32[]{:S(2)}) collective-permute-start(bf16[16,128]{1,0:T(8,128)(2,1)S(1)} %get-tuple-element.31.refs_0_), channel_id=1, source_target_pairs={{0,12},{4,8},{8,4},{12,0},{1,13},{5,9},{9,5},{13,1},{2,14},{6,10},... | collective-permute-start | bytes 12296 | tf_op jit(solution)/shard_map/ppermute | solution.py:93
  15.4 4.5 %collective-permute-start.4 = (bf16[16,128]{1,0:T(8,128)(2,1)S(1)}, bf16[16,128]{1,0:T(8,128)(2,1)S(1)}, u32[]{:S(2)}, u32[]{:S(2)}) collective-permute-start(bf16[16,128]{1,0:T(8,128)(2,1)S(1)} %get-tuple-element.31.refs_0_), channel_id=1, source_target_pairs={{0,8},{4,12},{8,0},{12,4},{1,9},{5,13},{9,1},{13,5},{2,10},{6,14},... | collective-permute-start | bytes 12296 | tf_op jit(solution)/shard_map/ppermute | solution.py:93
  16.0 3.9 %collective-permute-start.3 = (bf16[16,128]{1,0:T(8,128)(2,1)S(1)}, bf16[16,128]{1,0:T(8,128)(2,1)S(1)}, u32[]{:S(2)}, u32[]{:S(2)}) collective-permute-start(bf16[16,128]{1,0:T(8,128)(2,1)S(1)} %get-tuple-element.31.refs_0_), channel_id=1, source_target_pairs={{0,4},{4,0},{8,12},{12,8},{1,5},{5,1},{9,13},{13,9},{2,6},{6,2},{1... | collective-permute-start | bytes 12296 | tf_op jit(solution)/shard_map/ppermute | solution.py:93
  20.3 3.7 %collective-permute-start.8 = (bf16[16,1024]{1,0:T(8,128)(2,1)S(1)}, bf16[16,1024]{1,0:T(8,128)(2,1)S(1)}, u32[]{:S(2)}, u32[]{:S(2)}) collective-permute-start(bf16[16,1024]{1,0:T(8,128)(2,1)S(1)} %get-tuple-element.33), channel_id=1, source_target_pairs={{0,3},{1,2},{2,1},{3,0},{4,7},{5,6},{6,5},{7,4},{8,11},{9,10},{10,... | collective-permute-start | bytes 98312 | tf_op jit(solution)/shard_map/ppermute | solution.py:93
  20.3 4.0 %collective-permute-start.7 = (bf16[16,1024]{1,0:T(8,128)(2,1)S(1)}, bf16[16,1024]{1,0:T(8,128)(2,1)S(1)}, u32[]{:S(2)}, u32[]{:S(2)}) collective-permute-start(bf16[16,1024]{1,0:T(8,128)(2,1)S(1)} %get-tuple-element.33), channel_id=1, source_target_pairs={{0,2},{1,3},{2,0},{3,1},{4,6},{5,7},{6,4},{7,5},{8,10},{9,11},{10,... | collective-permute-start | bytes 98312 | tf_op jit(solution)/shard_map/ppermute | solution.py:93
  21.8 2.5 %collective-permute-start.6 = (bf16[16,1024]{1,0:T(8,128)(2,1)S(1)}, bf16[16,1024]{1,0:T(8,128)(2,1)S(1)}, u32[]{:S(2)}, u32[]{:S(2)}) collective-permute-start(bf16[16,1024]{1,0:T(8,128)(2,1)S(1)} %get-tuple-element.33), channel_id=1, source_target_pairs={{0,1},{1,0},{2,3},{3,2},{4,5},{5,4},{6,7},{7,6},{8,9},{9,8},{10,11... | collective-permute-start | bytes 98312 | tf_op jit(solution)/shard_map/ppermute | solution.py:93
  25.3 6.0 %collective-permute-start.9 = (bf16[16,1152]{1,0:T(8,128)(2,1)S(1)}, bf16[16,1152]{1,0:T(8,128)(2,1)S(1)}, u32[]{:S(2)}, u32[]{:S(2)}) collective-permute-start(bf16[16,1152]{1,0:T(8,128)(2,1)S(1)} %get-tuple-element.37), channel_id=1, source_target_pairs={{0,12},{4,8},{8,4},{12,0},{1,13},{5,9},{9,5},{13,1},{2,14},{6,10},... | collective-permute-start | bytes 110600 | tf_op jit(solution)/shard_map/ppermute | solution.py:93
  27.9 5.0 %collective-permute-start.10 = (bf16[16,1152]{1,0:T(8,128)(2,1)S(1)}, bf16[16,1152]{1,0:T(8,128)(2,1)S(1)}, u32[]{:S(2)}, u32[]{:S(2)}) collective-permute-start(bf16[16,1152]{1,0:T(8,128)(2,1)S(1)} %get-tuple-element.38), channel_id=1, source_target_pairs={{0,8},{4,12},{8,0},{12,4},{1,9},{5,13},{9,1},{13,5},{2,10},{6,14},... | collective-permute-start | bytes 110600 | tf_op jit(solution)/shard_map/ppermute | solution.py:93
  28.8 4.5 %collective-permute-start.11 = (bf16[16,1152]{1,0:T(8,128)(2,1)S(1)}, bf16[16,1152]{1,0:T(8,128)(2,1)S(1)}, u32[]{:S(2)}, u32[]{:S(2)}) collective-permute-start(bf16[16,1152]{1,0:T(8,128)(2,1)S(1)} %get-tuple-element.39), channel_id=1, source_target_pairs={{0,4},{4,0},{8,12},{12,8},{1,5},{5,1},{9,13},{13,9},{2,6},{6,2},{1... | collective-permute-start | bytes 110600 | tf_op jit(solution)/shard_map/ppermute | solution.py:93
  29.7 8.1 %slice-start.2 = ((s8[8388608]{0:T(1024)(128)(4,1)}), s8[4194304]{0:T(1024)(128)(4,1)S(1)}, s32[]{:S(2)}) async-start(s8[8388608]{0:T(1024)(128)(4,1)} %bitcast.4), calls=%async_computation.2 | async-start | bytes 8388608
  30.1 7.8 %slice-start.3 = ((s8[8388608]{0:T(1024)(128)(4,1)}), s8[4194304]{0:T(1024)(128)(4,1)S(1)}, s32[]{:S(2)}) async-start(s8[8388608]{0:T(1024)(128)(4,1)} %bitcast.4), calls=%async_computation.3 | async-start | bytes 8388608
  33.4 5.8 %collective-permute-start.14 = (bf16[16,1024]{1,0:T(8,128)(2,1)S(1)}, bf16[16,1024]{1,0:T(8,128)(2,1)S(1)}, u32[]{:S(2)}, u32[]{:S(2)}) collective-permute-start(bf16[16,1024]{1,0:T(8,128)(2,1)S(1)} %hidden.1.refs_0_), channel_id=1, source_target_pairs={{0,12},{4,8},{8,4},{12,0},{1,13},{5,9},{9,5},{13,1},{2,14},{6,10},... | collective-permute-start | bytes 98312 | tf_op jit(solution)/shard_map/ppermute | solution.py:93
  35.2 5.1 %collective-permute-start.13 = (bf16[16,1024]{1,0:T(8,128)(2,1)S(1)}, bf16[16,1024]{1,0:T(8,128)(2,1)S(1)}, u32[]{:S(2)}, u32[]{:S(2)}) collective-permute-start(bf16[16,1024]{1,0:T(8,128)(2,1)S(1)} %hidden.1.refs_0_), channel_id=1, source_target_pairs={{0,8},{4,12},{8,0},{12,4},{1,9},{5,13},{9,1},{13,5},{2,10},{6,14},... | collective-permute-start | bytes 98312 | tf_op jit(solution)/shard_map/ppermute | solution.py:93
  35.4 5.3 %collective-permute-start.12 = (bf16[16,1024]{1,0:T(8,128)(2,1)S(1)}, bf16[16,1024]{1,0:T(8,128)(2,1)S(1)}, u32[]{:S(2)}, u32[]{:S(2)}) collective-permute-start(bf16[16,1024]{1,0:T(8,128)(2,1)S(1)} %hidden.1.refs_0_), channel_id=1, source_target_pairs={{0,4},{4,0},{8,12},{12,8},{1,5},{5,1},{9,13},{13,9},{2,6},{6,2},{1... | collective-permute-start | bytes 98312 | tf_op jit(solution)/shard_map/ppermute | solution.py:93
  41.0 3.4 %collective-permute-start.17 = (bf16[16,1024]{1,0:T(8,128)(2,1)S(1)}, bf16[16,1024]{1,0:T(8,128)(2,1)S(1)}, u32[]{:S(2)}, u32[]{:S(2)}) collective-permute-start(bf16[16,1024]{1,0:T(8,128)(2,1)S(1)} %get-tuple-element.41), channel_id=1, source_target_pairs={{0,3},{1,2},{2,1},{3,0},{4,7},{5,6},{6,5},{7,4},{8,11},{9,10},{10,... | collective-permute-start | bytes 98312 | tf_op jit(solution)/shard_map/ppermute | solution.py:93
  41.1 4.0 %collective-permute-start.16 = (bf16[16,1024]{1,0:T(8,128)(2,1)S(1)}, bf16[16,1024]{1,0:T(8,128)(2,1)S(1)}, u32[]{:S(2)}, u32[]{:S(2)}) collective-permute-start(bf16[16,1024]{1,0:T(8,128)(2,1)S(1)} %get-tuple-element.41), channel_id=1, source_target_pairs={{0,2},{1,3},{2,0},{3,1},{4,6},{5,7},{6,4},{7,5},{8,10},{9,11},{10,... | collective-permute-start | bytes 98312 | tf_op jit(solution)/shard_map/ppermute | solution.py:93
  42.3 2.8 %collective-permute-start.15 = (bf16[16,1024]{1,0:T(8,128)(2,1)S(1)}, bf16[16,1024]{1,0:T(8,128)(2,1)S(1)}, u32[]{:S(2)}, u32[]{:S(2)}) collective-permute-start(bf16[16,1024]{1,0:T(8,128)(2,1)S(1)} %get-tuple-element.41), channel_id=1, source_target_pairs={{0,1},{1,0},{2,3},{3,2},{4,5},{5,4},{6,7},{7,6},{8,9},{9,8},{10,11... | collective-permute-start | bytes 98312 | tf_op jit(solution)/shard_map/ppermute | solution.py:93

commit v7 on v6

--- a/solution.py
+++ b/solution.py
@@ -11,6 +11,7 @@
 HEADS = 16
 DIRECT = 8
 LANES = 128
+ORDERS = ((2, 3, 1), (2, 3, 1), (3, 2, 1), (2, 3, 1), (2, 3, 1), (3, 2, 1))
 RATE = 1 << 33
 F32, BF16 = jnp.float32, jnp.bfloat16
 
@@ -87,6 +88,13 @@
     down_terms = jnp.dot(hidden, w_down, preferred_element_type=jnp.float32)
     layer_out = (middle + lax.psum(down_terms, "tp")).astype(jnp.bfloat16)
     return (layer_out, new_state)
+
+
+def exchange(values, axis, n, order):
+    steps = [s for s in order if s < n] + [s for s in reversed(range(1, n)) if s not in order]
+    if not isinstance(values, list):
+        steps, values = steps[::-1], [values] * (n - 1)
+    return [swap(values[s - 1], axis, n, s) for s in steps], steps
 
 
 def swap(value, axis, n, step):
@@ -224,7 +232,8 @@
         copy.wait()
 
 
-def out_kernel(n, *refs):
+def out_kernel(steps, *refs):
+    n = len(steps)
     parts, (w_ref, own_ref, sent_ref) = refs[:n], refs[n:]
     kept = jnp.concatenate([p[...] for p in parts], axis=0)
     many, size = kept.shape
@@ -235,7 +244,9 @@
     to = lax.broadcasted_iota(jnp.int32, (many, many), 0)
     of = lax.broadcasted_iota(jnp.int32, (many, many), 1)
     head, row = to // rows, to % rows
-    hot = ((row // block) ^ me) * (heads * block) + head * block + row % block == of
+    part = of // (heads * block)
+    owner = sum(jnp.where(part == i, me ^ s, 0) for i, s in enumerate(steps))
+    hot = (owner == row // block) & (of % (heads * block) == head * block + row % block)
     kept = jnp.dot(hot.astype(F32).astype(BF16), kept, preferred_element_type=F32).astype(BF16)
     kept = jnp.concatenate([kept[h * rows : (h + 1) * rows] for h in range(heads)], axis=1)
     terms = jnp.dot(kept, w_ref[...], preferred_element_type=F32)
@@ -359,7 +370,7 @@
             ],
             us=2,
         )
-        got = [swap(sent[s - 1], "kv", n, s) for s in reversed(range(1, n))]
+        got, _ = exchange(sent, "kv", n, ORDERS[0])
         half = size // 2
         freq = 10000.0 ** (-(jnp.arange(half, dtype=F32) * 2.0) / size)
         angle = positions.astype(F32)[:, None] * freq[None, :]
@@ -384,15 +395,16 @@
             gamma,
             prepared,
         )
-        kept = [kept] + [swap(kept, "kv", n, s) for s in range(1, n)]
+        got, steps = exchange(kept, "kv", n, ORDERS[1])
         own, sent = call(
-            functools.partial(out_kernel, n),
+            functools.partial(out_kernel, (0, *steps)),
             "out",
             [((rows, depth), F32), ((rows, depth), BF16)],
-            *kept,
+            kept,
+            *got,
             near(w_out),
         )
-        got = [swap(sent, "tp", n_tp, s) for s in range(1, n_tp)]
+        got, _ = exchange(sent, "tp", n_tp, ORDERS[2])
         part = w_up.shape[1] // n
         w_up = near(w_up)
         mixed, normed, split, *sent = call(
@@ -406,7 +418,7 @@
             own,
             *got,
         )
-        got = [swap(sent[s - 1], "kv", n, s) for s in reversed(range(1, n))]
+        got, _ = exchange(sent, "kv", n, ORDERS[3])
         (new_state,) = call(
             update_kernel,
             "update",
@@ -424,23 +436,23 @@
             functools.partial(up_own_kernel, n), "up_own", [((rows, part), F32)], normed, w_up
         )
         (hidden,) = call(hidden_kernel, "hidden", [((rows, part), BF16)], own, split, *got)
-        got = [swap(hidden, "kv", n, s) for s in range(1, n)]
+        got, steps = exchange(hidden, "kv", n, ORDERS[4])
         w_down = near(w_down)
         (own,) = call(
             functools.partial(down_kernel, n, 0, False), "down_own", [((rows, depth), F32)], hidden, w_down
         )
-        for s in reversed(range(1, n)):
-            last = s == 1
+        for i, s in reversed(list(enumerate(steps))):
+            last = i == 0
             own, *sent = call(
                 functools.partial(down_kernel, n, s, last),
                 f"down_{s}",
                 [((rows, depth), F32)] + [((rows, depth), BF16)] * last,
-                got[s - 1],
+                got[i],
                 w_down,
                 own,
             )
         (sent,) = sent
-        got = [swap(sent, "tp", n_tp, s) for s in range(1, n_tp)]
+        got, _ = exchange(sent, "tp", n_tp, ORDERS[5])
         (layer_out,) = call(final_kernel, "final", [((rows, depth), BF16)], mixed, own, *got, kept=False)
         return (layer_out, new_state)
 

time: 45.9 us -> 45.5 us (level)
  starting transfers between devices: 22.8 us -> 20.1 us
  waiting for transfers between devices: 12.9 us -> 15.3 us
    ppermute x18, starting transfers between devices: 22.8 us -> 20.1 us  [swap(): return lax.ppermute(value, axis, [(i, i ^ step) for i in range(n)])]
    ppermute x18, waiting for transfers between devices: 12.9 us -> 15.3 us  [swap(): return lax.ppermute(value, axis, [(i, i ^ step) for i in range(n)])]
where the time goes in v7:
time: 45.5 us; the launch traced here: 45.3 us
  starting transfers between devices  20.1 us (44%)
  waiting for transfers between devices  15.3 us (34%)
  Pallas kernels  9.05 us (20%)
  between operations  0.77 us (2%)
    ppermute x18, starting transfers between devices, swap(): return lax.ppermute(value, axis, [(i, i ^ step) for i in range(n)])  20.1 us
    ppermute x18, waiting for transfers between devices, swap(): return lax.ppermute(value, axis, [(i, i ^ step) for i in range(n)])  15.3 us
    pallas_call x13, Pallas kernels, call(): pl.pallas_call(kernel, name=name, out_shape=[(pltpu.VMEM if kept else jax...  9.05 us
  transfers between devices with their start and end apart: 18, of which 12 were waited for; matrix products, arithmetic and copies ran while one was open for 0% of the time, Pallas kernels for 7%

profile of v7, /device:TPU:0, one launch (start us, length us, event | category | flops | bytes accessed | tf_op | source)
XLA Modules:
  0.0 45.3 jit_solution(16367026543384877018)
XLA Ops:
  0.6 0.0 copy-start.4
  0.6 0.0 copy-start.1
  0.7 2.8 %project.1 = (f32[80,128]{1,0:T(8,128)S(1)}, bf16[80,128]{1,0:T(8,128)(2,1)S(1)}, bf16[80,128]{1,0:T(8,128)(2,1)S(1)}, bf16[80,128]{1,0:T(8,128)(2,1)S(1)}) custom-call(bf16[16,1024]{1,0:T(8,128)(2,1)} %x_ref.1, f32[1,1024]{1,0:T(1,128)} %bitcast.7, bf16[1024,512]{1,0:T(8,128)(2,1)} %refs_0_.1, bf16[1024,512]{1,0:T(8,128)(2,1)} %refs_1_.5, ...), custom_call_target="tpu_custom_call" | custom-call | flops 17179869184 | tf_op jit(solution)/shard_map/project/pallas_call | solution.py:324
  3.5 4.1 %collective-permute-start = (bf16[80,128]{1,0:T(8,128)(2,1)S(1)}, bf16[80,128]{1,0:T(8,128)(2,1)S(1)}, u32[]{:S(2)}, u32[]{:S(2)}) collective-permute-start(bf16[80,128]{1,0:T(8,128)(2,1)S(1)} %get-tuple-element.24), channel_id=1, source_target_pairs={{0,8},{4,12},{8,0},{12,4},{1,9},{5,13},{9,1},{13,5},{2,10},{6,14},... | collective-permute-start | bytes 61448 | tf_op jit(solution)/shard_map/ppermute | solution.py:101
  7.6 1.3 %collective-permute-start.1 = (bf16[80,128]{1,0:T(8,128)(2,1)S(1)}, bf16[80,128]{1,0:T(8,128)(2,1)S(1)}, u32[]{:S(2)}, u32[]{:S(2)}) collective-permute-start(bf16[80,128]{1,0:T(8,128)(2,1)S(1)} %get-tuple-element.25), channel_id=1, source_target_pairs={{0,12},{4,8},{8,4},{12,0},{1,13},{5,9},{9,5},{13,1},{2,14},{6,10},... | collective-permute-start | bytes 61448 | tf_op jit(solution)/shard_map/ppermute | solution.py:101
  9.0 0.2 collective-permute-start.2
  9.2 0.0 copy-done.4
  9.2 0.1 multiply_sine_fusion
  9.3 0.0 copy-done.1
  9.3 0.2 prepare.1
  9.5 0.0 collective-permute-done.refs_0_
  9.5 3.7 %collective-permute-done.1.refs_1_ = bf16[80,128]{1,0:T(8,128)(2,1)S(1)} collective-permute-done((bf16[80,128]{1,0:T(8,128)(2,1)S(1)}, bf16[80,128]{1,0:T(8,128)(2,1)S(1)}, u32[]{:S(2)}, u32[]{:S(2)}) %collective-permute-start.1) | collective-permute-done | bytes 20512 | tf_op jit(solution)/shard_map/ppermute | solution.py:101
  13.2 0.0 collective-permute-done.2.refs_2_
  13.2 0.0 copy-start
  13.2 0.5 %read.1 = (bf16[16,128]{1,0:T(8,128)(2,1)S(1)}, f32[16,128]{1,0:T(8,128)S(1)}, f32[16,128]{1,0:T(8,128)S(1)}) custom-call(f32[80,128]{1,0:T(8,128)S(1)} %get-tuple-element.23.own_ref, bf16[80,128]{1,0:T(8,128)(2,1)S(1)} %collective-permute-done.refs_0_, bf16[80,128]{1,0:T(8,128)(2,1)S(1)} %collective-permute-done.1.refs_1_, ...), custom_call_target="tpu_custom_call" | custom-call | flops 8589934592 | tf_op jit(solution)/shard_map/read/pallas_call | solution.py:324
  13.7 0.0 copy-start.2
  13.7 0.0 copy-start.3
  13.8 1.3 %collective-permute-start.5 = (bf16[16,128]{1,0:T(8,128)(2,1)S(1)}, bf16[16,128]{1,0:T(8,128)(2,1)S(1)}, u32[]{:S(2)}, u32[]{:S(2)}) collective-permute-start(bf16[16,128]{1,0:T(8,128)(2,1)S(1)} %get-tuple-element.31.refs_0_), channel_id=1, source_target_pairs={{0,8},{4,12},{8,0},{12,4},{1,9},{5,13},{9,1},{13,5},{2,10},{6,14},... | collective-permute-start | bytes 12296 | tf_op jit(solution)/shard_map/ppermute | solution.py:101
  15.1 0.9 %collective-permute-start.4 = (bf16[16,128]{1,0:T(8,128)(2,1)S(1)}, bf16[16,128]{1,0:T(8,128)(2,1)S(1)}, u32[]{:S(2)}, u32[]{:S(2)}) collective-permute-start(bf16[16,128]{1,0:T(8,128)(2,1)S(1)} %get-tuple-element.31.refs_0_), channel_id=1, source_target_pairs={{0,12},{4,8},{8,4},{12,0},{1,13},{5,9},{9,5},{13,1},{2,14},{6,10},... | collective-permute-start | bytes 12296 | tf_op jit(solution)/shard_map/ppermute | solution.py:101
  16.0 1.3 %collective-permute-start.3 = (bf16[16,128]{1,0:T(8,128)(2,1)S(1)}, bf16[16,128]{1,0:T(8,128)(2,1)S(1)}, u32[]{:S(2)}, u32[]{:S(2)}) collective-permute-start(bf16[16,128]{1,0:T(8,128)(2,1)S(1)} %get-tuple-element.31.refs_0_), channel_id=1, source_target_pairs={{0,4},{4,0},{8,12},{12,8},{1,5},{5,1},{9,13},{13,9},{2,6},{6,2},{1... | collective-permute-start | bytes 12296 | tf_op jit(solution)/shard_map/ppermute | solution.py:101
  17.3 1.0 %collective-permute-done.5.refs_3_ = bf16[16,128]{1,0:T(8,128)(2,1)S(1)} collective-permute-done((bf16[16,128]{1,0:T(8,128)(2,1)S(1)}, bf16[16,128]{1,0:T(8,128)(2,1)S(1)}, u32[]{:S(2)}, u32[]{:S(2)}) %collective-permute-start.5) | collective-permute-done | bytes 4128 | tf_op jit(solution)/shard_map/ppermute | solution.py:101
  18.3 2.1 %collective-permute-done.4.refs_2_ = bf16[16,128]{1,0:T(8,128)(2,1)S(1)} collective-permute-done((bf16[16,128]{1,0:T(8,128)(2,1)S(1)}, bf16[16,128]{1,0:T(8,128)(2,1)S(1)}, u32[]{:S(2)}, u32[]{:S(2)}) %collective-permute-start.4) | collective-permute-done | bytes 4128 | tf_op jit(solution)/shard_map/ppermute | solution.py:101
  20.5 0.0 collective-permute-done.3.refs_1_
  20.5 0.0 copy-done
  20.5 0.3 out.1
  20.8 0.0 collective-permute-start.8
  20.8 1.5 %collective-permute-start.7 = (bf16[16,1024]{1,0:T(8,128)(2,1)S(1)}, bf16[16,1024]{1,0:T(8,128)(2,1)S(1)}, u32[]{:S(2)}, u32[]{:S(2)}) collective-permute-start(bf16[16,1024]{1,0:T(8,128)(2,1)S(1)} %get-tuple-element.33), channel_id=1, source_target_pairs={{0,2},{1,3},{2,0},{3,1},{4,6},{5,7},{6,4},{7,5},{8,10},{9,11},{10,... | collective-permute-start | bytes 98312 | tf_op jit(solution)/shard_map/ppermute | solution.py:101
  22.4 0.3 collective-permute-start.6
  22.7 1.8 %collective-permute-done.8.refs_2_ = bf16[16,1024]{1,0:T(8,128)(2,1)S(1)} collective-permute-done((bf16[16,1024]{1,0:T(8,128)(2,1)S(1)}, bf16[16,1024]{1,0:T(8,128)(2,1)S(1)}, u32[]{:S(2)}, u32[]{:S(2)}) %collective-permute-start.8) | collective-permute-done | bytes 32800 | tf_op jit(solution)/shard_map/ppermute | solution.py:101
  24.5 0.4 collective-permute-done.7.refs_1_
  24.9 0.0 collective-permute-done.6.refs_0_
  24.9 0.0 slice-done
  24.9 0.0 slice-done.1
  24.9 0.0 copy-done.2
  24.9 0.0 copy-done.3
  24.9 0.9 %up.1 = (bf16[16,1024]{1,0:T(8,128)(2,1)S(1)}, bf16[16,1024]{1,0:T(8,128)(2,1)S(1)}, f32[16,128]{1,0:T(8,128)S(1)}, bf16[16,1152]{1,0:T(8,128)(2,1)S(1)}, bf16[1...) custom-call(bf16[16,1024]{1,0:T(8,128)(2,1)S(1)} %copy-done.2, f32[1,1024]{1,0:T(1,128)S(1)} %bitcast.6, ...), custom_call_target="tpu_custom_call" | custom-call | flops 8589934592 | tf_op jit(solution)/shard_map/up/pallas_call | solution.py:324
  25.8 1.0 %collective-permute-start.9 = (bf16[16,1152]{1,0:T(8,128)(2,1)S(1)}, bf16[16,1152]{1,0:T(8,128)(2,1)S(1)}, u32[]{:S(2)}, u32[]{:S(2)}) collective-permute-start(bf16[16,1152]{1,0:T(8,128)(2,1)S(1)} %get-tuple-element.37), channel_id=1, source_target_pairs={{0,8},{4,12},{8,0},{12,4},{1,9},{5,13},{9,1},{13,5},{2,10},{6,14},... | collective-permute-start | bytes 110600 | tf_op jit(solution)/shard_map/ppermute | solution.py:101
  26.9 1.8 %collective-permute-start.10 = (bf16[16,1152]{1,0:T(8,128)(2,1)S(1)}, bf16[16,1152]{1,0:T(8,128)(2,1)S(1)}, u32[]{:S(2)}, u32[]{:S(2)}) collective-permute-start(bf16[16,1152]{1,0:T(8,128)(2,1)S(1)} %get-tuple-element.38), channel_id=1, source_target_pairs={{0,12},{4,8},{8,4},{12,0},{1,13},{5,9},{9,5},{13,1},{2,14},{6,10},... | collective-permute-start | bytes 110600 | tf_op jit(solution)/shard_map/ppermute | solution.py:101
  28.7 0.7 %collective-permute-start.11 = (bf16[16,1152]{1,0:T(8,128)(2,1)S(1)}, bf16[16,1152]{1,0:T(8,128)(2,1)S(1)}, u32[]{:S(2)}, u32[]{:S(2)}) collective-permute-start(bf16[16,1152]{1,0:T(8,128)(2,1)S(1)} %get-tuple-element.39), channel_id=1, source_target_pairs={{0,4},{4,0},{8,12},{12,8},{1,5},{5,1},{9,13},{13,9},{2,6},{6,2},{1... | collective-permute-start | bytes 110600 | tf_op jit(solution)/shard_map/ppermute | solution.py:101
  29.4 0.4 up_own.1.own_ref
  29.7 1.7 %collective-permute-done.9.refs_0_ = bf16[16,1152]{1,0:T(8,128)(2,1)S(1)} collective-permute-done((bf16[16,1152]{1,0:T(8,128)(2,1)S(1)}, bf16[16,1152]{1,0:T(8,128)(2,1)S(1)}, u32[]{:S(2)}, u32[]{:S(2)}) %collective-permute-start.9) | collective-permute-done | bytes 36896 | tf_op jit(solution)/shard_map/ppermute | solution.py:101
  31.5 1.2 %collective-permute-done.10.refs_1_ = bf16[16,1152]{1,0:T(8,128)(2,1)S(1)} collective-permute-done((bf16[16,1152]{1,0:T(8,128)(2,1)S(1)}, bf16[16,1152]{1,0:T(8,128)(2,1)S(1)}, u32[]{:S(2)}, u32[]{:S(2)}) %collective-permute-start.10) | collective-permute-done | bytes 36896 | tf_op jit(solution)/shard_map/ppermute | solution.py:101
  32.6 0.4 collective-permute-done.11.refs_2_
  33.0 0.2 hidden.1.refs_0_
  33.2 0.9 %collective-permute-start.14 = (bf16[16,1024]{1,0:T(8,128)(2,1)S(1)}, bf16[16,1024]{1,0:T(8,128)(2,1)S(1)}, u32[]{:S(2)}, u32[]{:S(2)}) collective-permute-start(bf16[16,1024]{1,0:T(8,128)(2,1)S(1)} %hidden.1.refs_0_), channel_id=1, source_target_pairs={{0,8},{4,12},{8,0},{12,4},{1,9},{5,13},{9,1},{13,5},{2,10},{6,14},... | collective-permute-start | bytes 98312 | tf_op jit(solution)/shard_map/ppermute | solution.py:101
  34.1 1.8 %collective-permute-start.13 = (bf16[16,1024]{1,0:T(8,128)(2,1)S(1)}, bf16[16,1024]{1,0:T(8,128)(2,1)S(1)}, u32[]{:S(2)}, u32[]{:S(2)}) collective-permute-start(bf16[16,1024]{1,0:T(8,128)(2,1)S(1)} %hidden.1.refs_0_), channel_id=1, source_target_pairs={{0,12},{4,8},{8,4},{12,0},{1,13},{5,9},{9,5},{13,1},{2,14},{6,10},... | collective-permute-start | bytes 98312 | tf_op jit(solution)/shard_map/ppermute | solution.py:101
  35.9 0.8 %collective-permute-start.12 = (bf16[16,1024]{1,0:T(8,128)(2,1)S(1)}, bf16[16,1024]{1,0:T(8,128)(2,1)S(1)}, u32[]{:S(2)}, u32[]{:S(2)}) collective-permute-start(bf16[16,1024]{1,0:T(8,128)(2,1)S(1)} %hidden.1.refs_0_), channel_id=1, source_target_pairs={{0,4},{4,0},{8,12},{12,8},{1,5},{5,1},{9,13},{13,9},{2,6},{6,2},{1... | collective-permute-start | bytes 98312 | tf_op jit(solution)/shard_map/ppermute | solution.py:101
  36.7 0.0 slice-done.2
  36.7 0.0 slice-done.3
  36.8 0.4 down_own.1.refs_2_
  37.1 1.4 %collective-permute-done.14.refs_0_ = bf16[16,1024]{1,0:T(8,128)(2,1)S(1)} collective-permute-done((bf16[16,1024]{1,0:T(8,128)(2,1)S(1)}, bf16[16,1024]{1,0:T(8,128)(2,1)S(1)}, u32[]{:S(2)}, u32[]{:S(2)}) %collective-permute-start.14) | collective-permute-done | bytes 32800 | tf_op jit(solution)/shard_map/ppermute | solution.py:101
  38.5 0.4 down_2.1.refs_2_
  38.9 1.0 %collective-permute-done.13.refs_0_ = bf16[16,1024]{1,0:T(8,128)(2,1)S(1)} collective-permute-done((bf16[16,1024]{1,0:T(8,128)(2,1)S(1)}, bf16[16,1024]{1,0:T(8,128)(2,1)S(1)}, u32[]{:S(2)}, u32[]{:S(2)}) %collective-permute-start.13) | collective-permute-done | bytes 32800 | tf_op jit(solution)/shard_map/ppermute | solution.py:101
  39.8 0.4 down_3.1.refs_2_
  40.2 0.0 collective-permute-done.12.refs_0_
  40.2 0.4 down_1.1
  40.6 0.0 collective-permute-start.17
  40.6 1.5 %collective-permute-start.16 = (bf16[16,1024]{1,0:T(8,128)(2,1)S(1)}, bf16[16,1024]{1,0:T(8,128)(2,1)S(1)}, u32[]{:S(2)}, u32[]{:S(2)}) collective-permute-start(bf16[16,1024]{1,0:T(8,128)(2,1)S(1)} %get-tuple-element.41), channel_id=1, source_target_pairs={{0,2},{1,3},{2,0},{3,1},{4,6},{5,7},{6,4},{7,5},{8,10},{9,11},{10,... | collective-permute-start | bytes 98312 | tf_op jit(solution)/shard_map/ppermute | solution.py:101
  42.2 0.3 collective-permute-start.15
  42.5 1.5 %update.1 = f32[4,4,128,128]{3,2,1,0:T(8,128)} custom-call(f32[16,128]{1,0:T(8,128)S(1)} %get-tuple-element.42.key_ref, f32[16,128]{1,0:T(8,128)S(1)} %get-tuple-element.43.value_ref, f32[16,128]{1,0:T(8,128)S(1)} %get-tuple-element.29.refs_5_.gamma_ref, f32[16,128]{1,0:T(8,128)S(1)} %get-tuple-element.36.split_ref.after_ref, f32[4,4,128,128]{3,2,1,0:T(8,128)S(1)} %copy-done.1), custom_call_target="tpu_custom_call" | custom-call | flops 8589934592 | tf_op jit(solution)/shard_map/update/pallas_call | solution.py:324
  44.0 0.3 collective-permute-done.17.refs_2_
  44.3 0.4 collective-permute-done.16.refs_1_
  44.7 0.0 collective-permute-done.15.refs_0_
  44.7 0.6 %final.1 = bf16[16,1024]{1,0:T(8,128)(2,1)} custom-call(bf16[16,1024]{1,0:T(8,128)(2,1)S(1)} %get-tuple-element.34.mixed_ref, f32[16,1024]{1,0:T(8,128)S(1)} %get-tuple-element.40.own_ref, bf16[16,1024]{1,0:T(8,128)(2,1)S(1)} %collective-permute-done.15.refs_0_, bf16[16,1024]{1,0:T(8,128)(2,1)S(1)} %collective-permute-done.16.refs_1_, ...), custom_call_target="tpu_custom_call" | custom-call | flops 8589934592 | tf_op jit(solution)/shard_map/final/pallas_call | solution.py:324
  (8 shorter events, 0.0 us)
Async XLA Ops:
  0.6 8.6 %copy-start.4 = (s32[4]{0:T(128)S(1)}, s32[4]{0:T(128)}, u32[]{:S(2)}) copy-start(s32[4]{0:T(128)} %param.13) | copy-start | bytes 52
  0.6 8.7 %copy-start.1 = (f32[4,4,128,128]{3,2,1,0:T(8,128)S(1)}, f32[4,4,128,128]{3,2,1,0:T(8,128)}, u32[]{:S(2)}) copy-start(f32[4,4,128,128]{3,2,1,0:T(8,128)} %state_ref.3) | copy-start | bytes 3145732
  3.5 6.0 %collective-permute-start = (bf16[80,128]{1,0:T(8,128)(2,1)S(1)}, bf16[80,128]{1,0:T(8,128)(2,1)S(1)}, u32[]{:S(2)}, u32[]{:S(2)}) collective-permute-start(bf16[80,128]{1,0:T(8,128)(2,1)S(1)} %get-tuple-element.24), channel_id=1, source_target_pairs={{0,8},{4,12},{8,0},{12,4},{1,9},{5,13},{9,1},{13,5},{2,10},{6,14},... | collective-permute-start | bytes 61448 | tf_op jit(solution)/shard_map/ppermute | solution.py:101
  7.6 5.6 %collective-permute-start.1 = (bf16[80,128]{1,0:T(8,128)(2,1)S(1)}, bf16[80,128]{1,0:T(8,128)(2,1)S(1)}, u32[]{:S(2)}, u32[]{:S(2)}) collective-permute-start(bf16[80,128]{1,0:T(8,128)(2,1)S(1)} %get-tuple-element.25), channel_id=1, source_target_pairs={{0,12},{4,8},{8,4},{12,0},{1,13},{5,9},{9,5},{13,1},{2,14},{6,10},... | collective-permute-start | bytes 61448 | tf_op jit(solution)/shard_map/ppermute | solution.py:101
  9.0 4.2 %collective-permute-start.2 = (bf16[80,128]{1,0:T(8,128)(2,1)S(1)}, bf16[80,128]{1,0:T(8,128)(2,1)S(1)}, u32[]{:S(2)}, u32[]{:S(2)}) collective-permute-start(bf16[80,128]{1,0:T(8,128)(2,1)S(1)} %get-tuple-element.26), channel_id=1, source_target_pairs={{0,4},{4,0},{8,12},{12,8},{1,5},{5,1},{9,13},{13,9},{2,6},{6,2},{1... | collective-permute-start | bytes 61448 | tf_op jit(solution)/shard_map/ppermute | solution.py:101
  13.2 7.3 %copy-start = (bf16[512,1024]{1,0:T(8,128)(2,1)S(1)}, bf16[512,1024]{1,0:T(8,128)(2,1)}, u32[]{:S(2)}) copy-start(bf16[512,1024]{1,0:T(8,128)(2,1)} %refs_4_.1) | copy-start | bytes 3145732
  13.7 11.1 %slice-start = ((s8[8388608]{0:T(1024)(128)(4,1)}), s8[4194304]{0:T(1024)(128)(4,1)S(1)}, s32[]{:S(2)}) async-start(s8[8388608]{0:T(1024)(128)(4,1)} %bitcast.2), calls=%async_computation | async-start | bytes 8388608
  13.7 11.1 %slice-start.1 = ((s8[8388608]{0:T(1024)(128)(4,1)}), s8[4194304]{0:T(1024)(128)(4,1)S(1)}, s32[]{:S(2)}) async-start(s8[8388608]{0:T(1024)(128)(4,1)} %bitcast.2), calls=%async_computation.1 | async-start | bytes 8388608
  13.7 11.2 %copy-start.2 = (bf16[16,1024]{1,0:T(8,128)(2,1)S(1)}, bf16[16,1024]{1,0:T(8,128)(2,1)}, u32[]{:S(2)}) copy-start(bf16[16,1024]{1,0:T(8,128)(2,1)} %x_ref.1) | copy-start | bytes 98308
  13.7 11.1 %copy-start.3 = (f32[1024]{0:T(1024)S(1)}, f32[1024]{0:T(1024)}, u32[]{:S(2)}) copy-start(f32[1024]{0:T(1024)} %param.21) | copy-start | bytes 12292
  13.8 4.6 %collective-permute-start.5 = (bf16[16,128]{1,0:T(8,128)(2,1)S(1)}, bf16[16,128]{1,0:T(8,128)(2,1)S(1)}, u32[]{:S(2)}, u32[]{:S(2)}) collective-permute-start(bf16[16,128]{1,0:T(8,128)(2,1)S(1)} %get-tuple-element.31.refs_0_), channel_id=1, source_target_pairs={{0,8},{4,12},{8,0},{12,4},{1,9},{5,13},{9,1},{13,5},{2,10},{6,14},... | collective-permute-start | bytes 12296 | tf_op jit(solution)/shard_map/ppermute | solution.py:101
  15.1 5.4 %collective-permute-start.4 = (bf16[16,128]{1,0:T(8,128)(2,1)S(1)}, bf16[16,128]{1,0:T(8,128)(2,1)S(1)}, u32[]{:S(2)}, u32[]{:S(2)}) collective-permute-start(bf16[16,128]{1,0:T(8,128)(2,1)S(1)} %get-tuple-element.31.refs_0_), channel_id=1, source_target_pairs={{0,12},{4,8},{8,4},{12,0},{1,13},{5,9},{9,5},{13,1},{2,14},{6,10},... | collective-permute-start | bytes 12296 | tf_op jit(solution)/shard_map/ppermute | solution.py:101
  16.0 4.5 %collective-permute-start.3 = (bf16[16,128]{1,0:T(8,128)(2,1)S(1)}, bf16[16,128]{1,0:T(8,128)(2,1)S(1)}, u32[]{:S(2)}, u32[]{:S(2)}) collective-permute-start(bf16[16,128]{1,0:T(8,128)(2,1)S(1)} %get-tuple-element.31.refs_0_), channel_id=1, source_target_pairs={{0,4},{4,0},{8,12},{12,8},{1,5},{5,1},{9,13},{13,9},{2,6},{6,2},{1... | collective-permute-start | bytes 12296 | tf_op jit(solution)/shard_map/ppermute | solution.py:101
  20.8 3.7 %collective-permute-start.8 = (bf16[16,1024]{1,0:T(8,128)(2,1)S(1)}, bf16[16,1024]{1,0:T(8,128)(2,1)S(1)}, u32[]{:S(2)}, u32[]{:S(2)}) collective-permute-start(bf16[16,1024]{1,0:T(8,128)(2,1)S(1)} %get-tuple-element.33), channel_id=1, source_target_pairs={{0,3},{1,2},{2,1},{3,0},{4,7},{5,6},{6,5},{7,4},{8,11},{9,10},{10,... | collective-permute-start | bytes 98312 | tf_op jit(solution)/shard_map/ppermute | solution.py:101
  20.8 4.0 %collective-permute-start.7 = (bf16[16,1024]{1,0:T(8,128)(2,1)S(1)}, bf16[16,1024]{1,0:T(8,128)(2,1)S(1)}, u32[]{:S(2)}, u32[]{:S(2)}) collective-permute-start(bf16[16,1024]{1,0:T(8,128)(2,1)S(1)} %get-tuple-element.33), channel_id=1, source_target_pairs={{0,2},{1,3},{2,0},{3,1},{4,6},{5,7},{6,4},{7,5},{8,10},{9,11},{10,... | collective-permute-start | bytes 98312 | tf_op jit(solution)/shard_map/ppermute | solution.py:101
  22.4 2.5 %collective-permute-start.6 = (bf16[16,1024]{1,0:T(8,128)(2,1)S(1)}, bf16[16,1024]{1,0:T(8,128)(2,1)S(1)}, u32[]{:S(2)}, u32[]{:S(2)}) collective-permute-start(bf16[16,1024]{1,0:T(8,128)(2,1)S(1)} %get-tuple-element.33), channel_id=1, source_target_pairs={{0,1},{1,0},{2,3},{3,2},{4,5},{5,4},{6,7},{7,6},{8,9},{9,8},{10,11... | collective-permute-start | bytes 98312 | tf_op jit(solution)/shard_map/ppermute | solution.py:101
  25.8 5.6 %collective-permute-start.9 = (bf16[16,1152]{1,0:T(8,128)(2,1)S(1)}, bf16[16,1152]{1,0:T(8,128)(2,1)S(1)}, u32[]{:S(2)}, u32[]{:S(2)}) collective-permute-start(bf16[16,1152]{1,0:T(8,128)(2,1)S(1)} %get-tuple-element.37), channel_id=1, source_target_pairs={{0,8},{4,12},{8,0},{12,4},{1,9},{5,13},{9,1},{13,5},{2,10},{6,14},... | collective-permute-start | bytes 110600 | tf_op jit(solution)/shard_map/ppermute | solution.py:101
  26.9 5.8 %collective-permute-start.10 = (bf16[16,1152]{1,0:T(8,128)(2,1)S(1)}, bf16[16,1152]{1,0:T(8,128)(2,1)S(1)}, u32[]{:S(2)}, u32[]{:S(2)}) collective-permute-start(bf16[16,1152]{1,0:T(8,128)(2,1)S(1)} %get-tuple-element.38), channel_id=1, source_target_pairs={{0,12},{4,8},{8,4},{12,0},{1,13},{5,9},{9,5},{13,1},{2,14},{6,10},... | collective-permute-start | bytes 110600 | tf_op jit(solution)/shard_map/ppermute | solution.py:101
  28.7 4.4 %collective-permute-start.11 = (bf16[16,1152]{1,0:T(8,128)(2,1)S(1)}, bf16[16,1152]{1,0:T(8,128)(2,1)S(1)}, u32[]{:S(2)}, u32[]{:S(2)}) collective-permute-start(bf16[16,1152]{1,0:T(8,128)(2,1)S(1)} %get-tuple-element.39), channel_id=1, source_target_pairs={{0,4},{4,0},{8,12},{12,8},{1,5},{5,1},{9,13},{13,9},{2,6},{6,2},{1... | collective-permute-start | bytes 110600 | tf_op jit(solution)/shard_map/ppermute | solution.py:101
  29.3 7.4 %slice-start.2 = ((s8[8388608]{0:T(1024)(128)(4,1)}), s8[4194304]{0:T(1024)(128)(4,1)S(1)}, s32[]{:S(2)}) async-start(s8[8388608]{0:T(1024)(128)(4,1)} %bitcast.4), calls=%async_computation.2 | async-start | bytes 8388608
  29.7 7.0 %slice-start.3 = ((s8[8388608]{0:T(1024)(128)(4,1)}), s8[4194304]{0:T(1024)(128)(4,1)S(1)}, s32[]{:S(2)}) async-start(s8[8388608]{0:T(1024)(128)(4,1)} %bitcast.4), calls=%async_computation.3 | async-start | bytes 8388608
  33.2 5.3 %collective-permute-start.14 = (bf16[16,1024]{1,0:T(8,128)(2,1)S(1)}, bf16[16,1024]{1,0:T(8,128)(2,1)S(1)}, u32[]{:S(2)}, u32[]{:S(2)}) collective-permute-start(bf16[16,1024]{1,0:T(8,128)(2,1)S(1)} %hidden.1.refs_0_), channel_id=1, source_target_pairs={{0,8},{4,12},{8,0},{12,4},{1,9},{5,13},{9,1},{13,5},{2,10},{6,14},... | collective-permute-start | bytes 98312 | tf_op jit(solution)/shard_map/ppermute | solution.py:101
  34.1 5.7 %collective-permute-start.13 = (bf16[16,1024]{1,0:T(8,128)(2,1)S(1)}, bf16[16,1024]{1,0:T(8,128)(2,1)S(1)}, u32[]{:S(2)}, u32[]{:S(2)}) collective-permute-start(bf16[16,1024]{1,0:T(8,128)(2,1)S(1)} %hidden.1.refs_0_), channel_id=1, source_target_pairs={{0,12},{4,8},{8,4},{12,0},{1,13},{5,9},{9,5},{13,1},{2,14},{6,10},... | collective-permute-start | bytes 98312 | tf_op jit(solution)/shard_map/ppermute | solution.py:101
  35.9 4.3 %collective-permute-start.12 = (bf16[16,1024]{1,0:T(8,128)(2,1)S(1)}, bf16[16,1024]{1,0:T(8,128)(2,1)S(1)}, u32[]{:S(2)}, u32[]{:S(2)}) collective-permute-start(bf16[16,1024]{1,0:T(8,128)(2,1)S(1)} %hidden.1.refs_0_), channel_id=1, source_target_pairs={{0,4},{4,0},{8,12},{12,8},{1,5},{5,1},{9,13},{13,9},{2,6},{6,2},{1... | collective-permute-start | bytes 98312 | tf_op jit(solution)/shard_map/ppermute | solution.py:101
  40.6 3.7 %collective-permute-start.17 = (bf16[16,1024]{1,0:T(8,128)(2,1)S(1)}, bf16[16,1024]{1,0:T(8,128)(2,1)S(1)}, u32[]{:S(2)}, u32[]{:S(2)}) collective-permute-start(bf16[16,1024]{1,0:T(8,128)(2,1)S(1)} %get-tuple-element.41), channel_id=1, source_target_pairs={{0,3},{1,2},{2,1},{3,0},{4,7},{5,6},{6,5},{7,4},{8,11},{9,10},{10,... | collective-permute-start | bytes 98312 | tf_op jit(solution)/shard_map/ppermute | solution.py:101
  40.6 4.1 %collective-permute-start.16 = (bf16[16,1024]{1,0:T(8,128)(2,1)S(1)}, bf16[16,1024]{1,0:T(8,128)(2,1)S(1)}, u32[]{:S(2)}, u32[]{:S(2)}) collective-permute-start(bf16[16,1024]{1,0:T(8,128)(2,1)S(1)} %get-tuple-element.41), channel_id=1, source_target_pairs={{0,2},{1,3},{2,0},{3,1},{4,6},{5,7},{6,4},{7,5},{8,10},{9,11},{10,... | collective-permute-start | bytes 98312 | tf_op jit(solution)/shard_map/ppermute | solution.py:101
  42.2 2.5 %collective-permute-start.15 = (bf16[16,1024]{1,0:T(8,128)(2,1)S(1)}, bf16[16,1024]{1,0:T(8,128)(2,1)S(1)}, u32[]{:S(2)}, u32[]{:S(2)}) collective-permute-start(bf16[16,1024]{1,0:T(8,128)(2,1)S(1)} %get-tuple-element.41), channel_id=1, source_target_pairs={{0,1},{1,0},{2,3},{3,2},{4,5},{5,4},{6,7},{7,6},{8,9},{9,8},{10,11... | collective-permute-start | bytes 98312 | tf_op jit(solution)/shard_map/ppermute | solution.py:101

commit v8 on v6

--- a/solution.py
+++ b/solution.py
@@ -7,10 +7,15 @@
 from jax.experimental.pallas import tpu as pltpu
 from jax.sharding import PartitionSpec as P
 
+
 D = 4096
 HEADS = 16
 DIRECT = 8
 LANES = 128
+X1, X2, X3 = (1, 0, 3, 2), (2, 3, 0, 1), (3, 2, 1, 0)
+C, R = (1, 3, 0, 2), (2, 0, 3, 1)
+PERMS = ((X2, X3, X1), (X2, X3, X1), (X3, X2, X1), (X2, X3, X1), (C, X3, R), (X3, X2, X1))
+TURNS = (0, 1, 2)
 RATE = 1 << 33
 F32, BF16 = jnp.float32, jnp.bfloat16
 
@@ -89,8 +94,28 @@
     return (layer_out, new_state)
 
 
-def swap(value, axis, n, step):
-    return lax.ppermute(value, axis, [(i, i ^ step) for i in range(n)])
+def partners(n, i):
+    if n == 4:
+        return PERMS[i]
+    return [tuple(j ^ s for j in range(n)) for s in reversed(range(1, n))]
+
+
+def inverse(perm):
+    return tuple(perm.index(j) for j in range(len(perm)))
+
+
+def lookup(axis, perm):
+    me = lax.axis_index(axis)
+    return sum(jnp.where(me == j, entry, 0) for j, entry in enumerate(perm))
+
+
+def exchange(values, axis, perms):
+    if not isinstance(values, list):
+        values = [values] * len(perms)
+    got = []
+    for value, perm in zip(values, perms):
+        got.append(lax.ppermute(value, axis, list(enumerate(perm))))
+    return got
 
 
 def pieces(value):
@@ -100,17 +125,18 @@
     return high, middle, rest - middle
 
 
-def reorder(n, values):
-    me = lax.axis_index("kv")
+def reorder(perms, values):
     rows = values.shape[0]
-    block = rows // n
+    block = rows // len(perms)
     to = lax.broadcasted_iota(jnp.int32, (rows, rows), 0)
     of = lax.broadcasted_iota(jnp.int32, (rows, rows), 1)
-    hot = ((to // block) ^ me) * block + to % block == of
+    owner = sum(jnp.where(to // block == k, lookup("kv", perm), 0) for k, perm in enumerate(perms))
+    hot = owner * block + to % block == of
     return jnp.dot(hot.astype(F32).astype(BF16), values, preferred_element_type=F32)
 
 
-def project_kernel(n, chunks, flight, x_hbm, gain_hbm, *refs):
+def project_kernel(perms, chunks, flight, x_hbm, gain_hbm, *refs):
+    n = len(perms)
     weights, outs, (x_ref, gain_ref, held, sems, small) = refs[:4], refs[4 : 4 + n], refs[4 + n :]
     first = [
         pltpu.make_async_copy(x_hbm, x_ref, small.at[0]),
@@ -128,7 +154,7 @@
     for copy in first + copies[:flight]:
         copy.start()
     first[0].wait()
-    x = reorder(n, x_ref[...])
+    x = reorder(perms, x_ref[...])
     lane = lax.broadcasted_iota(jnp.int32, (rows, LANES), 1)
     high, mid, low = pieces(jnp.sum(x * x, axis=1, keepdims=True))
     split = jnp.where(lane == 0, high, jnp.where(lane == 1, mid, jnp.where(lane == 2, low, 0.0)))
@@ -209,7 +235,7 @@
 
 def update_kernel(key_ref, value_ref, gamma_ref, after_ref, state_ref, new_hbm, new_ref, sems):
     del after_ref
-    block, head_dev, size, _ = state_ref.shape
+    block, head_dev, _, _ = state_ref.shape
     copies = []
     for h in range(head_dev):
         rows = slice(h * block, (h + 1) * block)
@@ -224,18 +250,20 @@
         copy.wait()
 
 
-def out_kernel(n, *refs):
+def out_kernel(perms, *refs):
+    n = len(perms)
     parts, (w_ref, own_ref, sent_ref) = refs[:n], refs[n:]
     kept = jnp.concatenate([p[...] for p in parts], axis=0)
     many, size = kept.shape
     heads = w_ref.shape[0] // size
     block = many // n // heads
     rows = n * block
-    me = lax.axis_index("kv")
     to = lax.broadcasted_iota(jnp.int32, (many, many), 0)
     of = lax.broadcasted_iota(jnp.int32, (many, many), 1)
     head, row = to // rows, to % rows
-    hot = ((row // block) ^ me) * (heads * block) + head * block + row % block == of
+    part = of // (heads * block)
+    owner = sum(jnp.where(part == k, lookup("kv", inverse(perm)), 0) for k, perm in enumerate(perms))
+    hot = (owner == row // block) & (of % (heads * block) == head * block + row % block)
     kept = jnp.dot(hot.astype(F32).astype(BF16), kept, preferred_element_type=F32).astype(BF16)
     kept = jnp.concatenate([kept[h * rows : (h + 1) * rows] for h in range(heads)], axis=1)
     terms = jnp.dot(kept, w_ref[...], preferred_element_type=F32)
@@ -243,7 +271,7 @@
     sent_ref[...] = terms.astype(BF16)
 
 
-def up_kernel(n_tp, n, x_ref, gain_ref, w_ref, own_ref, *refs):
+def up_kernel(n_tp, perms, x_ref, gain_ref, w_ref, own_ref, *refs):
     got, (mixed_ref, normed_ref, split_ref, *sent) = refs[: n_tp - 1], refs[n_tp - 1 :]
     total = own_ref[...]
     for g in got:
@@ -258,11 +286,9 @@
     lane = lax.broadcasted_iota(jnp.int32, (rows, LANES), 1)
     split = jnp.where(lane == 0, high, jnp.where(lane == 1, mid, jnp.where(lane == 2, low, 0.0)))
     split_ref[...] = split
-    part = w_ref.shape[1] // n
-    me = lax.axis_index("kv")
-    for s in reversed(range(1, n)):
-        at = pl.ds(pl.multiple_of((me ^ s) * part, part), part)
-        out = sent[s - 1]
+    part = sent[0].shape[1] - LANES
+    for perm, out in zip(perms, sent):
+        at = pl.ds(pl.multiple_of(lookup("kv", perm) * part, part), part)
         out[:, :part] = jnp.dot(normed, w_ref[:, at], preferred_element_type=F32).astype(out.dtype)
         out[:, part:] = split.astype(out.dtype)
 
@@ -285,12 +311,12 @@
     out_ref[...] = jnp.square(jnp.maximum(total * scale, 0.0)).astype(BF16)
 
 
-def down_kernel(n, s, last, *refs):
+def down_kernel(perm, first, last, *refs):
     part_ref, w_ref, *refs = refs
-    part = w_ref.shape[0] // n
-    at = pl.ds(pl.multiple_of((lax.axis_index("kv") ^ s) * part, part), part)
+    part = part_ref.shape[1]
+    at = pl.ds(pl.multiple_of(lookup("kv", inverse(perm)) * part, part), part)
     total = jnp.dot(part_ref[...], w_ref[at, :], preferred_element_type=F32)
-    if s:
+    if not first:
         total = total + refs.pop(0)[...]
     refs[0][...] = total
     if last:
@@ -309,10 +335,9 @@
 HBM = pl.BlockSpec(memory_space=pltpu.HBM)
 
 
-def call(kernel, name, outs, *args, specs=None, out_specs=None, scratch=(), limit=8, us=1, kept=True):
+def call(kernel, outs, *args, specs=None, out_specs=None, scratch=(), limit=8, us=1, kept=True):
     return pl.pallas_call(
         kernel,
-        name=name,
         out_shape=[(pltpu.VMEM if kept else jax.ShapeDtypeStruct)(*o) for o in outs],
         in_specs=specs or [VMEM] * len(args),
         out_specs=out_specs or [VMEM] * len(outs),
@@ -339,9 +364,10 @@
         width = head_dev * size
         group = head_dev * block
         chunks, flight = 1, 4
+        same = tuple(range(n))
+        perms = partners(n, 0)
         own, *sent = call(
-            functools.partial(project_kernel, n, chunks, flight),
-            "project",
+            functools.partial(project_kernel, [same, *perms], chunks, flight),
             [((5 * group, size), F32)] + [((5 * group, size), BF16)] * (n - 1),
             far(tokens),
             far(norm_gain[None]),
@@ -359,7 +385,7 @@
             ],
             us=2,
         )
-        got = [swap(sent[s - 1], "kv", n, s) for s in reversed(range(1, n))]
+        got = exchange(sent, "kv", perms)
         half = size // 2
         freq = 10000.0 ** (-(jnp.arange(half, dtype=F32) * 2.0) / size)
         angle = positions.astype(F32)[:, None] * freq[None, :]
@@ -367,7 +393,6 @@
         state = near(state)
         prepared, cosine, sine, gamma = call(
             prepare_kernel,
-            "prepare",
             [((head_dev, 2 * size, block * size), BF16)] + [((group, size), F32)] * 3,
             state,
             cosine,
@@ -375,7 +400,6 @@
         )
         kept, key, value = call(
             functools.partial(read_kernel, n, block),
-            "read",
             [((group, size), BF16), ((group, size), F32), ((group, size), F32)],
             own,
             *got,
@@ -384,20 +408,21 @@
             gamma,
             prepared,
         )
-        kept = [kept] + [swap(kept, "kv", n, s) for s in range(1, n)]
+        perms = partners(n, 1)
+        got = exchange(kept, "kv", perms)
         own, sent = call(
-            functools.partial(out_kernel, n),
-            "out",
+            functools.partial(out_kernel, [same, *perms]),
             [((rows, depth), F32), ((rows, depth), BF16)],
-            *kept,
+            kept,
+            *got,
             near(w_out),
         )
-        got = [swap(sent, "tp", n_tp, s) for s in range(1, n_tp)]
+        got = exchange(sent, "tp", partners(n_tp, 2))
         part = w_up.shape[1] // n
         w_up = near(w_up)
+        perms = partners(n, 3)
         mixed, normed, split, *sent = call(
-            functools.partial(up_kernel, n_tp, n),
-            "up",
+            functools.partial(up_kernel, n_tp, perms),
             [((rows, depth), BF16), ((rows, depth), BF16), ((rows, LANES), F32)]
             + [((rows, part + LANES), BF16)] * (n - 1),
             tokens,
@@ -406,10 +431,9 @@
             own,
             *got,
         )
-        got = [swap(sent[s - 1], "kv", n, s) for s in reversed(range(1, n))]
+        got = exchange(sent, "kv", perms)
         (new_state,) = call(
             update_kernel,
-            "update",
             [(state.shape, F32)],
             key,
             value,
@@ -420,28 +444,25 @@
             scratch=[pltpu.VMEM(state.shape, F32), pltpu.SemaphoreType.DMA((block, head_dev))],
             kept=False,
         )
-        (own,) = call(
-            functools.partial(up_own_kernel, n), "up_own", [((rows, part), F32)], normed, w_up
-        )
-        (hidden,) = call(hidden_kernel, "hidden", [((rows, part), BF16)], own, split, *got)
-        got = [swap(hidden, "kv", n, s) for s in range(1, n)]
+        (own,) = call(functools.partial(up_own_kernel, n), [((rows, part), F32)], normed, w_up)
+        (hidden,) = call(hidden_kernel, [((rows, part), BF16)], own, split, *got)
+        perms = partners(n, 4)
+        got = exchange(hidden, "kv", perms)
         w_down = near(w_down)
-        (own,) = call(
-            functools.partial(down_kernel, n, 0, False), "down_own", [((rows, depth), F32)], hidden, w_down
-        )
-        for s in reversed(range(1, n)):
-            last = s == 1
+        (own,) = call(functools.partial(down_kernel, same, True, False), [((rows, depth), F32)], hidden, w_down)
+        turns = TURNS if n == 4 else range(n - 1)
+        for k in turns:
+            last = k == turns[-1]
             own, *sent = call(
-                functools.partial(down_kernel, n, s, last),
-                f"down_{s}",
+                functools.partial(down_kernel, perms[k], False, last),
                 [((rows, depth), F32)] + [((rows, depth), BF16)] * last,
-                got[s - 1],
+                got[k],
                 w_down,
                 own,
             )
         (sent,) = sent
-        got = [swap(sent, "tp", n_tp, s) for s in range(1, n_tp)]
-        (layer_out,) = call(final_kernel, "final", [((rows, depth), BF16)], mixed, own, *got, kept=False)
+        got = exchange(sent, "tp", partners(n_tp, 5))
+        (layer_out,) = call(final_kernel, [((rows, depth), BF16)], mixed, own, *got, kept=False)
         return (layer_out, new_state)
 
     return shards

time: 45.9 us -> 46.6 us (1.015)
  waiting for transfers between devices: 12.9 us -> 16 us
  starting transfers between devices: 22.8 us -> 20.5 us
    ppermute x18, waiting for transfers between devices: 12.9 us -> 16 us  [exchange(): got.append(lax.ppermute(value, axis, list(enumerate(perm))))]
    ppermute x18, starting transfers between devices: 22.8 us -> 20.5 us  [exchange(): got.append(lax.ppermute(value, axis, list(enumerate(perm))))]
  transfers between devices with their start and end apart: 18 -> 18, of which waited for: 12 -> 13; matrix products, arithmetic and copies ran while one was open for 0% -> 0% of each run, Pallas kernels for 7% -> 7%
where the time goes in v8:
time: 46.6 us; the launch traced here: 46.5 us
  starting transfers between devices  20.5 us (44%)
  waiting for transfers between devices  16 us (34%)
  Pallas kernels  9.05 us (19%)
  between operations  0.78 us (2%)
    ppermute x18, starting transfers between devices, exchange(): got.append(lax.ppermute(value, axis, list(enumerate(perm))))  20.5 us
    ppermute x18, waiting for transfers between devices, exchange(): got.append(lax.ppermute(value, axis, list(enumerate(perm))))  16 us
    pallas_call x13, Pallas kernels, call(): pl.pallas_call(kernel, out_shape=[(pltpu.VMEM if kept else jax.ShapeDtype...  9.05 us
  transfers between devices with their start and end apart: 18, of which 13 were waited for; matrix products, arithmetic and copies ran while one was open for 0% of the time, Pallas kernels for 7%

profile of v8, /device:TPU:0, one launch (start us, length us, event | category | flops | bytes accessed | tf_op | source)
XLA Modules:
  0.0 46.5 jit_solution(779921924470753499)
XLA Ops:
  0.6 0.0 copy-start.4
  0.6 0.0 copy-start.1
  0.7 2.8 %shard_map.131 = (f32[80,128]{1,0:T(8,128)S(1)}, bf16[80,128]{1,0:T(8,128)(2,1)S(1)}, bf16[80,128]{1,0:T(8,128)(2,1)S(1)}, bf16[80,128]{1,0:T(8,128)(2,1)S(1)}) custom-call(bf16[16,1024]{1,0:T(8,128)(2,1)} %x_ref.1, f32[1,1024]{1,0:T(1,128)} %bitcast.7, bf16[1024,512]{1,0:T(8,128)(2,1)} %refs_0_.1, bf16[1024,512]{1,0:T(8,128)(2,1)} %refs_1_.5, ...), custom_call_target="tpu_custom_call" | custom-call | flops 17179869184 | tf_op jit(solution)/shard_map/pallas_call | solution.py:339
  3.5 4.1 %collective-permute-start = (bf16[80,128]{1,0:T(8,128)(2,1)S(1)}, bf16[80,128]{1,0:T(8,128)(2,1)S(1)}, u32[]{:S(2)}, u32[]{:S(2)}) collective-permute-start(bf16[80,128]{1,0:T(8,128)(2,1)S(1)} %get-tuple-element.24), channel_id=1, source_target_pairs={{0,8},{4,12},{8,0},{12,4},{1,9},{5,13},{9,1},{13,5},{2,10},{6,14},... | collective-permute-start | bytes 61448 | tf_op jit(solution)/shard_map/ppermute | solution.py:117
  7.6 1.3 %collective-permute-start.1 = (bf16[80,128]{1,0:T(8,128)(2,1)S(1)}, bf16[80,128]{1,0:T(8,128)(2,1)S(1)}, u32[]{:S(2)}, u32[]{:S(2)}) collective-permute-start(bf16[80,128]{1,0:T(8,128)(2,1)S(1)} %get-tuple-element.25), channel_id=1, source_target_pairs={{0,12},{4,8},{8,4},{12,0},{1,13},{5,9},{9,5},{13,1},{2,14},{6,10},... | collective-permute-start | bytes 61448 | tf_op jit(solution)/shard_map/ppermute | solution.py:117
  9.0 0.2 collective-permute-start.2
  9.2 0.0 copy-done.4
  9.2 0.1 multiply_sine_fusion
  9.3 0.0 copy-done.1
  9.3 0.2 shard_map.132
  9.5 0.0 collective-permute-done.refs_0_
  9.5 3.7 %collective-permute-done.1.refs_1_ = bf16[80,128]{1,0:T(8,128)(2,1)S(1)} collective-permute-done((bf16[80,128]{1,0:T(8,128)(2,1)S(1)}, bf16[80,128]{1,0:T(8,128)(2,1)S(1)}, u32[]{:S(2)}, u32[]{:S(2)}) %collective-permute-start.1) | collective-permute-done | bytes 20512 | tf_op jit(solution)/shard_map/ppermute | solution.py:117
  13.2 0.0 collective-permute-done.2.refs_2_
  13.2 0.5 %shard_map.133 = (bf16[16,128]{1,0:T(8,128)(2,1)S(1)}, f32[16,128]{1,0:T(8,128)S(1)}, f32[16,128]{1,0:T(8,128)S(1)}) custom-call(f32[80,128]{1,0:T(8,128)S(1)} %get-tuple-element.23.own_ref, bf16[80,128]{1,0:T(8,128)(2,1)S(1)} %collective-permute-done.refs_0_, bf16[80,128]{1,0:T(8,128)(2,1)S(1)} %collective-permute-done.1.refs_1_, ...), custom_call_target="tpu_custom_call" | custom-call | flops 8589934592 | tf_op jit(solution)/shard_map/pallas_call | solution.py:339
  13.7 0.0 slice-start
  13.7 0.0 copy-start.2
  13.7 0.0 copy-start.3
  13.8 0.1 collective-permute-start.5
  13.8 2.7 %collective-permute-start.4 = (bf16[16,128]{1,0:T(8,128)(2,1)S(1)}, bf16[16,128]{1,0:T(8,128)(2,1)S(1)}, u32[]{:S(2)}, u32[]{:S(2)}) collective-permute-start(bf16[16,128]{1,0:T(8,128)(2,1)S(1)} %get-tuple-element.31.refs_0_), channel_id=1, source_target_pairs={{0,12},{4,8},{8,4},{12,0},{1,13},{5,9},{9,5},{13,1},{2,14},{6,10},... | collective-permute-start | bytes 12296 | tf_op jit(solution)/shard_map/ppermute | solution.py:117
  16.5 0.8 %collective-permute-start.3 = (bf16[16,128]{1,0:T(8,128)(2,1)S(1)}, bf16[16,128]{1,0:T(8,128)(2,1)S(1)}, u32[]{:S(2)}, u32[]{:S(2)}) collective-permute-start(bf16[16,128]{1,0:T(8,128)(2,1)S(1)} %get-tuple-element.31.refs_0_), channel_id=1, source_target_pairs={{0,8},{4,12},{8,0},{12,4},{1,9},{5,13},{9,1},{13,5},{2,10},{6,14},... | collective-permute-start | bytes 12296 | tf_op jit(solution)/shard_map/ppermute | solution.py:117
  17.3 0.1 collective-permute-done.5.refs_3_
  17.4 1.9 %collective-permute-done.4.refs_2_ = bf16[16,128]{1,0:T(8,128)(2,1)S(1)} collective-permute-done((bf16[16,128]{1,0:T(8,128)(2,1)S(1)}, bf16[16,128]{1,0:T(8,128)(2,1)S(1)}, u32[]{:S(2)}, u32[]{:S(2)}) %collective-permute-start.4) | collective-permute-done | bytes 4128 | tf_op jit(solution)/shard_map/ppermute | solution.py:117
  19.3 1.7 %collective-permute-done.3.refs_1_ = bf16[16,128]{1,0:T(8,128)(2,1)S(1)} collective-permute-done((bf16[16,128]{1,0:T(8,128)(2,1)S(1)}, bf16[16,128]{1,0:T(8,128)(2,1)S(1)}, u32[]{:S(2)}, u32[]{:S(2)}) %collective-permute-start.3) | collective-permute-done | bytes 4128 | tf_op jit(solution)/shard_map/ppermute | solution.py:117
  21.0 0.0 copy-done
  21.0 0.4 shard_map.134
  21.4 0.0 collective-permute-start.8
  21.4 1.5 %collective-permute-start.7 = (bf16[16,1024]{1,0:T(8,128)(2,1)S(1)}, bf16[16,1024]{1,0:T(8,128)(2,1)S(1)}, u32[]{:S(2)}, u32[]{:S(2)}) collective-permute-start(bf16[16,1024]{1,0:T(8,128)(2,1)S(1)} %get-tuple-element.33), channel_id=1, source_target_pairs={{0,2},{1,3},{2,0},{3,1},{4,6},{5,7},{6,4},{7,5},{8,10},{9,11},{10,... | collective-permute-start | bytes 98312 | tf_op jit(solution)/shard_map/ppermute | solution.py:117
  22.9 0.3 collective-permute-start.6
  23.2 0.0 collective-permute-done.8.refs_2_
  23.3 2.1 %collective-permute-done.7.refs_1_ = bf16[16,1024]{1,0:T(8,128)(2,1)S(1)} collective-permute-done((bf16[16,1024]{1,0:T(8,128)(2,1)S(1)}, bf16[16,1024]{1,0:T(8,128)(2,1)S(1)}, u32[]{:S(2)}, u32[]{:S(2)}) %collective-permute-start.7) | collective-permute-done | bytes 32800 | tf_op jit(solution)/shard_map/ppermute | solution.py:117
  25.3 0.9 %collective-permute-done.6.refs_0_ = bf16[16,1024]{1,0:T(8,128)(2,1)S(1)} collective-permute-done((bf16[16,1024]{1,0:T(8,128)(2,1)S(1)}, bf16[16,1024]{1,0:T(8,128)(2,1)S(1)}, u32[]{:S(2)}, u32[]{:S(2)}) %collective-permute-start.6) | collective-permute-done | bytes 32800 | tf_op jit(solution)/shard_map/ppermute | solution.py:117
  26.3 0.0 slice-done
  26.3 0.0 slice-done.1
  26.3 0.0 copy-done.2
  26.3 0.0 copy-done.3
  26.3 0.9 %shard_map.135 = (bf16[16,1024]{1,0:T(8,128)(2,1)S(1)}, bf16[16,1024]{1,0:T(8,128)(2,1)S(1)}, f32[16,128]{1,0:T(8,128)S(1)}, bf16[16,1152]{1,0:T(8,128)(2,1)S(1)...) custom-call(bf16[16,1024]{1,0:T(8,128)(2,1)S(1)} %copy-done.2, f32[1,1024]{1,0:T(1,128)S(1)} %bitcast.6, ...), custom_call_target="tpu_custom_call" | custom-call | flops 8589934592 | tf_op jit(solution)/shard_map/pallas_call | solution.py:339
  27.2 0.8 %collective-permute-start.9 = (bf16[16,1152]{1,0:T(8,128)(2,1)S(1)}, bf16[16,1152]{1,0:T(8,128)(2,1)S(1)}, u32[]{:S(2)}, u32[]{:S(2)}) collective-permute-start(bf16[16,1152]{1,0:T(8,128)(2,1)S(1)} %get-tuple-element.37), channel_id=1, source_target_pairs={{0,8},{4,12},{8,0},{12,4},{1,9},{5,13},{9,1},{13,5},{2,10},{6,14},... | collective-permute-start | bytes 110600 | tf_op jit(solution)/shard_map/ppermute | solution.py:117
  28.0 2.0 %collective-permute-start.10 = (bf16[16,1152]{1,0:T(8,128)(2,1)S(1)}, bf16[16,1152]{1,0:T(8,128)(2,1)S(1)}, u32[]{:S(2)}, u32[]{:S(2)}) collective-permute-start(bf16[16,1152]{1,0:T(8,128)(2,1)S(1)} %get-tuple-element.38), channel_id=1, source_target_pairs={{0,12},{4,8},{8,4},{12,0},{1,13},{5,9},{9,5},{13,1},{2,14},{6,10},... | collective-permute-start | bytes 110600 | tf_op jit(solution)/shard_map/ppermute | solution.py:117
  30.1 0.7 %collective-permute-start.11 = (bf16[16,1152]{1,0:T(8,128)(2,1)S(1)}, bf16[16,1152]{1,0:T(8,128)(2,1)S(1)}, u32[]{:S(2)}, u32[]{:S(2)}) collective-permute-start(bf16[16,1152]{1,0:T(8,128)(2,1)S(1)} %get-tuple-element.39), channel_id=1, source_target_pairs={{0,4},{4,0},{8,12},{12,8},{1,5},{5,1},{9,13},{13,9},{2,6},{6,2},{1... | collective-permute-start | bytes 110600 | tf_op jit(solution)/shard_map/ppermute | solution.py:117
  30.7 0.4 shard_map.136.own_ref
  31.1 2.1 %collective-permute-done.9.refs_0_ = bf16[16,1152]{1,0:T(8,128)(2,1)S(1)} collective-permute-done((bf16[16,1152]{1,0:T(8,128)(2,1)S(1)}, bf16[16,1152]{1,0:T(8,128)(2,1)S(1)}, u32[]{:S(2)}, u32[]{:S(2)}) %collective-permute-start.9) | collective-permute-done | bytes 36896 | tf_op jit(solution)/shard_map/ppermute | solution.py:117
  33.2 0.7 %collective-permute-done.10.refs_1_ = bf16[16,1152]{1,0:T(8,128)(2,1)S(1)} collective-permute-done((bf16[16,1152]{1,0:T(8,128)(2,1)S(1)}, bf16[16,1152]{1,0:T(8,128)(2,1)S(1)}, u32[]{:S(2)}, u32[]{:S(2)}) %collective-permute-start.10) | collective-permute-done | bytes 36896 | tf_op jit(solution)/shard_map/ppermute | solution.py:117
  33.9 0.4 collective-permute-done.11.refs_2_
  34.3 0.2 shard_map.137.refs_0_
  34.5 0.5 collective-permute-start.14
  34.9 1.6 %collective-permute-start.13 = (bf16[16,1024]{1,0:T(8,128)(2,1)S(1)}, bf16[16,1024]{1,0:T(8,128)(2,1)S(1)}, u32[]{:S(2)}, u32[]{:S(2)}) collective-permute-start(bf16[16,1024]{1,0:T(8,128)(2,1)S(1)} %shard_map.137.refs_0_), channel_id=1, source_target_pairs={{0,12},{4,8},{8,4},{12,0},{1,13},{5,9},{9,5},{13,1},{2,14},{6,10},... | collective-permute-start | bytes 98312 | tf_op jit(solution)/shard_map/ppermute | solution.py:117
  36.5 1.9 %collective-permute-start.12 = (bf16[16,1024]{1,0:T(8,128)(2,1)S(1)}, bf16[16,1024]{1,0:T(8,128)(2,1)S(1)}, u32[]{:S(2)}, u32[]{:S(2)}) collective-permute-start(bf16[16,1024]{1,0:T(8,128)(2,1)S(1)} %shard_map.137.refs_0_), channel_id=1, source_target_pairs={{0,8},{4,0},{8,12},{12,4},{1,9},{5,1},{9,13},{13,5},{2,10},{6,2},{... | collective-permute-start | bytes 98312 | tf_op jit(solution)/shard_map/ppermute | solution.py:117
  38.5 0.0 slice-done.2
  38.5 0.0 slice-done.3
  38.5 0.4 shard_map.138.refs_2_
  38.9 0.5 %collective-permute-done.14.refs_0_ = bf16[16,1024]{1,0:T(8,128)(2,1)S(1)} collective-permute-done((bf16[16,1024]{1,0:T(8,128)(2,1)S(1)}, bf16[16,1024]{1,0:T(8,128)(2,1)S(1)}, u32[]{:S(2)}, u32[]{:S(2)}) %collective-permute-start.14) | collective-permute-done | bytes 32800 | tf_op jit(solution)/shard_map/ppermute | solution.py:117
  39.3 0.4 shard_map.139.refs_2_
  39.7 1.0 %collective-permute-done.13.refs_0_ = bf16[16,1024]{1,0:T(8,128)(2,1)S(1)} collective-permute-done((bf16[16,1024]{1,0:T(8,128)(2,1)S(1)}, bf16[16,1024]{1,0:T(8,128)(2,1)S(1)}, u32[]{:S(2)}, u32[]{:S(2)}) %collective-permute-start.13) | collective-permute-done | bytes 32800 | tf_op jit(solution)/shard_map/ppermute | solution.py:117
  40.7 0.4 shard_map.140.refs_2_
  41.1 0.0 collective-permute-done.12.refs_0_
  41.1 0.4 shard_map.141
  41.5 0.0 collective-permute-start.17
  41.5 1.0 %collective-permute-start.16 = (bf16[16,1024]{1,0:T(8,128)(2,1)S(1)}, bf16[16,1024]{1,0:T(8,128)(2,1)S(1)}, u32[]{:S(2)}, u32[]{:S(2)}) collective-permute-start(bf16[16,1024]{1,0:T(8,128)(2,1)S(1)} %get-tuple-element.41), channel_id=1, source_target_pairs={{0,2},{1,3},{2,0},{3,1},{4,6},{5,7},{6,4},{7,5},{8,10},{9,11},{10,... | collective-permute-start | bytes 98312 | tf_op jit(solution)/shard_map/ppermute | solution.py:117
  42.5 0.9 %collective-permute-start.15 = (bf16[16,1024]{1,0:T(8,128)(2,1)S(1)}, bf16[16,1024]{1,0:T(8,128)(2,1)S(1)}, u32[]{:S(2)}, u32[]{:S(2)}) collective-permute-start(bf16[16,1024]{1,0:T(8,128)(2,1)S(1)} %get-tuple-element.41), channel_id=1, source_target_pairs={{0,3},{1,2},{2,1},{3,0},{4,7},{5,6},{6,5},{7,4},{8,11},{9,10},{10,... | collective-permute-start | bytes 98312 | tf_op jit(solution)/shard_map/ppermute | solution.py:117
  43.4 1.5 %shard_map.143 = f32[4,4,128,128]{3,2,1,0:T(8,128)} custom-call(f32[16,128]{1,0:T(8,128)S(1)} %get-tuple-element.42.key_ref, f32[16,128]{1,0:T(8,128)S(1)} %get-tuple-element.43.value_ref, f32[16,128]{1,0:T(8,128)S(1)} %get-tuple-element.29.refs_5_.gamma_ref, f32[16,128]{1,0:T(8,128)S(1)} %get-tuple-element.36.split_ref.after_ref, ...), custom_call_target="tpu_custom_call" | custom-call | flops 8589934592 | tf_op jit(solution)/shard_map/pallas_call | solution.py:339
  44.9 0.0 collective-permute-done.17.refs_2_
  44.9 0.6 %collective-permute-done.16.refs_1_ = bf16[16,1024]{1,0:T(8,128)(2,1)S(1)} collective-permute-done((bf16[16,1024]{1,0:T(8,128)(2,1)S(1)}, bf16[16,1024]{1,0:T(8,128)(2,1)S(1)}, u32[]{:S(2)}, u32[]{:S(2)}) %collective-permute-start.16) | collective-permute-done | bytes 32800 | tf_op jit(solution)/shard_map/ppermute | solution.py:117
  45.5 0.3 collective-permute-done.15.refs_0_
  45.9 0.6 %shard_map.142 = bf16[16,1024]{1,0:T(8,128)(2,1)} custom-call(bf16[16,1024]{1,0:T(8,128)(2,1)S(1)} %get-tuple-element.34.mixed_ref, f32[16,1024]{1,0:T(8,128)S(1)} %get-tuple-element.40.own_ref, bf16[16,1024]{1,0:T(8,128)(2,1)S(1)} %collective-permute-done.15.refs_0_, bf16[16,1024]{1,0:T(8,128)(2,1)S(1)} %collective-permute-done.16.refs_1_, ...), custom_call_target="tpu_custom_call" | custom-call | flops 8589934592 | tf_op jit(solution)/shard_map/pallas_call | solution.py:339
  (8 shorter events, 0.0 us)
Async XLA Ops:
  0.6 8.6 %copy-start.4 = (s32[4]{0:T(128)S(1)}, s32[4]{0:T(128)}, u32[]{:S(2)}) copy-start(s32[4]{0:T(128)} %param.13) | copy-start | bytes 52
  0.6 8.7 %copy-start.1 = (f32[4,4,128,128]{3,2,1,0:T(8,128)S(1)}, f32[4,4,128,128]{3,2,1,0:T(8,128)}, u32[]{:S(2)}) copy-start(f32[4,4,128,128]{3,2,1,0:T(8,128)} %state_ref.3) | copy-start | bytes 3145732
  3.5 6.0 %collective-permute-start = (bf16[80,128]{1,0:T(8,128)(2,1)S(1)}, bf16[80,128]{1,0:T(8,128)(2,1)S(1)}, u32[]{:S(2)}, u32[]{:S(2)}) collective-permute-start(bf16[80,128]{1,0:T(8,128)(2,1)S(1)} %get-tuple-element.24), channel_id=1, source_target_pairs={{0,8},{4,12},{8,0},{12,4},{1,9},{5,13},{9,1},{13,5},{2,10},{6,14},... | collective-permute-start | bytes 61448 | tf_op jit(solution)/shard_map/ppermute | solution.py:117
  7.6 5.6 %collective-permute-start.1 = (bf16[80,128]{1,0:T(8,128)(2,1)S(1)}, bf16[80,128]{1,0:T(8,128)(2,1)S(1)}, u32[]{:S(2)}, u32[]{:S(2)}) collective-permute-start(bf16[80,128]{1,0:T(8,128)(2,1)S(1)} %get-tuple-element.25), channel_id=1, source_target_pairs={{0,12},{4,8},{8,4},{12,0},{1,13},{5,9},{9,5},{13,1},{2,14},{6,10},... | collective-permute-start | bytes 61448 | tf_op jit(solution)/shard_map/ppermute | solution.py:117
  9.0 4.2 %collective-permute-start.2 = (bf16[80,128]{1,0:T(8,128)(2,1)S(1)}, bf16[80,128]{1,0:T(8,128)(2,1)S(1)}, u32[]{:S(2)}, u32[]{:S(2)}) collective-permute-start(bf16[80,128]{1,0:T(8,128)(2,1)S(1)} %get-tuple-element.26), channel_id=1, source_target_pairs={{0,4},{4,0},{8,12},{12,8},{1,5},{5,1},{9,13},{13,9},{2,6},{6,2},{1... | collective-permute-start | bytes 61448 | tf_op jit(solution)/shard_map/ppermute | solution.py:117
  13.2 7.8 %copy-start = (bf16[512,1024]{1,0:T(8,128)(2,1)S(1)}, bf16[512,1024]{1,0:T(8,128)(2,1)}, u32[]{:S(2)}) copy-start(bf16[512,1024]{1,0:T(8,128)(2,1)} %refs_4_.1) | copy-start | bytes 3145732
  13.7 12.6 %slice-start = ((s8[8388608]{0:T(1024)(128)(4,1)}), s8[4194304]{0:T(1024)(128)(4,1)S(1)}, s32[]{:S(2)}) async-start(s8[8388608]{0:T(1024)(128)(4,1)} %bitcast.2), calls=%async_computation | async-start | bytes 8388608
  13.7 12.6 %slice-start.1 = ((s8[8388608]{0:T(1024)(128)(4,1)}), s8[4194304]{0:T(1024)(128)(4,1)S(1)}, s32[]{:S(2)}) async-start(s8[8388608]{0:T(1024)(128)(4,1)} %bitcast.2), calls=%async_computation.1 | async-start | bytes 8388608
  13.7 12.6 %copy-start.2 = (bf16[16,1024]{1,0:T(8,128)(2,1)S(1)}, bf16[16,1024]{1,0:T(8,128)(2,1)}, u32[]{:S(2)}) copy-start(bf16[16,1024]{1,0:T(8,128)(2,1)} %x_ref.1) | copy-start | bytes 98308
  13.7 12.5 %copy-start.3 = (f32[1024]{0:T(1024)S(1)}, f32[1024]{0:T(1024)}, u32[]{:S(2)}) copy-start(f32[1024]{0:T(1024)} %param.21) | copy-start | bytes 12292
  13.8 3.7 %collective-permute-start.5 = (bf16[16,128]{1,0:T(8,128)(2,1)S(1)}, bf16[16,128]{1,0:T(8,128)(2,1)S(1)}, u32[]{:S(2)}, u32[]{:S(2)}) collective-permute-start(bf16[16,128]{1,0:T(8,128)(2,1)S(1)} %get-tuple-element.31.refs_0_), channel_id=1, source_target_pairs={{0,4},{4,0},{8,12},{12,8},{1,5},{5,1},{9,13},{13,9},{2,6},{6,2},{1... | collective-permute-start | bytes 12296 | tf_op jit(solution)/shard_map/ppermute | solution.py:117
  13.8 5.5 %collective-permute-start.4 = (bf16[16,128]{1,0:T(8,128)(2,1)S(1)}, bf16[16,128]{1,0:T(8,128)(2,1)S(1)}, u32[]{:S(2)}, u32[]{:S(2)}) collective-permute-start(bf16[16,128]{1,0:T(8,128)(2,1)S(1)} %get-tuple-element.31.refs_0_), channel_id=1, source_target_pairs={{0,12},{4,8},{8,4},{12,0},{1,13},{5,9},{9,5},{13,1},{2,14},{6,10},... | collective-permute-start | bytes 12296 | tf_op jit(solution)/shard_map/ppermute | solution.py:117
  16.5 4.5 %collective-permute-start.3 = (bf16[16,128]{1,0:T(8,128)(2,1)S(1)}, bf16[16,128]{1,0:T(8,128)(2,1)S(1)}, u32[]{:S(2)}, u32[]{:S(2)}) collective-permute-start(bf16[16,128]{1,0:T(8,128)(2,1)S(1)} %get-tuple-element.31.refs_0_), channel_id=1, source_target_pairs={{0,8},{4,12},{8,0},{12,4},{1,9},{5,13},{9,1},{13,5},{2,10},{6,14},... | collective-permute-start | bytes 12296 | tf_op jit(solution)/shard_map/ppermute | solution.py:117
  21.4 1.9 %collective-permute-start.8 = (bf16[16,1024]{1,0:T(8,128)(2,1)S(1)}, bf16[16,1024]{1,0:T(8,128)(2,1)S(1)}, u32[]{:S(2)}, u32[]{:S(2)}) collective-permute-start(bf16[16,1024]{1,0:T(8,128)(2,1)S(1)} %get-tuple-element.33), channel_id=1, source_target_pairs={{0,1},{1,0},{2,3},{3,2},{4,5},{5,4},{6,7},{7,6},{8,9},{9,8},{10,11... | collective-permute-start | bytes 98312 | tf_op jit(solution)/shard_map/ppermute | solution.py:117
  21.4 4.0 %collective-permute-start.7 = (bf16[16,1024]{1,0:T(8,128)(2,1)S(1)}, bf16[16,1024]{1,0:T(8,128)(2,1)S(1)}, u32[]{:S(2)}, u32[]{:S(2)}) collective-permute-start(bf16[16,1024]{1,0:T(8,128)(2,1)S(1)} %get-tuple-element.33), channel_id=1, source_target_pairs={{0,2},{1,3},{2,0},{3,1},{4,6},{5,7},{6,4},{7,5},{8,10},{9,11},{10,... | collective-permute-start | bytes 98312 | tf_op jit(solution)/shard_map/ppermute | solution.py:117
  22.9 3.3 %collective-permute-start.6 = (bf16[16,1024]{1,0:T(8,128)(2,1)S(1)}, bf16[16,1024]{1,0:T(8,128)(2,1)S(1)}, u32[]{:S(2)}, u32[]{:S(2)}) collective-permute-start(bf16[16,1024]{1,0:T(8,128)(2,1)S(1)} %get-tuple-element.33), channel_id=1, source_target_pairs={{0,3},{1,2},{2,1},{3,0},{4,7},{5,6},{6,5},{7,4},{8,11},{9,10},{10,... | collective-permute-start | bytes 98312 | tf_op jit(solution)/shard_map/ppermute | solution.py:117
  27.2 5.9 %collective-permute-start.9 = (bf16[16,1152]{1,0:T(8,128)(2,1)S(1)}, bf16[16,1152]{1,0:T(8,128)(2,1)S(1)}, u32[]{:S(2)}, u32[]{:S(2)}) collective-permute-start(bf16[16,1152]{1,0:T(8,128)(2,1)S(1)} %get-tuple-element.37), channel_id=1, source_target_pairs={{0,8},{4,12},{8,0},{12,4},{1,9},{5,13},{9,1},{13,5},{2,10},{6,14},... | collective-permute-start | bytes 110600 | tf_op jit(solution)/shard_map/ppermute | solution.py:117
  28.0 5.9 %collective-permute-start.10 = (bf16[16,1152]{1,0:T(8,128)(2,1)S(1)}, bf16[16,1152]{1,0:T(8,128)(2,1)S(1)}, u32[]{:S(2)}, u32[]{:S(2)}) collective-permute-start(bf16[16,1152]{1,0:T(8,128)(2,1)S(1)} %get-tuple-element.38), channel_id=1, source_target_pairs={{0,12},{4,8},{8,4},{12,0},{1,13},{5,9},{9,5},{13,1},{2,14},{6,10},... | collective-permute-start | bytes 110600 | tf_op jit(solution)/shard_map/ppermute | solution.py:117
  30.1 4.2 %collective-permute-start.11 = (bf16[16,1152]{1,0:T(8,128)(2,1)S(1)}, bf16[16,1152]{1,0:T(8,128)(2,1)S(1)}, u32[]{:S(2)}, u32[]{:S(2)}) collective-permute-start(bf16[16,1152]{1,0:T(8,128)(2,1)S(1)} %get-tuple-element.39), channel_id=1, source_target_pairs={{0,4},{4,0},{8,12},{12,8},{1,5},{5,1},{9,13},{13,9},{2,6},{6,2},{1... | collective-permute-start | bytes 110600 | tf_op jit(solution)/shard_map/ppermute | solution.py:117
  30.7 7.7 %slice-start.2 = ((s8[8388608]{0:T(1024)(128)(4,1)}), s8[4194304]{0:T(1024)(128)(4,1)S(1)}, s32[]{:S(2)}) async-start(s8[8388608]{0:T(1024)(128)(4,1)} %bitcast.4), calls=%async_computation.2 | async-start | bytes 8388608
  31.1 7.3 %slice-start.3 = ((s8[8388608]{0:T(1024)(128)(4,1)}), s8[4194304]{0:T(1024)(128)(4,1)S(1)}, s32[]{:S(2)}) async-start(s8[8388608]{0:T(1024)(128)(4,1)} %bitcast.4), calls=%async_computation.3 | async-start | bytes 8388608
  34.5 4.9 %collective-permute-start.14 = (bf16[16,1024]{1,0:T(8,128)(2,1)S(1)}, bf16[16,1024]{1,0:T(8,128)(2,1)S(1)}, u32[]{:S(2)}, u32[]{:S(2)}) collective-permute-start(bf16[16,1024]{1,0:T(8,128)(2,1)S(1)} %shard_map.137.refs_0_), channel_id=1, source_target_pairs={{0,4},{4,12},{8,0},{12,8},{1,5},{5,13},{9,1},{13,9},{2,6},{6,14},{... | collective-permute-start | bytes 98312 | tf_op jit(solution)/shard_map/ppermute | solution.py:117
  34.9 5.8 %collective-permute-start.13 = (bf16[16,1024]{1,0:T(8,128)(2,1)S(1)}, bf16[16,1024]{1,0:T(8,128)(2,1)S(1)}, u32[]{:S(2)}, u32[]{:S(2)}) collective-permute-start(bf16[16,1024]{1,0:T(8,128)(2,1)S(1)} %shard_map.137.refs_0_), channel_id=1, source_target_pairs={{0,12},{4,8},{8,4},{12,0},{1,13},{5,9},{9,5},{13,1},{2,14},{6,10},... | collective-permute-start | bytes 98312 | tf_op jit(solution)/shard_map/ppermute | solution.py:117
  36.5 4.6 %collective-permute-start.12 = (bf16[16,1024]{1,0:T(8,128)(2,1)S(1)}, bf16[16,1024]{1,0:T(8,128)(2,1)S(1)}, u32[]{:S(2)}, u32[]{:S(2)}) collective-permute-start(bf16[16,1024]{1,0:T(8,128)(2,1)S(1)} %shard_map.137.refs_0_), channel_id=1, source_target_pairs={{0,8},{4,0},{8,12},{12,4},{1,9},{5,1},{9,13},{13,5},{2,10},{6,2},{... | collective-permute-start | bytes 98312 | tf_op jit(solution)/shard_map/ppermute | solution.py:117
  41.5 3.4 %collective-permute-start.17 = (bf16[16,1024]{1,0:T(8,128)(2,1)S(1)}, bf16[16,1024]{1,0:T(8,128)(2,1)S(1)}, u32[]{:S(2)}, u32[]{:S(2)}) collective-permute-start(bf16[16,1024]{1,0:T(8,128)(2,1)S(1)} %get-tuple-element.41), channel_id=1, source_target_pairs={{0,1},{1,0},{2,3},{3,2},{4,5},{5,4},{6,7},{7,6},{8,9},{9,8},{10,11... | collective-permute-start | bytes 98312 | tf_op jit(solution)/shard_map/ppermute | solution.py:117
  41.5 4.0 %collective-permute-start.16 = (bf16[16,1024]{1,0:T(8,128)(2,1)S(1)}, bf16[16,1024]{1,0:T(8,128)(2,1)S(1)}, u32[]{:S(2)}, u32[]{:S(2)}) collective-permute-start(bf16[16,1024]{1,0:T(8,128)(2,1)S(1)} %get-tuple-element.41), channel_id=1, source_target_pairs={{0,2},{1,3},{2,0},{3,1},{4,6},{5,7},{6,4},{7,5},{8,10},{9,11},{10,... | collective-permute-start | bytes 98312 | tf_op jit(solution)/shard_map/ppermute | solution.py:117
  42.5 3.4 %collective-permute-start.15 = (bf16[16,1024]{1,0:T(8,128)(2,1)S(1)}, bf16[16,1024]{1,0:T(8,128)(2,1)S(1)}, u32[]{:S(2)}, u32[]{:S(2)}) collective-permute-start(bf16[16,1024]{1,0:T(8,128)(2,1)S(1)} %get-tuple-element.41), channel_id=1, source_target_pairs={{0,3},{1,2},{2,1},{3,0},{4,7},{5,6},{6,5},{7,4},{8,11},{9,10},{10,... | collective-permute-start | bytes 98312 | tf_op jit(solution)/shard_map/ppermute | solution.py:117

commit v9 on v8

--- a/solution.py
+++ b/solution.py
@@ -253,19 +253,21 @@
 def out_kernel(perms, *refs):
     n = len(perms)
     parts, (w_ref, own_ref, sent_ref) = refs[:n], refs[n:]
-    kept = jnp.concatenate([p[...] for p in parts], axis=0)
-    many, size = kept.shape
+    size = parts[0].shape[1]
     heads = w_ref.shape[0] // size
-    block = many // n // heads
-    rows = n * block
-    to = lax.broadcasted_iota(jnp.int32, (many, many), 0)
-    of = lax.broadcasted_iota(jnp.int32, (many, many), 1)
-    head, row = to // rows, to % rows
-    part = of // (heads * block)
-    owner = sum(jnp.where(part == k, lookup("kv", inverse(perm)), 0) for k, perm in enumerate(perms))
-    hot = (owner == row // block) & (of % (heads * block) == head * block + row % block)
-    kept = jnp.dot(hot.astype(F32).astype(BF16), kept, preferred_element_type=F32).astype(BF16)
-    kept = jnp.concatenate([kept[h * rows : (h + 1) * rows] for h in range(heads)], axis=1)
+    block = parts[0].shape[0] // heads
+    values = [p[...].astype(F32) for p in parts]
+    places = [lookup("kv", inverse(perm)) for perm in perms]
+    ordered = []
+    for t in range(n):
+        value = values[0]
+        for place, other in zip(places[1:], values[1:]):
+            value = jnp.where(place == t, other, value)
+        ordered.append(value)
+    columns = [
+        jnp.concatenate([value[h * block : (h + 1) * block] for value in ordered], axis=0) for h in range(heads)
+    ]
+    kept = jnp.concatenate(columns, axis=1).astype(BF16)
     terms = jnp.dot(kept, w_ref[...], preferred_element_type=F32)
     own_ref[...] = terms
     sent_ref[...] = terms.astype(BF16)

time: 46.6 us -> 46.5 us (level)
  no operation moved by 1% of the time
where the time goes in v9:
time: 46.5 us; the launch traced here: 46.4 us
  starting transfers between devices  20.5 us (44%)
  waiting for transfers between devices  16 us (34%)
  Pallas kernels  8.94 us (19%)
  between operations  0.78 us (2%)
    ppermute x18, starting transfers between devices, exchange(): got.append(lax.ppermute(value, axis, list(enumerate(perm))))  20.5 us
    ppermute x18, waiting for transfers between devices, exchange(): got.append(lax.ppermute(value, axis, list(enumerate(perm))))  16 us
    pallas_call x13, Pallas kernels, call(): pl.pallas_call(kernel, out_shape=[(pltpu.VMEM if kept else jax.ShapeDtype...  8.94 us
  transfers between devices with their start and end apart: 18, of which 13 were waited for; matrix products, arithmetic and copies ran while one was open for 0% of the time, Pallas kernels for 7%

profile of v9, /device:TPU:0, one launch (start us, length us, event | category | flops | bytes accessed | tf_op | source)
XLA Modules:
  0.0 46.4 jit_solution(17856296549695229799)
XLA Ops:
  0.6 0.0 copy-start.4
  0.6 0.0 copy-start.1
  0.7 2.8 %shard_map.131 = (f32[80,128]{1,0:T(8,128)S(1)}, bf16[80,128]{1,0:T(8,128)(2,1)S(1)}, bf16[80,128]{1,0:T(8,128)(2,1)S(1)}, bf16[80,128]{1,0:T(8,128)(2,1)S(1)}) custom-call(bf16[16,1024]{1,0:T(8,128)(2,1)} %x_ref.1, f32[1,1024]{1,0:T(1,128)} %bitcast.7, bf16[1024,512]{1,0:T(8,128)(2,1)} %refs_0_.1, bf16[1024,512]{1,0:T(8,128)(2,1)} %refs_1_.5, ...), custom_call_target="tpu_custom_call" | custom-call | flops 17179869184 | tf_op jit(solution)/shard_map/pallas_call | solution.py:341
  3.5 4.1 %collective-permute-start = (bf16[80,128]{1,0:T(8,128)(2,1)S(1)}, bf16[80,128]{1,0:T(8,128)(2,1)S(1)}, u32[]{:S(2)}, u32[]{:S(2)}) collective-permute-start(bf16[80,128]{1,0:T(8,128)(2,1)S(1)} %get-tuple-element.24), channel_id=1, source_target_pairs={{0,8},{4,12},{8,0},{12,4},{1,9},{5,13},{9,1},{13,5},{2,10},{6,14},... | collective-permute-start | bytes 61448 | tf_op jit(solution)/shard_map/ppermute | solution.py:117
  7.6 1.3 %collective-permute-start.1 = (bf16[80,128]{1,0:T(8,128)(2,1)S(1)}, bf16[80,128]{1,0:T(8,128)(2,1)S(1)}, u32[]{:S(2)}, u32[]{:S(2)}) collective-permute-start(bf16[80,128]{1,0:T(8,128)(2,1)S(1)} %get-tuple-element.25), channel_id=1, source_target_pairs={{0,12},{4,8},{8,4},{12,0},{1,13},{5,9},{9,5},{13,1},{2,14},{6,10},... | collective-permute-start | bytes 61448 | tf_op jit(solution)/shard_map/ppermute | solution.py:117
  9.0 0.2 collective-permute-start.2
  9.2 0.0 copy-done.4
  9.2 0.1 multiply_sine_fusion
  9.3 0.0 copy-done.1
  9.3 0.2 shard_map.132
  9.5 0.0 collective-permute-done.refs_0_
  9.5 3.7 %collective-permute-done.1.refs_1_ = bf16[80,128]{1,0:T(8,128)(2,1)S(1)} collective-permute-done((bf16[80,128]{1,0:T(8,128)(2,1)S(1)}, bf16[80,128]{1,0:T(8,128)(2,1)S(1)}, u32[]{:S(2)}, u32[]{:S(2)}) %collective-permute-start.1) | collective-permute-done | bytes 20512 | tf_op jit(solution)/shard_map/ppermute | solution.py:117
  13.2 0.0 collective-permute-done.2.refs_2_
  13.2 0.5 %shard_map.133 = (bf16[16,128]{1,0:T(8,128)(2,1)S(1)}, f32[16,128]{1,0:T(8,128)S(1)}, f32[16,128]{1,0:T(8,128)S(1)}) custom-call(f32[80,128]{1,0:T(8,128)S(1)} %get-tuple-element.23.own_ref, bf16[80,128]{1,0:T(8,128)(2,1)S(1)} %collective-permute-done.refs_0_, bf16[80,128]{1,0:T(8,128)(2,1)S(1)} %collective-permute-done.1.refs_1_, ...), custom_call_target="tpu_custom_call" | custom-call | flops 8589934592 | tf_op jit(solution)/shard_map/pallas_call | solution.py:341
  13.7 0.0 slice-start
  13.7 0.0 copy-start.2
  13.7 0.0 copy-start.3
  13.8 0.1 collective-permute-start.5
  13.8 2.7 %collective-permute-start.4 = (bf16[16,128]{1,0:T(8,128)(2,1)S(1)}, bf16[16,128]{1,0:T(8,128)(2,1)S(1)}, u32[]{:S(2)}, u32[]{:S(2)}) collective-permute-start(bf16[16,128]{1,0:T(8,128)(2,1)S(1)} %get-tuple-element.31.refs_0_), channel_id=1, source_target_pairs={{0,12},{4,8},{8,4},{12,0},{1,13},{5,9},{9,5},{13,1},{2,14},{6,10},... | collective-permute-start | bytes 12296 | tf_op jit(solution)/shard_map/ppermute | solution.py:117
  16.5 0.8 %collective-permute-start.3 = (bf16[16,128]{1,0:T(8,128)(2,1)S(1)}, bf16[16,128]{1,0:T(8,128)(2,1)S(1)}, u32[]{:S(2)}, u32[]{:S(2)}) collective-permute-start(bf16[16,128]{1,0:T(8,128)(2,1)S(1)} %get-tuple-element.31.refs_0_), channel_id=1, source_target_pairs={{0,8},{4,12},{8,0},{12,4},{1,9},{5,13},{9,1},{13,5},{2,10},{6,14},... | collective-permute-start | bytes 12296 | tf_op jit(solution)/shard_map/ppermute | solution.py:117
  17.3 0.1 collective-permute-done.5.refs_3_
  17.4 1.9 %collective-permute-done.4.refs_2_ = bf16[16,128]{1,0:T(8,128)(2,1)S(1)} collective-permute-done((bf16[16,128]{1,0:T(8,128)(2,1)S(1)}, bf16[16,128]{1,0:T(8,128)(2,1)S(1)}, u32[]{:S(2)}, u32[]{:S(2)}) %collective-permute-start.4) | collective-permute-done | bytes 4128 | tf_op jit(solution)/shard_map/ppermute | solution.py:117
  19.3 1.7 %collective-permute-done.3.refs_1_ = bf16[16,128]{1,0:T(8,128)(2,1)S(1)} collective-permute-done((bf16[16,128]{1,0:T(8,128)(2,1)S(1)}, bf16[16,128]{1,0:T(8,128)(2,1)S(1)}, u32[]{:S(2)}, u32[]{:S(2)}) %collective-permute-start.3) | collective-permute-done | bytes 4128 | tf_op jit(solution)/shard_map/ppermute | solution.py:117
  21.0 0.0 copy-done
  21.0 0.2 shard_map.134
  21.3 0.0 collective-permute-start.8
  21.3 1.5 %collective-permute-start.7 = (bf16[16,1024]{1,0:T(8,128)(2,1)S(1)}, bf16[16,1024]{1,0:T(8,128)(2,1)S(1)}, u32[]{:S(2)}, u32[]{:S(2)}) collective-permute-start(bf16[16,1024]{1,0:T(8,128)(2,1)S(1)} %get-tuple-element.33), channel_id=1, source_target_pairs={{0,2},{1,3},{2,0},{3,1},{4,6},{5,7},{6,4},{7,5},{8,10},{9,11},{10,... | collective-permute-start | bytes 98312 | tf_op jit(solution)/shard_map/ppermute | solution.py:117
  22.8 0.3 collective-permute-start.6
  23.1 0.0 collective-permute-done.8.refs_2_
  23.1 2.1 %collective-permute-done.7.refs_1_ = bf16[16,1024]{1,0:T(8,128)(2,1)S(1)} collective-permute-done((bf16[16,1024]{1,0:T(8,128)(2,1)S(1)}, bf16[16,1024]{1,0:T(8,128)(2,1)S(1)}, u32[]{:S(2)}, u32[]{:S(2)}) %collective-permute-start.7) | collective-permute-done | bytes 32800 | tf_op jit(solution)/shard_map/ppermute | solution.py:117
  25.2 0.9 %collective-permute-done.6.refs_0_ = bf16[16,1024]{1,0:T(8,128)(2,1)S(1)} collective-permute-done((bf16[16,1024]{1,0:T(8,128)(2,1)S(1)}, bf16[16,1024]{1,0:T(8,128)(2,1)S(1)}, u32[]{:S(2)}, u32[]{:S(2)}) %collective-permute-start.6) | collective-permute-done | bytes 32800 | tf_op jit(solution)/shard_map/ppermute | solution.py:117
  26.1 0.0 slice-done
  26.2 0.0 slice-done.1
  26.2 0.0 copy-done.2
  26.2 0.0 copy-done.3
  26.2 0.9 %shard_map.135 = (bf16[16,1024]{1,0:T(8,128)(2,1)S(1)}, bf16[16,1024]{1,0:T(8,128)(2,1)S(1)}, f32[16,128]{1,0:T(8,128)S(1)}, bf16[16,1152]{1,0:T(8,128)(2,1)S(1)...) custom-call(bf16[16,1024]{1,0:T(8,128)(2,1)S(1)} %copy-done.2, f32[1,1024]{1,0:T(1,128)S(1)} %bitcast.6, ...), custom_call_target="tpu_custom_call" | custom-call | flops 8589934592 | tf_op jit(solution)/shard_map/pallas_call | solution.py:341
  27.1 0.8 %collective-permute-start.9 = (bf16[16,1152]{1,0:T(8,128)(2,1)S(1)}, bf16[16,1152]{1,0:T(8,128)(2,1)S(1)}, u32[]{:S(2)}, u32[]{:S(2)}) collective-permute-start(bf16[16,1152]{1,0:T(8,128)(2,1)S(1)} %get-tuple-element.37), channel_id=1, source_target_pairs={{0,8},{4,12},{8,0},{12,4},{1,9},{5,13},{9,1},{13,5},{2,10},{6,14},... | collective-permute-start | bytes 110600 | tf_op jit(solution)/shard_map/ppermute | solution.py:117
  27.9 2.0 %collective-permute-start.10 = (bf16[16,1152]{1,0:T(8,128)(2,1)S(1)}, bf16[16,1152]{1,0:T(8,128)(2,1)S(1)}, u32[]{:S(2)}, u32[]{:S(2)}) collective-permute-start(bf16[16,1152]{1,0:T(8,128)(2,1)S(1)} %get-tuple-element.38), channel_id=1, source_target_pairs={{0,12},{4,8},{8,4},{12,0},{1,13},{5,9},{9,5},{13,1},{2,14},{6,10},... | collective-permute-start | bytes 110600 | tf_op jit(solution)/shard_map/ppermute | solution.py:117
  30.0 0.7 %collective-permute-start.11 = (bf16[16,1152]{1,0:T(8,128)(2,1)S(1)}, bf16[16,1152]{1,0:T(8,128)(2,1)S(1)}, u32[]{:S(2)}, u32[]{:S(2)}) collective-permute-start(bf16[16,1152]{1,0:T(8,128)(2,1)S(1)} %get-tuple-element.39), channel_id=1, source_target_pairs={{0,4},{4,0},{8,12},{12,8},{1,5},{5,1},{9,13},{13,9},{2,6},{6,2},{1... | collective-permute-start | bytes 110600 | tf_op jit(solution)/shard_map/ppermute | solution.py:117
  30.6 0.4 shard_map.136.own_ref
  31.0 2.1 %collective-permute-done.9.refs_0_ = bf16[16,1152]{1,0:T(8,128)(2,1)S(1)} collective-permute-done((bf16[16,1152]{1,0:T(8,128)(2,1)S(1)}, bf16[16,1152]{1,0:T(8,128)(2,1)S(1)}, u32[]{:S(2)}, u32[]{:S(2)}) %collective-permute-start.9) | collective-permute-done | bytes 36896 | tf_op jit(solution)/shard_map/ppermute | solution.py:117
  33.1 0.7 %collective-permute-done.10.refs_1_ = bf16[16,1152]{1,0:T(8,128)(2,1)S(1)} collective-permute-done((bf16[16,1152]{1,0:T(8,128)(2,1)S(1)}, bf16[16,1152]{1,0:T(8,128)(2,1)S(1)}, u32[]{:S(2)}, u32[]{:S(2)}) %collective-permute-start.10) | collective-permute-done | bytes 36896 | tf_op jit(solution)/shard_map/ppermute | solution.py:117
  33.8 0.4 collective-permute-done.11.refs_2_
  34.2 0.2 shard_map.137.refs_0_
  34.3 0.5 collective-permute-start.14
  34.8 1.6 %collective-permute-start.13 = (bf16[16,1024]{1,0:T(8,128)(2,1)S(1)}, bf16[16,1024]{1,0:T(8,128)(2,1)S(1)}, u32[]{:S(2)}, u32[]{:S(2)}) collective-permute-start(bf16[16,1024]{1,0:T(8,128)(2,1)S(1)} %shard_map.137.refs_0_), channel_id=1, source_target_pairs={{0,12},{4,8},{8,4},{12,0},{1,13},{5,9},{9,5},{13,1},{2,14},{6,10},... | collective-permute-start | bytes 98312 | tf_op jit(solution)/shard_map/ppermute | solution.py:117
  36.4 1.9 %collective-permute-start.12 = (bf16[16,1024]{1,0:T(8,128)(2,1)S(1)}, bf16[16,1024]{1,0:T(8,128)(2,1)S(1)}, u32[]{:S(2)}, u32[]{:S(2)}) collective-permute-start(bf16[16,1024]{1,0:T(8,128)(2,1)S(1)} %shard_map.137.refs_0_), channel_id=1, source_target_pairs={{0,8},{4,0},{8,12},{12,4},{1,9},{5,1},{9,13},{13,5},{2,10},{6,2},{... | collective-permute-start | bytes 98312 | tf_op jit(solution)/shard_map/ppermute | solution.py:117
  38.3 0.0 slice-done.2
  38.4 0.0 slice-done.3
  38.4 0.4 shard_map.138.refs_2_
  38.7 0.5 %collective-permute-done.14.refs_0_ = bf16[16,1024]{1,0:T(8,128)(2,1)S(1)} collective-permute-done((bf16[16,1024]{1,0:T(8,128)(2,1)S(1)}, bf16[16,1024]{1,0:T(8,128)(2,1)S(1)}, u32[]{:S(2)}, u32[]{:S(2)}) %collective-permute-start.14) | collective-permute-done | bytes 32800 | tf_op jit(solution)/shard_map/ppermute | solution.py:117
  39.2 0.4 shard_map.139.refs_2_
  39.6 1.0 %collective-permute-done.13.refs_0_ = bf16[16,1024]{1,0:T(8,128)(2,1)S(1)} collective-permute-done((bf16[16,1024]{1,0:T(8,128)(2,1)S(1)}, bf16[16,1024]{1,0:T(8,128)(2,1)S(1)}, u32[]{:S(2)}, u32[]{:S(2)}) %collective-permute-start.13) | collective-permute-done | bytes 32800 | tf_op jit(solution)/shard_map/ppermute | solution.py:117
  40.6 0.4 shard_map.140.refs_2_
  41.0 0.0 collective-permute-done.12.refs_0_
  41.0 0.4 shard_map.141
  41.4 0.0 collective-permute-start.17
  41.4 1.0 %collective-permute-start.16 = (bf16[16,1024]{1,0:T(8,128)(2,1)S(1)}, bf16[16,1024]{1,0:T(8,128)(2,1)S(1)}, u32[]{:S(2)}, u32[]{:S(2)}) collective-permute-start(bf16[16,1024]{1,0:T(8,128)(2,1)S(1)} %get-tuple-element.41), channel_id=1, source_target_pairs={{0,2},{1,3},{2,0},{3,1},{4,6},{5,7},{6,4},{7,5},{8,10},{9,11},{10,... | collective-permute-start | bytes 98312 | tf_op jit(solution)/shard_map/ppermute | solution.py:117
  42.4 0.9 %collective-permute-start.15 = (bf16[16,1024]{1,0:T(8,128)(2,1)S(1)}, bf16[16,1024]{1,0:T(8,128)(2,1)S(1)}, u32[]{:S(2)}, u32[]{:S(2)}) collective-permute-start(bf16[16,1024]{1,0:T(8,128)(2,1)S(1)} %get-tuple-element.41), channel_id=1, source_target_pairs={{0,3},{1,2},{2,1},{3,0},{4,7},{5,6},{6,5},{7,4},{8,11},{9,10},{10,... | collective-permute-start | bytes 98312 | tf_op jit(solution)/shard_map/ppermute | solution.py:117
  43.3 1.5 %shard_map.143 = f32[4,4,128,128]{3,2,1,0:T(8,128)} custom-call(f32[16,128]{1,0:T(8,128)S(1)} %get-tuple-element.42.key_ref, f32[16,128]{1,0:T(8,128)S(1)} %get-tuple-element.43.value_ref, f32[16,128]{1,0:T(8,128)S(1)} %get-tuple-element.29.refs_5_.gamma_ref, f32[16,128]{1,0:T(8,128)S(1)} %get-tuple-element.36.split_ref.after_ref, ...), custom_call_target="tpu_custom_call" | custom-call | flops 8589934592 | tf_op jit(solution)/shard_map/pallas_call | solution.py:341
  44.8 0.0 collective-permute-done.17.refs_2_
  44.8 0.6 %collective-permute-done.16.refs_1_ = bf16[16,1024]{1,0:T(8,128)(2,1)S(1)} collective-permute-done((bf16[16,1024]{1,0:T(8,128)(2,1)S(1)}, bf16[16,1024]{1,0:T(8,128)(2,1)S(1)}, u32[]{:S(2)}, u32[]{:S(2)}) %collective-permute-start.16) | collective-permute-done | bytes 32800 | tf_op jit(solution)/shard_map/ppermute | solution.py:117
  45.4 0.3 collective-permute-done.15.refs_0_
  45.7 0.6 %shard_map.142 = bf16[16,1024]{1,0:T(8,128)(2,1)} custom-call(bf16[16,1024]{1,0:T(8,128)(2,1)S(1)} %get-tuple-element.34.mixed_ref, f32[16,1024]{1,0:T(8,128)S(1)} %get-tuple-element.40.own_ref, bf16[16,1024]{1,0:T(8,128)(2,1)S(1)} %collective-permute-done.15.refs_0_, bf16[16,1024]{1,0:T(8,128)(2,1)S(1)} %collective-permute-done.16.refs_1_, ...), custom_call_target="tpu_custom_call" | custom-call | flops 8589934592 | tf_op jit(solution)/shard_map/pallas_call | solution.py:341
  (8 shorter events, 0.0 us)
Async XLA Ops:
  0.6 8.6 %copy-start.4 = (s32[4]{0:T(128)S(1)}, s32[4]{0:T(128)}, u32[]{:S(2)}) copy-start(s32[4]{0:T(128)} %param.13) | copy-start | bytes 52
  0.6 8.7 %copy-start.1 = (f32[4,4,128,128]{3,2,1,0:T(8,128)S(1)}, f32[4,4,128,128]{3,2,1,0:T(8,128)}, u32[]{:S(2)}) copy-start(f32[4,4,128,128]{3,2,1,0:T(8,128)} %state_ref.3) | copy-start | bytes 3145732
  3.5 6.0 %collective-permute-start = (bf16[80,128]{1,0:T(8,128)(2,1)S(1)}, bf16[80,128]{1,0:T(8,128)(2,1)S(1)}, u32[]{:S(2)}, u32[]{:S(2)}) collective-permute-start(bf16[80,128]{1,0:T(8,128)(2,1)S(1)} %get-tuple-element.24), channel_id=1, source_target_pairs={{0,8},{4,12},{8,0},{12,4},{1,9},{5,13},{9,1},{13,5},{2,10},{6,14},... | collective-permute-start | bytes 61448 | tf_op jit(solution)/shard_map/ppermute | solution.py:117
  7.6 5.6 %collective-permute-start.1 = (bf16[80,128]{1,0:T(8,128)(2,1)S(1)}, bf16[80,128]{1,0:T(8,128)(2,1)S(1)}, u32[]{:S(2)}, u32[]{:S(2)}) collective-permute-start(bf16[80,128]{1,0:T(8,128)(2,1)S(1)} %get-tuple-element.25), channel_id=1, source_target_pairs={{0,12},{4,8},{8,4},{12,0},{1,13},{5,9},{9,5},{13,1},{2,14},{6,10},... | collective-permute-start | bytes 61448 | tf_op jit(solution)/shard_map/ppermute | solution.py:117
  9.0 4.2 %collective-permute-start.2 = (bf16[80,128]{1,0:T(8,128)(2,1)S(1)}, bf16[80,128]{1,0:T(8,128)(2,1)S(1)}, u32[]{:S(2)}, u32[]{:S(2)}) collective-permute-start(bf16[80,128]{1,0:T(8,128)(2,1)S(1)} %get-tuple-element.26), channel_id=1, source_target_pairs={{0,4},{4,0},{8,12},{12,8},{1,5},{5,1},{9,13},{13,9},{2,6},{6,2},{1... | collective-permute-start | bytes 61448 | tf_op jit(solution)/shard_map/ppermute | solution.py:117
  13.2 7.8 %copy-start = (bf16[512,1024]{1,0:T(8,128)(2,1)S(1)}, bf16[512,1024]{1,0:T(8,128)(2,1)}, u32[]{:S(2)}) copy-start(bf16[512,1024]{1,0:T(8,128)(2,1)} %refs_4_.1) | copy-start | bytes 3145732
  13.7 12.4 %slice-start = ((s8[8388608]{0:T(1024)(128)(4,1)}), s8[4194304]{0:T(1024)(128)(4,1)S(1)}, s32[]{:S(2)}) async-start(s8[8388608]{0:T(1024)(128)(4,1)} %bitcast.2), calls=%async_computation | async-start | bytes 8388608
  13.7 12.4 %slice-start.1 = ((s8[8388608]{0:T(1024)(128)(4,1)}), s8[4194304]{0:T(1024)(128)(4,1)S(1)}, s32[]{:S(2)}) async-start(s8[8388608]{0:T(1024)(128)(4,1)} %bitcast.2), calls=%async_computation.1 | async-start | bytes 8388608
  13.7 12.4 %copy-start.2 = (bf16[16,1024]{1,0:T(8,128)(2,1)S(1)}, bf16[16,1024]{1,0:T(8,128)(2,1)}, u32[]{:S(2)}) copy-start(bf16[16,1024]{1,0:T(8,128)(2,1)} %x_ref.1) | copy-start | bytes 98308
  13.7 12.4 %copy-start.3 = (f32[1024]{0:T(1024)S(1)}, f32[1024]{0:T(1024)}, u32[]{:S(2)}) copy-start(f32[1024]{0:T(1024)} %param.21) | copy-start | bytes 12292
  13.8 3.7 %collective-permute-start.5 = (bf16[16,128]{1,0:T(8,128)(2,1)S(1)}, bf16[16,128]{1,0:T(8,128)(2,1)S(1)}, u32[]{:S(2)}, u32[]{:S(2)}) collective-permute-start(bf16[16,128]{1,0:T(8,128)(2,1)S(1)} %get-tuple-element.31.refs_0_), channel_id=1, source_target_pairs={{0,4},{4,0},{8,12},{12,8},{1,5},{5,1},{9,13},{13,9},{2,6},{6,2},{1... | collective-permute-start | bytes 12296 | tf_op jit(solution)/shard_map/ppermute | solution.py:117
  13.8 5.5 %collective-permute-start.4 = (bf16[16,128]{1,0:T(8,128)(2,1)S(1)}, bf16[16,128]{1,0:T(8,128)(2,1)S(1)}, u32[]{:S(2)}, u32[]{:S(2)}) collective-permute-start(bf16[16,128]{1,0:T(8,128)(2,1)S(1)} %get-tuple-element.31.refs_0_), channel_id=1, source_target_pairs={{0,12},{4,8},{8,4},{12,0},{1,13},{5,9},{9,5},{13,1},{2,14},{6,10},... | collective-permute-start | bytes 12296 | tf_op jit(solution)/shard_map/ppermute | solution.py:117
  16.5 4.5 %collective-permute-start.3 = (bf16[16,128]{1,0:T(8,128)(2,1)S(1)}, bf16[16,128]{1,0:T(8,128)(2,1)S(1)}, u32[]{:S(2)}, u32[]{:S(2)}) collective-permute-start(bf16[16,128]{1,0:T(8,128)(2,1)S(1)} %get-tuple-element.31.refs_0_), channel_id=1, source_target_pairs={{0,8},{4,12},{8,0},{12,4},{1,9},{5,13},{9,1},{13,5},{2,10},{6,14},... | collective-permute-start | bytes 12296 | tf_op jit(solution)/shard_map/ppermute | solution.py:117
  21.3 1.9 %collective-permute-start.8 = (bf16[16,1024]{1,0:T(8,128)(2,1)S(1)}, bf16[16,1024]{1,0:T(8,128)(2,1)S(1)}, u32[]{:S(2)}, u32[]{:S(2)}) collective-permute-start(bf16[16,1024]{1,0:T(8,128)(2,1)S(1)} %get-tuple-element.33), channel_id=1, source_target_pairs={{0,1},{1,0},{2,3},{3,2},{4,5},{5,4},{6,7},{7,6},{8,9},{9,8},{10,11... | collective-permute-start | bytes 98312 | tf_op jit(solution)/shard_map/ppermute | solution.py:117
  21.3 4.0 %collective-permute-start.7 = (bf16[16,1024]{1,0:T(8,128)(2,1)S(1)}, bf16[16,1024]{1,0:T(8,128)(2,1)S(1)}, u32[]{:S(2)}, u32[]{:S(2)}) collective-permute-start(bf16[16,1024]{1,0:T(8,128)(2,1)S(1)} %get-tuple-element.33), channel_id=1, source_target_pairs={{0,2},{1,3},{2,0},{3,1},{4,6},{5,7},{6,4},{7,5},{8,10},{9,11},{10,... | collective-permute-start | bytes 98312 | tf_op jit(solution)/shard_map/ppermute | solution.py:117
  22.8 3.3 %collective-permute-start.6 = (bf16[16,1024]{1,0:T(8,128)(2,1)S(1)}, bf16[16,1024]{1,0:T(8,128)(2,1)S(1)}, u32[]{:S(2)}, u32[]{:S(2)}) collective-permute-start(bf16[16,1024]{1,0:T(8,128)(2,1)S(1)} %get-tuple-element.33), channel_id=1, source_target_pairs={{0,3},{1,2},{2,1},{3,0},{4,7},{5,6},{6,5},{7,4},{8,11},{9,10},{10,... | collective-permute-start | bytes 98312 | tf_op jit(solution)/shard_map/ppermute | solution.py:117
  27.1 5.9 %collective-permute-start.9 = (bf16[16,1152]{1,0:T(8,128)(2,1)S(1)}, bf16[16,1152]{1,0:T(8,128)(2,1)S(1)}, u32[]{:S(2)}, u32[]{:S(2)}) collective-permute-start(bf16[16,1152]{1,0:T(8,128)(2,1)S(1)} %get-tuple-element.37), channel_id=1, source_target_pairs={{0,8},{4,12},{8,0},{12,4},{1,9},{5,13},{9,1},{13,5},{2,10},{6,14},... | collective-permute-start | bytes 110600 | tf_op jit(solution)/shard_map/ppermute | solution.py:117
  27.9 5.9 %collective-permute-start.10 = (bf16[16,1152]{1,0:T(8,128)(2,1)S(1)}, bf16[16,1152]{1,0:T(8,128)(2,1)S(1)}, u32[]{:S(2)}, u32[]{:S(2)}) collective-permute-start(bf16[16,1152]{1,0:T(8,128)(2,1)S(1)} %get-tuple-element.38), channel_id=1, source_target_pairs={{0,12},{4,8},{8,4},{12,0},{1,13},{5,9},{9,5},{13,1},{2,14},{6,10},... | collective-permute-start | bytes 110600 | tf_op jit(solution)/shard_map/ppermute | solution.py:117
  30.0 4.2 %collective-permute-start.11 = (bf16[16,1152]{1,0:T(8,128)(2,1)S(1)}, bf16[16,1152]{1,0:T(8,128)(2,1)S(1)}, u32[]{:S(2)}, u32[]{:S(2)}) collective-permute-start(bf16[16,1152]{1,0:T(8,128)(2,1)S(1)} %get-tuple-element.39), channel_id=1, source_target_pairs={{0,4},{4,0},{8,12},{12,8},{1,5},{5,1},{9,13},{13,9},{2,6},{6,2},{1... | collective-permute-start | bytes 110600 | tf_op jit(solution)/shard_map/ppermute | solution.py:117
  30.6 7.7 %slice-start.2 = ((s8[8388608]{0:T(1024)(128)(4,1)}), s8[4194304]{0:T(1024)(128)(4,1)S(1)}, s32[]{:S(2)}) async-start(s8[8388608]{0:T(1024)(128)(4,1)} %bitcast.4), calls=%async_computation.2 | async-start | bytes 8388608
  31.0 7.3 %slice-start.3 = ((s8[8388608]{0:T(1024)(128)(4,1)}), s8[4194304]{0:T(1024)(128)(4,1)S(1)}, s32[]{:S(2)}) async-start(s8[8388608]{0:T(1024)(128)(4,1)} %bitcast.4), calls=%async_computation.3 | async-start | bytes 8388608
  34.3 4.9 %collective-permute-start.14 = (bf16[16,1024]{1,0:T(8,128)(2,1)S(1)}, bf16[16,1024]{1,0:T(8,128)(2,1)S(1)}, u32[]{:S(2)}, u32[]{:S(2)}) collective-permute-start(bf16[16,1024]{1,0:T(8,128)(2,1)S(1)} %shard_map.137.refs_0_), channel_id=1, source_target_pairs={{0,4},{4,12},{8,0},{12,8},{1,5},{5,13},{9,1},{13,9},{2,6},{6,14},{... | collective-permute-start | bytes 98312 | tf_op jit(solution)/shard_map/ppermute | solution.py:117
  34.8 5.8 %collective-permute-start.13 = (bf16[16,1024]{1,0:T(8,128)(2,1)S(1)}, bf16[16,1024]{1,0:T(8,128)(2,1)S(1)}, u32[]{:S(2)}, u32[]{:S(2)}) collective-permute-start(bf16[16,1024]{1,0:T(8,128)(2,1)S(1)} %shard_map.137.refs_0_), channel_id=1, source_target_pairs={{0,12},{4,8},{8,4},{12,0},{1,13},{5,9},{9,5},{13,1},{2,14},{6,10},... | collective-permute-start | bytes 98312 | tf_op jit(solution)/shard_map/ppermute | solution.py:117
  36.4 4.6 %collective-permute-start.12 = (bf16[16,1024]{1,0:T(8,128)(2,1)S(1)}, bf16[16,1024]{1,0:T(8,128)(2,1)S(1)}, u32[]{:S(2)}, u32[]{:S(2)}) collective-permute-start(bf16[16,1024]{1,0:T(8,128)(2,1)S(1)} %shard_map.137.refs_0_), channel_id=1, source_target_pairs={{0,8},{4,0},{8,12},{12,4},{1,9},{5,1},{9,13},{13,5},{2,10},{6,2},{... | collective-permute-start | bytes 98312 | tf_op jit(solution)/shard_map/ppermute | solution.py:117
  41.4 3.4 %collective-permute-start.17 = (bf16[16,1024]{1,0:T(8,128)(2,1)S(1)}, bf16[16,1024]{1,0:T(8,128)(2,1)S(1)}, u32[]{:S(2)}, u32[]{:S(2)}) collective-permute-start(bf16[16,1024]{1,0:T(8,128)(2,1)S(1)} %get-tuple-element.41), channel_id=1, source_target_pairs={{0,1},{1,0},{2,3},{3,2},{4,5},{5,4},{6,7},{7,6},{8,9},{9,8},{10,11... | collective-permute-start | bytes 98312 | tf_op jit(solution)/shard_map/ppermute | solution.py:117
  41.4 4.0 %collective-permute-start.16 = (bf16[16,1024]{1,0:T(8,128)(2,1)S(1)}, bf16[16,1024]{1,0:T(8,128)(2,1)S(1)}, u32[]{:S(2)}, u32[]{:S(2)}) collective-permute-start(bf16[16,1024]{1,0:T(8,128)(2,1)S(1)} %get-tuple-element.41), channel_id=1, source_target_pairs={{0,2},{1,3},{2,0},{3,1},{4,6},{5,7},{6,4},{7,5},{8,10},{9,11},{10,... | collective-permute-start | bytes 98312 | tf_op jit(solution)/shard_map/ppermute | solution.py:117
  42.4 3.4 %collective-permute-start.15 = (bf16[16,1024]{1,0:T(8,128)(2,1)S(1)}, bf16[16,1024]{1,0:T(8,128)(2,1)S(1)}, u32[]{:S(2)}, u32[]{:S(2)}) collective-permute-start(bf16[16,1024]{1,0:T(8,128)(2,1)S(1)} %get-tuple-element.41), channel_id=1, source_target_pairs={{0,3},{1,2},{2,1},{3,0},{4,7},{5,6},{6,5},{7,4},{8,11},{9,10},{10,... | collective-permute-start | bytes 98312 | tf_op jit(solution)/shard_map/ppermute | solution.py:117

commit v10 on v9

--- a/solution.py
+++ b/solution.py
@@ -180,8 +180,11 @@
             out[i * group : (i + 1) * group] = mine.astype(out.dtype)
 
 
-def prepare_kernel(state_ref, cos_ref, sin_ref, out_ref, cosine_ref, sine_ref, gamma_ref):
+def prepare_kernel(state_hbm, cos_ref, sin_ref, out_ref, cosine_ref, sine_ref, gamma_ref, state_ref, sem):
     block, head_dev, size, _ = state_ref.shape
+    copy = pltpu.make_async_copy(state_hbm, state_ref, sem)
+    copy.start()
+    copy.wait()
     for h in range(head_dev):
         for b in range(block):
             value = state_ref[b, h]
@@ -392,13 +395,14 @@
         freq = 10000.0 ** (-(jnp.arange(half, dtype=F32) * 2.0) / size)
         angle = positions.astype(F32)[:, None] * freq[None, :]
         cosine, sine = jnp.cos(angle), jnp.sin(angle)
-        state = near(state)
         prepared, cosine, sine, gamma = call(
             prepare_kernel,
             [((head_dev, 2 * size, block * size), BF16)] + [((group, size), F32)] * 3,
-            state,
+            far(state),
             cosine,
             sine,
+            specs=[HBM, VMEM, VMEM],
+            scratch=[pltpu.VMEM(state.shape, F32), pltpu.SemaphoreType.DMA],
         )
         kept, key, value = call(
             functools.partial(read_kernel, n, block),
@@ -441,7 +445,7 @@
             value,
             gamma,
             split,
-            state,
+            near(state),
             out_specs=[HBM],
             scratch=[pltpu.VMEM(state.shape, F32), pltpu.SemaphoreType.DMA((block, head_dev))],
             kept=False,

time: 46.5 us -> 46.5 us (level)
  waiting for transfers between devices: 16 us -> 14.8 us
  Pallas kernels: 8.94 us -> 10.1 us
    ppermute x18, waiting for transfers between devices: 16 us -> 14.8 us  [exchange(): got.append(lax.ppermute(value, axis, list(enumerate(perm))))]
    pallas_call x13, Pallas kernels: 8.94 us -> 10.1 us  [call(): pl.pallas_call(kernel, out_shape=[(pltpu.VMEM if kept else jax.ShapeDtype...]
  transfers between devices with their start and end apart: 18 -> 18, of which waited for: 13 -> 13; matrix products, arithmetic and copies ran while one was open for 0% -> 0% of each run, Pallas kernels for 7% -> 10%
where the time goes in v10:
time: 46.5 us; the launch traced here: 46.3 us
  starting transfers between devices  20.5 us (44%)
  waiting for transfers between devices  14.8 us (32%)
  Pallas kernels  10.1 us (22%)
  between operations  0.76 us (2%)
    ppermute x18, starting transfers between devices, exchange(): got.append(lax.ppermute(value, axis, list(enumerate(perm))))  20.5 us
    ppermute x18, waiting for transfers between devices, exchange(): got.append(lax.ppermute(value, axis, list(enumerate(perm))))  14.8 us
    pallas_call x13, Pallas kernels, call(): pl.pallas_call(kernel, out_shape=[(pltpu.VMEM if kept else jax.ShapeDtype...  10.1 us
  transfers between devices with their start and end apart: 18, of which 13 were waited for; matrix products, arithmetic and copies ran while one was open for 0% of the time, Pallas kernels for 10%

profile of v10, /device:TPU:0, one launch (start us, length us, event | category | flops | bytes accessed | tf_op | source)
XLA Modules:
  0.0 46.3 jit_solution(10331026467680101407)
XLA Ops:
  0.6 0.0 copy-start.4
  0.6 2.8 %shard_map.131 = (f32[80,128]{1,0:T(8,128)S(1)}, bf16[80,128]{1,0:T(8,128)(2,1)S(1)}, bf16[80,128]{1,0:T(8,128)(2,1)S(1)}, bf16[80,128]{1,0:T(8,128)(2,1)S(1)}) custom-call(bf16[16,1024]{1,0:T(8,128)(2,1)} %x_ref.1, f32[1,1024]{1,0:T(1,128)} %bitcast.7, bf16[1024,512]{1,0:T(8,128)(2,1)} %refs_0_.1, bf16[1024,512]{1,0:T(8,128)(2,1)} %refs_1_.5, ...), custom_call_target="tpu_custom_call" | custom-call | flops 17179869184 | tf_op jit(solution)/shard_map/pallas_call | solution.py:344
  3.4 4.1 %collective-permute-start = (bf16[80,128]{1,0:T(8,128)(2,1)S(1)}, bf16[80,128]{1,0:T(8,128)(2,1)S(1)}, u32[]{:S(2)}, u32[]{:S(2)}) collective-permute-start(bf16[80,128]{1,0:T(8,128)(2,1)S(1)} %get-tuple-element.24), channel_id=1, source_target_pairs={{0,8},{4,12},{8,0},{12,4},{1,9},{5,13},{9,1},{13,5},{2,10},{6,14},... | collective-permute-start | bytes 61448 | tf_op jit(solution)/shard_map/ppermute | solution.py:117
  7.5 1.3 %collective-permute-start.1 = (bf16[80,128]{1,0:T(8,128)(2,1)S(1)}, bf16[80,128]{1,0:T(8,128)(2,1)S(1)}, u32[]{:S(2)}, u32[]{:S(2)}) collective-permute-start(bf16[80,128]{1,0:T(8,128)(2,1)S(1)} %get-tuple-element.25), channel_id=1, source_target_pairs={{0,12},{4,8},{8,4},{12,0},{1,13},{5,9},{9,5},{13,1},{2,14},{6,10},... | collective-permute-start | bytes 61448 | tf_op jit(solution)/shard_map/ppermute | solution.py:117
  8.9 0.2 collective-permute-start.2
  9.1 0.0 copy-done.4
  9.2 0.1 multiply_sine_fusion
  9.3 1.4 %shard_map.132 = (bf16[4,256,512]{2,1,0:T(8,128)(2,1)S(1)}, f32[16,128]{1,0:T(8,128)S(1)}, f32[16,128]{1,0:T(8,128)S(1)}, f32[16,128]{1,0:T(8,128)S(1)}) custom-call(f32[4,4,128,128]{3,2,1,0:T(8,128)} %state_ref.1, f32[4,64]{1,0:T(4,128)S(1)} %get-tuple-element.45.cos_ref, f32[4,64]{1,0:T(4,128)S(1)} %get-tuple-element.44.sin_ref), custom_call_target="tpu_custom_call" | custom-call | flops 8589934592 | tf_op jit(solution)/shard_map/pallas_call | solution.py:344
  10.7 0.0 collective-permute-done.refs_0_
  10.7 2.4 %collective-permute-done.1.refs_1_ = bf16[80,128]{1,0:T(8,128)(2,1)S(1)} collective-permute-done((bf16[80,128]{1,0:T(8,128)(2,1)S(1)}, bf16[80,128]{1,0:T(8,128)(2,1)S(1)}, u32[]{:S(2)}, u32[]{:S(2)}) %collective-permute-start.1) | collective-permute-done | bytes 20512 | tf_op jit(solution)/shard_map/ppermute | solution.py:117
  13.1 0.0 collective-permute-done.2.refs_2_
  13.1 0.0 copy-start
  13.1 0.5 %shard_map.133 = (bf16[16,128]{1,0:T(8,128)(2,1)S(1)}, f32[16,128]{1,0:T(8,128)S(1)}, f32[16,128]{1,0:T(8,128)S(1)}) custom-call(f32[80,128]{1,0:T(8,128)S(1)} %get-tuple-element.23.own_ref, bf16[80,128]{1,0:T(8,128)(2,1)S(1)} %collective-permute-done.refs_0_, bf16[80,128]{1,0:T(8,128)(2,1)S(1)} %collective-permute-done.1.refs_1_, ...), custom_call_target="tpu_custom_call" | custom-call | flops 8589934592 | tf_op jit(solution)/shard_map/pallas_call | solution.py:344
  13.7 0.0 slice-start
  13.7 0.0 copy-start.2
  13.7 0.0 copy-start.3
  13.7 0.1 collective-permute-start.5
  13.8 2.7 %collective-permute-start.4 = (bf16[16,128]{1,0:T(8,128)(2,1)S(1)}, bf16[16,128]{1,0:T(8,128)(2,1)S(1)}, u32[]{:S(2)}, u32[]{:S(2)}) collective-permute-start(bf16[16,128]{1,0:T(8,128)(2,1)S(1)} %get-tuple-element.31.refs_0_), channel_id=1, source_target_pairs={{0,12},{4,8},{8,4},{12,0},{1,13},{5,9},{9,5},{13,1},{2,14},{6,10},... | collective-permute-start | bytes 12296 | tf_op jit(solution)/shard_map/ppermute | solution.py:117
  16.5 0.8 %collective-permute-start.3 = (bf16[16,128]{1,0:T(8,128)(2,1)S(1)}, bf16[16,128]{1,0:T(8,128)(2,1)S(1)}, u32[]{:S(2)}, u32[]{:S(2)}) collective-permute-start(bf16[16,128]{1,0:T(8,128)(2,1)S(1)} %get-tuple-element.31.refs_0_), channel_id=1, source_target_pairs={{0,8},{4,12},{8,0},{12,4},{1,9},{5,13},{9,1},{13,5},{2,10},{6,14},... | collective-permute-start | bytes 12296 | tf_op jit(solution)/shard_map/ppermute | solution.py:117
  17.3 0.1 collective-permute-done.5.refs_3_
  17.4 1.9 %collective-permute-done.4.refs_2_ = bf16[16,128]{1,0:T(8,128)(2,1)S(1)} collective-permute-done((bf16[16,128]{1,0:T(8,128)(2,1)S(1)}, bf16[16,128]{1,0:T(8,128)(2,1)S(1)}, u32[]{:S(2)}, u32[]{:S(2)}) %collective-permute-start.4) | collective-permute-done | bytes 4128 | tf_op jit(solution)/shard_map/ppermute | solution.py:117
  19.2 1.7 %collective-permute-done.3.refs_1_ = bf16[16,128]{1,0:T(8,128)(2,1)S(1)} collective-permute-done((bf16[16,128]{1,0:T(8,128)(2,1)S(1)}, bf16[16,128]{1,0:T(8,128)(2,1)S(1)}, u32[]{:S(2)}, u32[]{:S(2)}) %collective-permute-start.3) | collective-permute-done | bytes 4128 | tf_op jit(solution)/shard_map/ppermute | solution.py:117
  21.0 0.0 copy-done
  21.0 0.2 shard_map.134
  21.2 0.0 collective-permute-start.8
  21.2 1.5 %collective-permute-start.7 = (bf16[16,1024]{1,0:T(8,128)(2,1)S(1)}, bf16[16,1024]{1,0:T(8,128)(2,1)S(1)}, u32[]{:S(2)}, u32[]{:S(2)}) collective-permute-start(bf16[16,1024]{1,0:T(8,128)(2,1)S(1)} %get-tuple-element.33), channel_id=1, source_target_pairs={{0,2},{1,3},{2,0},{3,1},{4,6},{5,7},{6,4},{7,5},{8,10},{9,11},{10,... | collective-permute-start | bytes 98312 | tf_op jit(solution)/shard_map/ppermute | solution.py:117
  22.8 0.3 collective-permute-start.6
  23.1 0.0 collective-permute-done.8.refs_2_
  23.1 2.1 %collective-permute-done.7.refs_1_ = bf16[16,1024]{1,0:T(8,128)(2,1)S(1)} collective-permute-done((bf16[16,1024]{1,0:T(8,128)(2,1)S(1)}, bf16[16,1024]{1,0:T(8,128)(2,1)S(1)}, u32[]{:S(2)}, u32[]{:S(2)}) %collective-permute-start.7) | collective-permute-done | bytes 32800 | tf_op jit(solution)/shard_map/ppermute | solution.py:117
  25.2 0.9 %collective-permute-done.6.refs_0_ = bf16[16,1024]{1,0:T(8,128)(2,1)S(1)} collective-permute-done((bf16[16,1024]{1,0:T(8,128)(2,1)S(1)}, bf16[16,1024]{1,0:T(8,128)(2,1)S(1)}, u32[]{:S(2)}, u32[]{:S(2)}) %collective-permute-start.6) | collective-permute-done | bytes 32800 | tf_op jit(solution)/shard_map/ppermute | solution.py:117
  26.1 0.0 slice-done
  26.1 0.0 slice-done.1
  26.1 0.0 copy-done.2
  26.1 0.0 copy-done.3
  26.1 0.9 %shard_map.135 = (bf16[16,1024]{1,0:T(8,128)(2,1)S(1)}, bf16[16,1024]{1,0:T(8,128)(2,1)S(1)}, f32[16,128]{1,0:T(8,128)S(1)}, bf16[16,1152]{1,0:T(8,128)(2,1)S(1)...) custom-call(bf16[16,1024]{1,0:T(8,128)(2,1)S(1)} %copy-done.2, f32[1,1024]{1,0:T(1,128)S(1)} %bitcast.6, ...), custom_call_target="tpu_custom_call" | custom-call | flops 8589934592 | tf_op jit(solution)/shard_map/pallas_call | solution.py:344
  27.1 0.8 %collective-permute-start.9 = (bf16[16,1152]{1,0:T(8,128)(2,1)S(1)}, bf16[16,1152]{1,0:T(8,128)(2,1)S(1)}, u32[]{:S(2)}, u32[]{:S(2)}) collective-permute-start(bf16[16,1152]{1,0:T(8,128)(2,1)S(1)} %get-tuple-element.37), channel_id=1, source_target_pairs={{0,8},{4,12},{8,0},{12,4},{1,9},{5,13},{9,1},{13,5},{2,10},{6,14},... | collective-permute-start | bytes 110600 | tf_op jit(solution)/shard_map/ppermute | solution.py:117
  27.9 2.0 %collective-permute-start.10 = (bf16[16,1152]{1,0:T(8,128)(2,1)S(1)}, bf16[16,1152]{1,0:T(8,128)(2,1)S(1)}, u32[]{:S(2)}, u32[]{:S(2)}) collective-permute-start(bf16[16,1152]{1,0:T(8,128)(2,1)S(1)} %get-tuple-element.38), channel_id=1, source_target_pairs={{0,12},{4,8},{8,4},{12,0},{1,13},{5,9},{9,5},{13,1},{2,14},{6,10},... | collective-permute-start | bytes 110600 | tf_op jit(solution)/shard_map/ppermute | solution.py:117
  29.9 0.7 %collective-permute-start.11 = (bf16[16,1152]{1,0:T(8,128)(2,1)S(1)}, bf16[16,1152]{1,0:T(8,128)(2,1)S(1)}, u32[]{:S(2)}, u32[]{:S(2)}) collective-permute-start(bf16[16,1152]{1,0:T(8,128)(2,1)S(1)} %get-tuple-element.39), channel_id=1, source_target_pairs={{0,4},{4,0},{8,12},{12,8},{1,5},{5,1},{9,13},{13,9},{2,6},{6,2},{1... | collective-permute-start | bytes 110600 | tf_op jit(solution)/shard_map/ppermute | solution.py:117
  30.6 0.4 shard_map.136.own_ref
  31.0 2.1 %collective-permute-done.9.refs_0_ = bf16[16,1152]{1,0:T(8,128)(2,1)S(1)} collective-permute-done((bf16[16,1152]{1,0:T(8,128)(2,1)S(1)}, bf16[16,1152]{1,0:T(8,128)(2,1)S(1)}, u32[]{:S(2)}, u32[]{:S(2)}) %collective-permute-start.9) | collective-permute-done | bytes 36896 | tf_op jit(solution)/shard_map/ppermute | solution.py:117
  33.0 0.7 %collective-permute-done.10.refs_1_ = bf16[16,1152]{1,0:T(8,128)(2,1)S(1)} collective-permute-done((bf16[16,1152]{1,0:T(8,128)(2,1)S(1)}, bf16[16,1152]{1,0:T(8,128)(2,1)S(1)}, u32[]{:S(2)}, u32[]{:S(2)}) %collective-permute-start.10) | collective-permute-done | bytes 36896 | tf_op jit(solution)/shard_map/ppermute | solution.py:117
  33.7 0.4 collective-permute-done.11.refs_2_
  34.1 0.2 shard_map.137.refs_0_
  34.3 0.5 collective-permute-start.14
  34.8 1.6 %collective-permute-start.13 = (bf16[16,1024]{1,0:T(8,128)(2,1)S(1)}, bf16[16,1024]{1,0:T(8,128)(2,1)S(1)}, u32[]{:S(2)}, u32[]{:S(2)}) collective-permute-start(bf16[16,1024]{1,0:T(8,128)(2,1)S(1)} %shard_map.137.refs_0_), channel_id=1, source_target_pairs={{0,12},{4,8},{8,4},{12,0},{1,13},{5,9},{9,5},{13,1},{2,14},{6,10},... | collective-permute-start | bytes 98312 | tf_op jit(solution)/shard_map/ppermute | solution.py:117
  36.3 1.9 %collective-permute-start.12 = (bf16[16,1024]{1,0:T(8,128)(2,1)S(1)}, bf16[16,1024]{1,0:T(8,128)(2,1)S(1)}, u32[]{:S(2)}, u32[]{:S(2)}) collective-permute-start(bf16[16,1024]{1,0:T(8,128)(2,1)S(1)} %shard_map.137.refs_0_), channel_id=1, source_target_pairs={{0,8},{4,0},{8,12},{12,4},{1,9},{5,1},{9,13},{13,5},{2,10},{6,2},{... | collective-permute-start | bytes 98312 | tf_op jit(solution)/shard_map/ppermute | solution.py:117
  38.3 0.0 slice-done.2
  38.3 0.0 slice-done.3
  38.3 0.4 shard_map.138.refs_2_
  38.7 0.5 %collective-permute-done.14.refs_0_ = bf16[16,1024]{1,0:T(8,128)(2,1)S(1)} collective-permute-done((bf16[16,1024]{1,0:T(8,128)(2,1)S(1)}, bf16[16,1024]{1,0:T(8,128)(2,1)S(1)}, u32[]{:S(2)}, u32[]{:S(2)}) %collective-permute-start.14) | collective-permute-done | bytes 32800 | tf_op jit(solution)/shard_map/ppermute | solution.py:117
  39.2 0.4 shard_map.139.refs_2_
  39.5 1.0 %collective-permute-done.13.refs_0_ = bf16[16,1024]{1,0:T(8,128)(2,1)S(1)} collective-permute-done((bf16[16,1024]{1,0:T(8,128)(2,1)S(1)}, bf16[16,1024]{1,0:T(8,128)(2,1)S(1)}, u32[]{:S(2)}, u32[]{:S(2)}) %collective-permute-start.13) | collective-permute-done | bytes 32800 | tf_op jit(solution)/shard_map/ppermute | solution.py:117
  40.6 0.4 shard_map.140.refs_2_
  41.0 0.0 collective-permute-done.12.refs_0_
  41.0 0.4 shard_map.141
  41.4 0.0 collective-permute-start.17
  41.4 1.0 %collective-permute-start.16 = (bf16[16,1024]{1,0:T(8,128)(2,1)S(1)}, bf16[16,1024]{1,0:T(8,128)(2,1)S(1)}, u32[]{:S(2)}, u32[]{:S(2)}) collective-permute-start(bf16[16,1024]{1,0:T(8,128)(2,1)S(1)} %get-tuple-element.41), channel_id=1, source_target_pairs={{0,2},{1,3},{2,0},{3,1},{4,6},{5,7},{6,4},{7,5},{8,10},{9,11},{10,... | collective-permute-start | bytes 98312 | tf_op jit(solution)/shard_map/ppermute | solution.py:117
  42.3 0.9 %collective-permute-start.15 = (bf16[16,1024]{1,0:T(8,128)(2,1)S(1)}, bf16[16,1024]{1,0:T(8,128)(2,1)S(1)}, u32[]{:S(2)}, u32[]{:S(2)}) collective-permute-start(bf16[16,1024]{1,0:T(8,128)(2,1)S(1)} %get-tuple-element.41), channel_id=1, source_target_pairs={{0,3},{1,2},{2,1},{3,0},{4,7},{5,6},{6,5},{7,4},{8,11},{9,10},{10,... | collective-permute-start | bytes 98312 | tf_op jit(solution)/shard_map/ppermute | solution.py:117
  43.2 0.0 copy-done.1
  43.2 1.5 %shard_map.143 = f32[4,4,128,128]{3,2,1,0:T(8,128)} custom-call(f32[16,128]{1,0:T(8,128)S(1)} %get-tuple-element.42.key_ref, f32[16,128]{1,0:T(8,128)S(1)} %get-tuple-element.43.value_ref, f32[16,128]{1,0:T(8,128)S(1)} %get-tuple-element.29.refs_5_.gamma_ref, f32[16,128]{1,0:T(8,128)S(1)} %get-tuple-element.36.split_ref.after_ref, ...), custom_call_target="tpu_custom_call" | custom-call | flops 8589934592 | tf_op jit(solution)/shard_map/pallas_call | solution.py:344
  44.8 0.0 collective-permute-done.17.refs_2_
  44.8 0.6 %collective-permute-done.16.refs_1_ = bf16[16,1024]{1,0:T(8,128)(2,1)S(1)} collective-permute-done((bf16[16,1024]{1,0:T(8,128)(2,1)S(1)}, bf16[16,1024]{1,0:T(8,128)(2,1)S(1)}, u32[]{:S(2)}, u32[]{:S(2)}) %collective-permute-start.16) | collective-permute-done | bytes 32800 | tf_op jit(solution)/shard_map/ppermute | solution.py:117
  45.4 0.3 collective-permute-done.15.refs_0_
  45.7 0.6 %shard_map.142 = bf16[16,1024]{1,0:T(8,128)(2,1)} custom-call(bf16[16,1024]{1,0:T(8,128)(2,1)S(1)} %get-tuple-element.34.mixed_ref, f32[16,1024]{1,0:T(8,128)S(1)} %get-tuple-element.40.own_ref, bf16[16,1024]{1,0:T(8,128)(2,1)S(1)} %collective-permute-done.15.refs_0_, bf16[16,1024]{1,0:T(8,128)(2,1)S(1)} %collective-permute-done.16.refs_1_, ...), custom_call_target="tpu_custom_call" | custom-call | flops 8589934592 | tf_op jit(solution)/shard_map/pallas_call | solution.py:344
  (8 shorter events, 0.0 us)
Async XLA Ops:
  0.6 8.5 %copy-start.4 = (s32[4]{0:T(128)S(1)}, s32[4]{0:T(128)}, u32[]{:S(2)}) copy-start(s32[4]{0:T(128)} %param.13) | copy-start | bytes 52
  3.4 7.3 %collective-permute-start = (bf16[80,128]{1,0:T(8,128)(2,1)S(1)}, bf16[80,128]{1,0:T(8,128)(2,1)S(1)}, u32[]{:S(2)}, u32[]{:S(2)}) collective-permute-start(bf16[80,128]{1,0:T(8,128)(2,1)S(1)} %get-tuple-element.24), channel_id=1, source_target_pairs={{0,8},{4,12},{8,0},{12,4},{1,9},{5,13},{9,1},{13,5},{2,10},{6,14},... | collective-permute-start | bytes 61448 | tf_op jit(solution)/shard_map/ppermute | solution.py:117
  7.5 5.6 %collective-permute-start.1 = (bf16[80,128]{1,0:T(8,128)(2,1)S(1)}, bf16[80,128]{1,0:T(8,128)(2,1)S(1)}, u32[]{:S(2)}, u32[]{:S(2)}) collective-permute-start(bf16[80,128]{1,0:T(8,128)(2,1)S(1)} %get-tuple-element.25), channel_id=1, source_target_pairs={{0,12},{4,8},{8,4},{12,0},{1,13},{5,9},{9,5},{13,1},{2,14},{6,10},... | collective-permute-start | bytes 61448 | tf_op jit(solution)/shard_map/ppermute | solution.py:117
  8.9 4.2 %collective-permute-start.2 = (bf16[80,128]{1,0:T(8,128)(2,1)S(1)}, bf16[80,128]{1,0:T(8,128)(2,1)S(1)}, u32[]{:S(2)}, u32[]{:S(2)}) collective-permute-start(bf16[80,128]{1,0:T(8,128)(2,1)S(1)} %get-tuple-element.26), channel_id=1, source_target_pairs={{0,4},{4,0},{8,12},{12,8},{1,5},{5,1},{9,13},{13,9},{2,6},{6,2},{1... | collective-permute-start | bytes 61448 | tf_op jit(solution)/shard_map/ppermute | solution.py:117
  13.1 7.8 %copy-start = (bf16[512,1024]{1,0:T(8,128)(2,1)S(1)}, bf16[512,1024]{1,0:T(8,128)(2,1)}, u32[]{:S(2)}) copy-start(bf16[512,1024]{1,0:T(8,128)(2,1)} %refs_4_.1) | copy-start | bytes 3145732
  13.7 12.4 %slice-start = ((s8[8388608]{0:T(1024)(128)(4,1)}), s8[4194304]{0:T(1024)(128)(4,1)S(1)}, s32[]{:S(2)}) async-start(s8[8388608]{0:T(1024)(128)(4,1)} %bitcast.2), calls=%async_computation | async-start | bytes 8388608
  13.7 12.4 %slice-start.1 = ((s8[8388608]{0:T(1024)(128)(4,1)}), s8[4194304]{0:T(1024)(128)(4,1)S(1)}, s32[]{:S(2)}) async-start(s8[8388608]{0:T(1024)(128)(4,1)} %bitcast.2), calls=%async_computation.1 | async-start | bytes 8388608
  13.7 12.4 %copy-start.2 = (bf16[16,1024]{1,0:T(8,128)(2,1)S(1)}, bf16[16,1024]{1,0:T(8,128)(2,1)}, u32[]{:S(2)}) copy-start(bf16[16,1024]{1,0:T(8,128)(2,1)} %x_ref.1) | copy-start | bytes 98308
  13.7 12.4 %copy-start.3 = (f32[1024]{0:T(1024)S(1)}, f32[1024]{0:T(1024)}, u32[]{:S(2)}) copy-start(f32[1024]{0:T(1024)} %param.21) | copy-start | bytes 12292
  13.7 3.7 %collective-permute-start.5 = (bf16[16,128]{1,0:T(8,128)(2,1)S(1)}, bf16[16,128]{1,0:T(8,128)(2,1)S(1)}, u32[]{:S(2)}, u32[]{:S(2)}) collective-permute-start(bf16[16,128]{1,0:T(8,128)(2,1)S(1)} %get-tuple-element.31.refs_0_), channel_id=1, source_target_pairs={{0,4},{4,0},{8,12},{12,8},{1,5},{5,1},{9,13},{13,9},{2,6},{6,2},{1... | collective-permute-start | bytes 12296 | tf_op jit(solution)/shard_map/ppermute | solution.py:117
  13.8 5.5 %collective-permute-start.4 = (bf16[16,128]{1,0:T(8,128)(2,1)S(1)}, bf16[16,128]{1,0:T(8,128)(2,1)S(1)}, u32[]{:S(2)}, u32[]{:S(2)}) collective-permute-start(bf16[16,128]{1,0:T(8,128)(2,1)S(1)} %get-tuple-element.31.refs_0_), channel_id=1, source_target_pairs={{0,12},{4,8},{8,4},{12,0},{1,13},{5,9},{9,5},{13,1},{2,14},{6,10},... | collective-permute-start | bytes 12296 | tf_op jit(solution)/shard_map/ppermute | solution.py:117
  16.5 4.5 %collective-permute-start.3 = (bf16[16,128]{1,0:T(8,128)(2,1)S(1)}, bf16[16,128]{1,0:T(8,128)(2,1)S(1)}, u32[]{:S(2)}, u32[]{:S(2)}) collective-permute-start(bf16[16,128]{1,0:T(8,128)(2,1)S(1)} %get-tuple-element.31.refs_0_), channel_id=1, source_target_pairs={{0,8},{4,12},{8,0},{12,4},{1,9},{5,13},{9,1},{13,5},{2,10},{6,14},... | collective-permute-start | bytes 12296 | tf_op jit(solution)/shard_map/ppermute | solution.py:117
  21.2 1.9 %collective-permute-start.8 = (bf16[16,1024]{1,0:T(8,128)(2,1)S(1)}, bf16[16,1024]{1,0:T(8,128)(2,1)S(1)}, u32[]{:S(2)}, u32[]{:S(2)}) collective-permute-start(bf16[16,1024]{1,0:T(8,128)(2,1)S(1)} %get-tuple-element.33), channel_id=1, source_target_pairs={{0,1},{1,0},{2,3},{3,2},{4,5},{5,4},{6,7},{7,6},{8,9},{9,8},{10,11... | collective-permute-start | bytes 98312 | tf_op jit(solution)/shard_map/ppermute | solution.py:117
  21.2 4.0 %collective-permute-start.7 = (bf16[16,1024]{1,0:T(8,128)(2,1)S(1)}, bf16[16,1024]{1,0:T(8,128)(2,1)S(1)}, u32[]{:S(2)}, u32[]{:S(2)}) collective-permute-start(bf16[16,1024]{1,0:T(8,128)(2,1)S(1)} %get-tuple-element.33), channel_id=1, source_target_pairs={{0,2},{1,3},{2,0},{3,1},{4,6},{5,7},{6,4},{7,5},{8,10},{9,11},{10,... | collective-permute-start | bytes 98312 | tf_op jit(solution)/shard_map/ppermute | solution.py:117
  22.8 3.3 %collective-permute-start.6 = (bf16[16,1024]{1,0:T(8,128)(2,1)S(1)}, bf16[16,1024]{1,0:T(8,128)(2,1)S(1)}, u32[]{:S(2)}, u32[]{:S(2)}) collective-permute-start(bf16[16,1024]{1,0:T(8,128)(2,1)S(1)} %get-tuple-element.33), channel_id=1, source_target_pairs={{0,3},{1,2},{2,1},{3,0},{4,7},{5,6},{6,5},{7,4},{8,11},{9,10},{10,... | collective-permute-start | bytes 98312 | tf_op jit(solution)/shard_map/ppermute | solution.py:117
  27.1 5.9 %collective-permute-start.9 = (bf16[16,1152]{1,0:T(8,128)(2,1)S(1)}, bf16[16,1152]{1,0:T(8,128)(2,1)S(1)}, u32[]{:S(2)}, u32[]{:S(2)}) collective-permute-start(bf16[16,1152]{1,0:T(8,128)(2,1)S(1)} %get-tuple-element.37), channel_id=1, source_target_pairs={{0,8},{4,12},{8,0},{12,4},{1,9},{5,13},{9,1},{13,5},{2,10},{6,14},... | collective-permute-start | bytes 110600 | tf_op jit(solution)/shard_map/ppermute | solution.py:117
  27.9 5.9 %collective-permute-start.10 = (bf16[16,1152]{1,0:T(8,128)(2,1)S(1)}, bf16[16,1152]{1,0:T(8,128)(2,1)S(1)}, u32[]{:S(2)}, u32[]{:S(2)}) collective-permute-start(bf16[16,1152]{1,0:T(8,128)(2,1)S(1)} %get-tuple-element.38), channel_id=1, source_target_pairs={{0,12},{4,8},{8,4},{12,0},{1,13},{5,9},{9,5},{13,1},{2,14},{6,10},... | collective-permute-start | bytes 110600 | tf_op jit(solution)/shard_map/ppermute | solution.py:117
  29.9 4.2 %collective-permute-start.11 = (bf16[16,1152]{1,0:T(8,128)(2,1)S(1)}, bf16[16,1152]{1,0:T(8,128)(2,1)S(1)}, u32[]{:S(2)}, u32[]{:S(2)}) collective-permute-start(bf16[16,1152]{1,0:T(8,128)(2,1)S(1)} %get-tuple-element.39), channel_id=1, source_target_pairs={{0,4},{4,0},{8,12},{12,8},{1,5},{5,1},{9,13},{13,9},{2,6},{6,2},{1... | collective-permute-start | bytes 110600 | tf_op jit(solution)/shard_map/ppermute | solution.py:117
  30.6 7.7 %slice-start.2 = ((s8[8388608]{0:T(1024)(128)(4,1)}), s8[4194304]{0:T(1024)(128)(4,1)S(1)}, s32[]{:S(2)}) async-start(s8[8388608]{0:T(1024)(128)(4,1)} %bitcast.4), calls=%async_computation.2 | async-start | bytes 8388608
  31.0 7.3 %slice-start.3 = ((s8[8388608]{0:T(1024)(128)(4,1)}), s8[4194304]{0:T(1024)(128)(4,1)S(1)}, s32[]{:S(2)}) async-start(s8[8388608]{0:T(1024)(128)(4,1)} %bitcast.4), calls=%async_computation.3 | async-start | bytes 8388608
  34.3 4.9 %collective-permute-start.14 = (bf16[16,1024]{1,0:T(8,128)(2,1)S(1)}, bf16[16,1024]{1,0:T(8,128)(2,1)S(1)}, u32[]{:S(2)}, u32[]{:S(2)}) collective-permute-start(bf16[16,1024]{1,0:T(8,128)(2,1)S(1)} %shard_map.137.refs_0_), channel_id=1, source_target_pairs={{0,4},{4,12},{8,0},{12,8},{1,5},{5,13},{9,1},{13,9},{2,6},{6,14},{... | collective-permute-start | bytes 98312 | tf_op jit(solution)/shard_map/ppermute | solution.py:117
  34.8 5.8 %collective-permute-start.13 = (bf16[16,1024]{1,0:T(8,128)(2,1)S(1)}, bf16[16,1024]{1,0:T(8,128)(2,1)S(1)}, u32[]{:S(2)}, u32[]{:S(2)}) collective-permute-start(bf16[16,1024]{1,0:T(8,128)(2,1)S(1)} %shard_map.137.refs_0_), channel_id=1, source_target_pairs={{0,12},{4,8},{8,4},{12,0},{1,13},{5,9},{9,5},{13,1},{2,14},{6,10},... | collective-permute-start | bytes 98312 | tf_op jit(solution)/shard_map/ppermute | solution.py:117
  36.3 4.6 %collective-permute-start.12 = (bf16[16,1024]{1,0:T(8,128)(2,1)S(1)}, bf16[16,1024]{1,0:T(8,128)(2,1)S(1)}, u32[]{:S(2)}, u32[]{:S(2)}) collective-permute-start(bf16[16,1024]{1,0:T(8,128)(2,1)S(1)} %shard_map.137.refs_0_), channel_id=1, source_target_pairs={{0,8},{4,0},{8,12},{12,4},{1,9},{5,1},{9,13},{13,5},{2,10},{6,2},{... | collective-permute-start | bytes 98312 | tf_op jit(solution)/shard_map/ppermute | solution.py:117
  40.9 2.3 %copy-start.1 = (f32[4,4,128,128]{3,2,1,0:T(8,128)S(1)}, f32[4,4,128,128]{3,2,1,0:T(8,128)}, u32[]{:S(2)}) copy-start(f32[4,4,128,128]{3,2,1,0:T(8,128)} %state_ref.1) | copy-start | bytes 3145732
  41.4 3.4 %collective-permute-start.17 = (bf16[16,1024]{1,0:T(8,128)(2,1)S(1)}, bf16[16,1024]{1,0:T(8,128)(2,1)S(1)}, u32[]{:S(2)}, u32[]{:S(2)}) collective-permute-start(bf16[16,1024]{1,0:T(8,128)(2,1)S(1)} %get-tuple-element.41), channel_id=1, source_target_pairs={{0,1},{1,0},{2,3},{3,2},{4,5},{5,4},{6,7},{7,6},{8,9},{9,8},{10,11... | collective-permute-start | bytes 98312 | tf_op jit(solution)/shard_map/ppermute | solution.py:117
  41.4 4.0 %collective-permute-start.16 = (bf16[16,1024]{1,0:T(8,128)(2,1)S(1)}, bf16[16,1024]{1,0:T(8,128)(2,1)S(1)}, u32[]{:S(2)}, u32[]{:S(2)}) collective-permute-start(bf16[16,1024]{1,0:T(8,128)(2,1)S(1)} %get-tuple-element.41), channel_id=1, source_target_pairs={{0,2},{1,3},{2,0},{3,1},{4,6},{5,7},{6,4},{7,5},{8,10},{9,11},{10,... | collective-permute-start | bytes 98312 | tf_op jit(solution)/shard_map/ppermute | solution.py:117
  42.3 3.4 %collective-permute-start.15 = (bf16[16,1024]{1,0:T(8,128)(2,1)S(1)}, bf16[16,1024]{1,0:T(8,128)(2,1)S(1)}, u32[]{:S(2)}, u32[]{:S(2)}) collective-permute-start(bf16[16,1024]{1,0:T(8,128)(2,1)S(1)} %get-tuple-element.41), channel_id=1, source_target_pairs={{0,3},{1,2},{2,1},{3,0},{4,7},{5,6},{6,5},{7,4},{8,11},{9,10},{10,... | collective-permute-start | bytes 98312 | tf_op jit(solution)/shard_map/ppermute | solution.py:117
